TPU v7x, 128 devices: a whole 4x4x4 slice. The times are simulated.
128 devices in a mesh: sp: 32 (over z, y, core), tp: 4 (over x).
Axes of the slice: x: 4, y: 4, z: 4, core: 2. Of those that a mesh axis runs over, the one named last changes fastest.
Arguments:
- query_narrow: bfloat16 [4096, 2048], P('sp', 'tp'), may hold values from -48 to 48
- key_narrow: bfloat16 [4096, 512], P('sp', 'tp'), may hold values from -15 to 15
- value_narrow: bfloat16 [4096, 512], P('sp', 'tp'), may hold values from -6 to 6
- gates_narrow: float32 [4096, 16], P(None, 'tp'), may hold values from -514 to 0, as said below
- query_broad: bfloat16 [4096, 2048], P('sp', 'tp'), may hold values from -48 to 48
- key_broad: bfloat16 [4096, 1024], P('sp', 'tp'), may hold values from -15 to 15
- value_broad: bfloat16 [4096, 1024], P('sp', 'tp'), may hold values from -6 to 6
- gates_broad: float32 [4096, 8], P(None, 'tp'), may hold values from -514 to 0, as said below
- project_narrow: bfloat16 [2048, 4096], P('tp'), may hold values from -0.1875 to 0.1875
- project_broad: bfloat16 [2048, 4096], P('tp'), may hold values from -0.1875 to 0.1875
- residual: bfloat16 [4096, 4096], P('sp'), may hold values from -6 to 6
- norm_gain: float32 [4096], replicated, may hold values from 0.1 to 1.9
- route_ids: int32 [4096, 4], P(('sp', 'tp')), may hold values from 0 to 127, all different within a row; in each aligned block of 32 rows (0 to 31, 32 to 63, ...) at most 2 rows name the same one
- route_weight: float32 [4096, 4], P(('sp', 'tp')), may hold values from 0.2 to 1.2
- expert_gate: bfloat16 [128, 4096, 256], P(('sp', 'tp')), may hold values from -0.09375 to 0.09375
- expert_up: bfloat16 [128, 4096, 256], P(('sp', 'tp')), may hold values from -0.09375 to 0.09375
- expert_down: bfloat16 [128, 256, 4096], P(('sp', 'tp')), may hold values from -0.375 to 0.375
- shared_gate: bfloat16 [4096, 1024], P(None, 'tp'), may hold values from -0.09375 to 0.09375
- shared_up: bfloat16 [4096, 1024], P(None, 'tp'), may hold values from -0.09375 to 0.09375
- shared_down: bfloat16 [1024, 4096], P('tp'), may hold values from -0.1875 to 0.1875
Outputs:
- layer_out: bfloat16 [4096, 4096], P(('sp', 'tp'))
Inputs may be any that keep to these rules, and one draw needn't show every extreme that they name: `gates_narrow`: Non-increasing along positions in each head. `gates_broad`: Non-increasing along positions in each head. `route_ids`: each row names 4 different experts; among the rows of one device no expert is named by more than 2 rows, and that number is reached.
All inputs are finite; a program needn't handle non-finite values.
Results may differ from a plain program's by a relative error of at most 0.014.
Values may be sent and summed in bfloat16 or wider, within the bound.
No kernel may reach another device: no remote copies, remote signals or barrier semaphores. Data moves between devices by JAX's collectives and lax.ppermute only.
A program may use at most 128 MiB of HBM per device.

v0:
```python
import math

import jax
import jax.numpy as jnp
from jax import lax
from jax.sharding import PartitionSpec as P

NARROW_SIZE = 128
BROAD_SIZE = 256


norm_epsilon = 1e-06


def in_one_piece(arrays, axis, dim, along):
    both = jnp.concatenate(arrays, axis=along)
    whole, at, outs = (lax.all_gather(both, axis, axis=dim, tiled=True), 0, [])
    for a in arrays:
        outs.append(lax.slice_in_dim(whole, at, at + a.shape[along], axis=along))
        at += a.shape[along]
    return tuple(outs)


def split_up(shard, dim, length):
    dims = shard.shape
    parts = shard.reshape(*dims[:dim], length, dims[dim] // length, *dims[dim + 1 :])
    return jnp.moveaxis(parts, dim, 0)


def sum_at_owner(shard, axis, dim):
    length = lax.axis_size(axis)
    parts = lax.all_to_all(split_up(shard, dim, length), axis, 0, 0, tiled=True)
    return jnp.sum(parts.astype(jnp.float32), axis=0)


def span_for(length):
    common = math.gcd(length, 512)
    return common


def split_heads(rows, kv_local, head_size):
    tokens = rows.shape[0]
    group_size = rows.shape[1] // (kv_local * head_size)
    return rows.reshape(tokens, kv_local, group_size, head_size).transpose(1, 2, 0, 3)


def attend_span(
    states,
    queries,
    query_gates,
    key_rows,
    value_rows,
    key_gates,
    query_place,
    key_place,
    key_limit,
    scaling,
):
    kv_local, group_size, tokens, head_size = queries.shape
    length = key_rows.shape[0]
    key_heads = key_rows.reshape(length, kv_local, head_size)
    value_heads = value_rows.reshape(length, kv_local, head_size)
    scores = (
        jnp.einsum("kgtd,skd->kgts", queries, key_heads, preferred_element_type=jnp.float32)
        * scaling
    )
    scores = scores + query_gates[..., None] - key_gates.T.reshape(kv_local, group_size, 1, length)
    allowed = (key_place[None, :] <= query_place[:, None]) & (key_place[None, :] < key_limit)
    scores = jnp.where(allowed, scores, -jnp.inf)
    running_max, running_sum, weighted = states
    newest = jnp.maximum(running_max, jnp.max(scores, axis=-1))
    anchor = jnp.where(newest == -jnp.inf, 0.0, newest)
    weights = jnp.exp(scores - anchor[..., None])
    factor = jnp.exp(running_max - anchor)
    weighted = weighted * factor[..., None] + jnp.einsum(
        "kgts,skd->kgtd",
        weights.astype(jnp.bfloat16),
        value_heads,
        preferred_element_type=jnp.float32,
    )
    running_sum = running_sum * factor + jnp.sum(weights, axis=-1)
    return (newest, running_sum, weighted)


def local(
    query_narrow,
    key_narrow,
    value_narrow,
    gates_narrow,
    query_broad,
    key_broad,
    value_broad,
    gates_broad,
    project_narrow,
    project_broad,
    residual,
    norm_gain,
    route_ids,
    route_weight,
    expert_gate,
    expert_up,
    expert_down,
    shared_gate,
    shared_up,
    shared_down,
):
    tokens = query_narrow.shape[0]
    first_row = lax.axis_index("sp") * tokens
    query_place = first_row + jnp.arange(tokens, dtype=jnp.int32)
    groups_info = []
    for queries, all_gates, head_size, key_width in (
        (query_narrow, gates_narrow, NARROW_SIZE, key_narrow.shape[1]),
        (query_broad, gates_broad, BROAD_SIZE, key_broad.shape[1]),
    ):
        kv_local = key_width // head_size
        split = split_heads(queries, kv_local, head_size)
        own_gates = lax.dynamic_slice_in_dim(all_gates, first_row, tokens, 0)
        own_gates = own_gates.reshape(tokens, kv_local, -1).transpose(1, 2, 0)
        groups_info.append((split, own_gates, all_gates, head_size ** (-0.5)))

    def update(states, pairs, key_first, key_limit):
        length = pairs[0][0].shape[0]
        key_place = key_first + jnp.arange(length, dtype=jnp.int32)
        result = []
        for details, member, key_value in zip(groups_info, states, pairs):
            split, own_gates, all_gates, scaling = details
            key_gates = lax.dynamic_slice_in_dim(all_gates, key_first, length, 0)
            result.append(
                attend_span(
                    member,
                    split,
                    own_gates,
                    key_value[0],
                    key_value[1],
                    key_gates,
                    query_place,
                    key_place,
                    key_limit,
                    scaling,
                )
            )
        return tuple(result)

    empty = tuple(
        (
            (
                jnp.full(details[0].shape[:3], -jnp.inf, jnp.float32),
                jnp.zeros(details[0].shape[:3], jnp.float32),
                jnp.zeros(details[0].shape, jnp.float32),
            )
            for details in groups_info
        )
    )
    key_limit = first_row + tokens
    narrow_keys, narrow_values, broad_keys, broad_values = in_one_piece(
        (key_narrow, value_narrow, key_broad, value_broad), "sp", 0, 1
    )
    length = narrow_keys.shape[0]
    stride = span_for(length)

    def one_span(round_index, carried):
        offset = round_index * stride

        def cut(array):
            return lax.dynamic_slice_in_dim(array, offset, stride, 0)

        def take(inner):
            return update(
                inner,
                ((cut(narrow_keys), cut(narrow_values)), (cut(broad_keys), cut(broad_values))),
                offset,
                key_limit,
            )

        def leave(inner):
            return inner

        return lax.cond(offset < key_limit, take, leave, carried)

    finished = lax.fori_loop(0, length // stride, one_span, empty)
    heads_out = []
    for running_max, running_sum, weighted in finished:
        normalized = (weighted / running_sum[..., None]).astype(jnp.bfloat16)
        heads_out.append(normalized.transpose(2, 0, 1, 3).reshape(tokens, -1))
    partial_value = jnp.dot(heads_out[0], project_narrow, preferred_element_type=jnp.float32)
    partial_value = partial_value + jnp.dot(
        heads_out[1], project_broad, preferred_element_type=jnp.float32
    )
    mixture = lax.psum(partial_value.astype(jnp.bfloat16), "tp").astype(jnp.float32)
    stream = residual.astype(jnp.float32) + mixture
    normed = (
        stream
        * lax.rsqrt(jnp.mean(stream * stream, axis=-1, keepdims=True) + norm_epsilon)
        * norm_gain
    ).astype(jnp.bfloat16)
    shared_hidden = (
        jax.nn.silu(jnp.dot(normed, shared_gate, preferred_element_type=jnp.float32))
        * jnp.dot(normed, shared_up, preferred_element_type=jnp.float32)
    ).astype(jnp.bfloat16)
    sub_rows = route_ids.shape[0]
    own_first = lax.axis_index("tp") * sub_rows
    shared = sum_at_owner(
        jnp.dot(shared_hidden, shared_down, preferred_element_type=jnp.float32).astype(
            jnp.bfloat16
        ),
        "tp",
        0,
    )
    top_count = route_ids.shape[1]
    local_experts = expert_gate.shape[0]
    expert_total = lax.axis_size("sp") * lax.axis_size("tp") * local_experts
    capacity = 2 * sub_rows * top_count // expert_total
    flat_ids = route_ids.reshape(-1)
    one_hot = (flat_ids[:, None] == jnp.arange(expert_total, dtype=jnp.int32)[None, :]).astype(
        jnp.int32
    )
    slot_of = jnp.sum(one_hot * (jnp.cumsum(one_hot, axis=0) - 1), axis=1)
    target = (flat_ids * capacity + slot_of).reshape(sub_rows, top_count)
    slot_total = expert_total * capacity
    matches = target[None, :, :] == jnp.arange(slot_total, dtype=jnp.int32)[:, None, None]
    dispatch = jnp.any(matches, axis=-1).astype(jnp.bfloat16)
    own_normed = lax.dynamic_slice_in_dim(normed, own_first, sub_rows, 0)
    outbound = (
        jnp.dot(dispatch, own_normed, preferred_element_type=jnp.float32)
        .astype(jnp.bfloat16)
        .reshape(expert_total, capacity, -1)
    )
    weight_rounded = route_weight.astype(jnp.bfloat16)
    combiner = jnp.sum(
        jnp.where(matches, weight_rounded[None], jnp.zeros((), jnp.bfloat16)), axis=-1
    ).T
    inbound = lax.all_to_all(outbound, ("sp", "tp"), split_axis=0, concat_axis=0, tiled=True)
    senders = inbound.shape[0] // local_experts
    grouped = inbound.reshape(senders, local_experts, inbound.shape[1], inbound.shape[2])
    gate_out = jnp.einsum(
        "secd,edh->sech", grouped, expert_gate, preferred_element_type=jnp.float32
    )
    up_out = jnp.einsum("secd,edh->sech", grouped, expert_up, preferred_element_type=jnp.float32)
    hidden = (jax.nn.silu(gate_out) * up_out).astype(jnp.bfloat16)
    result = jnp.einsum(
        "sech,ehd->secd", hidden, expert_down, preferred_element_type=jnp.float32
    ).astype(jnp.bfloat16)
    results = result.reshape(inbound.shape)
    returned = lax.all_to_all(results, ("sp", "tp"), split_axis=0, concat_axis=0, tiled=True)
    routed = jnp.dot(combiner, returned.reshape(slot_total, -1), preferred_element_type=jnp.float32)
    own_stream = lax.dynamic_slice_in_dim(stream, own_first, sub_rows, 0)
    return (own_stream + shared + routed).astype(jnp.bfloat16)


def solution(mesh):
    placed = (
        P("sp", "tp"),
        P("sp", "tp"),
        P("sp", "tp"),
        P(None, "tp"),
        P("sp", "tp"),
        P("sp", "tp"),
        P("sp", "tp"),
        P(None, "tp"),
        P("tp", None),
        P("tp", None),
        P("sp", None),
        P(),
        P(("sp", "tp"), None),
        P(("sp", "tp"), None),
        P(("sp", "tp"), None, None),
        P(("sp", "tp"), None, None),
        P(("sp", "tp"), None, None),
        P(None, "tp"),
        P(None, "tp"),
        P("tp", None),
    )
    return jax.shard_map(
        local, mesh=mesh, in_specs=placed, out_specs=P(("sp", "tp"), None), check_vma=False
    )
```

profile of v0, /device:TPU:0, one launch (start us, length us, event | category | flops | bytes accessed | tf_op | source)
XLA Modules:
  0.0 297.9 jit_solution(1453185535958948922)
XLA Ops:
  6.5 1.7 pad_maximum_fusion
  8.3 1.0 copy.74
  9.4 0.1 copy.76
  9.5 1.0 copy.75
  10.5 0.1 copy.77
  10.7 0.7 dynamic-slice_bitcast_fusion.3
  11.4 0.7 dynamic-slice_bitcast_fusion.2
  12.0 49.2 %all-gather.2.cloned.1.call-done = bf16[4096,768]{1,0:T(8,128)(2,1)} async-done(((bf16[128,768]{1,0:T(8,128)(2,1)}), bf16[4096,768]{1,0:T(8,128)(2,1)}) %all-gather.2.cloned.1.call-update) | async-done | bytes 6291472 | tf_op jit(solution)/shard_map/all_gather | solution.py:17
  61.3 4.5 %fusion.99 = (bf16[4096,256]{1,0:T(8,128)(2,1)}, bf16[4096,256]{1,0:T(8,128)(2,1)}) fusion(bf16[4096,768]{1,0:T(8,128)(2,1)} %all-gather.2.cloned.1.call-done), kind=kLoop, calls=%fused_computation.112 | loop fusion | bytes 8388608 | tf_op jit(solution)/shard_map/slice | solution.py:19
  65.8 3.0 %fusion.100 = (bf16[4096,128]{1,0:T(8,128)(2,1)}, bf16[4096,128]{1,0:T(8,128)(2,1)}) fusion(bf16[4096,768]{1,0:T(8,128)(2,1)} %all-gather.2.cloned.1.call-done), kind=kLoop, calls=%fused_computation.113 | loop fusion | bytes 4194304 | tf_op jit(solution)/shard_map/slice | solution.py:19
  68.9 7.7 %while.24 = (s32[]{:T(128)}, f32[1,4,128]{2,1,0:T(4,128)S(1)}, f32[1,4,128]{2,1,0:T(4,128)S(1)}, f32[1,4,128,128]{3,2,1,0:T(8,128)S(1)}, f32[1,2,128]{2,1,0:T(2,...) while((s32[]{:T(128)}, f32[1,4,128]{2,1,0:T(4,128)S(1)}, ...), condition=%wide.region_7.8_spmd.clone, body=%wide.region_0.7_spmd.clone.sunk | while | flops 272376192 | bytes 7115305 | solution.py:180
  68.9 7.2 %conditional.3 = ((f32[1,4,128]{2,1,0:T(4,128)S(1)}, f32[1,4,128]{2,1,0:T(4,128)S(1)}, f32[1,4,128,128]{3,2,1,0:T(8,128)S(1)}, f32[1,2,128]{2,1,0:T(2,128)S(1)},...) conditional(s32[]{:T(128)} %convert_element_type.115, (f32[1,4,128]{2,1,0:T(4,128)S(1)}, ...), branch_computations={%region_1.0_spmd, %region_2.6_spmd} | conditional | flops 272376192 | bytes 7114370 | solution.py:178
  69.0 0.7 dynamic-slice_bitcast_fusion.1
  69.7 0.2 compare_and_fusion
  69.9 1.3 fusion.98
  71.2 1.3 fusion.11
  72.6 0.7 dynamic-slice_bitcast_fusion
  73.3 1.3 fusion.97
  74.6 1.3 fusion.10
  75.9 0.2 fusion.13
  76.6 0.1 copy.79
  76.7 0.1 copy.78
  76.9 3.1 %fusion.101 = f32[128,4096]{1,0:T(8,128)S(1)} fusion(bf16[128,512]{0,1:T(8,128)(2,1)S(1)} %bitcast.155, bf16[512,4096]{1,0:T(8,128)(2,1)} %param.32), kind=kOutput, calls=%fused_computation.114 | convolution fusion | flops 536870912 | bytes 6422528 | tf_op jit(solution)/shard_map/dot_general | solution.py:185
  80.0 0.4 copy-done.1
  80.4 1.7 fusion.38
  82.2 0.1 eq.34
  82.4 0.2 reduce_window_sum.11
  82.6 0.2 select_reduce_fusion
  82.8 0.1 reduce_sum.66
  83.0 0.1 fusion.84
  83.1 94.2 %all-reduce.2.cloned.1.call-done = bf16[128,4096]{1,0:T(8,128)(2,1)} async-done(((bf16[128,4096]{1,0:T(8,128)(2,1)}), bf16[128,4096]{1,0:T(8,128)(2,1)}) %all-reduce.2.cloned.1.call-update) | async-done | bytes 1048592 | tf_op jit(solution)/shard_map/psum | solution.py:189
  177.4 3.1 %convert_add_fusion = (f32[128,4096]{1,0:T(8,128)}, f32[128]{0:T(128)S(1)}) fusion(bf16[128,4096]{1,0:T(8,128)(2,1)} %all-reduce.2.cloned.1.call-done, bf16[128,4096]{1,0:T(8,128)(2,1)S(1)} %copy-done.2), kind=kLoop, calls=%fused_computation.70 | loop fusion | flops 2621312 | bytes 4194816 | tf_op jit(solution)/shard_map/add | solution.py:190
  180.4 0.5 multiply_convert_fusion
  180.9 2.0 convolution_convert_fusion.1
  183.0 4.4 %reshape.159 = bf16[128,2,4096]{2,1,0:T(2,128)(2,1)} reshape(bf16[256,4096]{1,0:T(8,128)(2,1)} %convolution_convert_fusion.1) | data formatting | bytes 4194304 | tf_op jit(solution)/shard_map/reshape | solution.py:226
  187.4 10.2 %all-to-all-start.1 = ((bf16[128,2,4096]{2,1,0:T(2,128)(2,1)}), bf16[128,2,4096]{2,1,0:T(2,128)(2,1)}, u32[]{:S(2)}, u32[]{:S(2)}) async-start(bf16[128,2,4096]{2,1,0:T(2,128)(2,1)} %reshape.159), calls=%async_computation.1 | async-start | bytes 4194304 | tf_op jit(solution)/shard_map/all_to_all | solution.py:232
  197.5 2.0 fusion.102
  199.6 4.6 %convolution_convert_fusion.2 = bf16[128,4096]{1,0:T(8,128)(2,1)} fusion(bf16[256,4096]{1,0:T(8,128)(2,1)} %param.43, bf16[128,4096]{1,0:T(8,128)(2,1)S(1)} %multiply_convert_fusion, bf16[4096,256]{1,0:T(8,128)(2,1)} %param.42, f32[128,256]{1,0:T(8,128)S(1)} %fusion.102), kind=kOutput, calls=%fused_computation.59 | convolution fusion | flops 537591808 | bytes 6422528 | tf_op jit(solution)/shard_map/dot_general | solution.py:203
  204.1 23.0 %all-to-all-done.1 = bf16[128,2,4096]{2,1,0:T(2,128)(2,1)} async-done(((bf16[128,2,4096]{2,1,0:T(2,128)(2,1)}), bf16[128,2,4096]{2,1,0:T(2,128)(2,1)}, u32[]{:S(2)}, u32[]{:S(2)}) %all-to-all-start.1) | async-done | bytes 2097184 | tf_op jit(solution)/shard_map/all_to_all | solution.py:232
  227.1 3.7 %all-to-all-start = ((bf16[4,32,4096]{2,1,0:T(8,128)(2,1)}), bf16[4,32,4096]{2,1,0:T(8,128)(2,1)S(1)}, u32[]{:S(2)}, u32[]{:S(2)}) async-start(bf16[4,32,4096]{2,1,0:T(8,128)(2,1)} %bitcast.153), calls=%async_computation | async-start | bytes 2097152 | tf_op jit(solution)/shard_map/all_to_all | solution.py:32
  230.8 4.6 %fusion.47 = f32[128,1,2,256]{3,0,2,1:T(8,128)S(1)} fusion(bf16[1,4096,256]{2,1,0:T(8,128)(2,1)} %param.38, bf16[128,2,4096]{2,1,0:T(2,128)(2,1)} %all-to-all-done.1), kind=kOutput, calls=%fused_computation.73 | convolution fusion | flops 536870912 | bytes 4456448 | tf_op jit(solution)/shard_map/secd,edh->sech/dot_general | solution.py:235
  235.5 7.1 %convolution_convert_fusion = bf16[128,2,4096]{2,0,1:T(8,128)(2,1)} fusion(bf16[1,256,4096]{2,1,0:T(8,128)(2,1)S(1)} %copy-done, bf16[1,4096,256]{2,1,0:T(8,128)(2,1)} %param.39, bf16[128,2,4096]{2,1,0:T(2,128)(2,1)} %all-to-all-done.1, f32[128,1,2,256]{3,0,2,1:T(8,128)S(1)} %fusion.47), kind=kOutput, calls=%fused_computation.55 | convolution fusion | flops 1075183616 | bytes 8650752 | tf_op jit(solution)/shard_map/sech,ehd->secd/dot_general | solution.py:240
  242.6 5.1 %copy.84 = bf16[128,2,4096]{2,1,0:T(2,128)(2,1)} copy(bf16[128,2,4096]{2,0,1:T(8,128)(2,1)} %convolution_convert_fusion) | data formatting | bytes 4194304 | tf_op jit(solution)/shard_map/convert_element_type | solution.py:242
  247.6 6.8 %all-to-all-start.2 = ((bf16[128,2,4096]{2,1,0:T(2,128)(2,1)}), bf16[128,2,4096]{2,1,0:T(2,128)(2,1)}, u32[]{:S(2)}, u32[]{:S(2)}) async-start(bf16[128,2,4096]{2,1,0:T(2,128)(2,1)} %copy.84), calls=%async_computation.2 | async-start | bytes 4194304 | tf_op jit(solution)/shard_map/all_to_all | solution.py:244
  254.6 1.0 convert_reduce_fusion
  255.6 28.5 %all-to-all-done.2 = bf16[128,2,4096]{2,1,0:T(2,128)(2,1)} async-done(((bf16[128,2,4096]{2,1,0:T(2,128)(2,1)}), bf16[128,2,4096]{2,1,0:T(2,128)(2,1)}, u32[]{:S(2)}, u32[]{:S(2)}) %all-to-all-start.2) | async-done | bytes 2097184 | tf_op jit(solution)/shard_map/all_to_all | solution.py:244
  284.1 4.1 %reshape.164 = bf16[256,4096]{1,0:T(8,128)(2,1)} reshape(bf16[128,2,4096]{2,1,0:T(2,128)(2,1)} %all-to-all-done.2) | data formatting | bytes 4194304 | tf_op jit(solution)/shard_map/reshape | solution.py:245
  288.2 2.8 fusion.39
  (64 shorter events, 0.9 us)
Async XLA Ops:
  6.5 228.9 %copy-start = (bf16[1,256,4096]{2,1,0:T(8,128)(2,1)S(1)}, bf16[1,256,4096]{2,1,0:T(8,128)(2,1)}, u32[]{:S(2)}) copy-start(bf16[1,256,4096]{2,1,0:T(8,128)(2,1)} %param.40) | copy-start | bytes 6291460
  6.5 54.7 %all-gather.2.cloned.1.call-start = ((), (), s32[]{:S(2)}) async-start(), calls=%async_computation.3 | async-start | bytes 6488064 | tf_op jit(solution)/shard_map/all_gather | solution.py:17
  8.3 169.1 %all-reduce.2.cloned.1.call-start = ((), (), s32[]{:S(2)}) async-start(), calls=%async_computation.4 | async-start | bytes 2097152 | tf_op jit(solution)/shard_map/psum | solution.py:189
  76.9 3.5 %copy-start.1 = (bf16[512,4096]{1,0:T(8,128)(2,1)S(1)}, bf16[512,4096]{1,0:T(8,128)(2,1)}, u32[]{:S(2)}) copy-start(bf16[512,4096]{1,0:T(8,128)(2,1)} %param.33) | copy-start | bytes 12582916
  80.4 1.8 copy-start.7
  82.1 95.2 %copy-start.2 = (bf16[128,4096]{1,0:T(8,128)(2,1)S(1)}, bf16[128,4096]{1,0:T(8,128)(2,1)}, u32[]{:S(2)}) copy-start(bf16[128,4096]{1,0:T(8,128)(2,1)} %param.34) | copy-start | bytes 3145732
  83.1 97.3 %copy-start.6 = (f32[4096]{0:T(1024)S(1)}, f32[4096]{0:T(1024)}, u32[]{:S(2)}) copy-start(f32[4096]{0:T(1024)} %param.35) | copy-start | bytes 49156
  177.3 3.1 %copy-start.3 = (bf16[128,4096]{1,0:T(8,128)(2,1)S(1)}, bf16[128,4096]{1,0:T(8,128)(2,1)}, u32[]{:S(2)}) copy-start(bf16[128,4096]{1,0:T(8,128)(2,1)} %param.34) | copy-start | bytes 3145732
  177.4 3.1 %copy-start.4 = (bf16[128,4096]{1,0:T(8,128)(2,1)S(1)}, bf16[128,4096]{1,0:T(8,128)(2,1)}, u32[]{:S(2)}) copy-start(bf16[128,4096]{1,0:T(8,128)(2,1)} %all-reduce.2.cloned.1.call-done) | copy-start | bytes 3145732
  187.4 39.8 %all-to-all-start.1 = ((bf16[128,2,4096]{2,1,0:T(2,128)(2,1)}), bf16[128,2,4096]{2,1,0:T(2,128)(2,1)}, u32[]{:S(2)}, u32[]{:S(2)}) async-start(bf16[128,2,4096]{2,1,0:T(2,128)(2,1)} %reshape.159), calls=%async_computation.1 | async-start | bytes 4194304 | tf_op jit(solution)/shard_map/all_to_all | solution.py:232
  227.1 20.5 %all-to-all-start = ((bf16[4,32,4096]{2,1,0:T(8,128)(2,1)}), bf16[4,32,4096]{2,1,0:T(8,128)(2,1)S(1)}, u32[]{:S(2)}, u32[]{:S(2)}) async-start(bf16[4,32,4096]{2,1,0:T(8,128)(2,1)} %bitcast.153), calls=%async_computation | async-start | bytes 2097152 | tf_op jit(solution)/shard_map/all_to_all | solution.py:32
  247.6 6.9 %copy-start.8 = (f32[32,4]{0,1:T(4,128)S(1)}, f32[32,4]{0,1:T(4,128)}, u32[]{:S(2)}) copy-start(f32[32,4]{0,1:T(4,128)} %param.37) | copy-start | bytes 1540
  247.6 36.5 %all-to-all-start.2 = ((bf16[128,2,4096]{2,1,0:T(2,128)(2,1)}), bf16[128,2,4096]{2,1,0:T(2,128)(2,1)}, u32[]{:S(2)}, u32[]{:S(2)}) async-start(bf16[128,2,4096]{2,1,0:T(2,128)(2,1)} %copy.84), calls=%async_computation.2 | async-start | bytes 4194304 | tf_op jit(solution)/shard_map/all_to_all | solution.py:244
  255.6 32.6 %copy-start.5 = (f32[32,4096]{1,0:T(8,128)S(1)}, f32[32,4096]{1,0:T(8,128)}, u32[]{:S(2)}) copy-start(f32[32,4096]{1,0:T(8,128)} %convert_reduce_fusion) | copy-start | bytes 1572868
Sparse Core Ops, SparseCore 0:
  9.6 51.6 all-gather.1
  82.3 95.0 all-reduce.1
where the time goes:
time: 301 us; the launch traced here: 298 us
  waiting for transfers between devices  195 us (65%)
  matrix products  33.2 us (11%)
  local copies, waits for them, and re-layouts  27.3 us (9%)
  starting transfers between devices  20.7 us (7%)
  between operations  13.7 us (5%)
  other arithmetic  7.44 us (2%)
    psum x1, waiting for transfers between devices, local(): lax.psum(partial_value.astype(jnp.bfloat16), 'tp').astype(jnp.float32)  94.2 us
    all_gather x1, waiting for transfers between devices, in_one_piece(): whole, at, outs = (lax.all_gather(both, axis, axis=dim, tiled=True), 0, [])  49.2 us
    all_to_all x1, waiting for transfers between devices, local(): lax.all_to_all(results, ('sp', 'tp'), split_axis=0, concat_axis=0, tiled=...  28.5 us
    all_to_all x1, waiting for transfers between devices, local(): lax.all_to_all(outbound, ('sp', 'tp'), split_axis=0, concat_axis=0, tiled...  23 us
    all_to_all x1, starting transfers between devices, local(): lax.all_to_all(outbound, ('sp', 'tp'), split_axis=0, concat_axis=0, tiled...  10.2 us
    slice x2, local copies, waits for them, and re-layouts, in_one_piece(): outs.append(lax.slice_in_dim(whole, at, at + a.shape[along], axis=along))  7.53 us
    dot_general x1, matrix products, local(): jnp.einsum('sech,ehd->secd', hidden, expert_down, preferred_element_type=...  7.08 us
    all_to_all x1, starting transfers between devices, local(): lax.all_to_all(results, ('sp', 'tp'), split_axis=0, concat_axis=0, tiled=...  6.84 us
  transfers between devices with their start and end apart: 5, of which 4 were waited for; matrix products, arithmetic and copies ran while one was open for 10% of the time, Pallas kernels for 0%

commit v1 on v0

v1 whole, which is shorter than its diff:
```python
import functools

import jax
import jax.numpy as jnp
from jax import lax
from jax.experimental import pallas as pl
from jax.experimental.pallas import tpu as pltpu
from jax.sharding import Mesh
from jax.sharding import PartitionSpec as P

SP = ("z", "y", "c")
NARROW_SIZE = 128
BROAD_SIZE = 256
LOG2E = 1.4426950408889634
MASKED = -1e30
EPSILON = 1e-06
ORDER = (0, 1, 3, 2)
BF = jnp.bfloat16
F32 = jnp.float32


def shift(x, axis, k):
    return lax.ppermute(x, axis, [(i, (i + k) % 4) for i in range(4)])


def swap_core(x):
    return lax.ppermute(x, "c", [(0, 1), (1, 0)])


def direct_ring(x, axis):
    return jnp.stack([x] + [shift(x, axis, k) for k in ORDER[1:]])


def halved_ring(g, axis):
    back = shift(g, axis, 1)
    ahead = shift(g, axis, 3)
    far_low = shift(back[:2], axis, 1)
    far_high = shift(ahead[2:], axis, 3)
    return back, ahead, far_low, far_high


def scatter_sum(partial):
    t = lax.axis_index("tp")
    rows, width = partial.shape[0] // 4, partial.shape[1] // 2

    def part(k, half):
        return lax.dynamic_slice(partial, (((t + k) % 4) * rows, half * width), (rows, width))

    far_a = shift(part(2, 0), "tp", 1)
    far_b = shift(part(2, 1), "tp", 3)
    near_b = shift(part(1, 1), "tp", 1)
    near_a = shift(part(3, 0), "tp", 3)
    sum_a = shift((part(1, 0).astype(F32) + far_a.astype(F32)).astype(BF), "tp", 1)
    sum_b = shift((part(3, 1).astype(F32) + far_b.astype(F32)).astype(BF), "tp", 3)
    low = part(0, 0).astype(F32) + sum_a.astype(F32) + near_a.astype(F32)
    high = part(0, 1).astype(F32) + sum_b.astype(F32) + near_b.astype(F32)
    return jnp.concatenate([low, high], axis=1)


def gather_rows(own):
    t = lax.axis_index("tp")
    rows, width = own.shape
    back = shift(own, "tp", 1)
    ahead = shift(own, "tp", 3)
    far_a = shift(back[:, : width // 2], "tp", 1)
    far_b = shift(ahead[:, width // 2 :], "tp", 3)
    far = jnp.concatenate([far_a, far_b], axis=1)
    out = jnp.zeros((4 * rows, width), own.dtype)
    for k, piece in ((0, own), (1, back), (2, far), (3, ahead)):
        out = lax.dynamic_update_slice(out, piece, (((t - k) % 4) * rows, 0))
    return out


def attend_kernel(counts, first, last, *refs):
    at = 0

    def take(n):
        nonlocal at
        at += n
        return refs[at - n : at]

    q_own, q_other, core = take(3)
    tiles = []
    for n, own_block in counts:
        tiles.append((take(n), take(1)[0], own_block))
    if not first:
        m_in, l_in, an_in, ab_in = take(4)
    if last:
        own_out, send_out = take(2)
    else:
        m_out, l_out, an_out, ab_out = take(4)

    def keys(ref, lo, hi):
        value = ref[..., lo:hi]
        return value.reshape(-1, hi - lo)

    results = {}
    for group, size, heads, lo in (("n", NARROW_SIZE, 4, 0), ("b", BROAD_SIZE, 2, 256)):
        scale = size**-0.5 * LOG2E
        base = 0 if group == "n" else 4
        row_base = 0 if group == "n" else 1024
        loaded = []
        for arrays, bias, own_block in tiles:
            k = jnp.concatenate([keys(r, lo, lo + size) for r in arrays], axis=0)
            v = jnp.concatenate([keys(r, lo + size, lo + 2 * size) for r in arrays], axis=0)
            loaded.append((k, v, bias, own_block))
        for side, q_ref in ((0, q_own), (1, q_other)):
            for h0 in range(0, heads, 2):
                col = (0 if group == "n" else 512) + h0 * size
                q = jnp.concatenate([q_ref[:, col + i * size : col + (i + 1) * size] for i in range(2)], axis=0)
                rows = row_base + side * heads * 128 + h0 * 128
                arow = rows - row_base
                scores = []
                for k, v, bias, own_block in loaded:
                    s = lax.dot_general(q, k, (((1,), (1,)), ((), ())), preferred_element_type=F32) * scale
                    n = k.shape[0]
                    b = bias[base + h0 : base + h0 + 2, :]
                    s = (s.reshape(2, 128, n) + b[:, None, :]).reshape(256, n)
                    if own_block:
                        qi = lax.broadcasted_iota(jnp.int32, (256, n), 0) % 128
                        ki = lax.broadcasted_iota(jnp.int32, (256, n), 1)
                        offset = 0 if side == 0 else 128 * (1 - 2 * core[0])
                        s = jnp.where(ki <= qi + offset, s, MASKED)
                    scores.append(s)
                m = functools.reduce(jnp.maximum, [jnp.max(s, axis=1, keepdims=True) for s in scores])
                if not first:
                    m_old = m_in[pl.ds(rows, 256), :][:, :1]
                    m = jnp.maximum(m, m_old)
                l = jnp.zeros((256, 1), F32)
                acc = jnp.zeros((256, size), F32)
                for s, (k, v, bias, own_block) in zip(scores, loaded):
                    p = jnp.exp2(s - m)
                    l = l + jnp.sum(p, axis=1, keepdims=True)
                    acc = acc + jnp.dot(p.astype(BF), v, preferred_element_type=F32)
                acc_in, acc_out = (None, None)
                if not first:
                    a_in = an_in if group == "n" else ab_in
                    factor = jnp.exp2(m_old - m)
                    l = l + l_in[pl.ds(rows, 256), :][:, :1] * factor
                    acc = acc + a_in[pl.ds(arow, 256), :] * factor
                if last:
                    out = own_out if side == 0 else send_out
                    o = acc / l
                    lse = m + jnp.log2(l)
                    for i in range(2):
                        out[:, col + i * size : col + (i + 1) * size] = o[i * 128 : (i + 1) * 128]
                        results[(side, base + h0 + i)] = lse[i * 128 : (i + 1) * 128]
                else:
                    a_out = an_out if group == "n" else ab_out
                    m_out[pl.ds(rows, 256), :] = jnp.broadcast_to(m, (256, 128))
                    l_out[pl.ds(rows, 256), :] = jnp.broadcast_to(l, (256, 128))
                    a_out[pl.ds(arow, 256), :] = acc
    if last:
        lane = lax.broadcasted_iota(jnp.int32, (128, 128), 1)
        for side, out in ((0, own_out), (1, send_out)):
            stats = jnp.zeros((128, 128), F32)
            for h in range(6):
                stats = jnp.where(lane == h, results[(side, h)], stats)
            out[:, 1024:1152] = stats


def attend(q_own, q_other, core, tiles, state, last):
    counts = tuple((len(arrays), own_block) for arrays, _, own_block in tiles)
    operands = [q_own, q_other, core]
    n_keys = 0
    for arrays, bias, _ in tiles:
        operands += list(arrays) + [bias]
        n_keys += bias.shape[1]
    vmem = pl.BlockSpec(memory_space=pltpu.VMEM)
    specs = [vmem] * len(operands)
    specs[2] = pl.BlockSpec(memory_space=pltpu.SMEM)
    if state is not None:
        operands += list(state)
        specs += [vmem] * 4
    if last:
        shapes = [jax.ShapeDtypeStruct((128, 1152), F32)] * 2
    else:
        shapes = [
            jax.ShapeDtypeStruct((1536, 128), F32),
            jax.ShapeDtypeStruct((1536, 128), F32),
            jax.ShapeDtypeStruct((1024, 128), F32),
            jax.ShapeDtypeStruct((512, 256), F32),
        ]
    return pl.pallas_call(
        functools.partial(attend_kernel, counts, state is None, last),
        out_shape=shapes,
        in_specs=specs,
        out_specs=[vmem] * len(shapes),
        compiler_params=pltpu.CompilerParams(vmem_limit_bytes=40 * 1024 * 1024),
        cost_estimate=pl.CostEstimate(
            flops=4 * n_keys * 256 * 1024, transcendentals=n_keys * 1536, bytes_accessed=4 * 1024 * 1024
        ),
    )(*operands)


def key_biases(gates_narrow, gates_broad, z, y, c):
    gates = jnp.concatenate([gates_narrow, gates_broad], axis=1) * (-LOG2E)
    gates = gates.reshape(4, 4, 2, 128, 6)
    gates = lax.dynamic_index_in_dim(gates, c, 2, keepdims=False).transpose(0, 1, 3, 2)
    planes = []
    for i in ORDER:
        zs = (z - i) % 4
        plane = lax.dynamic_index_in_dim(gates, zs, 0, keepdims=False)
        blocks = []
        for k in ORDER:
            ys = (y - k) % 4
            block = lax.dynamic_index_in_dim(plane, ys, 0, keepdims=False)
            blocks.append(jnp.where(zs * 4 + ys > z * 4 + y, MASKED, block))
        planes.append(jnp.stack(blocks))
    return jnp.stack(planes)


def flat_bias(*pieces):
    rows = [p.reshape(-1, 6, 64) for p in pieces]
    return jnp.concatenate(rows, axis=0).transpose(1, 0, 2).reshape(6, -1)


def local(
    query_narrow,
    key_narrow,
    value_narrow,
    gates_narrow,
    query_broad,
    key_broad,
    value_broad,
    gates_broad,
    project_narrow,
    project_broad,
    residual,
    norm_gain,
    route_ids,
    route_weight,
    expert_gate,
    expert_up,
    expert_down,
    shared_gate,
    shared_up,
    shared_down,
):
    z, y, c, t = (lax.axis_index(n) for n in ("z", "y", "c", "tp"))

    own_kv = jnp.concatenate([key_narrow, value_narrow, key_broad, value_broad], axis=1)
    plane_a = direct_ring(own_kv[:64], "y")
    plane_b = direct_ring(own_kv[64:], "z")
    q_own = jnp.concatenate([query_narrow, query_broad], axis=1)
    q_other = swap_core(q_own)
    a_back, a_ahead, a_far_low, a_far_high = halved_ring(plane_a, "z")
    b_back, b_ahead, b_far_low, b_far_high = halved_ring(plane_b, "y")

    bias = key_biases(gates_narrow, gates_broad, z, y, c)
    bias_a, bias_b = bias[..., :64], bias[..., 64:].swapaxes(0, 1)
    core = c.astype(jnp.int32).reshape(1)
    own_bias = bias[0, 0]

    state = attend(
        q_own,
        q_other,
        core,
        [
            ((own_kv,), own_bias, True),
            ((plane_a[1:], plane_b[1:]), flat_bias(bias_a[0, 1:], bias_b[0, 1:]), False),
        ],
        None,
        False,
    )
    state = attend(
        q_own,
        q_other,
        core,
        [
            ((a_back, a_ahead), flat_bias(bias_a[1], bias_a[2]), False),
            ((b_back, b_ahead), flat_bias(bias_b[1], bias_b[2]), False),
        ],
        state,
        False,
    )
    own_part, send_part = attend(
        q_own,
        q_other,
        core,
        [
            (
                (a_far_low, a_far_high, b_far_low, b_far_high),
                flat_bias(bias_a[3], bias_b[3]),
                False,
            ),
        ],
        state,
        True,
    )
    other_part = swap_core(send_part)
    lse_own, lse_other = own_part[:, 1024:1030], other_part[:, 1024:1030]
    top = jnp.maximum(lse_own, lse_other)
    w_own, w_other = jnp.exp2(lse_own - top), jnp.exp2(lse_other - top)
    total = w_own + w_other
    w_own, w_other = w_own / total, w_other / total

    def spread(w):
        n = jnp.broadcast_to(w[:, :4, None], (128, 4, 128)).reshape(128, 512)
        b = jnp.broadcast_to(w[:, 4:, None], (128, 2, 256)).reshape(128, 512)
        return jnp.concatenate([n, b], axis=1)

    attn = (own_part[:, :1024] * spread(w_own) + other_part[:, :1024] * spread(w_other)).astype(BF)
    head_part = jnp.dot(attn[:, :512], project_narrow, preferred_element_type=F32)
    head_part = head_part + jnp.dot(attn[:, 512:], project_broad, preferred_element_type=F32)
    mixture = scatter_sum(head_part.astype(BF))

    line_ids = lax.all_gather(route_ids, "tp", axis=0, tiled=True)
    line_weight = lax.all_gather(route_weight.astype(BF).astype(F32), "tp", axis=0, tiled=True)
    tokens = line_ids.shape[0]
    experts = jnp.arange(32, dtype=jnp.int32) * 4 + t
    hit = line_ids[:, :, None] == experts[None, None, :]
    named = jnp.any(hit, axis=1)
    weight_of = jnp.sum(jnp.where(hit, line_weight[:, :, None], 0.0), axis=1)
    before = jnp.tril(jnp.ones((tokens, tokens), BF), -1)
    slot_of = jnp.dot(before, named.astype(BF), preferred_element_type=F32).astype(jnp.int32)
    taken = named[:, :, None] & (slot_of[:, :, None] == jnp.arange(8, dtype=jnp.int32))
    taken = taken.reshape(tokens, 256)
    dispatch = taken.astype(BF).T
    combiner = jnp.where(taken, jnp.repeat(weight_of, 8, axis=1), 0.0).astype(BF)

    sub_rows = route_ids.shape[0]
    own_rows = lax.dynamic_slice_in_dim(residual, t * sub_rows, sub_rows, 0)
    stream = own_rows.astype(F32) + mixture
    normed = stream * lax.rsqrt(jnp.mean(stream * stream, axis=-1, keepdims=True) + EPSILON) * norm_gain
    line_normed = gather_rows(normed.astype(BF))

    outbound = jnp.dot(dispatch, line_normed, preferred_element_type=F32).astype(BF)
    inbound = lax.all_to_all(outbound.reshape(32, 8, -1), SP, 0, 0, tiled=True).reshape(256, -1)

    gate = jnp.dot(line_normed, shared_gate, preferred_element_type=F32)
    up = jnp.dot(line_normed, shared_up, preferred_element_type=F32)
    shared_hidden = (jax.nn.silu(gate) * up).astype(BF)
    shared = jnp.dot(shared_hidden, shared_down, preferred_element_type=F32)

    gate = jnp.dot(inbound, expert_gate[0], preferred_element_type=F32)
    up = jnp.dot(inbound, expert_up[0], preferred_element_type=F32)
    hidden = (jax.nn.silu(gate) * up).astype(BF)
    result = jnp.dot(hidden, expert_down[0], preferred_element_type=F32).astype(BF)
    returned = lax.all_to_all(result.reshape(32, 8, -1), SP, 0, 0, tiled=True).reshape(256, -1)
    routed = jnp.dot(combiner, returned, preferred_element_type=F32)
    return (stream + scatter_sum((routed + shared).astype(BF))).astype(BF)


def solution(mesh):
    mesh = Mesh(mesh.devices.reshape(4, 4, 2, 4), ("z", "y", "c", "tp"))
    every = SP + ("tp",)
    placed = (
        P(SP, "tp"),
        P(SP, "tp"),
        P(SP, "tp"),
        P(None, "tp"),
        P(SP, "tp"),
        P(SP, "tp"),
        P(SP, "tp"),
        P(None, "tp"),
        P("tp", None),
        P("tp", None),
        P(SP, None),
        P(),
        P(every, None),
        P(every, None),
        P(every, None, None),
        P(every, None, None),
        P(every, None, None),
        P(None, "tp"),
        P(None, "tp"),
        P("tp", None),
    )
    return jax.shard_map(local, mesh=mesh, in_specs=placed, out_specs=P(every, None), check_vma=False)
```

time: 301 us -> 224 us (0.74)
  waiting for transfers between devices: 195 us -> 44.9 us
  blocking collectives: 0 us -> 53.6 us
  starting transfers between devices: 20.7 us -> 50.8 us
  between operations: 13.7 us -> 0.62 us
  other arithmetic: 7.44 us -> 19.6 us
  matrix products: 33.2 us -> 22 us
  Pallas kernels: 0 us -> 10.6 us
  local copies, waits for them, and re-layouts: 27.3 us -> 20.8 us
    psum x1 -> x0, waiting for transfers between devices: 94.2 us -> none  [local(): lax.psum(partial_value.astype(jnp.bfloat16), 'tp').astype(jnp.float32)]
    all_gather x1 -> x0, waiting for transfers between devices: 49.2 us -> none  [in_one_piece(): whole, at, outs = (lax.all_gather(both, axis, axis=dim, tiled=True), 0, [])]
    ppermute x0 -> x32, starting transfers between devices: none -> 45.9 us  [the longest x30 45.9 us: shift(): return lax.ppermute(x, axis, [(i, (i + k) % 4) for i in range(4)])]
    all_to_all x3 -> x1, waiting for transfers between devices: 51.5 us -> 16.3 us  [local(): lax.all_to_all(result.reshape(32, 8, -1), SP, 0, 0, tiled=True)]
    all_to_all x0 -> x1, blocking collectives: none -> 32.3 us  [local(): lax.all_to_all(outbound.reshape(32, 8, -1), SP, 0, 0, tiled=True)]
    ppermute x0 -> x32, waiting for transfers between devices: none -> 28.6 us  [the longest x30 26.2 us: shift(): return lax.ppermute(x, axis, [(i, (i + k) % 4) for i in range(4)])]
    all_gather x0 -> x2, blocking collectives: none -> 21.4 us  [the longest x1 10.9 us: local(): lax.all_gather(route_weight.astype(BF).astype(F32), 'tp', axis=0, tiled=T...]
    all_to_all x3 -> x1, starting transfers between devices: 20.7 us -> 4.9 us  [local(): lax.all_to_all(result.reshape(32, 8, -1), SP, 0, 0, tiled=True)]
  transfers between devices with their start and end apart: 5 -> 33, of which waited for: 4 -> 13; matrix products, arithmetic and copies ran while one was open for 10% -> 10% of each run, Pallas kernels for 0% -> 3%
where the time goes in v1:
time: 224 us; the launch traced here: 223 us
  blocking collectives  53.6 us (24%)
  starting transfers between devices  50.8 us (23%)
  waiting for transfers between devices  44.9 us (20%)
  matrix products  22 us (10%)
  local copies, waits for them, and re-layouts  20.8 us (9%)
  other arithmetic  19.6 us (9%)
  Pallas kernels  10.6 us (5%)
    ppermute x30, starting transfers between devices, shift(): return lax.ppermute(x, axis, [(i, (i + k) % 4) for i in range(4)])  45.9 us
    all_to_all x1, blocking collectives, local(): lax.all_to_all(outbound.reshape(32, 8, -1), SP, 0, 0, tiled=True)  32.3 us
    ppermute x30, waiting for transfers between devices, shift(): return lax.ppermute(x, axis, [(i, (i + k) % 4) for i in range(4)])  26.2 us
    all_to_all x1, waiting for transfers between devices, local(): lax.all_to_all(result.reshape(32, 8, -1), SP, 0, 0, tiled=True)  16.3 us
    all_gather x1, blocking collectives, local(): lax.all_gather(route_weight.astype(BF).astype(F32), 'tp', axis=0, tiled=T...  10.9 us
    pallas_call x3, Pallas kernels, attend(): pl.pallas_call(functools.partial(attend_kernel, counts, state is None, la...  10.6 us
    all_gather x1, blocking collectives, local(): line_ids = lax.all_gather(route_ids, 'tp', axis=0, tiled=True)  10.4 us
    unnamed x64, local copies, waits for them, and re-layouts  6.11 us
  transfers between devices with their start and end apart: 33, of which 13 were waited for; matrix products, arithmetic and copies ran while one was open for 10% of the time, Pallas kernels for 3%

profile of v1, /device:TPU:0, one launch (start us, length us, event | category | flops | bytes accessed | tf_op | source)
XLA Modules:
  0.0 222.9 jit_solution(1501685362041328739)
XLA Ops:
  4.8 1.7 collective-permute-start.1
  6.5 1.5 collective-permute-start.2
  8.0 2.0 collective-permute-start.8
  10.0 2.1 collective-permute-start.9
  12.2 1.9 collective-permute-start.10
  15.3 2.1 collective-permute-start.3
  20.1 2.9 %collective-permute-start.13 = (bf16[4,64,768]{2,1,0:T(8,128)(2,1)}, bf16[4,64,768]{2,1,0:T(8,128)(2,1)S(1)}, u32[]{:S(2)}, u32[]{:S(2)}) collective-permute-start(bf16[4,64,768]{2,1,0:T(8,128)(2,1)} %pad_maximum_fusion.1), channel_id=1, source_target_pairs={{0,24},{8,0},{16,8},{24,16},{1,25},{9,1},{17,9},{25,17},{2,26},{10... | collective-permute-start | bytes 1179656 | tf_op jit(solution)/shard_map/ppermute | solution.py:23
  23.0 1.8 pad_maximum_fusion
  25.4 2.7 %collective-permute-start.6 = (bf16[4,64,768]{2,1,0:T(8,128)(2,1)}, bf16[4,64,768]{2,1,0:T(8,128)(2,1)}, u32[]{:S(2)}, u32[]{:S(2)}) collective-permute-start(bf16[4,64,768]{2,1,0:T(8,128)(2,1)} %pad_maximum_fusion), channel_id=1, source_target_pairs={{0,96},{32,0},{64,32},{96,64},{1,97},{33,1},{65,33},{97,65},{2,98}... | collective-permute-start | bytes 1179656 | tf_op jit(solution)/shard_map/ppermute | solution.py:23
  32.4 1.1 pad_maximum_fusion.2.refs_5_
  33.7 3.3 %collective-permute-start.14 = (bf16[2,64,768]{2,1,0:T(8,128)(2,1)S(1)}, bf16[2,64,768]{2,1,0:T(8,128)(2,1)S(1)}, u32[]{:S(2)}, u32[]{:S(2)}) collective-permute-start(bf16[2,64,768]{2,1,0:T(8,128)(2,1)S(1)} %slice.130), channel_id=1, source_target_pairs={{0,24},{8,0},{16,8},{24,16},{1,25},{9,1},{17,9},{25,17},{2,26},{10... | collective-permute-start | bytes 589832 | tf_op jit(solution)/shard_map/ppermute | solution.py:23
  38.9 3.5 %collective-permute-start.7 = (bf16[2,64,768]{2,1,0:T(8,128)(2,1)S(1)}, bf16[2,64,768]{2,1,0:T(8,128)(2,1)S(1)}, u32[]{:S(2)}, u32[]{:S(2)}) collective-permute-start(bf16[2,64,768]{2,1,0:T(8,128)(2,1)S(1)} %slice.127), channel_id=1, source_target_pairs={{0,96},{32,0},{64,32},{96,64},{1,97},{33,1},{65,33},{97,65},{2,98}... | collective-permute-start | bytes 589832 | tf_op jit(solution)/shard_map/ppermute | solution.py:23
  42.5 2.3 %shard_map.190 = (f32[1536,128]{1,0:T(8,128)S(1)}, f32[1536,128]{1,0:T(8,128)S(1)}, f32[1024,128]{1,0:T(8,128)S(1)}, f32[512,256]{1,0:T(8,128)S(1)}) custom-call(bf16[128,1024]{1,0:T(8,128)(2,1)S(1)} %constant_dynamic-update-slice_fusion.refs_0_, bf16[128,1024]{1,0:T(8,128)(2,1)S(1)} %collective-permute-done.refs_1_, s32[1]{0:T(128)} %bitcast.refs_2_, ...), custom_call_target="tpu_custom_call" | custom-call | flops 536870912 | bytes 4194304 | tf_op jit(solution)/shard_map/pallas_call | solution.py:184
  44.7 4.9 %shard_map.191 = (f32[1536,128]{1,0:T(8,128)S(1)}, f32[1536,128]{1,0:T(8,128)S(1)}, f32[1024,128]{1,0:T(8,128)S(1)}, f32[512,256]{1,0:T(8,128)S(1)}) custom-call(bf16[128,1024]{1,0:T(8,128)(2,1)S(1)} %constant_dynamic-update-slice_fusion.refs_0_, bf16[128,1024]{1,0:T(8,128)(2,1)S(1)} %collective-permute-done.refs_1_, s32[1]{0:T(128)} %bitcast.refs_2_, ...), custom_call_target="tpu_custom_call" | custom-call | flops 1073741824 | bytes 4194304 | tf_op jit(solution)/shard_map/pallas_call | solution.py:184
  49.7 3.4 %shard_map.192 = (f32[128,1152]{1,0:T(8,128)S(1)}, f32[128,1152]{1,0:T(8,128)}) custom-call(bf16[128,1024]{1,0:T(8,128)(2,1)S(1)} %constant_dynamic-update-slice_fusion.refs_0_, bf16[128,1024]{1,0:T(8,128)(2,1)S(1)} %collective-permute-done.refs_1_, s32[1]{0:T(128)} %bitcast.refs_2_, bf16[2,64,768]{2,1,0:T(8,128)(2,1)S(1)} %collective-permute-done.5.refs_3_, ...), custom_call_target="tpu_custom_call" | custom-call | flops 536870912 | bytes 4194304 | tf_op jit(solution)/shard_map/pallas_call | solution.py:184
  53.1 2.3 %collective-permute-done.15 = f32[128,1152]{1,0:T(8,128)} collective-permute-done((f32[128,1152]{1,0:T(8,128)}, f32[128,1152]{1,0:T(8,128)}, u32[]{:S(2)}, u32[]{:S(2)}) %collective-permute-start.15) | collective-permute-done | bytes 589856 | tf_op jit(solution)/shard_map/ppermute | solution.py:27
  57.4 1.4 fusion.26
  60.0 1.5 copy-done.3
  62.9 1.5 collective-permute-start.16
  64.4 1.7 collective-permute-start.18
  66.2 1.6 collective-permute-start.19
  67.7 2.0 collective-permute-done.16
  70.6 1.5 collective-permute-start.21
  72.8 5.2 %collective-permute-done.17 = bf16[32,2048]{1,0:T(8,128)(2,1)} collective-permute-done((bf16[32,2048]{1,0:T(8,128)(2,1)}, bf16[32,2048]{1,0:T(8,128)(2,1)}, u32[]{:S(2)}, u32[]{:S(2)}) %collective-permute-start.17) | collective-permute-done | bytes 131104 | tf_op jit(solution)/shard_map/ppermute | solution.py:23
  77.9 1.8 convert_add_fusion.3
  80.1 10.4 %all-gather = s32[4,32,4]{1,2,0:T(4,128)S(1)} all-gather(s32[1,32,4]{1,2,0:T(4,128)S(1)} %bitcast.239), channel_id=1, replica_groups=mesh['z'=4,'y'=4,'c'=2,'tp'=4] {'tp'}, dimensions={0}, use_global_device_ids=true | all-gather | bytes 2560 | tf_op jit(solution)/shard_map/all_gather | solution.py:308
  92.3 1.2 multiply_reduce_fusion
  93.7 1.8 constant_dynamic-update-slice_fusion.8
  95.5 1.4 collective-permute-start.22
  96.9 1.8 collective-permute-start.24
  99.0 5.7 %collective-permute-done.22 = bf16[32,4096]{1,0:T(8,128)(2,1)} collective-permute-done((bf16[32,4096]{1,0:T(8,128)(2,1)}, bf16[32,4096]{1,0:T(8,128)(2,1)}, u32[]{:S(2)}, u32[]{:S(2)}) %collective-permute-start.22) | collective-permute-done | bytes 262176 | tf_op jit(solution)/shard_map/ppermute | solution.py:23
  106.9 3.1 %collective-permute-start.25 = (bf16[32,2048]{1,0:T(8,128)(2,1)S(1)}, bf16[32,2048]{1,0:T(8,128)(2,1)S(1)}, u32[]{:S(2)}, u32[]{:S(2)}) collective-permute-start(bf16[32,2048]{1,0:T(8,128)(2,1)S(1)} %slice.149), channel_id=1, source_target_pairs={{0,3},{1,0},{2,1},{3,2},{4,7},{5,4},{6,5},{7,6},{8,11},{9,8},{10,9... | collective-permute-start | bytes 393224 | tf_op jit(solution)/shard_map/ppermute | solution.py:23
  114.3 32.3 %all_to_all.10 = bf16[32,8,4096]{2,1,0:T(8,128)(2,1)} all-to-all(bf16[32,8,4096]{2,1,0:T(8,128)(2,1)S(1)} %fusion.1), channel_id=1, replica_groups=mesh['z'=4,'y'=4,'c'=2,'tp'=4] {'z','y','c'}, dimensions={0} | all-to-all | bytes 4194304 | tf_op jit(solution)/shard_map/all_to_all | solution.py:329
  146.5 3.0 %fusion.7 = f32[256,256]{1,0:T(8,128)} fusion(bf16[1,4096,256]{2,1,0:T(8,128)(2,1)S(1)} %copy-done.7, bf16[32,8,4096]{2,1,0:T(8,128)(2,1)} %all_to_all.10), kind=kOutput, calls=%fused_computation.12 | convolution fusion | flops 536870912 | bytes 4456448 | tf_op jit(solution)/shard_map/dot_general | solution.py:336
  149.5 6.0 %fusion = bf16[32,8,4096]{2,1,0:T(8,128)(2,1)} fusion(bf16[1,256,4096]{2,1,0:T(8,128)(2,1)S(1)} %copy-done, bf16[1,4096,256]{2,1,0:T(8,128)(2,1)} %param.35, bf16[32,8,4096]{2,1,0:T(8,128)(2,1)} %all_to_all.10, f32[256,256]{1,0:T(8,128)} %fusion.7), kind=kOutput, calls=%fused_computation.2 | convolution fusion | flops 1075183616 | bytes 8650752 | tf_op jit(solution)/shard_map/dot_general | solution.py:339
  155.5 4.9 %all-to-all-start.1 = ((bf16[32,8,4096]{2,1,0:T(8,128)(2,1)}), bf16[32,8,4096]{2,1,0:T(8,128)(2,1)}, u32[]{:S(2)}, u32[]{:S(2)}) async-start(bf16[32,8,4096]{2,1,0:T(8,128)(2,1)} %fusion), calls=%async_computation.1 | async-start | bytes 4194304 | tf_op jit(solution)/shard_map/all_to_all | solution.py:340
  160.4 10.9 %all-gather.1 = f32[4,32,4]{1,2,0:T(4,128)S(1)} all-gather(f32[1,32,4]{1,2,0:T(4,128)S(1)} %bitcast_convert_fusion), channel_id=1, replica_groups=mesh['z'=4,'y'=4,'c'=2,'tp'=4] {'tp'}, dimensions={0}, use_global_device_ids=true | all-gather | bytes 2560 | tf_op jit(solution)/shard_map/all_gather | solution.py:309
  172.1 2.0 fusion.98
  174.2 16.3 %all-to-all-done.1 = bf16[32,8,4096]{2,1,0:T(8,128)(2,1)} async-done(((bf16[32,8,4096]{2,1,0:T(8,128)(2,1)}), bf16[32,8,4096]{2,1,0:T(8,128)(2,1)}, u32[]{:S(2)}, u32[]{:S(2)}) %all-to-all-start.1) | async-done | bytes 2097184 | tf_op jit(solution)/shard_map/all_to_all | solution.py:340
  190.5 3.5 %convolution_bitcast_fusion = f32[128,4096]{1,0:T(8,128)} fusion(bf16[32,8,4096]{2,1,0:T(8,128)(2,1)} %all-to-all-done.1, bf16[128,32]{0,1:T(8,128)(2,1)} %fusion.41, s32[128,32]{0,1:T(8,128)S(1)} %convolution_convert_fusion.2, pred[128,32]{0,1:T(8,128)(4,1)} %compare_reduce_fusion), kind=kOutput, calls=%fused_computation.5 | convolution fusion | flops 268533760 | bytes 4222976 | tf_op jit(solution)/shard_map/dot_general | solution.py:341
  193.9 5.2 %fusion.3 = bf16[128,4096]{1,0:T(8,128)(2,1)} fusion(f32[128,4096]{1,0:T(8,128)} %convolution_bitcast_fusion, bf16[256,4096]{1,0:T(8,128)(2,1)} %param.39, f32[128,256]{1,0:T(8,128)S(1)} %fusion.98, bf16[128,4096]{1,0:T(8,128)(2,1)S(1)} %constant_dynamic-update-slice_fusion.6, bf16[4096,256]{1,0:T(8,128)(2,1)} %param.38), kind=kOutput, calls=%fused_computation.8 | convolution fusion | flops 538116096 | bytes 8519680 | tf_op jit(solution)/shard_map/dot_general | solution.py:334
  199.1 1.2 constant_dynamic-slice_fusion.1
  200.4 3.7 %collective-permute-start.28 = (bf16[32,2048]{1,0:T(8,128)(2,1)S(1)}, bf16[32,2048]{1,0:T(8,128)(2,1)S(1)}, u32[]{:S(2)}, u32[]{:S(2)}) collective-permute-start(bf16[32,2048]{1,0:T(8,128)(2,1)S(1)} %get-tuple-element.34), channel_id=1, source_target_pairs={{0,3},{1,0},{2,1},{3,2},{4,7},{5,4},{6,5},{7,6},{8,11},{9,8},{10,9... | collective-permute-start | bytes 393224 | tf_op jit(solution)/shard_map/ppermute | solution.py:23
  204.1 1.9 collective-permute-start.29
  209.1 5.1 %collective-permute-done.27 = bf16[32,2048]{1,0:T(8,128)(2,1)S(1)} collective-permute-done((bf16[32,2048]{1,0:T(8,128)(2,1)S(1)}, bf16[32,2048]{1,0:T(8,128)(2,1)S(1)}, u32[]{:S(2)}, u32[]{:S(2)}) %collective-permute-start.27) | collective-permute-done | bytes 131104 | tf_op jit(solution)/shard_map/ppermute | solution.py:23
  214.2 1.0 convert_add_fusion.1
  216.1 4.2 %collective-permute-done.30 = bf16[32,2048]{1,0:T(8,128)(2,1)S(1)} collective-permute-done((bf16[32,2048]{1,0:T(8,128)(2,1)S(1)}, bf16[32,2048]{1,0:T(8,128)(2,1)S(1)}, u32[]{:S(2)}, u32[]{:S(2)}) %collective-permute-start.30) | collective-permute-done | bytes 131104 | tf_op jit(solution)/shard_map/ppermute | solution.py:23
  221.2 1.7 fusion.27
  (169 shorter events, 36.5 us)
Async XLA Ops:
  0.0 149.5 %copy-start = (bf16[1,256,4096]{2,1,0:T(8,128)(2,1)S(1)}, bf16[1,256,4096]{2,1,0:T(8,128)(2,1)}, u32[]{:S(2)}) copy-start(bf16[1,256,4096]{2,1,0:T(8,128)(2,1)} %param.36) | copy-start | bytes 6291460
  0.0 15.3 %copy-start.17 = (bf16[128,512]{1,0:T(8,128)(2,1)S(1)}, bf16[128,512]{1,0:T(8,128)(2,1)}, u32[]{:S(2)}) copy-start(bf16[128,512]{1,0:T(8,128)(2,1)} %param.20) | copy-start | bytes 393220
  0.0 15.3 %copy-start.18 = (bf16[128,512]{1,0:T(8,128)(2,1)S(1)}, bf16[128,512]{1,0:T(8,128)(2,1)}, u32[]{:S(2)}) copy-start(bf16[128,512]{1,0:T(8,128)(2,1)} %param.24) | copy-start | bytes 393220
  4.8 15.4 %collective-permute-start.1 = (bf16[64,768]{1,0:T(8,128)(2,1)}, bf16[64,768]{1,0:T(8,128)(2,1)}, u32[]{:S(2)}, u32[]{:S(2)}) collective-permute-start(bf16[64,768]{1,0:T(8,128)(2,1)} %get-tuple-element.44), channel_id=1, source_target_pairs={{0,8},{8,16},{16,24},{24,0},{1,9},{9,17},{17,25},{25,1},{2,10},{10... | collective-permute-start | bytes 294920 | tf_op jit(solution)/shard_map/ppermute | solution.py:23
  6.5 16.6 %collective-permute-start.2 = (bf16[64,768]{1,0:T(8,128)(2,1)}, bf16[64,768]{1,0:T(8,128)(2,1)}, u32[]{:S(2)}, u32[]{:S(2)}) collective-permute-start(bf16[64,768]{1,0:T(8,128)(2,1)} %get-tuple-element.44), channel_id=1, source_target_pairs={{0,24},{8,0},{16,8},{24,16},{1,25},{9,1},{17,9},{25,17},{2,26},{10... | collective-permute-start | bytes 294920 | tf_op jit(solution)/shard_map/ppermute | solution.py:23
  8.0 7.3 %collective-permute-start.8 = (bf16[64,768]{1,0:T(8,128)(2,1)S(1)}, bf16[64,768]{1,0:T(8,128)(2,1)S(1)}, u32[]{:S(2)}, u32[]{:S(2)}) collective-permute-start(bf16[64,768]{1,0:T(8,128)(2,1)S(1)} %get-tuple-element.43), channel_id=1, source_target_pairs={{0,32},{32,64},{64,96},{96,0},{1,33},{33,65},{65,97},{97,1},{2,34}... | collective-permute-start | bytes 294920 | tf_op jit(solution)/shard_map/ppermute | solution.py:23
  10.0 7.4 %collective-permute-start.9 = (bf16[64,768]{1,0:T(8,128)(2,1)S(1)}, bf16[64,768]{1,0:T(8,128)(2,1)S(1)}, u32[]{:S(2)}, u32[]{:S(2)}) collective-permute-start(bf16[64,768]{1,0:T(8,128)(2,1)S(1)} %get-tuple-element.43), channel_id=1, source_target_pairs={{0,96},{32,0},{64,32},{96,64},{1,97},{33,1},{65,33},{97,65},{2,98}... | collective-permute-start | bytes 294920 | tf_op jit(solution)/shard_map/ppermute | solution.py:23
  12.2 6.2 %collective-permute-start.10 = (bf16[64,768]{1,0:T(8,128)(2,1)S(1)}, bf16[64,768]{1,0:T(8,128)(2,1)S(1)}, u32[]{:S(2)}, u32[]{:S(2)}) collective-permute-start(bf16[64,768]{1,0:T(8,128)(2,1)S(1)} %get-tuple-element.43), channel_id=1, source_target_pairs={{0,64},{32,96},{64,0},{96,32},{1,65},{33,97},{65,1},{97,33},{2,66}... | collective-permute-start | bytes 294920 | tf_op jit(solution)/shard_map/ppermute | solution.py:23
  14.0 9.0 %copy-start.14 = (bf16[1,64,768]{2,1,0:T(8,128)(2,1)S(1)}, bf16[1,64,768]{2,1,0:T(8,128)(2,1)}, u32[]{:S(2)}) copy-start(bf16[1,64,768]{2,1,0:T(8,128)(2,1)} %get-tuple-element.42) | copy-start | bytes 294916
  15.3 7.7 %collective-permute-start.3 = (bf16[64,768]{1,0:T(8,128)(2,1)}, bf16[64,768]{1,0:T(8,128)(2,1)S(1)}, u32[]{:S(2)}, u32[]{:S(2)}) collective-permute-start(bf16[64,768]{1,0:T(8,128)(2,1)} %get-tuple-element.44), channel_id=1, source_target_pairs={{0,16},{8,24},{16,0},{24,8},{1,17},{9,25},{17,1},{25,9},{2,18},{10... | collective-permute-start | bytes 294920 | tf_op jit(solution)/shard_map/ppermute | solution.py:23
  17.4 25.0 %collective-permute-start = (bf16[128,1024]{1,0:T(8,128)(2,1)S(1)}, bf16[128,1024]{1,0:T(8,128)(2,1)S(1)}, u32[]{:S(2)}, u32[]{:S(2)}) collective-permute-start(bf16[128,1024]{1,0:T(8,128)(2,1)S(1)} %constant_dynamic-update-slice_fusion.refs_0_), channel_id=1, source_target_pairs={{0,4},{4,0},{1,5},{5,1},{2,6},{6,2},{3,7},{7,3},{8,12},{12,8},{9,1... | collective-permute-start | bytes 786440 | tf_op jit(solution)/shard_map/ppermute | solution.py:27
  19.8 13.8 %collective-permute-start.11 = (bf16[4,64,768]{2,1,0:T(8,128)(2,1)}, bf16[4,64,768]{2,1,0:T(8,128)(2,1)S(1)}, u32[]{:S(2)}, u32[]{:S(2)}) collective-permute-start(bf16[4,64,768]{2,1,0:T(8,128)(2,1)} %pad_maximum_fusion.1), channel_id=1, source_target_pairs={{0,8},{8,16},{16,24},{24,0},{1,9},{9,17},{17,25},{25,1},{2,10},{10... | collective-permute-start | bytes 1179656 | tf_op jit(solution)/shard_map/ppermute | solution.py:23
  20.1 13.5 %collective-permute-start.13 = (bf16[4,64,768]{2,1,0:T(8,128)(2,1)}, bf16[4,64,768]{2,1,0:T(8,128)(2,1)S(1)}, u32[]{:S(2)}, u32[]{:S(2)}) collective-permute-start(bf16[4,64,768]{2,1,0:T(8,128)(2,1)} %pad_maximum_fusion.1), channel_id=1, source_target_pairs={{0,24},{8,0},{16,8},{24,16},{1,25},{9,1},{17,9},{25,17},{2,26},{10... | collective-permute-start | bytes 1179656 | tf_op jit(solution)/shard_map/ppermute | solution.py:23
  24.8 12.1 %collective-permute-start.4 = (bf16[4,64,768]{2,1,0:T(8,128)(2,1)}, bf16[4,64,768]{2,1,0:T(8,128)(2,1)}, u32[]{:S(2)}, u32[]{:S(2)}) collective-permute-start(bf16[4,64,768]{2,1,0:T(8,128)(2,1)} %pad_maximum_fusion), channel_id=1, source_target_pairs={{0,32},{32,64},{64,96},{96,0},{1,33},{33,65},{65,97},{97,1},{2,34}... | collective-permute-start | bytes 1179656 | tf_op jit(solution)/shard_map/ppermute | solution.py:23
  25.4 12.6 %collective-permute-start.6 = (bf16[4,64,768]{2,1,0:T(8,128)(2,1)}, bf16[4,64,768]{2,1,0:T(8,128)(2,1)}, u32[]{:S(2)}, u32[]{:S(2)}) collective-permute-start(bf16[4,64,768]{2,1,0:T(8,128)(2,1)} %pad_maximum_fusion), channel_id=1, source_target_pairs={{0,96},{32,0},{64,32},{96,64},{1,97},{33,1},{65,33},{97,65},{2,98}... | collective-permute-start | bytes 1179656 | tf_op jit(solution)/shard_map/ppermute | solution.py:23
  32.4 10.0 %copy-start.9 = (bf16[64,768]{1,0:T(8,128)(2,1)S(1)}, bf16[64,768]{1,0:T(8,128)(2,1)}, u32[]{:S(2)}) copy-start(bf16[64,768]{1,0:T(8,128)(2,1)} %copy-done.8) | copy-start | bytes 294916
  32.4 10.0 %copy-start.11 = (bf16[64,768]{1,0:T(8,128)(2,1)S(1)}, bf16[64,768]{1,0:T(8,128)(2,1)}, u32[]{:S(2)}) copy-start(bf16[64,768]{1,0:T(8,128)(2,1)} %copy-done.10) | copy-start | bytes 294916
  32.4 10.0 %copy-start.13 = (bf16[64,768]{1,0:T(8,128)(2,1)S(1)}, bf16[64,768]{1,0:T(8,128)(2,1)}, u32[]{:S(2)}) copy-start(bf16[64,768]{1,0:T(8,128)(2,1)} %copy-done.12) | copy-start | bytes 294916
  32.4 10.0 %copy-start.2 = (bf16[128,768]{1,0:T(8,128)(2,1)S(1)}, bf16[128,768]{1,0:T(8,128)(2,1)}, u32[]{:S(2)}) copy-start(bf16[128,768]{1,0:T(8,128)(2,1)} %copy-done.1) | copy-start | bytes 589828
  33.6 16.1 %collective-permute-start.12 = (bf16[2,64,768]{2,1,0:T(8,128)(2,1)S(1)}, bf16[2,64,768]{2,1,0:T(8,128)(2,1)S(1)}, u32[]{:S(2)}, u32[]{:S(2)}) collective-permute-start(bf16[2,64,768]{2,1,0:T(8,128)(2,1)S(1)} %slice.129), channel_id=1, source_target_pairs={{0,8},{8,16},{16,24},{24,0},{1,9},{9,17},{17,25},{25,1},{2,10},{10... | collective-permute-start | bytes 589832 | tf_op jit(solution)/shard_map/ppermute | solution.py:23
  33.7 16.0 %collective-permute-start.14 = (bf16[2,64,768]{2,1,0:T(8,128)(2,1)S(1)}, bf16[2,64,768]{2,1,0:T(8,128)(2,1)S(1)}, u32[]{:S(2)}, u32[]{:S(2)}) collective-permute-start(bf16[2,64,768]{2,1,0:T(8,128)(2,1)S(1)} %slice.130), channel_id=1, source_target_pairs={{0,24},{8,0},{16,8},{24,16},{1,25},{9,1},{17,9},{25,17},{2,26},{10... | collective-permute-start | bytes 589832 | tf_op jit(solution)/shard_map/ppermute | solution.py:23
  37.9 11.8 %collective-permute-start.5 = (bf16[2,64,768]{2,1,0:T(8,128)(2,1)S(1)}, bf16[2,64,768]{2,1,0:T(8,128)(2,1)S(1)}, u32[]{:S(2)}, u32[]{:S(2)}) collective-permute-start(bf16[2,64,768]{2,1,0:T(8,128)(2,1)S(1)} %slice.126), channel_id=1, source_target_pairs={{0,32},{32,64},{64,96},{96,0},{1,33},{33,65},{65,97},{97,1},{2,34}... | collective-permute-start | bytes 589832 | tf_op jit(solution)/shard_map/ppermute | solution.py:23
  38.9 10.8 %collective-permute-start.7 = (bf16[2,64,768]{2,1,0:T(8,128)(2,1)S(1)}, bf16[2,64,768]{2,1,0:T(8,128)(2,1)S(1)}, u32[]{:S(2)}, u32[]{:S(2)}) collective-permute-start(bf16[2,64,768]{2,1,0:T(8,128)(2,1)S(1)} %slice.127), channel_id=1, source_target_pairs={{0,96},{32,0},{64,32},{96,64},{1,97},{33,1},{65,33},{97,65},{2,98}... | collective-permute-start | bytes 589832 | tf_op jit(solution)/shard_map/ppermute | solution.py:23
  53.1 2.3 %collective-permute-start.15 = (f32[128,1152]{1,0:T(8,128)}, f32[128,1152]{1,0:T(8,128)}, u32[]{:S(2)}, u32[]{:S(2)}) collective-permute-start(f32[128,1152]{1,0:T(8,128)} %get-tuple-element.24), channel_id=1, source_target_pairs={{0,4},{4,0},{1,5},{5,1},{2,6},{6,2},{3,7},{7,3},{8,12},{12,8},{9,1... | collective-permute-start | bytes 1769480 | tf_op jit(solution)/shard_map/ppermute | solution.py:27
  62.2 17.9 %copy-start.23 = (s32[32,4]{0,1:T(4,128)S(1)}, s32[32,4]{0,1:T(4,128)}, u32[]{:S(2)}) copy-start(s32[32,4]{0,1:T(4,128)} %param.32) | copy-start | bytes 1540
  62.9 6.7 %collective-permute-start.16 = (bf16[32,2048]{1,0:T(8,128)(2,1)S(1)}, bf16[32,2048]{1,0:T(8,128)(2,1)S(1)}, u32[]{:S(2)}, u32[]{:S(2)}) collective-permute-start(bf16[32,2048]{1,0:T(8,128)(2,1)S(1)} %get-tuple-element.37), channel_id=1, source_target_pairs={{0,1},{1,2},{2,3},{3,0},{4,5},{5,6},{6,7},{7,4},{8,9},{9,10},{10,1... | collective-permute-start | bytes 393224 | tf_op jit(solution)/shard_map/ppermute | solution.py:23
  64.4 7.7 %collective-permute-start.18 = (bf16[32,2048]{1,0:T(8,128)(2,1)}, bf16[32,2048]{1,0:T(8,128)(2,1)S(1)}, u32[]{:S(2)}, u32[]{:S(2)}) collective-permute-start(bf16[32,2048]{1,0:T(8,128)(2,1)} %get-tuple-element.40), channel_id=1, source_target_pairs={{0,3},{1,0},{2,1},{3,2},{4,7},{5,4},{6,5},{7,6},{8,11},{9,8},{10,9... | collective-permute-start | bytes 393224 | tf_op jit(solution)/shard_map/ppermute | solution.py:23
  66.2 6.6 %collective-permute-start.19 = (bf16[32,2048]{1,0:T(8,128)(2,1)S(1)}, bf16[32,2048]{1,0:T(8,128)(2,1)}, u32[]{:S(2)}, u32[]{:S(2)}) collective-permute-start(bf16[32,2048]{1,0:T(8,128)(2,1)S(1)} %get-tuple-element.39), channel_id=1, source_target_pairs={{0,3},{1,0},{2,1},{3,2},{4,7},{5,4},{6,5},{7,6},{8,11},{9,8},{10,9... | collective-permute-start | bytes 393224 | tf_op jit(solution)/shard_map/ppermute | solution.py:23
  70.3 7.6 %collective-permute-start.17 = (bf16[32,2048]{1,0:T(8,128)(2,1)}, bf16[32,2048]{1,0:T(8,128)(2,1)}, u32[]{:S(2)}, u32[]{:S(2)}) collective-permute-start(bf16[32,2048]{1,0:T(8,128)(2,1)} %add_convert_fusion.3), channel_id=1, source_target_pairs={{0,1},{1,2},{2,3},{3,0},{4,5},{5,6},{6,7},{7,4},{8,9},{9,10},{10,1... | collective-permute-start | bytes 393224 | tf_op jit(solution)/shard_map/ppermute | solution.py:23
  70.6 20.7 %collective-permute-start.21 = (bf16[32,2048]{1,0:T(8,128)(2,1)S(1)}, bf16[32,2048]{1,0:T(8,128)(2,1)}, u32[]{:S(2)}, u32[]{:S(2)}) collective-permute-start(bf16[32,2048]{1,0:T(8,128)(2,1)S(1)} %get-tuple-element.38), channel_id=1, source_target_pairs={{0,1},{1,2},{2,3},{3,0},{4,5},{5,6},{6,7},{7,4},{8,9},{9,10},{10,1... | collective-permute-start | bytes 393224 | tf_op jit(solution)/shard_map/ppermute | solution.py:23
  79.7 11.6 %collective-permute-start.20 = (bf16[32,2048]{1,0:T(8,128)(2,1)}, bf16[32,2048]{1,0:T(8,128)(2,1)}, u32[]{:S(2)}, u32[]{:S(2)}) collective-permute-start(bf16[32,2048]{1,0:T(8,128)(2,1)} %get-tuple-element.36), channel_id=1, source_target_pairs={{0,3},{1,0},{2,1},{3,2},{4,7},{5,4},{6,5},{7,6},{8,11},{9,8},{10,9... | collective-permute-start | bytes 393224 | tf_op jit(solution)/shard_map/ppermute | solution.py:23
  80.1 18.7 %copy-start.25 = (s32[32]{0:T(128)}, s32[32]{0:T(128)S(1)}, u32[]{:S(2)}) copy-start(s32[32]{0:T(128)S(1)} %multiply_add_fusion) | copy-start | bytes 388
  90.6 8.2 %copy-start.20 = (s32[128,4]{0,1:T(4,128)}, s32[128,4]{0,1:T(4,128)S(1)}, u32[]{:S(2)}) copy-start(s32[128,4]{0,1:T(4,128)S(1)} %reshape.394) | copy-start | bytes 6148
  95.5 9.3 %collective-permute-start.22 = (bf16[32,4096]{1,0:T(8,128)(2,1)}, bf16[32,4096]{1,0:T(8,128)(2,1)}, u32[]{:S(2)}, u32[]{:S(2)}) collective-permute-start(bf16[32,4096]{1,0:T(8,128)(2,1)} %get-tuple-element.26), channel_id=1, source_target_pairs={{0,1},{1,2},{2,3},{3,0},{4,5},{5,6},{6,7},{7,4},{8,9},{9,10},{10,1... | collective-permute-start | bytes 786440 | tf_op jit(solution)/shard_map/ppermute | solution.py:23
  96.9 9.1 %collective-permute-start.24 = (bf16[32,4096]{1,0:T(8,128)(2,1)}, bf16[32,4096]{1,0:T(8,128)(2,1)}, u32[]{:S(2)}, u32[]{:S(2)}) collective-permute-start(bf16[32,4096]{1,0:T(8,128)(2,1)} %get-tuple-element.26), channel_id=1, source_target_pairs={{0,3},{1,0},{2,1},{3,2},{4,7},{5,4},{6,5},{7,6},{8,11},{9,8},{10,9... | collective-permute-start | bytes 786440 | tf_op jit(solution)/shard_map/ppermute | solution.py:23
  105.7 6.2 %collective-permute-start.23 = (bf16[32,2048]{1,0:T(8,128)(2,1)S(1)}, bf16[32,2048]{1,0:T(8,128)(2,1)S(1)}, u32[]{:S(2)}, u32[]{:S(2)}) collective-permute-start(bf16[32,2048]{1,0:T(8,128)(2,1)S(1)} %slice.148), channel_id=1, source_target_pairs={{0,1},{1,2},{2,3},{3,0},{4,5},{5,6},{6,7},{7,4},{8,9},{9,10},{10,1... | collective-permute-start | bytes 393224 | tf_op jit(solution)/shard_map/ppermute | solution.py:23
  106.9 5.6 %collective-permute-start.25 = (bf16[32,2048]{1,0:T(8,128)(2,1)S(1)}, bf16[32,2048]{1,0:T(8,128)(2,1)S(1)}, u32[]{:S(2)}, u32[]{:S(2)}) collective-permute-start(bf16[32,2048]{1,0:T(8,128)(2,1)S(1)} %slice.149), channel_id=1, source_target_pairs={{0,3},{1,0},{2,1},{3,2},{4,7},{5,4},{6,5},{7,6},{8,11},{9,8},{10,9... | collective-permute-start | bytes 393224 | tf_op jit(solution)/shard_map/ppermute | solution.py:23
  114.3 32.3 %copy-start.7 = (bf16[1,4096,256]{2,1,0:T(8,128)(2,1)S(1)}, bf16[1,4096,256]{2,1,0:T(8,128)(2,1)}, u32[]{:S(2)}) copy-start(bf16[1,4096,256]{2,1,0:T(8,128)(2,1)} %param.34) | copy-start | bytes 6291460
  155.5 16.0 %copy-start.21 = (s32[128,4]{0,1:T(4,128)S(1)}, s32[128,4]{0,1:T(4,128)}, u32[]{:S(2)}) copy-start(s32[128,4]{0,1:T(4,128)} %copy-done.20) | copy-start | bytes 6148
  155.5 16.0 %copy-start.26 = (s32[32]{0:T(128)S(1)}, s32[32]{0:T(128)}, u32[]{:S(2)}) copy-start(s32[32]{0:T(128)} %copy-done.25) | copy-start | bytes 388
  155.5 35.0 %all-to-all-start.1 = ((bf16[32,8,4096]{2,1,0:T(8,128)(2,1)}), bf16[32,8,4096]{2,1,0:T(8,128)(2,1)}, u32[]{:S(2)}, u32[]{:S(2)}) async-start(bf16[32,8,4096]{2,1,0:T(8,128)(2,1)} %fusion), calls=%async_computation.1 | async-start | bytes 4194304 | tf_op jit(solution)/shard_map/all_to_all | solution.py:340
  199.1 22.1 %copy-start.6 = (f32[32,2048]{1,0:T(8,128)S(1)}, f32[32,2048]{1,0:T(8,128)}, u32[]{:S(2)}) copy-start(f32[32,2048]{1,0:T(8,128)} %copy-done.5) | copy-start | bytes 786436
  200.3 6.7 %collective-permute-start.26 = (bf16[32,2048]{1,0:T(8,128)(2,1)S(1)}, bf16[32,2048]{1,0:T(8,128)(2,1)S(1)}, u32[]{:S(2)}, u32[]{:S(2)}) collective-permute-start(bf16[32,2048]{1,0:T(8,128)(2,1)S(1)} %get-tuple-element.31), channel_id=1, source_target_pairs={{0,1},{1,2},{2,3},{3,0},{4,5},{5,6},{6,7},{7,4},{8,9},{9,10},{10,1... | collective-permute-start | bytes 393224 | tf_op jit(solution)/shard_map/ppermute | solution.py:23
  200.4 8.6 %collective-permute-start.28 = (bf16[32,2048]{1,0:T(8,128)(2,1)S(1)}, bf16[32,2048]{1,0:T(8,128)(2,1)S(1)}, u32[]{:S(2)}, u32[]{:S(2)}) collective-permute-start(bf16[32,2048]{1,0:T(8,128)(2,1)S(1)} %get-tuple-element.34), channel_id=1, source_target_pairs={{0,3},{1,0},{2,1},{3,2},{4,7},{5,4},{6,5},{7,6},{8,11},{9,8},{10,9... | collective-permute-start | bytes 393224 | tf_op jit(solution)/shard_map/ppermute | solution.py:23
  204.1 5.0 %collective-permute-start.29 = (bf16[32,2048]{1,0:T(8,128)(2,1)S(1)}, bf16[32,2048]{1,0:T(8,128)(2,1)S(1)}, u32[]{:S(2)}, u32[]{:S(2)}) collective-permute-start(bf16[32,2048]{1,0:T(8,128)(2,1)S(1)} %get-tuple-element.33), channel_id=1, source_target_pairs={{0,3},{1,0},{2,1},{3,2},{4,7},{5,4},{6,5},{7,6},{8,11},{9,8},{10,9... | collective-permute-start | bytes 393224 | tf_op jit(solution)/shard_map/ppermute | solution.py:23
  207.9 6.2 %collective-permute-start.27 = (bf16[32,2048]{1,0:T(8,128)(2,1)S(1)}, bf16[32,2048]{1,0:T(8,128)(2,1)S(1)}, u32[]{:S(2)}, u32[]{:S(2)}) collective-permute-start(bf16[32,2048]{1,0:T(8,128)(2,1)S(1)} %add_convert_fusion.1), channel_id=1, source_target_pairs={{0,1},{1,2},{2,3},{3,0},{4,5},{5,6},{6,7},{7,4},{8,9},{9,10},{10,1... | collective-permute-start | bytes 393224 | tf_op jit(solution)/shard_map/ppermute | solution.py:23
  208.0 8.1 %collective-permute-start.31 = (bf16[32,2048]{1,0:T(8,128)(2,1)S(1)}, bf16[32,2048]{1,0:T(8,128)(2,1)S(1)}, u32[]{:S(2)}, u32[]{:S(2)}) collective-permute-start(bf16[32,2048]{1,0:T(8,128)(2,1)S(1)} %get-tuple-element.32), channel_id=1, source_target_pairs={{0,1},{1,2},{2,3},{3,0},{4,5},{5,6},{6,7},{7,4},{8,9},{9,10},{10,1... | collective-permute-start | bytes 393224 | tf_op jit(solution)/shard_map/ppermute | solution.py:23
  215.2 5.0 %collective-permute-start.30 = (bf16[32,2048]{1,0:T(8,128)(2,1)S(1)}, bf16[32,2048]{1,0:T(8,128)(2,1)S(1)}, u32[]{:S(2)}, u32[]{:S(2)}) collective-permute-start(bf16[32,2048]{1,0:T(8,128)(2,1)S(1)} %get-tuple-element.30), channel_id=1, source_target_pairs={{0,3},{1,0},{2,1},{3,2},{4,7},{5,4},{6,5},{7,6},{8,11},{9,8},{10,9... | collective-permute-start | bytes 393224 | tf_op jit(solution)/shard_map/ppermute | solution.py:23
  (12 other events, 34.2 us)

commit v2 on v1

v2 whole, which is shorter than its diff:
```python
import functools

import jax
import jax.numpy as jnp
from jax import lax
from jax.experimental import pallas as pl
from jax.experimental.pallas import tpu as pltpu
from jax.sharding import Mesh
from jax.sharding import PartitionSpec as P

SP = ("z", "y", "c")
NARROW_SIZE = 128
BROAD_SIZE = 256
LOG2E = 1.4426950408889634
MASKED = -1e30
EPSILON = 1e-06
ORDER = (0, 1, 3, 2)
VMEM = pl.BlockSpec(memory_space=pltpu.VMEM)
SMEM = pl.BlockSpec(memory_space=pltpu.SMEM)
BF = jnp.bfloat16
F32 = jnp.float32


def shift(x, axis, k):
    return lax.ppermute(x, axis, [(i, (i + k) % 4) for i in range(4)])


def swap_core(x):
    return lax.ppermute(x, "c", [(0, 1), (1, 0)])


def call(kernel, operands, shapes, smem=(), scratch=(), mib=32, flops=0):
    return pl.pallas_call(
        kernel,
        out_shape=shapes,
        in_specs=[SMEM if i in smem else VMEM for i in range(len(operands))],
        out_specs=[VMEM] * len(shapes),
        scratch_shapes=list(scratch),
        compiler_params=pltpu.CompilerParams(vmem_limit_bytes=mib * 1024 * 1024),
        cost_estimate=pl.CostEstimate(flops=flops, transcendentals=0, bytes_accessed=2 * 1024 * 1024),
    )(*operands)


def shaped(shape, dtype):
    return jax.ShapeDtypeStruct(shape, dtype)


def pack_kernel(kn, vn, kb, vb, qn, qb, a, b, q):
    for at, ref in ((0, kn), (128, vn), (256, kb), (512, vb)):
        a[:, at : at + ref.shape[1]] = ref[:64]
        b[:, at : at + ref.shape[1]] = ref[64:]
    q[:, :512] = qn[...]
    q[:, 512:] = qb[...]


def stack_kernel(a, b, c, d, out):
    for i, ref in enumerate((a, b, c, d)):
        out[i] = ref[...]


def bias_kernel(place, gates, own, first, second, third):
    z, y = place[0], place[1]
    here = z * 4 + y
    own[...] = gates[here]

    def put(out, at, back_z, back_y, half):
        chip = ((z + 4 - back_z) % 4) * 4 + (y + 4 - back_y) % 4
        piece = gates[chip][:, half * 64 : half * 64 + 64]
        out[:, at : at + 64] = jnp.where(chip > here, MASKED, piece)

    for i in range(1, 4):
        put(first, (i - 1) * 64, 0, ORDER[i], 0)
        put(first, 192 + (i - 1) * 64, ORDER[i], 0, 1)
    for i in range(4):
        put(second, i * 64, 1, ORDER[i], 0)
        put(second, 256 + i * 64, 3, ORDER[i], 0)
        put(second, 512 + i * 64, ORDER[i], 1, 1)
        put(second, 768 + i * 64, ORDER[i], 3, 1)
        put(third, i * 64, 2, ORDER[i], 0)
        put(third, 256 + i * 64, ORDER[i], 2, 1)


def project_kernel(place, own, other, narrow, broad, *refs):
    outs, total, attn = refs[:4], refs[4], refs[5]
    a, b = own[:, 1024:], other[:, 1024:]
    top = jnp.maximum(a, b)
    wa, wb = jnp.exp2(a - top), jnp.exp2(b - top)
    joined = wa + wb
    wa, wb = wa / joined, wb / joined
    for h in range(6):
        lo, size = (h * 128, 128) if h < 4 else (512 + (h - 4) * 256, 256)
        value = own[:, lo : lo + size] * wa[:, h : h + 1] + other[:, lo : lo + size] * wb[:, h : h + 1]
        attn[:, lo : lo + size] = value.astype(BF)
    for at in range(0, 4096, 1024):
        part = jnp.dot(attn[:, :512], narrow[:, at : at + 1024], preferred_element_type=F32)
        total[:, at : at + 1024] = part + jnp.dot(attn[:, 512:], broad[:, at : at + 1024], preferred_element_type=F32)
    for k in range(4):
        outs[k][...] = total[pl.ds(((place[0] + k) % 4) * 32, 32), :].astype(BF)


def dispatch_kernel(p0, p1, p2, p3, residual, gain, target, stream_out, normed_out, out):
    mixture = p0[...].astype(F32) + p1[...].astype(F32) + p2[...].astype(F32) + p3[...].astype(F32)
    stream = residual[...].astype(F32) + mixture
    stream_out[...] = stream
    scale = lax.rsqrt(jnp.mean(stream * stream, axis=1, keepdims=True) + EPSILON)
    normed = (stream * scale * gain[...]).astype(BF)
    normed_out[...] = normed
    cut = jnp.concatenate([normed[:, g * 1024 : (g + 1) * 1024] for g in range(4)], axis=0)
    row = lax.broadcasted_iota(jnp.int32, (256, 128), 0)
    for at in range(0, 1024, 256):
        pick = row + at == target[0:1, :]
        for k in range(1, 4):
            pick = pick | (row + at == target[k : k + 1, :])
        out[at : at + 256, :] = jnp.dot(pick.astype(F32).astype(BF), cut, preferred_element_type=F32).astype(BF)


def silu(v):
    return v / (1.0 + jnp.exp(-v))


def shared_kernel(n0, n1, n2, n3, gate, up, down, o0, o1, o2, o3):
    x = jnp.concatenate([n0[...], n1[...], n2[...], n3[...]], axis=0)
    g = jnp.dot(x, gate[...], preferred_element_type=F32)
    u = jnp.dot(x, up[...], preferred_element_type=F32)
    hidden = (silu(g) * u).astype(BF)
    for at in range(0, 4096, 1024):
        part = jnp.dot(hidden, down[:, at : at + 1024], preferred_element_type=F32).astype(BF)
        for k, out in enumerate((o0, o1, o2, o3)):
            out[:, at : at + 1024] = part[k * 32 : (k + 1) * 32]


def expert_kernel(inbound, gate, up, down, out, x):
    i = lax.broadcasted_iota(jnp.int32, (256, 256), 0)
    j = lax.broadcasted_iota(jnp.int32, (256, 256), 1)
    order = (j == ((i % 64) // 2) * 8 + (i % 2) * 4 + i // 64).astype(F32).astype(BF)
    back = (i == ((j % 64) // 2) * 8 + (j % 2) * 4 + j // 64).astype(F32).astype(BF)
    for b in range(4):
        rows = jnp.dot(order, inbound[b * 256 : (b + 1) * 256, :], preferred_element_type=F32).astype(BF)
        for g in range(4):
            x[b * 64 : (b + 1) * 64, g * 1024 : (g + 1) * 1024] = rows[g * 64 : (g + 1) * 64]
    gated = jnp.dot(x[...], gate[0], preferred_element_type=F32)
    upped = jnp.dot(x[...], up[0], preferred_element_type=F32)
    hidden = (silu(gated) * upped).astype(BF)
    for g in range(4):
        part = jnp.dot(hidden, down[0, :, g * 1024 : (g + 1) * 1024], preferred_element_type=F32)
        x[:, g * 1024 : (g + 1) * 1024] = part.astype(BF)
    for b in range(4):
        rows = jnp.concatenate([x[b * 64 : (b + 1) * 64, g * 1024 : (g + 1) * 1024] for g in range(4)], axis=0)
        out[b * 256 : (b + 1) * 256, :] = jnp.dot(back, rows, preferred_element_type=F32).astype(BF)


def combine_kernel(returned, target, weight, stream, s0, s1, s2, s3, out):
    column = lax.broadcasted_iota(jnp.int32, (128, 1024), 1)
    mix = jnp.zeros((128, 1024), F32)
    for k in range(4):
        mix = mix + jnp.where(column == target[:, k : k + 1], weight[:, k : k + 1], 0.0)
    routed = jnp.dot(mix.astype(BF), returned[...], preferred_element_type=F32)
    for g in range(4):
        lo, hi = g * 1024, (g + 1) * 1024
        total = stream[:, lo:hi] + routed[g * 32 : (g + 1) * 32]
        for s in (s0, s1, s2, s3):
            total = total + s[:, lo:hi].astype(F32)
        out[:, lo:hi] = total.astype(BF)


def attend_kernel(counts, first, last, *refs):
    at = 0

    def take(n):
        nonlocal at
        at += n
        return refs[at - n : at]

    q_own, q_other, core = take(3)
    tiles, planes = [], []
    for n, own_block in counts:
        tiles.append((take(n), take(1)[0], own_block))
        if first and not own_block:
            planes += tiles[-1][0]
    if not first:
        m_in, l_in, an_in, ab_in = take(4)
    if last:
        own_out, send_out = take(2)
    else:
        m_out, l_out, an_out, ab_out = take(4)

    def keys(ref, lo, hi):
        value = ref[1:, :, lo:hi] if any(ref is p for p in planes) else ref[..., lo:hi]
        return value.reshape(-1, hi - lo)

    results = {}
    for group, size, heads, lo in (("n", NARROW_SIZE, 4, 0), ("b", BROAD_SIZE, 2, 256)):
        scale = size**-0.5 * LOG2E
        base = 0 if group == "n" else 4
        row_base = 0 if group == "n" else 1024
        loaded = []
        for arrays, bias, own_block in tiles:
            k = jnp.concatenate([keys(r, lo, lo + size) for r in arrays], axis=0)
            v = jnp.concatenate([keys(r, lo + size, lo + 2 * size) for r in arrays], axis=0)
            loaded.append((k, v, bias, own_block))
        for side, q_ref in ((0, q_own), (1, q_other)):
            for h0 in range(0, heads, 2):
                col = (0 if group == "n" else 512) + h0 * size
                q = jnp.concatenate([q_ref[:, col + i * size : col + (i + 1) * size] for i in range(2)], axis=0)
                rows = row_base + side * heads * 128 + h0 * 128
                arow = rows - row_base
                scores = []
                for k, v, bias, own_block in loaded:
                    s = lax.dot_general(q, k, (((1,), (1,)), ((), ())), preferred_element_type=F32) * scale
                    n = k.shape[0]
                    b = bias[base + h0 : base + h0 + 2, :]
                    s = (s.reshape(2, 128, n) + b[:, None, :]).reshape(256, n)
                    if own_block:
                        qi = lax.broadcasted_iota(jnp.int32, (256, n), 0) % 128
                        ki = lax.broadcasted_iota(jnp.int32, (256, n), 1)
                        offset = 0 if side == 0 else 128 * (1 - 2 * core[0])
                        s = jnp.where(ki <= qi + offset, s, MASKED)
                    scores.append(s)
                m = functools.reduce(jnp.maximum, [jnp.max(s, axis=1, keepdims=True) for s in scores])
                if not first:
                    m_old = m_in[pl.ds(rows, 256), :][:, :1]
                    m = jnp.maximum(m, m_old)
                l = jnp.zeros((256, 1), F32)
                acc = jnp.zeros((256, size), F32)
                for s, (k, v, bias, own_block) in zip(scores, loaded):
                    p = jnp.exp2(s - m)
                    l = l + jnp.sum(p, axis=1, keepdims=True)
                    acc = acc + jnp.dot(p.astype(BF), v, preferred_element_type=F32)
                acc_in, acc_out = (None, None)
                if not first:
                    a_in = an_in if group == "n" else ab_in
                    factor = jnp.exp2(m_old - m)
                    l = l + l_in[pl.ds(rows, 256), :][:, :1] * factor
                    acc = acc + a_in[pl.ds(arow, 256), :] * factor
                if last:
                    out = own_out if side == 0 else send_out
                    o = acc / l
                    lse = m + jnp.log2(l)
                    for i in range(2):
                        out[:, col + i * size : col + (i + 1) * size] = o[i * 128 : (i + 1) * 128]
                        results[(side, base + h0 + i)] = lse[i * 128 : (i + 1) * 128]
                else:
                    a_out = an_out if group == "n" else ab_out
                    m_out[pl.ds(rows, 256), :] = jnp.broadcast_to(m, (256, 128))
                    l_out[pl.ds(rows, 256), :] = jnp.broadcast_to(l, (256, 128))
                    a_out[pl.ds(arow, 256), :] = acc
    if last:
        lane = lax.broadcasted_iota(jnp.int32, (128, 128), 1)
        for side, out in ((0, own_out), (1, send_out)):
            stats = jnp.zeros((128, 128), F32)
            for h in range(6):
                stats = jnp.where(lane == h, results[(side, h)], stats)
            out[:, 1024:1152] = stats


def attend(q_own, q_other, core, tiles, state, last):
    counts = tuple((len(arrays), own_block) for arrays, _, own_block in tiles)
    operands = [q_own, q_other, core]
    n_keys = 0
    for arrays, bias, _ in tiles:
        operands += list(arrays) + [bias]
        n_keys += bias.shape[1]
    specs = [VMEM] * len(operands)
    specs[2] = SMEM
    if state is not None:
        operands += list(state)
        specs += [VMEM] * 4
    if last:
        shapes = [jax.ShapeDtypeStruct((128, 1152), F32)] * 2
    else:
        shapes = [
            jax.ShapeDtypeStruct((1536, 128), F32),
            jax.ShapeDtypeStruct((1536, 128), F32),
            jax.ShapeDtypeStruct((1024, 128), F32),
            jax.ShapeDtypeStruct((512, 256), F32),
        ]
    return pl.pallas_call(
        functools.partial(attend_kernel, counts, state is None, last),
        out_shape=shapes,
        in_specs=specs,
        out_specs=[VMEM] * len(shapes),
        compiler_params=pltpu.CompilerParams(vmem_limit_bytes=24 * 1024 * 1024),
        cost_estimate=pl.CostEstimate(
            flops=4 * n_keys * 256 * 1024, transcendentals=n_keys * 1536, bytes_accessed=4 * 1024 * 1024
        ),
    )(*operands)


def local(
    query_narrow,
    key_narrow,
    value_narrow,
    gates_narrow,
    query_broad,
    key_broad,
    value_broad,
    gates_broad,
    project_narrow,
    project_broad,
    residual,
    norm_gain,
    route_ids,
    route_weight,
    expert_gate,
    expert_up,
    expert_down,
    shared_gate,
    shared_up,
    shared_down,
):
    z, y, c, t = (lax.axis_index(n).astype(jnp.int32) for n in ("z", "y", "c", "tp"))

    own_a, own_b, q_own = call(
        pack_kernel,
        (key_narrow, value_narrow, key_broad, value_broad, query_narrow, query_broad),
        [shaped((64, 768), BF)] * 2 + [shaped((128, 1024), BF)],
    )
    first_a = [shift(own_a, "y", k) for k in ORDER[1:]]
    first_b = [shift(own_b, "z", k) for k in ORDER[1:]]
    q_other = swap_core(q_own)
    (plane_a,) = call(stack_kernel, [own_a] + first_a, [shaped((4, 64, 768), BF)])
    (plane_b,) = call(stack_kernel, [own_b] + first_b, [shaped((4, 64, 768), BF)])
    a_back, b_back, a_ahead, b_ahead, a_far, b_far = (
        shift(plane, axis, k) for k in ORDER[1:] for plane, axis in ((plane_a, "z"), (plane_b, "y"))
    )

    gates = jnp.concatenate([gates_narrow, gates_broad], axis=1) * (-LOG2E)
    gates = lax.dynamic_index_in_dim(gates.reshape(16, 2, 128, 6), c, 1, keepdims=False)
    gates = jnp.pad(gates.transpose(0, 2, 1), ((0, 0), (0, 2), (0, 0)))
    own_bias, bias_1, bias_2, bias_3 = call(
        bias_kernel,
        (jnp.stack([z, y]), gates),
        [shaped((8, n), F32) for n in (128, 384, 1024, 512)],
        smem=(0,),
    )
    core = c.reshape(1)
    state = attend(
        q_own,
        q_other,
        core,
        [((own_a, own_b), own_bias, True), ((plane_a, plane_b), bias_1, False)],
        None,
        False,
    )
    state = attend(q_own, q_other, core, [((a_back, a_ahead, b_back, b_ahead), bias_2, False)], state, False)
    own_part, send_part = attend(q_own, q_other, core, [((a_far, b_far), bias_3, False)], state, True)
    other_part = swap_core(send_part)

    p0, p1, p2, p3 = call(
        project_kernel,
        (t.reshape(1), own_part, other_part, project_narrow, project_broad),
        [shaped((32, 4096), BF)] * 4,
        smem=(0,),
        scratch=[pltpu.VMEM((128, 4096), F32), pltpu.VMEM((128, 1024), BF)],
        flops=2 * 128 * 1024 * 4096,
    )
    p1, p2, p3 = shift(p1, "tp", 1), shift(p2, "tp", 2), shift(p3, "tp", 3)

    flat = route_ids.reshape(-1)
    earlier = jnp.arange(128)[:, None] // 4 > jnp.arange(128)[None, :] // 4
    slot = jnp.sum((earlier & (flat[:, None] == flat[None, :])).astype(jnp.int32), axis=1).reshape(32, 4)
    target = jnp.tile(route_ids * 8 + slot * 4, (4, 1)) + jnp.arange(128, dtype=jnp.int32)[:, None] // 32
    weight = jnp.tile(route_weight.astype(BF).astype(F32), (4, 1))

    own_rows = lax.dynamic_slice_in_dim(residual, t * 32, 32, 0)
    stream, normed, outbound = call(
        dispatch_kernel,
        (p0, p1, p2, p3, own_rows, norm_gain.reshape(1, -1), target.T),
        [shaped((32, 4096), F32), shaped((32, 4096), BF), shaped((1024, 1024), BF)],
        flops=2 * 1024 * 128 * 1024,
    )
    every = SP + ("tp",)
    inbound = lax.all_to_all(outbound.reshape(128, 8, 1024), every, 0, 0, tiled=True)

    n1, n2, n3 = (shift(normed, "tp", k) for k in (1, 2, 3))
    s0, s1, s2, s3 = call(
        shared_kernel,
        (normed, n1, n2, n3, shared_gate, shared_up, shared_down),
        [shaped((32, 4096), BF)] * 4,
        flops=2 * 128 * 4096 * 768,
    )
    s1, s2, s3 = shift(s1, "tp", 3), shift(s2, "tp", 2), shift(s3, "tp", 1)

    (result,) = call(
        expert_kernel,
        (inbound.reshape(1024, 1024), expert_gate, expert_up, expert_down),
        [shaped((1024, 1024), BF)],
        scratch=[pltpu.VMEM((256, 4096), BF)],
        flops=2 * 256 * 4096 * 768,
    )
    returned = lax.all_to_all(result.reshape(128, 8, 1024), every, 0, 0, tiled=True)
    (out,) = call(
        combine_kernel,
        (returned.reshape(1024, 1024), target, weight, stream, s0, s1, s2, s3),
        [shaped((32, 4096), BF)],
        flops=2 * 128 * 1024 * 1024,
    )
    return out


def solution(mesh):
    mesh = Mesh(mesh.devices.reshape(4, 4, 2, 4), ("z", "y", "c", "tp"))
    every = SP + ("tp",)
    placed = (
        P(SP, "tp"),
        P(SP, "tp"),
        P(SP, "tp"),
        P(None, "tp"),
        P(SP, "tp"),
        P(SP, "tp"),
        P(SP, "tp"),
        P(None, "tp"),
        P("tp", None),
        P("tp", None),
        P(SP, None),
        P(),
        P(every, None),
        P(every, None),
        P(every, None, None),
        P(every, None, None),
        P(every, None, None),
        P(None, "tp"),
        P(None, "tp"),
        P("tp", None),
    )
    return jax.shard_map(local, mesh=mesh, in_specs=placed, out_specs=P(every, None), check_vma=False)
```

time: 224 us -> 198 us (0.88)
  waiting for transfers between devices: 44.9 us -> 70.1 us
  matrix products: 22 us -> 0 us
  other arithmetic: 19.6 us -> 1.77 us
  blocking collectives: 53.6 us -> 37.7 us
  Pallas kernels: 10.6 us -> 25.3 us
  starting transfers between devices: 50.8 us -> 36.9 us
  local copies, waits for them, and re-layouts: 20.8 us -> 23.7 us
    ppermute x30 -> x21, waiting for transfers between devices: 26.2 us -> 68.5 us  [shift(): return lax.ppermute(x, axis, [(i, (i + k) % 4) for i in range(4)])]
    dot_general x9 -> x0, matrix products: 22 us -> none  [the longest x1 5.95 us: local(): jnp.dot(hidden, expert_down[0], preferred_element_type=F32).astype(BF)]
    all_gather x2 -> x0, blocking collectives: 21.4 us -> none  [the longest x1 10.9 us: local(): lax.all_gather(route_weight.astype(BF).astype(F32), 'tp', axis=0, tiled=T...]
    all_to_all x1, waiting for transfers between devices: 16.3 us -> 0.01 us  [local(): lax.all_to_all(result.reshape(128, 8, 1024), every, 0, 0, tiled=True)]
    pallas_call x0 -> x9, Pallas kernels: none -> 13.8 us  [call(): pl.pallas_call(kernel, out_shape=shapes, in_specs=[SMEM if i in smem else...]
    ppermute x30 -> x21, starting transfers between devices: 45.9 us -> 32.1 us  [shift(): return lax.ppermute(x, axis, [(i, (i + k) % 4) for i in range(4)])]
    unnamed x64 -> x57, local copies, waits for them, and re-layouts: 6.11 us -> 19.6 us
    all_to_all x1, blocking collectives: 32.3 us -> 37.7 us  [local(): lax.all_to_all(outbound.reshape(128, 8, 1024), every, 0, 0, tiled=True)]
  transfers between devices with their start and end apart: 33 -> 24, of which waited for: 13 -> 14; matrix products, arithmetic and copies ran while one was open for 10% -> 3% of each run, Pallas kernels for 3% -> 5%
where the time goes in v2:
time: 198 us; the launch traced here: 196 us
  waiting for transfers between devices  70.1 us (35%)
  blocking collectives  37.7 us (19%)
  starting transfers between devices  36.9 us (19%)
  Pallas kernels  25.3 us (13%)
  local copies, waits for them, and re-layouts  23.7 us (12%)
    ppermute x21, waiting for transfers between devices, shift(): return lax.ppermute(x, axis, [(i, (i + k) % 4) for i in range(4)])  68.5 us
    all_to_all x1, blocking collectives, local(): lax.all_to_all(outbound.reshape(128, 8, 1024), every, 0, 0, tiled=True)  37.7 us
    ppermute x21, starting transfers between devices, shift(): return lax.ppermute(x, axis, [(i, (i + k) % 4) for i in range(4)])  32.1 us
    unnamed x57, local copies, waits for them, and re-layouts  19.6 us
    pallas_call x9, Pallas kernels, call(): pl.pallas_call(kernel, out_shape=shapes, in_specs=[SMEM if i in smem else...  13.8 us
    pallas_call x3, Pallas kernels, attend(): pl.pallas_call(functools.partial(attend_kernel, counts, state is None, la...  11.5 us
    all_to_all x1, starting transfers between devices, local(): lax.all_to_all(result.reshape(128, 8, 1024), every, 0, 0, tiled=True)  4.78 us
  transfers between devices with their start and end apart: 24, of which 14 were waited for; matrix products, arithmetic and copies ran while one was open for 3% of the time, Pallas kernels for 5%

profile of v2, /device:TPU:0, one launch (start us, length us, event | category | flops | bytes accessed | tf_op | source)
XLA Modules:
  0.0 195.7 jit_solution(12925543879013257141)
XLA Ops:
  0.0 1.0 copy-done.13
  1.0 0.9 copy-done.14
  5.2 1.8 collective-permute-start.1
  6.9 1.5 collective-permute-start.2
  8.5 2.1 %collective-permute-start.3 = (bf16[64,768]{1,0:T(8,128)(2,1)S(1)}, bf16[64,768]{1,0:T(8,128)(2,1)S(1)}, u32[]{:S(2)}, u32[]{:S(2)}) collective-permute-start(bf16[64,768]{1,0:T(8,128)(2,1)S(1)} %get-tuple-element.34.a.refs_3_), channel_id=1, source_target_pairs={{0,16},{8,24},{16,0},{24,8},{1,17},{9,25},{17,1},{25,9},{2,18},{10... | collective-permute-start | bytes 294920 | tf_op jit(solution)/shard_map/ppermute | solution.py:25
  12.0 2.6 %collective-permute-done.3.d = bf16[64,768]{1,0:T(8,128)(2,1)S(1)} collective-permute-done((bf16[64,768]{1,0:T(8,128)(2,1)S(1)}, bf16[64,768]{1,0:T(8,128)(2,1)S(1)}, u32[]{:S(2)}, u32[]{:S(2)}) %collective-permute-start.3) | collective-permute-done | bytes 98336 | tf_op jit(solution)/shard_map/ppermute | solution.py:25
  15.4 2.0 %collective-permute-start.9 = (bf16[4,64,768]{2,1,0:T(8,128)(2,1)}, bf16[4,64,768]{2,1,0:T(8,128)(2,1)S(1)}, u32[]{:S(2)}, u32[]{:S(2)}) collective-permute-start(bf16[4,64,768]{2,1,0:T(8,128)(2,1)} %shard_map.191.refs_6_), channel_id=1, source_target_pairs={{0,32},{32,64},{64,96},{96,0},{1,33},{33,65},{65,97},{97,1},{2,34}... | collective-permute-start | bytes 1179656 | tf_op jit(solution)/shard_map/ppermute | solution.py:25
  17.4 1.9 collective-permute-start.5
  19.3 1.3 collective-permute-start.6
  20.6 2.4 %collective-permute-start.7 = (bf16[64,768]{1,0:T(8,128)(2,1)S(1)}, bf16[64,768]{1,0:T(8,128)(2,1)S(1)}, u32[]{:S(2)}, u32[]{:S(2)}) collective-permute-start(bf16[64,768]{1,0:T(8,128)(2,1)S(1)} %get-tuple-element.35.a.refs_4_), channel_id=1, source_target_pairs={{0,64},{32,96},{64,0},{96,32},{1,65},{33,97},{65,1},{97,33},{2,66}... | collective-permute-start | bytes 294920 | tf_op jit(solution)/shard_map/ppermute | solution.py:25
  23.0 7.7 %collective-permute-done.5.b = bf16[64,768]{1,0:T(8,128)(2,1)S(1)} collective-permute-done((bf16[64,768]{1,0:T(8,128)(2,1)S(1)}, bf16[64,768]{1,0:T(8,128)(2,1)S(1)}, u32[]{:S(2)}, u32[]{:S(2)}) %collective-permute-start.5) | collective-permute-done | bytes 98336 | tf_op jit(solution)/shard_map/ppermute | solution.py:25
  30.8 1.7 collective-permute-start.10
  34.5 2.5 %collective-permute-start.12 = (bf16[4,64,768]{2,1,0:T(8,128)(2,1)}, bf16[4,64,768]{2,1,0:T(8,128)(2,1)S(1)}, u32[]{:S(2)}, u32[]{:S(2)}) collective-permute-start(bf16[4,64,768]{2,1,0:T(8,128)(2,1)} %shard_map.192.refs_7_), channel_id=1, source_target_pairs={{0,24},{8,0},{16,8},{24,16},{1,25},{9,1},{17,9},{25,17},{2,26},{10... | collective-permute-start | bytes 1179656 | tf_op jit(solution)/shard_map/ppermute | solution.py:25
  37.0 0.9 concatenate.8
  40.0 1.4 fusion.2
  46.2 3.3 %shard_map.194 = (f32[1536,128]{1,0:T(8,128)S(1)}, f32[1536,128]{1,0:T(8,128)S(1)}, f32[1024,128]{1,0:T(8,128)S(1)}, f32[512,256]{1,0:T(8,128)S(1)}) custom-call(bf16[128,1024]{1,0:T(8,128)(2,1)S(1)} %get-tuple-element.33.refs_0_, bf16[128,1024]{1,0:T(8,128)(2,1)S(1)} %collective-permute-done.refs_1_, s32[1]{0:T(128)} %bitcast.1.refs_2_, ...), custom_call_target="tpu_custom_call" | custom-call | flops 536870912 | bytes 4194304 | tf_op jit(solution)/shard_map/pallas_call | solution.py:277
  49.5 2.0 %collective-permute-done.12.refs_6_ = bf16[4,64,768]{2,1,0:T(8,128)(2,1)S(1)} collective-permute-done((bf16[4,64,768]{2,1,0:T(8,128)(2,1)}, bf16[4,64,768]{2,1,0:T(8,128)(2,1)S(1)}, u32[]{:S(2)}, u32[]{:S(2)}) %collective-permute-start.12) | collective-permute-done | bytes 393248 | tf_op jit(solution)/shard_map/ppermute | solution.py:25
  51.5 3.8 %shard_map.195 = (f32[1536,128]{1,0:T(8,128)S(1)}, f32[1536,128]{1,0:T(8,128)S(1)}, f32[1024,128]{1,0:T(8,128)S(1)}, f32[512,256]{1,0:T(8,128)S(1)}) custom-call(bf16[128,1024]{1,0:T(8,128)(2,1)S(1)} %get-tuple-element.33.refs_0_, bf16[128,1024]{1,0:T(8,128)(2,1)S(1)} %collective-permute-done.refs_1_, s32[1]{0:T(128)} %bitcast.1.refs_2_, ...), custom_call_target="tpu_custom_call" | custom-call | flops 1073741824 | bytes 4194304 | tf_op jit(solution)/shard_map/pallas_call | solution.py:277
  55.3 4.4 %shard_map.196 = (f32[128,1152]{1,0:T(8,128)S(1)}, f32[128,1152]{1,0:T(8,128)}) custom-call(bf16[128,1024]{1,0:T(8,128)(2,1)S(1)} %get-tuple-element.33.refs_0_, bf16[128,1024]{1,0:T(8,128)(2,1)S(1)} %collective-permute-done.refs_1_, s32[1]{0:T(128)} %bitcast.1.refs_2_, bf16[4,64,768]{2,1,0:T(8,128)(2,1)S(1)} %collective-permute-done.4.refs_3_, ...), custom_call_target="tpu_custom_call" | custom-call | flops 536870912 | bytes 4194304 | tf_op jit(solution)/shard_map/pallas_call | solution.py:277
  60.4 1.6 collective-permute-done.13.other
  61.9 2.2 %copy-done.1 = bf16[512,4096]{1,0:T(8,128)(2,1)S(1)} copy-done((bf16[512,4096]{1,0:T(8,128)(2,1)S(1)}, bf16[512,4096]{1,0:T(8,128)(2,1)}, u32[]{:S(2)}) %copy-start.1) | copy-done | bytes 4194328
  64.1 2.2 %copy-done.2 = bf16[512,4096]{1,0:T(8,128)(2,1)S(1)} copy-done((bf16[512,4096]{1,0:T(8,128)(2,1)S(1)}, bf16[512,4096]{1,0:T(8,128)(2,1)}, u32[]{:S(2)}) %copy-start.2) | copy-done | bytes 4194328
  66.3 1.5 shard_map.197
  67.8 1.6 collective-permute-start.14
  69.4 2.7 %collective-permute-start.15 = (bf16[32,4096]{1,0:T(8,128)(2,1)S(1)}, bf16[32,4096]{1,0:T(8,128)(2,1)S(1)}, u32[]{:S(2)}, u32[]{:S(2)}) collective-permute-start(bf16[32,4096]{1,0:T(8,128)(2,1)S(1)} %get-tuple-element.52), channel_id=1, source_target_pairs={{0,2},{1,3},{2,0},{3,1},{4,6},{5,7},{6,4},{7,5},{8,10},{9,11},{10,... | collective-permute-start | bytes 786440 | tf_op jit(solution)/shard_map/ppermute | solution.py:25
  72.1 1.4 collective-permute-start.16
  73.6 3.9 %collective-permute-done.14.p1 = bf16[32,4096]{1,0:T(8,128)(2,1)S(1)} collective-permute-done((bf16[32,4096]{1,0:T(8,128)(2,1)S(1)}, bf16[32,4096]{1,0:T(8,128)(2,1)S(1)}, u32[]{:S(2)}, u32[]{:S(2)}) %collective-permute-start.14) | collective-permute-done | bytes 262176 | tf_op jit(solution)/shard_map/ppermute | solution.py:25
  77.5 6.6 %collective-permute-done.15.p2 = bf16[32,4096]{1,0:T(8,128)(2,1)S(1)} collective-permute-done((bf16[32,4096]{1,0:T(8,128)(2,1)S(1)}, bf16[32,4096]{1,0:T(8,128)(2,1)S(1)}, u32[]{:S(2)}, u32[]{:S(2)}) %collective-permute-start.15) | collective-permute-done | bytes 262176 | tf_op jit(solution)/shard_map/ppermute | solution.py:25
  84.1 1.0 shard_map.198
  85.9 37.7 %all_to_all.10 = bf16[128,8,1024]{2,1,0:T(8,128)(2,1)S(1)} all-to-all(bf16[128,8,1024]{2,1,0:T(8,128)(2,1)S(1)} %bitcast.23), channel_id=1, replica_groups=mesh['z'=4,'y'=4,'c'=2,'tp'=4] {'z','y','c','tp'}, dimensions={0} | all-to-all | bytes 4194304 | tf_op jit(solution)/shard_map/all_to_all | solution.py:373
  123.6 4.4 %shard_map.199 = bf16[1024,1024]{1,0:T(8,128)(2,1)} custom-call(bf16[1024,1024]{1,0:T(8,128)(2,1)S(1)} %bitcast.21, bf16[1,4096,256]{2,1,0:T(8,128)(2,1)S(1)} %copy-done.3, bf16[1,4096,256]{2,1,0:T(8,128)(2,1)S(1)} %copy-done.4, bf16[1,256,4096]{2,1,0:T(8,128)(2,1)S(1)} %copy-done.5), custom_call_target="tpu_custom_call" | custom-call | flops 1610612736 | bytes 2097152 | tf_op jit(solution)/shard_map/pallas_call | solution.py:33
  127.9 4.8 %all-to-all-start.1 = ((bf16[128,8,1024]{2,1,0:T(8,128)(2,1)}), bf16[128,8,1024]{2,1,0:T(8,128)(2,1)S(1)}, u32[]{:S(2)}, u32[]{:S(2)}) async-start(bf16[128,8,1024]{2,1,0:T(8,128)(2,1)} %bitcast.11), calls=%async_computation.1 | async-start | bytes 4194304 | tf_op jit(solution)/shard_map/all_to_all | solution.py:391
  132.7 0.9 collective-permute-start.17
  133.6 2.7 %collective-permute-start.18 = (bf16[32,4096]{1,0:T(8,128)(2,1)S(1)}, bf16[32,4096]{1,0:T(8,128)(2,1)S(1)}, u32[]{:S(2)}, u32[]{:S(2)}) collective-permute-start(bf16[32,4096]{1,0:T(8,128)(2,1)S(1)} %get-tuple-element.56.n0), channel_id=1, source_target_pairs={{0,2},{1,3},{2,0},{3,1},{4,6},{5,7},{6,4},{7,5},{8,10},{9,11},{10,... | collective-permute-start | bytes 786440 | tf_op jit(solution)/shard_map/ppermute | solution.py:25
  136.3 1.4 collective-permute-start.19
  137.8 25.7 %collective-permute-done.17.n1 = bf16[32,4096]{1,0:T(8,128)(2,1)S(1)} collective-permute-done((bf16[32,4096]{1,0:T(8,128)(2,1)S(1)}, bf16[32,4096]{1,0:T(8,128)(2,1)S(1)}, u32[]{:S(2)}, u32[]{:S(2)}) %collective-permute-start.17) | collective-permute-done | bytes 262176 | tf_op jit(solution)/shard_map/ppermute | solution.py:25
  163.5 5.6 %collective-permute-done.18.n2 = bf16[32,4096]{1,0:T(8,128)(2,1)S(1)} collective-permute-done((bf16[32,4096]{1,0:T(8,128)(2,1)S(1)}, bf16[32,4096]{1,0:T(8,128)(2,1)S(1)}, u32[]{:S(2)}, u32[]{:S(2)}) %collective-permute-start.18) | collective-permute-done | bytes 262176 | tf_op jit(solution)/shard_map/ppermute | solution.py:25
  169.1 1.6 copy-done.6
  170.7 1.6 copy-done.7
  172.3 1.6 copy-done.8
  173.9 0.9 copy-done.12
  174.8 2.0 %shard_map.200 = (bf16[32,4096]{1,0:T(8,128)(2,1)S(1)}, bf16[32,4096]{1,0:T(8,128)(2,1)}, bf16[32,4096]{1,0:T(8,128)(2,1)}, bf16[32,4096]{1,0:T(8,128)(2,1)}) custom-call(bf16[32,4096]{1,0:T(8,128)(2,1)S(1)} %copy-done.12, bf16[32,4096]{1,0:T(8,128)(2,1)S(1)} %collective-permute-done.17.n1, bf16[32,4096]{1,0:T(8,128)(2,1)S(1)} %collective-permute-done.18.n2, ...), custom_call_target="tpu_custom_call" | custom-call | flops 805306368 | bytes 2097152 | tf_op jit(solution)/shard_map/pallas_call | solution.py:33
  176.9 2.0 %collective-permute-start.21 = (bf16[32,4096]{1,0:T(8,128)(2,1)}, bf16[32,4096]{1,0:T(8,128)(2,1)}, u32[]{:S(2)}, u32[]{:S(2)}) collective-permute-start(bf16[32,4096]{1,0:T(8,128)(2,1)} %get-tuple-element.59), channel_id=1, source_target_pairs={{0,2},{1,3},{2,0},{3,1},{4,6},{5,7},{6,4},{7,5},{8,10},{9,11},{10,... | collective-permute-start | bytes 786440 | tf_op jit(solution)/shard_map/ppermute | solution.py:25
  179.5 6.8 %collective-permute-done.20.s1 = bf16[32,4096]{1,0:T(8,128)(2,1)} collective-permute-done((bf16[32,4096]{1,0:T(8,128)(2,1)}, bf16[32,4096]{1,0:T(8,128)(2,1)}, u32[]{:S(2)}, u32[]{:S(2)}) %collective-permute-start.20) | collective-permute-done | bytes 262176 | tf_op jit(solution)/shard_map/ppermute | solution.py:25
  186.3 1.6 collective-permute-done.21.s2
  187.9 4.1 %collective-permute-done.22.s3 = bf16[32,4096]{1,0:T(8,128)(2,1)} collective-permute-done((bf16[32,4096]{1,0:T(8,128)(2,1)}, bf16[32,4096]{1,0:T(8,128)(2,1)}, u32[]{:S(2)}, u32[]{:S(2)}) %collective-permute-start.22) | collective-permute-done | bytes 262176 | tf_op jit(solution)/shard_map/ppermute | solution.py:25
  192.0 1.0 copy-done.10
  193.1 2.6 %shard_map.201 = bf16[32,4096]{1,0:T(8,128)(2,1)} custom-call(bf16[1024,1024]{1,0:T(8,128)(2,1)S(1)} %bitcast.22, s32[128,4]{1,0:T(8,128)S(1)} %bitcast_add_fusion.target, f32[128,4]{1,0:T(8,128)S(1)} %bitcast.25, f32[32,4096]{1,0:T(8,128)S(1)} %copy-done.10, bf16[32,4096]{1,0:T(8,128)(2,1)S(1)} %get-tuple-element.57.s0, ...), custom_call_target="tpu_custom_call" | custom-call | flops 268435456 | bytes 2097152 | tf_op jit(solution)/shard_map/pallas_call | solution.py:33
  (92 shorter events, 16.5 us)
Async XLA Ops:
  0.0 73.6 %copy-start = (bf16[128,4096]{1,0:T(8,128)(2,1)S(1)}, bf16[128,4096]{1,0:T(8,128)(2,1)}, u32[]{:S(2)}) copy-start(bf16[128,4096]{1,0:T(8,128)(2,1)} %param.30) | copy-start | bytes 3145732
  0.0 1.0 copy-start.13
  1.0 0.9 copy-start.14
  1.9 0.8 copy-start.19
  5.1 33.5 %copy-start.24 = (f32[4096,2]{0,1:T(2,128)S(1)}, f32[4096,2]{0,1:T(2,128)}, u32[]{:S(2)}) copy-start(f32[4096,2]{0,1:T(2,128)} %param.27) | copy-start | bytes 98308
  5.1 28.7 %copy-start.15 = (bf16[64,768]{1,0:T(8,128)(2,1)}, bf16[64,768]{1,0:T(8,128)(2,1)S(1)}, u32[]{:S(2)}) copy-start(bf16[64,768]{1,0:T(8,128)(2,1)S(1)} %get-tuple-element.34.a.refs_3_) | copy-start | bytes 294916
  5.2 29.4 %copy-start.17 = (bf16[64,768]{1,0:T(8,128)(2,1)}, bf16[64,768]{1,0:T(8,128)(2,1)S(1)}, u32[]{:S(2)}) copy-start(bf16[64,768]{1,0:T(8,128)(2,1)S(1)} %get-tuple-element.35.a.refs_4_) | copy-start | bytes 294916
  5.2 6.0 %collective-permute-start.1 = (bf16[64,768]{1,0:T(8,128)(2,1)S(1)}, bf16[64,768]{1,0:T(8,128)(2,1)S(1)}, u32[]{:S(2)}, u32[]{:S(2)}) collective-permute-start(bf16[64,768]{1,0:T(8,128)(2,1)S(1)} %get-tuple-element.34.a.refs_3_), channel_id=1, source_target_pairs={{0,8},{8,16},{16,24},{24,0},{1,9},{9,17},{17,25},{25,1},{2,10},{10... | collective-permute-start | bytes 294920 | tf_op jit(solution)/shard_map/ppermute | solution.py:25
  6.9 5.1 %collective-permute-start.2 = (bf16[64,768]{1,0:T(8,128)(2,1)S(1)}, bf16[64,768]{1,0:T(8,128)(2,1)S(1)}, u32[]{:S(2)}, u32[]{:S(2)}) collective-permute-start(bf16[64,768]{1,0:T(8,128)(2,1)S(1)} %get-tuple-element.34.a.refs_3_), channel_id=1, source_target_pairs={{0,24},{8,0},{16,8},{24,16},{1,25},{9,1},{17,9},{25,17},{2,26},{10... | collective-permute-start | bytes 294920 | tf_op jit(solution)/shard_map/ppermute | solution.py:25
  8.5 6.1 %collective-permute-start.3 = (bf16[64,768]{1,0:T(8,128)(2,1)S(1)}, bf16[64,768]{1,0:T(8,128)(2,1)S(1)}, u32[]{:S(2)}, u32[]{:S(2)}) collective-permute-start(bf16[64,768]{1,0:T(8,128)(2,1)S(1)} %get-tuple-element.34.a.refs_3_), channel_id=1, source_target_pairs={{0,16},{8,24},{16,0},{24,8},{1,17},{9,25},{17,1},{25,9},{2,18},{10... | collective-permute-start | bytes 294920 | tf_op jit(solution)/shard_map/ppermute | solution.py:25
  15.4 24.3 %collective-permute-start.9 = (bf16[4,64,768]{2,1,0:T(8,128)(2,1)}, bf16[4,64,768]{2,1,0:T(8,128)(2,1)S(1)}, u32[]{:S(2)}, u32[]{:S(2)}) collective-permute-start(bf16[4,64,768]{2,1,0:T(8,128)(2,1)} %shard_map.191.refs_6_), channel_id=1, source_target_pairs={{0,32},{32,64},{64,96},{96,0},{1,33},{33,65},{65,97},{97,1},{2,34}... | collective-permute-start | bytes 1179656 | tf_op jit(solution)/shard_map/ppermute | solution.py:25
  17.4 21.9 %collective-permute-start = (bf16[128,1024]{1,0:T(8,128)(2,1)S(1)}, bf16[128,1024]{1,0:T(8,128)(2,1)S(1)}, u32[]{:S(2)}, u32[]{:S(2)}) collective-permute-start(bf16[128,1024]{1,0:T(8,128)(2,1)S(1)} %get-tuple-element.33.refs_0_), channel_id=1, source_target_pairs={{0,4},{4,0},{1,5},{5,1},{2,6},{6,2},{3,7},{7,3},{8,12},{12,8},{9,1... | collective-permute-start | bytes 786440 | tf_op jit(solution)/shard_map/ppermute | solution.py:29
  17.4 13.3 %collective-permute-start.5 = (bf16[64,768]{1,0:T(8,128)(2,1)S(1)}, bf16[64,768]{1,0:T(8,128)(2,1)S(1)}, u32[]{:S(2)}, u32[]{:S(2)}) collective-permute-start(bf16[64,768]{1,0:T(8,128)(2,1)S(1)} %get-tuple-element.35.a.refs_4_), channel_id=1, source_target_pairs={{0,32},{32,64},{64,96},{96,0},{1,33},{33,65},{65,97},{97,1},{2,34}... | collective-permute-start | bytes 294920 | tf_op jit(solution)/shard_map/ppermute | solution.py:25
  19.3 13.2 %collective-permute-start.6 = (bf16[64,768]{1,0:T(8,128)(2,1)S(1)}, bf16[64,768]{1,0:T(8,128)(2,1)S(1)}, u32[]{:S(2)}, u32[]{:S(2)}) collective-permute-start(bf16[64,768]{1,0:T(8,128)(2,1)S(1)} %get-tuple-element.35.a.refs_4_), channel_id=1, source_target_pairs={{0,96},{32,0},{64,32},{96,64},{1,97},{33,1},{65,33},{97,65},{2,98}... | collective-permute-start | bytes 294920 | tf_op jit(solution)/shard_map/ppermute | solution.py:25
  20.6 12.3 %collective-permute-start.7 = (bf16[64,768]{1,0:T(8,128)(2,1)S(1)}, bf16[64,768]{1,0:T(8,128)(2,1)S(1)}, u32[]{:S(2)}, u32[]{:S(2)}) collective-permute-start(bf16[64,768]{1,0:T(8,128)(2,1)S(1)} %get-tuple-element.35.a.refs_4_), channel_id=1, source_target_pairs={{0,64},{32,96},{64,0},{96,32},{1,65},{33,97},{65,1},{97,33},{2,66}... | collective-permute-start | bytes 294920 | tf_op jit(solution)/shard_map/ppermute | solution.py:25
  30.8 18.7 %collective-permute-start.10 = (bf16[4,64,768]{2,1,0:T(8,128)(2,1)}, bf16[4,64,768]{2,1,0:T(8,128)(2,1)S(1)}, u32[]{:S(2)}, u32[]{:S(2)}) collective-permute-start(bf16[4,64,768]{2,1,0:T(8,128)(2,1)} %shard_map.191.refs_6_), channel_id=1, source_target_pairs={{0,96},{32,0},{64,32},{96,64},{1,97},{33,1},{65,33},{97,65},{2,98}... | collective-permute-start | bytes 1179656 | tf_op jit(solution)/shard_map/ppermute | solution.py:25
  33.8 15.7 %collective-permute-start.11 = (bf16[4,64,768]{2,1,0:T(8,128)(2,1)}, bf16[4,64,768]{2,1,0:T(8,128)(2,1)S(1)}, u32[]{:S(2)}, u32[]{:S(2)}) collective-permute-start(bf16[4,64,768]{2,1,0:T(8,128)(2,1)} %shard_map.192.refs_7_), channel_id=1, source_target_pairs={{0,8},{8,16},{16,24},{24,0},{1,9},{9,17},{17,25},{25,1},{2,10},{10... | collective-permute-start | bytes 1179656 | tf_op jit(solution)/shard_map/ppermute | solution.py:25
  34.5 17.0 %collective-permute-start.12 = (bf16[4,64,768]{2,1,0:T(8,128)(2,1)}, bf16[4,64,768]{2,1,0:T(8,128)(2,1)S(1)}, u32[]{:S(2)}, u32[]{:S(2)}) collective-permute-start(bf16[4,64,768]{2,1,0:T(8,128)(2,1)} %shard_map.192.refs_7_), channel_id=1, source_target_pairs={{0,24},{8,0},{16,8},{24,16},{1,25},{9,1},{17,9},{25,17},{2,26},{10... | collective-permute-start | bytes 1179656 | tf_op jit(solution)/shard_map/ppermute | solution.py:25
  39.3 16.0 %collective-permute-start.4 = (bf16[4,64,768]{2,1,0:T(8,128)(2,1)}, bf16[4,64,768]{2,1,0:T(8,128)(2,1)S(1)}, u32[]{:S(2)}, u32[]{:S(2)}) collective-permute-start(bf16[4,64,768]{2,1,0:T(8,128)(2,1)} %shard_map.191.refs_6_), channel_id=1, source_target_pairs={{0,64},{32,96},{64,0},{96,32},{1,65},{33,97},{65,1},{97,33},{2,66}... | collective-permute-start | bytes 1179656 | tf_op jit(solution)/shard_map/ppermute | solution.py:25
  39.7 15.6 %collective-permute-start.8 = (bf16[4,64,768]{2,1,0:T(8,128)(2,1)}, bf16[4,64,768]{2,1,0:T(8,128)(2,1)}, u32[]{:S(2)}, u32[]{:S(2)}) collective-permute-start(bf16[4,64,768]{2,1,0:T(8,128)(2,1)} %shard_map.192.refs_7_), channel_id=1, source_target_pairs={{0,16},{8,24},{16,0},{24,8},{1,17},{9,25},{17,1},{25,9},{2,18},{10... | collective-permute-start | bytes 1179656 | tf_op jit(solution)/shard_map/ppermute | solution.py:25
  44.4 0.9 copy-start.16
  45.3 0.9 copy-start.18
  55.3 4.4 %copy-start.26 = (s32[128]{0:T(128)S(1)}, s32[128]{0:T(128)}, u32[]{:S(2)}) copy-start(s32[128]{0:T(128)} %eq.15) | copy-start | bytes 1540
  55.3 4.8 %copy-start.25 = (s32[32,4]{0,1:T(4,128)S(1)}, s32[32,4]{0,1:T(4,128)}, u32[]{:S(2)}) copy-start(s32[32,4]{0,1:T(4,128)} %param.32) | copy-start | bytes 1540
  59.7 2.2 %collective-permute-start.13 = (f32[128,1152]{1,0:T(8,128)}, f32[128,1152]{1,0:T(8,128)S(1)}, u32[]{:S(2)}, u32[]{:S(2)}) collective-permute-start(f32[128,1152]{1,0:T(8,128)} %get-tuple-element.49), channel_id=1, source_target_pairs={{0,4},{4,0},{1,5},{5,1},{2,6},{6,2},{3,7},{7,3},{8,12},{12,8},{9,1... | collective-permute-start | bytes 1769480 | tf_op jit(solution)/shard_map/ppermute | solution.py:29
  61.9 2.2 %copy-start.1 = (bf16[512,4096]{1,0:T(8,128)(2,1)S(1)}, bf16[512,4096]{1,0:T(8,128)(2,1)}, u32[]{:S(2)}) copy-start(bf16[512,4096]{1,0:T(8,128)(2,1)} %narrow.1) | copy-start | bytes 12582916
  64.1 2.2 %copy-start.2 = (bf16[512,4096]{1,0:T(8,128)(2,1)S(1)}, bf16[512,4096]{1,0:T(8,128)(2,1)}, u32[]{:S(2)}) copy-start(bf16[512,4096]{1,0:T(8,128)(2,1)} %broad.1) | copy-start | bytes 12582916
  66.3 17.8 %copy-start.23 = (f32[4096]{0:T(1024)S(1)}, f32[4096]{0:T(1024)}, u32[]{:S(2)}) copy-start(f32[4096]{0:T(1024)} %param.31) | copy-start | bytes 49156
  66.3 57.3 %copy-start.5 = (bf16[1,256,4096]{2,1,0:T(8,128)(2,1)S(1)}, bf16[1,256,4096]{2,1,0:T(8,128)(2,1)}, u32[]{:S(2)}) copy-start(bf16[1,256,4096]{2,1,0:T(8,128)(2,1)} %down.2) | copy-start | bytes 6291460
  67.8 9.6 %collective-permute-start.14 = (bf16[32,4096]{1,0:T(8,128)(2,1)S(1)}, bf16[32,4096]{1,0:T(8,128)(2,1)S(1)}, u32[]{:S(2)}, u32[]{:S(2)}) collective-permute-start(bf16[32,4096]{1,0:T(8,128)(2,1)S(1)} %get-tuple-element.51), channel_id=1, source_target_pairs={{0,1},{1,2},{2,3},{3,0},{4,5},{5,6},{6,7},{7,4},{8,9},{9,10},{10,1... | collective-permute-start | bytes 786440 | tf_op jit(solution)/shard_map/ppermute | solution.py:25
  69.4 14.7 %collective-permute-start.15 = (bf16[32,4096]{1,0:T(8,128)(2,1)S(1)}, bf16[32,4096]{1,0:T(8,128)(2,1)S(1)}, u32[]{:S(2)}, u32[]{:S(2)}) collective-permute-start(bf16[32,4096]{1,0:T(8,128)(2,1)S(1)} %get-tuple-element.52), channel_id=1, source_target_pairs={{0,2},{1,3},{2,0},{3,1},{4,6},{5,7},{6,4},{7,5},{8,10},{9,11},{10,... | collective-permute-start | bytes 786440 | tf_op jit(solution)/shard_map/ppermute | solution.py:25
  72.1 11.9 %collective-permute-start.16 = (bf16[32,4096]{1,0:T(8,128)(2,1)S(1)}, bf16[32,4096]{1,0:T(8,128)(2,1)S(1)}, u32[]{:S(2)}, u32[]{:S(2)}) collective-permute-start(bf16[32,4096]{1,0:T(8,128)(2,1)S(1)} %get-tuple-element.53), channel_id=1, source_target_pairs={{0,3},{1,0},{2,1},{3,2},{4,7},{5,4},{6,5},{7,6},{8,11},{9,8},{10,9... | collective-permute-start | bytes 786440 | tf_op jit(solution)/shard_map/ppermute | solution.py:25
  85.9 50.4 %copy-start.11 = (bf16[32,4096]{1,0:T(8,128)(2,1)}, bf16[32,4096]{1,0:T(8,128)(2,1)S(1)}, u32[]{:S(2)}) copy-start(bf16[32,4096]{1,0:T(8,128)(2,1)S(1)} %get-tuple-element.56.n0) | copy-start | bytes 786436
  85.9 37.7 %copy-start.3 = (bf16[1,4096,256]{2,1,0:T(8,128)(2,1)S(1)}, bf16[1,4096,256]{2,1,0:T(8,128)(2,1)}, u32[]{:S(2)}) copy-start(bf16[1,4096,256]{2,1,0:T(8,128)(2,1)} %gate.2) | copy-start | bytes 6291460
  85.9 37.7 %copy-start.4 = (bf16[1,4096,256]{2,1,0:T(8,128)(2,1)S(1)}, bf16[1,4096,256]{2,1,0:T(8,128)(2,1)}, u32[]{:S(2)}) copy-start(bf16[1,4096,256]{2,1,0:T(8,128)(2,1)} %up.2) | copy-start | bytes 6291460
  127.9 51.5 %copy-start.27 = (f32[32,4]{0,1:T(4,128)S(1)}, f32[32,4]{0,1:T(4,128)}, u32[]{:S(2)}) copy-start(f32[32,4]{0,1:T(4,128)} %param.33) | copy-start | bytes 1540
  127.9 64.1 %all-to-all-start.1 = ((bf16[128,8,1024]{2,1,0:T(8,128)(2,1)}), bf16[128,8,1024]{2,1,0:T(8,128)(2,1)S(1)}, u32[]{:S(2)}, u32[]{:S(2)}) async-start(bf16[128,8,1024]{2,1,0:T(8,128)(2,1)} %bitcast.11), calls=%async_computation.1 | async-start | bytes 4194304 | tf_op jit(solution)/shard_map/all_to_all | solution.py:391
  132.7 30.8 %collective-permute-start.17 = (bf16[32,4096]{1,0:T(8,128)(2,1)S(1)}, bf16[32,4096]{1,0:T(8,128)(2,1)S(1)}, u32[]{:S(2)}, u32[]{:S(2)}) collective-permute-start(bf16[32,4096]{1,0:T(8,128)(2,1)S(1)} %get-tuple-element.56.n0), channel_id=1, source_target_pairs={{0,1},{1,2},{2,3},{3,0},{4,5},{5,6},{6,7},{7,4},{8,9},{9,10},{10,1... | collective-permute-start | bytes 786440 | tf_op jit(solution)/shard_map/ppermute | solution.py:25
  133.6 35.5 %collective-permute-start.18 = (bf16[32,4096]{1,0:T(8,128)(2,1)S(1)}, bf16[32,4096]{1,0:T(8,128)(2,1)S(1)}, u32[]{:S(2)}, u32[]{:S(2)}) collective-permute-start(bf16[32,4096]{1,0:T(8,128)(2,1)S(1)} %get-tuple-element.56.n0), channel_id=1, source_target_pairs={{0,2},{1,3},{2,0},{3,1},{4,6},{5,7},{6,4},{7,5},{8,10},{9,11},{10,... | collective-permute-start | bytes 786440 | tf_op jit(solution)/shard_map/ppermute | solution.py:25
  136.3 32.8 %collective-permute-start.19 = (bf16[32,4096]{1,0:T(8,128)(2,1)S(1)}, bf16[32,4096]{1,0:T(8,128)(2,1)S(1)}, u32[]{:S(2)}, u32[]{:S(2)}) collective-permute-start(bf16[32,4096]{1,0:T(8,128)(2,1)S(1)} %get-tuple-element.56.n0), channel_id=1, source_target_pairs={{0,3},{1,0},{2,1},{3,2},{4,7},{5,4},{6,5},{7,6},{8,11},{9,8},{10,9... | collective-permute-start | bytes 786440 | tf_op jit(solution)/shard_map/ppermute | solution.py:25
  169.1 1.6 copy-start.6
  170.7 1.6 copy-start.7
  172.3 1.6 copy-start.8
  173.9 0.9 copy-start.12
  176.8 9.5 %collective-permute-start.20 = (bf16[32,4096]{1,0:T(8,128)(2,1)}, bf16[32,4096]{1,0:T(8,128)(2,1)}, u32[]{:S(2)}, u32[]{:S(2)}) collective-permute-start(bf16[32,4096]{1,0:T(8,128)(2,1)} %get-tuple-element.58), channel_id=1, source_target_pairs={{0,3},{1,0},{2,1},{3,2},{4,7},{5,4},{6,5},{7,6},{8,11},{9,8},{10,9... | collective-permute-start | bytes 786440 | tf_op jit(solution)/shard_map/ppermute | solution.py:25
  176.9 11.0 %collective-permute-start.21 = (bf16[32,4096]{1,0:T(8,128)(2,1)}, bf16[32,4096]{1,0:T(8,128)(2,1)}, u32[]{:S(2)}, u32[]{:S(2)}) collective-permute-start(bf16[32,4096]{1,0:T(8,128)(2,1)} %get-tuple-element.59), channel_id=1, source_target_pairs={{0,2},{1,3},{2,0},{3,1},{4,6},{5,7},{6,4},{7,5},{8,10},{9,11},{10,... | collective-permute-start | bytes 786440 | tf_op jit(solution)/shard_map/ppermute | solution.py:25
  178.8 13.2 %collective-permute-start.22 = (bf16[32,4096]{1,0:T(8,128)(2,1)}, bf16[32,4096]{1,0:T(8,128)(2,1)}, u32[]{:S(2)}, u32[]{:S(2)}) collective-permute-start(bf16[32,4096]{1,0:T(8,128)(2,1)} %get-tuple-element.60), channel_id=1, source_target_pairs={{0,1},{1,2},{2,3},{3,0},{4,5},{5,6},{6,7},{7,4},{8,9},{9,10},{10,1... | collective-permute-start | bytes 786440 | tf_op jit(solution)/shard_map/ppermute | solution.py:25
  192.0 1.0 copy-start.10
  (4 other events, 3.2 us)

commit v3 on v2

--- a/solution.py
+++ b/solution.py
@@ -7,6 +7,7 @@
 from jax.experimental.pallas import tpu as pltpu
 from jax.sharding import Mesh
 from jax.sharding import PartitionSpec as P
+
 
 SP = ("z", "y", "c")
 NARROW_SIZE = 128
@@ -17,6 +18,7 @@
 ORDER = (0, 1, 3, 2)
 VMEM = pl.BlockSpec(memory_space=pltpu.VMEM)
 SMEM = pl.BlockSpec(memory_space=pltpu.SMEM)
+HBM = pl.BlockSpec(memory_space=pltpu.HBM)
 BF = jnp.bfloat16
 F32 = jnp.float32
 
@@ -29,11 +31,21 @@
     return lax.ppermute(x, "c", [(0, 1), (1, 0)])
 
 
-def call(kernel, operands, shapes, smem=(), scratch=(), mib=32, flops=0):
+def turn(x, k, phase):
+    pairs = []
+    for z in range(4):
+        for y in range(4):
+            for c in range(2):
+                to_z, to_y = (z, (y + k) % 4) if c == phase else ((z + k) % 4, y)
+                pairs.append(((z * 4 + y) * 2 + c, (to_z * 4 + to_y) * 2 + c))
+    return lax.ppermute(x, SP, pairs)
+
+
+def call(kernel, operands, shapes, smem=(), hbm=(), scratch=(), mib=16, flops=0):
     return pl.pallas_call(
         kernel,
         out_shape=shapes,
-        in_specs=[SMEM if i in smem else VMEM for i in range(len(operands))],
+        in_specs=[SMEM if i in smem else HBM if i in hbm else VMEM for i in range(len(operands))],
         out_specs=[VMEM] * len(shapes),
         scratch_shapes=list(scratch),
         compiler_params=pltpu.CompilerParams(vmem_limit_bytes=mib * 1024 * 1024),
@@ -45,12 +57,15 @@
     return jax.ShapeDtypeStruct(shape, dtype)
 
 
-def pack_kernel(kn, vn, kb, vb, qn, qb, a, b, q):
-    for at, ref in ((0, kn), (128, vn), (256, kb), (512, vb)):
-        a[:, at : at + ref.shape[1]] = ref[:64]
-        b[:, at : at + ref.shape[1]] = ref[64:]
-    q[:, :512] = qn[...]
-    q[:, 512:] = qb[...]
+def pack_kernel(kn, vn, kb, vb, qn, qb, kv, q, sems):
+    copies = []
+    for ref, out, at in ((kn, kv, 0), (vn, kv, 128), (kb, kv, 256), (vb, kv, 512), (qn, q, 0), (qb, q, 512)):
+        target = out.at[:, at : at + ref.shape[1]]
+        copies.append(pltpu.make_async_copy(ref, target, sems.at[len(copies)]))
+    for copy in copies:
+        copy.start()
+    for copy in copies:
+        copy.wait()
 
 
 def stack_kernel(a, b, c, d, out):
@@ -58,26 +73,27 @@
         out[i] = ref[...]
 
 
-def bias_kernel(place, gates, own, first, second, third):
-    z, y = place[0], place[1]
+def bias_kernel(place, narrow, broad, own, first, second, third):
+    z, y, c = place[0], place[1], place[2]
     here = z * 4 + y
-    own[...] = gates[here]
-
-    def put(out, at, back_z, back_y, half):
+
+    def put(out, at, early, late):
+        back_y = jnp.where(c == 0, early, late)
+        back_z = jnp.where(c == 0, late, early)
         chip = ((z + 4 - back_z) % 4) * 4 + (y + 4 - back_y) % 4
-        piece = gates[chip][:, half * 64 : half * 64 + 64]
-        out[:, at : at + 64] = jnp.where(chip > here, MASKED, piece)
-
+        block = pl.multiple_of(chip * 256 + c * 128, 128)
+        ahead = chip > here
+        for row, gates in ((0, narrow), (4, broad)):
+            piece = gates[:, pl.ds(block, 128)] * (-LOG2E)
+            out[row : row + gates.shape[0], at : at + 128] = jnp.where(ahead, MASKED, piece)
+
+    put(own, 0, 0, 0)
     for i in range(1, 4):
-        put(first, (i - 1) * 64, 0, ORDER[i], 0)
-        put(first, 192 + (i - 1) * 64, ORDER[i], 0, 1)
+        put(first, (i - 1) * 128, ORDER[i], 0)
     for i in range(4):
-        put(second, i * 64, 1, ORDER[i], 0)
-        put(second, 256 + i * 64, 3, ORDER[i], 0)
-        put(second, 512 + i * 64, ORDER[i], 1, 1)
-        put(second, 768 + i * 64, ORDER[i], 3, 1)
-        put(third, i * 64, 2, ORDER[i], 0)
-        put(third, 256 + i * 64, ORDER[i], 2, 1)
+        put(second, i * 128, ORDER[i], 1)
+        put(second, 512 + i * 128, ORDER[i], 3)
+        put(third, i * 128, ORDER[i], 2)
 
 
 def project_kernel(place, own, other, narrow, broad, *refs):
@@ -179,10 +195,17 @@
             planes += tiles[-1][0]
     if not first:
         m_in, l_in, an_in, ab_in = take(4)
+    if first:
+        weights_in = take(2)
     if last:
         own_out, send_out = take(2)
     else:
         m_out, l_out, an_out, ab_out = take(4)
+    if first:
+        weights_out, sems = take(2), take(1)[0]
+        copies = [pltpu.make_async_copy(weights_in[i], weights_out[i], sems.at[i]) for i in range(2)]
+        for copy in copies:
+            copy.start()
 
     def keys(ref, lo, hi):
         value = ref[1:, :, lo:hi] if any(ref is p for p in planes) else ref[..., lo:hi]
@@ -226,7 +249,6 @@
                     p = jnp.exp2(s - m)
                     l = l + jnp.sum(p, axis=1, keepdims=True)
                     acc = acc + jnp.dot(p.astype(BF), v, preferred_element_type=F32)
-                acc_in, acc_out = (None, None)
                 if not first:
                     a_in = an_in if group == "n" else ab_in
                     factor = jnp.exp2(m_old - m)
@@ -251,9 +273,12 @@
             for h in range(6):
                 stats = jnp.where(lane == h, results[(side, h)], stats)
             out[:, 1024:1152] = stats
-
-
-def attend(q_own, q_other, core, tiles, state, last):
+    if first:
+        for copy in copies:
+            copy.wait()
+
+
+def attend(q_own, q_other, core, tiles, state, last, weights=None):
     counts = tuple((len(arrays), own_block) for arrays, _, own_block in tiles)
     operands = [q_own, q_other, core]
     n_keys = 0
@@ -265,6 +290,9 @@
     if state is not None:
         operands += list(state)
         specs += [VMEM] * 4
+    else:
+        operands += list(weights)
+        specs += [HBM] * 2
     if last:
         shapes = [jax.ShapeDtypeStruct((128, 1152), F32)] * 2
     else:
@@ -274,11 +302,14 @@
             jax.ShapeDtypeStruct((1024, 128), F32),
             jax.ShapeDtypeStruct((512, 256), F32),
         ]
+    if state is None:
+        shapes += [jax.ShapeDtypeStruct(w.shape, w.dtype) for w in weights]
     return pl.pallas_call(
         functools.partial(attend_kernel, counts, state is None, last),
         out_shape=shapes,
         in_specs=specs,
         out_specs=[VMEM] * len(shapes),
+        scratch_shapes=[pltpu.SemaphoreType.DMA((2,))] if state is None else [],
         compiler_params=pltpu.CompilerParams(vmem_limit_bytes=24 * 1024 * 1024),
         cost_estimate=pl.CostEstimate(
             flops=4 * n_keys * 256 * 1024, transcendentals=n_keys * 1536, bytes_accessed=4 * 1024 * 1024
@@ -310,45 +341,36 @@
 ):
     z, y, c, t = (lax.axis_index(n).astype(jnp.int32) for n in ("z", "y", "c", "tp"))
 
-    own_a, own_b, q_own = call(
+    own_kv, q_own = call(
         pack_kernel,
         (key_narrow, value_narrow, key_broad, value_broad, query_narrow, query_broad),
-        [shaped((64, 768), BF)] * 2 + [shaped((128, 1024), BF)],
-    )
-    first_a = [shift(own_a, "y", k) for k in ORDER[1:]]
-    first_b = [shift(own_b, "z", k) for k in ORDER[1:]]
+        [shaped((128, 768), BF), shaped((128, 1024), BF)],
+        hbm=range(6),
+        scratch=[pltpu.SemaphoreType.DMA((6,))],
+    )
+    line = [turn(own_kv, k, 0) for k in ORDER[1:]]
     q_other = swap_core(q_own)
-    (plane_a,) = call(stack_kernel, [own_a] + first_a, [shaped((4, 64, 768), BF)])
-    (plane_b,) = call(stack_kernel, [own_b] + first_b, [shaped((4, 64, 768), BF)])
-    a_back, b_back, a_ahead, b_ahead, a_far, b_far = (
-        shift(plane, axis, k) for k in ORDER[1:] for plane, axis in ((plane_a, "z"), (plane_b, "y"))
-    )
-
-    gates = jnp.concatenate([gates_narrow, gates_broad], axis=1) * (-LOG2E)
-    gates = lax.dynamic_index_in_dim(gates.reshape(16, 2, 128, 6), c, 1, keepdims=False)
-    gates = jnp.pad(gates.transpose(0, 2, 1), ((0, 0), (0, 2), (0, 0)))
+    (plane,) = call(stack_kernel, [own_kv] + line, [shaped((4, 128, 768), BF)])
+    back, ahead, far = (turn(plane, k, 1) for k in ORDER[1:])
+
     own_bias, bias_1, bias_2, bias_3 = call(
         bias_kernel,
-        (jnp.stack([z, y]), gates),
+        (jnp.stack([z, y, c]), gates_narrow.T, gates_broad.T),
         [shaped((8, n), F32) for n in (128, 384, 1024, 512)],
         smem=(0,),
     )
     core = c.reshape(1)
-    state = attend(
-        q_own,
-        q_other,
-        core,
-        [((own_a, own_b), own_bias, True), ((plane_a, plane_b), bias_1, False)],
-        None,
-        False,
-    )
-    state = attend(q_own, q_other, core, [((a_back, a_ahead, b_back, b_ahead), bias_2, False)], state, False)
-    own_part, send_part = attend(q_own, q_other, core, [((a_far, b_far), bias_3, False)], state, True)
+    first_tiles = [((own_kv,), own_bias, True), ((plane,), bias_1, False)]
+    *state, narrow, broad = attend(
+        q_own, q_other, core, first_tiles, None, False, (project_narrow, project_broad)
+    )
+    state = attend(q_own, q_other, core, [((back, ahead), bias_2, False)], state, False)
+    own_part, send_part = attend(q_own, q_other, core, [((far,), bias_3, False)], state, True)
     other_part = swap_core(send_part)
 
     p0, p1, p2, p3 = call(
         project_kernel,
-        (t.reshape(1), own_part, other_part, project_narrow, project_broad),
+        (t.reshape(1), own_part, other_part, narrow, broad),
         [shaped((32, 4096), BF)] * 4,
         smem=(0,),
         scratch=[pltpu.VMEM((128, 4096), F32), pltpu.VMEM((128, 1024), BF)],
@@ -372,14 +394,18 @@
     every = SP + ("tp",)
     inbound = lax.all_to_all(outbound.reshape(128, 8, 1024), every, 0, 0, tiled=True)
 
-    n1, n2, n3 = (shift(normed, "tp", k) for k in (1, 2, 3))
+    n1 = shift(normed, "tp", 1)
+    n2 = shift(normed, "tp", 2)
+    n3 = shift(normed, "tp", 3)
     s0, s1, s2, s3 = call(
         shared_kernel,
         (normed, n1, n2, n3, shared_gate, shared_up, shared_down),
         [shaped((32, 4096), BF)] * 4,
         flops=2 * 128 * 4096 * 768,
     )
-    s1, s2, s3 = shift(s1, "tp", 3), shift(s2, "tp", 2), shift(s3, "tp", 1)
+    s1 = shift(s1, "tp", 3)
+    s2 = shift(s2, "tp", 2)
+    s3 = shift(s3, "tp", 1)
 
     (result,) = call(
         expert_kernel,
@@ -423,4 +449,5 @@
         P(None, "tp"),
         P("tp", None),
     )
+
     return jax.shard_map(local, mesh=mesh, in_specs=placed, out_specs=P(every, None), check_vma=False)

time: 198 us -> 186 us (0.939)
  starting transfers between devices: 36.9 us -> 29.9 us
  waiting for transfers between devices: 70.1 us -> 66.1 us
    ppermute x21 -> x9, starting transfers between devices: 32.1 us -> 13.4 us  [shift(): return lax.ppermute(x, axis, [(i, (i + k) % 4) for i in range(4)])]
    ppermute x21 -> x9, waiting for transfers between devices: 68.5 us -> 54.3 us  [shift(): return lax.ppermute(x, axis, [(i, (i + k) % 4) for i in range(4)])]
    ppermute x0 -> x6, starting transfers between devices: none -> 11.5 us  [turn(): return lax.ppermute(x, SP, pairs)]
    ppermute x0 -> x6, waiting for transfers between devices: none -> 10.4 us  [turn(): return lax.ppermute(x, SP, pairs)]
    unnamed x57, local copies, waits for them, and re-layouts: 19.6 us -> 24.1 us
    concatenate x4 -> x0, local copies, waits for them, and re-layouts: 2.25 us -> none  [local(): gates = jnp.concatenate([gates_narrow, gates_broad], axis=1) * -LOG2E]
    pallas_call x9 -> x8, Pallas kernels: 13.8 us -> 12.4 us  [call(): pl.pallas_call(kernel, out_shape=shapes, in_specs=[SMEM if i in smem else...]
  transfers between devices with their start and end apart: 24 -> 18, of which waited for: 14 -> 12; matrix products, arithmetic and copies ran while one was open for 3% -> 1% of each run, Pallas kernels for 5% -> 6%
where the time goes in v3:
time: 186 us; the launch traced here: 184 us
  waiting for transfers between devices  66.1 us (36%)
  blocking collectives  39.1 us (21%)
  starting transfers between devices  29.9 us (16%)
  local copies, waits for them, and re-layouts  24.7 us (13%)
  Pallas kernels  24 us (13%)
    ppermute x9, waiting for transfers between devices, shift(): return lax.ppermute(x, axis, [(i, (i + k) % 4) for i in range(4)])  54.3 us
    all_to_all x1, blocking collectives, local(): lax.all_to_all(outbound.reshape(128, 8, 1024), every, 0, 0, tiled=True)  39.1 us
    unnamed x57, local copies, waits for them, and re-layouts  24.1 us
    ppermute x9, starting transfers between devices, shift(): return lax.ppermute(x, axis, [(i, (i + k) % 4) for i in range(4)])  13.4 us
    pallas_call x8, Pallas kernels, call(): pl.pallas_call(kernel, out_shape=shapes, in_specs=[SMEM if i in smem else...  12.4 us
    pallas_call x3, Pallas kernels, attend(): pl.pallas_call(functools.partial(attend_kernel, counts, state is None, la...  11.6 us
    ppermute x6, starting transfers between devices, turn(): return lax.ppermute(x, SP, pairs)  11.5 us
    ppermute x6, waiting for transfers between devices, turn(): return lax.ppermute(x, SP, pairs)  10.4 us
  transfers between devices with their start and end apart: 18, of which 12 were waited for; matrix products, arithmetic and copies ran while one was open for 1% of the time, Pallas kernels for 6%

profile of v3, /device:TPU:0, one launch (start us, length us, event | category | flops | bytes accessed | tf_op | source)
XLA Modules:
  0.0 184.3 jit_solution(6829287210002630093)
XLA Ops:
  0.0 1.0 copy-done.17
  1.0 0.9 copy-done.18
  1.9 0.8 copy-done.19
  2.7 0.8 copy-done.20
  5.2 1.8 collective-permute-start.1
  7.0 1.5 collective-permute-start.2
  8.5 2.1 %collective-permute-start.3 = (bf16[128,768]{1,0:T(8,128)(2,1)S(1)}, bf16[128,768]{1,0:T(8,128)(2,1)S(1)}, u32[]{:S(2)}, u32[]{:S(2)}) collective-permute-start(bf16[128,768]{1,0:T(8,128)(2,1)S(1)} %get-tuple-element.35.a.refs_3_), channel_id=1, source_target_pairs={{0,16},{4,68},{8,24},{12,76},{16,0},{20,84},{24,8},{28,92},{32,48}... | collective-permute-start | bytes 589832 | tf_op jit(solution)/shard_map/ppermute | solution.py:41
  10.6 1.5 collective-permute-done.1.b
  12.7 3.1 %collective-permute-done.3.d = bf16[128,768]{1,0:T(8,128)(2,1)S(1)} collective-permute-done((bf16[128,768]{1,0:T(8,128)(2,1)S(1)}, bf16[128,768]{1,0:T(8,128)(2,1)S(1)}, u32[]{:S(2)}, u32[]{:S(2)}) %collective-permute-start.3) | collective-permute-done | bytes 196640 | tf_op jit(solution)/shard_map/ppermute | solution.py:41
  15.8 2.1 %collective-permute-start.5 = (bf16[4,128,768]{2,1,0:T(8,128)(2,1)S(1)}, bf16[4,128,768]{2,1,0:T(8,128)(2,1)S(1)}, u32[]{:S(2)}, u32[]{:S(2)}) collective-permute-start(bf16[4,128,768]{2,1,0:T(8,128)(2,1)S(1)} %shard_map.191.refs_5_), channel_id=1, source_target_pairs={{0,32},{4,12},{8,40},{12,20},{16,48},{20,28},{24,56},{28,4},{32,64... | collective-permute-start | bytes 2359304 | tf_op jit(solution)/shard_map/ppermute | solution.py:41
  17.9 2.2 %collective-permute-start.6 = (bf16[4,128,768]{2,1,0:T(8,128)(2,1)S(1)}, bf16[4,128,768]{2,1,0:T(8,128)(2,1)}, u32[]{:S(2)}, u32[]{:S(2)}) collective-permute-start(bf16[4,128,768]{2,1,0:T(8,128)(2,1)S(1)} %shard_map.191.refs_5_), channel_id=1, source_target_pairs={{0,96},{4,28},{8,104},{12,4},{16,112},{20,12},{24,120},{28,20},{32... | collective-permute-start | bytes 2359304 | tf_op jit(solution)/shard_map/ppermute | solution.py:41
  20.1 1.8 collective-permute-start.4
  23.5 2.2 %copy-done.1 = bf16[512,4096]{1,0:T(8,128)(2,1)S(1)} copy-done((bf16[512,4096]{1,0:T(8,128)(2,1)S(1)}, bf16[512,4096]{1,0:T(8,128)(2,1)}, u32[]{:S(2)}) %copy-start.1) | copy-done | bytes 4194328
  25.7 2.2 %copy-done.2 = bf16[512,4096]{1,0:T(8,128)(2,1)S(1)} copy-done((bf16[512,4096]{1,0:T(8,128)(2,1)S(1)}, bf16[512,4096]{1,0:T(8,128)(2,1)}, u32[]{:S(2)}) %copy-start.2) | copy-done | bytes 4194328
  27.9 2.8 %shard_map.193 = (f32[1536,128]{1,0:T(8,128)S(1)}, f32[1536,128]{1,0:T(8,128)S(1)}, f32[1024,128]{1,0:T(8,128)S(1)}, f32[512,256]{1,0:T(8,128)S(1)}, bf16[512,40...) custom-call(bf16[128,1024]{1,0:T(8,128)(2,1)S(1)} %get-tuple-element.34.refs_0_, ...), custom_call_target="tpu_custom_call" | custom-call | flops 536870912 | bytes 4194304 | tf_op jit(solution)/shard_map/pallas_call | solution.py:307
  30.7 2.0 %copy-done.5 = bf16[512,4096]{1,0:T(8,128)(2,1)} copy-done((bf16[512,4096]{1,0:T(8,128)(2,1)}, bf16[512,4096]{1,0:T(8,128)(2,1)S(1)}, u32[]{:S(2)}) %copy-start.5) | copy-done | bytes 4194328
  32.7 5.3 %collective-permute-done.6.refs_4_ = bf16[4,128,768]{2,1,0:T(8,128)(2,1)} collective-permute-done((bf16[4,128,768]{2,1,0:T(8,128)(2,1)S(1)}, bf16[4,128,768]{2,1,0:T(8,128)(2,1)}, u32[]{:S(2)}, u32[]{:S(2)}) %collective-permute-start.6) | collective-permute-done | bytes 786464 | tf_op jit(solution)/shard_map/ppermute | solution.py:41
  38.0 5.1 %shard_map.194 = (f32[1536,128]{1,0:T(8,128)S(1)}, f32[1536,128]{1,0:T(8,128)S(1)}, f32[1024,128]{1,0:T(8,128)S(1)}, f32[512,256]{1,0:T(8,128)S(1)}) custom-call(bf16[128,1024]{1,0:T(8,128)(2,1)S(1)} %get-tuple-element.34.refs_0_, bf16[128,1024]{1,0:T(8,128)(2,1)S(1)} %collective-permute-done.refs_1_, s32[1]{0:T(128)} %bitcast.1.refs_2_, ...), custom_call_target="tpu_custom_call" | custom-call | flops 1073741824 | bytes 4194304 | tf_op jit(solution)/shard_map/pallas_call | solution.py:307
  43.1 3.7 %shard_map.195 = (f32[128,1152]{1,0:T(8,128)S(1)}, f32[128,1152]{1,0:T(8,128)S(1)}) custom-call(bf16[128,1024]{1,0:T(8,128)(2,1)S(1)} %get-tuple-element.34.refs_0_, bf16[128,1024]{1,0:T(8,128)(2,1)S(1)} %collective-permute-done.refs_1_, s32[1]{0:T(128)} %bitcast.1.refs_2_, bf16[4,128,768]{2,1,0:T(8,128)(2,1)} %collective-permute-done.4.refs_3_, ...), custom_call_target="tpu_custom_call" | custom-call | flops 536870912 | bytes 4194304 | tf_op jit(solution)/shard_map/pallas_call | solution.py:307
  47.8 1.4 collective-permute-done.7.other
  49.1 2.2 %copy-done.4 = bf16[512,4096]{1,0:T(8,128)(2,1)S(1)} copy-done((bf16[512,4096]{1,0:T(8,128)(2,1)S(1)}, bf16[512,4096]{1,0:T(8,128)(2,1)}, u32[]{:S(2)}) %copy-start.4) | copy-done | bytes 4194328
  51.3 2.2 %copy-done.6 = bf16[512,4096]{1,0:T(8,128)(2,1)S(1)} copy-done((bf16[512,4096]{1,0:T(8,128)(2,1)S(1)}, bf16[512,4096]{1,0:T(8,128)(2,1)}, u32[]{:S(2)}) %copy-start.6) | copy-done | bytes 4194328
  53.5 1.5 shard_map.196
  55.0 1.6 collective-permute-start.8
  56.6 2.7 %collective-permute-start.9 = (bf16[32,4096]{1,0:T(8,128)(2,1)S(1)}, bf16[32,4096]{1,0:T(8,128)(2,1)S(1)}, u32[]{:S(2)}, u32[]{:S(2)}) collective-permute-start(bf16[32,4096]{1,0:T(8,128)(2,1)S(1)} %get-tuple-element.54), channel_id=1, source_target_pairs={{0,2},{1,3},{2,0},{3,1},{4,6},{5,7},{6,4},{7,5},{8,10},{9,11},{10,... | collective-permute-start | bytes 786440 | tf_op jit(solution)/shard_map/ppermute | solution.py:27
  59.3 1.4 collective-permute-start.10
  60.8 3.9 %collective-permute-done.8.p1 = bf16[32,4096]{1,0:T(8,128)(2,1)S(1)} collective-permute-done((bf16[32,4096]{1,0:T(8,128)(2,1)S(1)}, bf16[32,4096]{1,0:T(8,128)(2,1)S(1)}, u32[]{:S(2)}, u32[]{:S(2)}) %collective-permute-start.8) | collective-permute-done | bytes 262176 | tf_op jit(solution)/shard_map/ppermute | solution.py:27
  64.7 6.6 %collective-permute-done.9.p2 = bf16[32,4096]{1,0:T(8,128)(2,1)S(1)} collective-permute-done((bf16[32,4096]{1,0:T(8,128)(2,1)S(1)}, bf16[32,4096]{1,0:T(8,128)(2,1)S(1)}, u32[]{:S(2)}, u32[]{:S(2)}) %collective-permute-start.9) | collective-permute-done | bytes 262176 | tf_op jit(solution)/shard_map/ppermute | solution.py:27
  71.3 1.0 shard_map.197
  73.1 39.1 %all_to_all.10 = bf16[128,8,1024]{2,1,0:T(8,128)(2,1)S(1)} all-to-all(bf16[128,8,1024]{2,1,0:T(8,128)(2,1)S(1)} %bitcast.17), channel_id=1, replica_groups=mesh['z'=4,'y'=4,'c'=2,'tp'=4] {'z','y','c','tp'}, dimensions={0} | all-to-all | bytes 4194304 | tf_op jit(solution)/shard_map/all_to_all | solution.py:395
  112.2 4.3 %shard_map.198 = bf16[1024,1024]{1,0:T(8,128)(2,1)} custom-call(bf16[1024,1024]{1,0:T(8,128)(2,1)S(1)} %bitcast.15, bf16[1,4096,256]{2,1,0:T(8,128)(2,1)S(1)} %copy-done.7, bf16[1,4096,256]{2,1,0:T(8,128)(2,1)S(1)} %copy-done.8, bf16[1,256,4096]{2,1,0:T(8,128)(2,1)S(1)} %copy-done.9), custom_call_target="tpu_custom_call" | custom-call | flops 1610612736 | bytes 2097152 | tf_op jit(solution)/shard_map/pallas_call | solution.py:45
  116.5 4.8 %all-to-all-start.1 = ((bf16[128,8,1024]{2,1,0:T(8,128)(2,1)}), bf16[128,8,1024]{2,1,0:T(8,128)(2,1)S(1)}, u32[]{:S(2)}, u32[]{:S(2)}) async-start(bf16[128,8,1024]{2,1,0:T(8,128)(2,1)} %bitcast.11), calls=%async_computation.1 | async-start | bytes 4194304 | tf_op jit(solution)/shard_map/all_to_all | solution.py:417
  121.3 0.9 collective-permute-start.11
  122.2 2.7 %collective-permute-start.12 = (bf16[32,4096]{1,0:T(8,128)(2,1)S(1)}, bf16[32,4096]{1,0:T(8,128)(2,1)S(1)}, u32[]{:S(2)}, u32[]{:S(2)}) collective-permute-start(bf16[32,4096]{1,0:T(8,128)(2,1)S(1)} %get-tuple-element.58.n0), channel_id=1, source_target_pairs={{0,2},{1,3},{2,0},{3,1},{4,6},{5,7},{6,4},{7,5},{8,10},{9,11},{10,... | collective-permute-start | bytes 786440 | tf_op jit(solution)/shard_map/ppermute | solution.py:27
  124.9 1.4 collective-permute-start.13
  126.3 25.7 %collective-permute-done.11.n1 = bf16[32,4096]{1,0:T(8,128)(2,1)S(1)} collective-permute-done((bf16[32,4096]{1,0:T(8,128)(2,1)S(1)}, bf16[32,4096]{1,0:T(8,128)(2,1)S(1)}, u32[]{:S(2)}, u32[]{:S(2)}) %collective-permute-start.11) | collective-permute-done | bytes 262176 | tf_op jit(solution)/shard_map/ppermute | solution.py:27
  152.0 5.6 %collective-permute-done.12.n2 = bf16[32,4096]{1,0:T(8,128)(2,1)S(1)} collective-permute-done((bf16[32,4096]{1,0:T(8,128)(2,1)S(1)}, bf16[32,4096]{1,0:T(8,128)(2,1)S(1)}, u32[]{:S(2)}, u32[]{:S(2)}) %collective-permute-start.12) | collective-permute-done | bytes 262176 | tf_op jit(solution)/shard_map/ppermute | solution.py:27
  157.7 1.6 copy-done.10
  159.3 1.6 copy-done.11
  160.8 1.6 copy-done.12
  162.4 0.9 copy-done.16
  163.4 2.0 %shard_map.199 = (bf16[32,4096]{1,0:T(8,128)(2,1)S(1)}, bf16[32,4096]{1,0:T(8,128)(2,1)}, bf16[32,4096]{1,0:T(8,128)(2,1)}, bf16[32,4096]{1,0:T(8,128)(2,1)}) custom-call(bf16[32,4096]{1,0:T(8,128)(2,1)S(1)} %copy-done.16, bf16[32,4096]{1,0:T(8,128)(2,1)S(1)} %collective-permute-done.11.n1, bf16[32,4096]{1,0:T(8,128)(2,1)S(1)} %collective-permute-done.12.n2, ...), custom_call_target="tpu_custom_call" | custom-call | flops 805306368 | bytes 2097152 | tf_op jit(solution)/shard_map/pallas_call | solution.py:45
  165.4 2.0 %collective-permute-start.15 = (bf16[32,4096]{1,0:T(8,128)(2,1)}, bf16[32,4096]{1,0:T(8,128)(2,1)}, u32[]{:S(2)}, u32[]{:S(2)}) collective-permute-start(bf16[32,4096]{1,0:T(8,128)(2,1)} %get-tuple-element.61), channel_id=1, source_target_pairs={{0,2},{1,3},{2,0},{3,1},{4,6},{5,7},{6,4},{7,5},{8,10},{9,11},{10,... | collective-permute-start | bytes 786440 | tf_op jit(solution)/shard_map/ppermute | solution.py:27
  168.1 6.8 %collective-permute-done.14.s1 = bf16[32,4096]{1,0:T(8,128)(2,1)} collective-permute-done((bf16[32,4096]{1,0:T(8,128)(2,1)}, bf16[32,4096]{1,0:T(8,128)(2,1)}, u32[]{:S(2)}, u32[]{:S(2)}) %collective-permute-start.14) | collective-permute-done | bytes 262176 | tf_op jit(solution)/shard_map/ppermute | solution.py:27
  174.9 1.6 collective-permute-done.15.s2
  176.5 4.1 %collective-permute-done.16.s3 = bf16[32,4096]{1,0:T(8,128)(2,1)} collective-permute-done((bf16[32,4096]{1,0:T(8,128)(2,1)}, bf16[32,4096]{1,0:T(8,128)(2,1)}, u32[]{:S(2)}, u32[]{:S(2)}) %collective-permute-start.16) | collective-permute-done | bytes 262176 | tf_op jit(solution)/shard_map/ppermute | solution.py:27
  180.6 1.0 copy-done.14
  181.6 2.7 %shard_map.200 = bf16[32,4096]{1,0:T(8,128)(2,1)} custom-call(bf16[1024,1024]{1,0:T(8,128)(2,1)S(1)} %bitcast.16, s32[128,4]{1,0:T(8,128)S(1)} %bitcast_add_fusion.target, f32[128,4]{1,0:T(8,128)S(1)} %bitcast.19, f32[32,4096]{1,0:T(8,128)S(1)} %copy-done.14, bf16[32,4096]{1,0:T(8,128)(2,1)S(1)} %get-tuple-element.59.s0, ...), custom_call_target="tpu_custom_call" | custom-call | flops 268435456 | bytes 2097152 | tf_op jit(solution)/shard_map/pallas_call | solution.py:45
  (73 shorter events, 6.3 us)
Async XLA Ops:
  0.0 60.7 %copy-start = (bf16[128,4096]{1,0:T(8,128)(2,1)S(1)}, bf16[128,4096]{1,0:T(8,128)(2,1)}, u32[]{:S(2)}) copy-start(bf16[128,4096]{1,0:T(8,128)(2,1)} %param.30) | copy-start | bytes 3145732
  0.0 1.0 copy-start.17
  1.0 0.9 copy-start.18
  1.9 0.8 copy-start.19
  2.7 0.8 copy-start.20
  3.6 0.8 copy-start.22
  4.3 0.8 copy-start.23
  5.1 17.7 %copy-start.21 = (f32[4096,4]{0,1:T(4,128)S(1)}, f32[4096,4]{0,1:T(4,128)}, u32[]{:S(2)}) copy-start(f32[4096,4]{0,1:T(4,128)} %param.23) | copy-start | bytes 196612
  5.1 17.7 %copy-start.24 = (f32[4096,2]{0,1:T(2,128)S(1)}, f32[4096,2]{0,1:T(2,128)}, u32[]{:S(2)}) copy-start(f32[4096,2]{0,1:T(2,128)} %param.27) | copy-start | bytes 98308
  5.2 6.9 %collective-permute-start.1 = (bf16[128,768]{1,0:T(8,128)(2,1)S(1)}, bf16[128,768]{1,0:T(8,128)(2,1)S(1)}, u32[]{:S(2)}, u32[]{:S(2)}) collective-permute-start(bf16[128,768]{1,0:T(8,128)(2,1)S(1)} %get-tuple-element.35.a.refs_3_), channel_id=1, source_target_pairs={{0,8},{4,36},{8,16},{12,44},{16,24},{20,52},{24,0},{28,60},{32,40}... | collective-permute-start | bytes 589832 | tf_op jit(solution)/shard_map/ppermute | solution.py:41
  7.0 5.7 %collective-permute-start.2 = (bf16[128,768]{1,0:T(8,128)(2,1)S(1)}, bf16[128,768]{1,0:T(8,128)(2,1)S(1)}, u32[]{:S(2)}, u32[]{:S(2)}) collective-permute-start(bf16[128,768]{1,0:T(8,128)(2,1)S(1)} %get-tuple-element.35.a.refs_3_), channel_id=1, source_target_pairs={{0,24},{4,100},{8,0},{12,108},{16,8},{20,116},{24,16},{28,124},{32... | collective-permute-start | bytes 589832 | tf_op jit(solution)/shard_map/ppermute | solution.py:41
  8.5 7.2 %collective-permute-start.3 = (bf16[128,768]{1,0:T(8,128)(2,1)S(1)}, bf16[128,768]{1,0:T(8,128)(2,1)S(1)}, u32[]{:S(2)}, u32[]{:S(2)}) collective-permute-start(bf16[128,768]{1,0:T(8,128)(2,1)S(1)} %get-tuple-element.35.a.refs_3_), channel_id=1, source_target_pairs={{0,16},{4,68},{8,24},{12,76},{16,0},{20,84},{24,8},{28,92},{32,48}... | collective-permute-start | bytes 589832 | tf_op jit(solution)/shard_map/ppermute | solution.py:41
  15.8 16.9 %collective-permute-start.5 = (bf16[4,128,768]{2,1,0:T(8,128)(2,1)S(1)}, bf16[4,128,768]{2,1,0:T(8,128)(2,1)S(1)}, u32[]{:S(2)}, u32[]{:S(2)}) collective-permute-start(bf16[4,128,768]{2,1,0:T(8,128)(2,1)S(1)} %shard_map.191.refs_5_), channel_id=1, source_target_pairs={{0,32},{4,12},{8,40},{12,20},{16,48},{20,28},{24,56},{28,4},{32,64... | collective-permute-start | bytes 2359304 | tf_op jit(solution)/shard_map/ppermute | solution.py:41
  17.9 20.2 %collective-permute-start.6 = (bf16[4,128,768]{2,1,0:T(8,128)(2,1)S(1)}, bf16[4,128,768]{2,1,0:T(8,128)(2,1)}, u32[]{:S(2)}, u32[]{:S(2)}) collective-permute-start(bf16[4,128,768]{2,1,0:T(8,128)(2,1)S(1)} %shard_map.191.refs_5_), channel_id=1, source_target_pairs={{0,96},{4,28},{8,104},{12,4},{16,112},{20,12},{24,120},{28,20},{32... | collective-permute-start | bytes 2359304 | tf_op jit(solution)/shard_map/ppermute | solution.py:41
  20.1 23.1 %collective-permute-start.4 = (bf16[4,128,768]{2,1,0:T(8,128)(2,1)S(1)}, bf16[4,128,768]{2,1,0:T(8,128)(2,1)}, u32[]{:S(2)}, u32[]{:S(2)}) collective-permute-start(bf16[4,128,768]{2,1,0:T(8,128)(2,1)S(1)} %shard_map.191.refs_5_), channel_id=1, source_target_pairs={{0,64},{4,20},{8,72},{12,28},{16,80},{20,4},{24,88},{28,12},{32,96... | collective-permute-start | bytes 2359304 | tf_op jit(solution)/shard_map/ppermute | solution.py:41
  21.8 1.7 collective-permute-start
  23.5 2.2 %copy-start.1 = (bf16[512,4096]{1,0:T(8,128)(2,1)S(1)}, bf16[512,4096]{1,0:T(8,128)(2,1)}, u32[]{:S(2)}) copy-start(bf16[512,4096]{1,0:T(8,128)(2,1)} %refs_7_.1) | copy-start | bytes 12582916
  25.7 2.2 %copy-start.2 = (bf16[512,4096]{1,0:T(8,128)(2,1)S(1)}, bf16[512,4096]{1,0:T(8,128)(2,1)}, u32[]{:S(2)}) copy-start(bf16[512,4096]{1,0:T(8,128)(2,1)} %refs_8_.1) | copy-start | bytes 12582916
  30.7 2.0 %copy-start.5 = (bf16[512,4096]{1,0:T(8,128)(2,1)}, bf16[512,4096]{1,0:T(8,128)(2,1)S(1)}, u32[]{:S(2)}) copy-start(bf16[512,4096]{1,0:T(8,128)(2,1)S(1)} %get-tuple-element.51.broad) | copy-start | bytes 12582916
  32.7 10.4 %copy-start.3 = (bf16[512,4096]{1,0:T(8,128)(2,1)}, bf16[512,4096]{1,0:T(8,128)(2,1)S(1)}, u32[]{:S(2)}) copy-start(bf16[512,4096]{1,0:T(8,128)(2,1)S(1)} %get-tuple-element.50.narrow) | copy-start | bytes 12582916
  43.1 4.4 %copy-start.26 = (s32[32,4]{0,1:T(4,128)S(1)}, s32[32,4]{0,1:T(4,128)}, u32[]{:S(2)}) copy-start(s32[32,4]{0,1:T(4,128)} %param.32) | copy-start | bytes 1540
  46.9 2.3 %collective-permute-start.7 = (f32[128,1152]{1,0:T(8,128)S(1)}, f32[128,1152]{1,0:T(8,128)S(1)}, u32[]{:S(2)}, u32[]{:S(2)}) collective-permute-start(f32[128,1152]{1,0:T(8,128)S(1)} %get-tuple-element.49), channel_id=1, source_target_pairs={{0,4},{4,0},{1,5},{5,1},{2,6},{6,2},{3,7},{7,3},{8,12},{12,8},{9,1... | collective-permute-start | bytes 1769480 | tf_op jit(solution)/shard_map/ppermute | solution.py:31
  49.1 2.2 %copy-start.4 = (bf16[512,4096]{1,0:T(8,128)(2,1)S(1)}, bf16[512,4096]{1,0:T(8,128)(2,1)}, u32[]{:S(2)}) copy-start(bf16[512,4096]{1,0:T(8,128)(2,1)} %copy-done.3) | copy-start | bytes 12582916
  51.3 2.2 %copy-start.6 = (bf16[512,4096]{1,0:T(8,128)(2,1)S(1)}, bf16[512,4096]{1,0:T(8,128)(2,1)}, u32[]{:S(2)}) copy-start(bf16[512,4096]{1,0:T(8,128)(2,1)} %copy-done.5) | copy-start | bytes 12582916
  53.5 17.8 %copy-start.25 = (f32[4096]{0:T(1024)S(1)}, f32[4096]{0:T(1024)}, u32[]{:S(2)}) copy-start(f32[4096]{0:T(1024)} %param.31) | copy-start | bytes 49156
  53.5 58.6 %copy-start.9 = (bf16[1,256,4096]{2,1,0:T(8,128)(2,1)S(1)}, bf16[1,256,4096]{2,1,0:T(8,128)(2,1)}, u32[]{:S(2)}) copy-start(bf16[1,256,4096]{2,1,0:T(8,128)(2,1)} %down.2) | copy-start | bytes 6291460
  55.0 9.6 %collective-permute-start.8 = (bf16[32,4096]{1,0:T(8,128)(2,1)S(1)}, bf16[32,4096]{1,0:T(8,128)(2,1)S(1)}, u32[]{:S(2)}, u32[]{:S(2)}) collective-permute-start(bf16[32,4096]{1,0:T(8,128)(2,1)S(1)} %get-tuple-element.53), channel_id=1, source_target_pairs={{0,1},{1,2},{2,3},{3,0},{4,5},{5,6},{6,7},{7,4},{8,9},{9,10},{10,1... | collective-permute-start | bytes 786440 | tf_op jit(solution)/shard_map/ppermute | solution.py:27
  56.6 14.7 %collective-permute-start.9 = (bf16[32,4096]{1,0:T(8,128)(2,1)S(1)}, bf16[32,4096]{1,0:T(8,128)(2,1)S(1)}, u32[]{:S(2)}, u32[]{:S(2)}) collective-permute-start(bf16[32,4096]{1,0:T(8,128)(2,1)S(1)} %get-tuple-element.54), channel_id=1, source_target_pairs={{0,2},{1,3},{2,0},{3,1},{4,6},{5,7},{6,4},{7,5},{8,10},{9,11},{10,... | collective-permute-start | bytes 786440 | tf_op jit(solution)/shard_map/ppermute | solution.py:27
  59.3 11.9 %collective-permute-start.10 = (bf16[32,4096]{1,0:T(8,128)(2,1)S(1)}, bf16[32,4096]{1,0:T(8,128)(2,1)S(1)}, u32[]{:S(2)}, u32[]{:S(2)}) collective-permute-start(bf16[32,4096]{1,0:T(8,128)(2,1)S(1)} %get-tuple-element.55), channel_id=1, source_target_pairs={{0,3},{1,0},{2,1},{3,2},{4,7},{5,4},{6,5},{7,6},{8,11},{9,8},{10,9... | collective-permute-start | bytes 786440 | tf_op jit(solution)/shard_map/ppermute | solution.py:27
  72.3 0.8 copy-start.13
  73.1 51.8 %copy-start.15 = (bf16[32,4096]{1,0:T(8,128)(2,1)}, bf16[32,4096]{1,0:T(8,128)(2,1)S(1)}, u32[]{:S(2)}) copy-start(bf16[32,4096]{1,0:T(8,128)(2,1)S(1)} %get-tuple-element.58.n0) | copy-start | bytes 786436
  73.1 39.1 %copy-start.7 = (bf16[1,4096,256]{2,1,0:T(8,128)(2,1)S(1)}, bf16[1,4096,256]{2,1,0:T(8,128)(2,1)}, u32[]{:S(2)}) copy-start(bf16[1,4096,256]{2,1,0:T(8,128)(2,1)} %gate.2) | copy-start | bytes 6291460
  73.1 39.1 %copy-start.8 = (bf16[1,4096,256]{2,1,0:T(8,128)(2,1)S(1)}, bf16[1,4096,256]{2,1,0:T(8,128)(2,1)}, u32[]{:S(2)}) copy-start(bf16[1,4096,256]{2,1,0:T(8,128)(2,1)} %up.2) | copy-start | bytes 6291460
  116.5 51.5 %copy-start.27 = (f32[32,4]{0,1:T(4,128)S(1)}, f32[32,4]{0,1:T(4,128)}, u32[]{:S(2)}) copy-start(f32[32,4]{0,1:T(4,128)} %param.33) | copy-start | bytes 1540
  116.5 64.1 %all-to-all-start.1 = ((bf16[128,8,1024]{2,1,0:T(8,128)(2,1)}), bf16[128,8,1024]{2,1,0:T(8,128)(2,1)S(1)}, u32[]{:S(2)}, u32[]{:S(2)}) async-start(bf16[128,8,1024]{2,1,0:T(8,128)(2,1)} %bitcast.11), calls=%async_computation.1 | async-start | bytes 4194304 | tf_op jit(solution)/shard_map/all_to_all | solution.py:417
  121.3 30.8 %collective-permute-start.11 = (bf16[32,4096]{1,0:T(8,128)(2,1)S(1)}, bf16[32,4096]{1,0:T(8,128)(2,1)S(1)}, u32[]{:S(2)}, u32[]{:S(2)}) collective-permute-start(bf16[32,4096]{1,0:T(8,128)(2,1)S(1)} %get-tuple-element.58.n0), channel_id=1, source_target_pairs={{0,1},{1,2},{2,3},{3,0},{4,5},{5,6},{6,7},{7,4},{8,9},{9,10},{10,1... | collective-permute-start | bytes 786440 | tf_op jit(solution)/shard_map/ppermute | solution.py:27
  122.2 35.5 %collective-permute-start.12 = (bf16[32,4096]{1,0:T(8,128)(2,1)S(1)}, bf16[32,4096]{1,0:T(8,128)(2,1)S(1)}, u32[]{:S(2)}, u32[]{:S(2)}) collective-permute-start(bf16[32,4096]{1,0:T(8,128)(2,1)S(1)} %get-tuple-element.58.n0), channel_id=1, source_target_pairs={{0,2},{1,3},{2,0},{3,1},{4,6},{5,7},{6,4},{7,5},{8,10},{9,11},{10,... | collective-permute-start | bytes 786440 | tf_op jit(solution)/shard_map/ppermute | solution.py:27
  124.9 32.8 %collective-permute-start.13 = (bf16[32,4096]{1,0:T(8,128)(2,1)S(1)}, bf16[32,4096]{1,0:T(8,128)(2,1)S(1)}, u32[]{:S(2)}, u32[]{:S(2)}) collective-permute-start(bf16[32,4096]{1,0:T(8,128)(2,1)S(1)} %get-tuple-element.58.n0), channel_id=1, source_target_pairs={{0,3},{1,0},{2,1},{3,2},{4,7},{5,4},{6,5},{7,6},{8,11},{9,8},{10,9... | collective-permute-start | bytes 786440 | tf_op jit(solution)/shard_map/ppermute | solution.py:27
  157.7 1.6 copy-start.10
  159.2 1.6 copy-start.11
  160.8 1.6 copy-start.12
  162.4 0.9 copy-start.16
  165.4 9.5 %collective-permute-start.14 = (bf16[32,4096]{1,0:T(8,128)(2,1)}, bf16[32,4096]{1,0:T(8,128)(2,1)}, u32[]{:S(2)}, u32[]{:S(2)}) collective-permute-start(bf16[32,4096]{1,0:T(8,128)(2,1)} %get-tuple-element.60), channel_id=1, source_target_pairs={{0,3},{1,0},{2,1},{3,2},{4,7},{5,4},{6,5},{7,6},{8,11},{9,8},{10,9... | collective-permute-start | bytes 786440 | tf_op jit(solution)/shard_map/ppermute | solution.py:27
  165.4 11.0 %collective-permute-start.15 = (bf16[32,4096]{1,0:T(8,128)(2,1)}, bf16[32,4096]{1,0:T(8,128)(2,1)}, u32[]{:S(2)}, u32[]{:S(2)}) collective-permute-start(bf16[32,4096]{1,0:T(8,128)(2,1)} %get-tuple-element.61), channel_id=1, source_target_pairs={{0,2},{1,3},{2,0},{3,1},{4,6},{5,7},{6,4},{7,5},{8,10},{9,11},{10,... | collective-permute-start | bytes 786440 | tf_op jit(solution)/shard_map/ppermute | solution.py:27
  167.4 13.2 %collective-permute-start.16 = (bf16[32,4096]{1,0:T(8,128)(2,1)}, bf16[32,4096]{1,0:T(8,128)(2,1)}, u32[]{:S(2)}, u32[]{:S(2)}) collective-permute-start(bf16[32,4096]{1,0:T(8,128)(2,1)} %get-tuple-element.62), channel_id=1, source_target_pairs={{0,1},{1,2},{2,3},{3,0},{4,5},{5,6},{6,7},{7,4},{8,9},{9,10},{10,1... | collective-permute-start | bytes 786440 | tf_op jit(solution)/shard_map/ppermute | solution.py:27
  180.6 1.0 copy-start.14

commit v4 on v3

--- a/solution.py
+++ b/solution.py
@@ -41,7 +41,7 @@
     return lax.ppermute(x, SP, pairs)
 
 
-def call(kernel, operands, shapes, smem=(), hbm=(), scratch=(), mib=16, flops=0):
+def call(kernel, operands, shapes, smem=(), hbm=(), scratch=(), mib=16, flops=0, moved=2**21):
     return pl.pallas_call(
         kernel,
         out_shape=shapes,
@@ -49,7 +49,7 @@
         out_specs=[VMEM] * len(shapes),
         scratch_shapes=list(scratch),
         compiler_params=pltpu.CompilerParams(vmem_limit_bytes=mib * 1024 * 1024),
-        cost_estimate=pl.CostEstimate(flops=flops, transcendentals=0, bytes_accessed=2 * 1024 * 1024),
+        cost_estimate=pl.CostEstimate(flops=flops, transcendentals=0, bytes_accessed=moved),
     )(*operands)
 
 
@@ -68,9 +68,29 @@
         copy.wait()
 
 
-def stack_kernel(a, b, c, d, out):
-    for i, ref in enumerate((a, b, c, d)):
+def stack_kernel(a, b, c, d, ready, low, high):
+    for out, i, ref in ((low, 0, a), (low, 1, b), (high, 0, c), (high, 1, d)):
         out[i] = ref[...]
+
+
+def route_kernel(ids_in, weight_in, target, mix):
+    ids = jnp.concatenate([ids_in[...]] * 4, axis=1)
+    weight = jnp.concatenate([weight_in[...].astype(BF).astype(F32)] * 4, axis=1)
+    expert = lax.broadcasted_iota(jnp.int32, (128, 128), 0)
+    column = lax.broadcasted_iota(jnp.int32, (128, 128), 1)
+    named = jnp.zeros((128, 128), F32)
+    for k in range(4):
+        named = named + jnp.where(expert == ids[k : k + 1, :], 1.0, 0.0)
+    earlier = jnp.where((expert < 32) & (expert < column % 32), 1.0, 0.0).astype(BF)
+    before = jnp.dot(named.astype(BF), earlier, preferred_element_type=F32)
+    row = lax.broadcasted_iota(jnp.int32, (1024, 128), 0)
+    total = jnp.zeros((1024, 128), F32)
+    for k in range(4):
+        slot = jnp.sum(jnp.where(expert == ids[k : k + 1, :], before, 0.0), axis=0, keepdims=True)
+        start = ids[k : k + 1, :] * 8 + slot.astype(jnp.int32) * 4 + column[:1] // 32
+        target[k : k + 1, :] = start
+        total = total + jnp.where(row == start, weight[k : k + 1, :], 0.0)
+    mix[...] = total.T.astype(BF)
 
 
 def bias_kernel(place, narrow, broad, own, first, second, third):
@@ -91,13 +111,20 @@
     for i in range(1, 4):
         put(first, (i - 1) * 128, ORDER[i], 0)
     for i in range(4):
-        put(second, i * 128, ORDER[i], 1)
-        put(second, 512 + i * 128, ORDER[i], 3)
+        put(second, i * 128, ORDER[i % 2], 1 if i < 2 else 3)
+        put(second, 512 + i * 128, ORDER[2 + i % 2], 1 if i < 2 else 3)
         put(third, i * 128, ORDER[i], 2)
 
 
 def project_kernel(place, own, other, narrow, broad, *refs):
-    outs, total, attn = refs[:4], refs[4], refs[5]
+    outs, total, attn, weights, sems = refs[:4], *refs[4:]
+    copies = []
+    for at in range(0, 4096, 1024):
+        for i, ref in enumerate((narrow, broad)):
+            source, target = ref.at[:, at : at + 1024], weights.at[i, :, at : at + 1024]
+            copies.append(pltpu.make_async_copy(source, target, sems.at[len(copies)]))
+    for copy in copies:
+        copy.start()
     a, b = own[:, 1024:], other[:, 1024:]
     top = jnp.maximum(a, b)
     wa, wb = jnp.exp2(a - top), jnp.exp2(b - top)
@@ -108,15 +135,18 @@
         value = own[:, lo : lo + size] * wa[:, h : h + 1] + other[:, lo : lo + size] * wb[:, h : h + 1]
         attn[:, lo : lo + size] = value.astype(BF)
     for at in range(0, 4096, 1024):
-        part = jnp.dot(attn[:, :512], narrow[:, at : at + 1024], preferred_element_type=F32)
-        total[:, at : at + 1024] = part + jnp.dot(attn[:, 512:], broad[:, at : at + 1024], preferred_element_type=F32)
+        copies[at // 512].wait()
+        copies[at // 512 + 1].wait()
+        part = jnp.dot(attn[:, :512], weights[0, :, at : at + 1024], preferred_element_type=F32)
+        part = part + jnp.dot(attn[:, 512:], weights[1, :, at : at + 1024], preferred_element_type=F32)
+        total[:, at : at + 1024] = part
     for k in range(4):
-        outs[k][...] = total[pl.ds(((place[0] + k) % 4) * 32, 32), :].astype(BF)
-
-
-def dispatch_kernel(p0, p1, p2, p3, residual, gain, target, stream_out, normed_out, out):
+        outs[k][...] = total[pl.ds(((place[3] + k) % 4) * 32, 32), :].astype(BF)
+
+
+def dispatch_kernel(place, p0, p1, p2, p3, residual, gain, target, stream_out, normed_out, out):
     mixture = p0[...].astype(F32) + p1[...].astype(F32) + p2[...].astype(F32) + p3[...].astype(F32)
-    stream = residual[...].astype(F32) + mixture
+    stream = residual[pl.ds(place[3] * 32, 32), :].astype(F32) + mixture
     stream_out[...] = stream
     scale = lax.rsqrt(jnp.mean(stream * stream, axis=1, keepdims=True) + EPSILON)
     normed = (stream * scale * gain[...]).astype(BF)
@@ -145,7 +175,15 @@
             out[:, at : at + 1024] = part[k * 32 : (k + 1) * 32]
 
 
-def expert_kernel(inbound, gate, up, down, out, x):
+def expert_kernel(inbound, gate, up, down, out, x, gate_up, down_copy, sems):
+    copies = []
+    for g in range(4):
+        for i, ref in enumerate((gate, up)):
+            part = pl.ds(g * 1024, 1024)
+            copies.append(pltpu.make_async_copy(ref.at[0, part], gate_up.at[i, part], sems.at[len(copies)]))
+    copies.append(pltpu.make_async_copy(down.at[0], down_copy, sems.at[len(copies)]))
+    for copy in copies:
+        copy.start()
     i = lax.broadcasted_iota(jnp.int32, (256, 256), 0)
     j = lax.broadcasted_iota(jnp.int32, (256, 256), 1)
     order = (j == ((i % 64) // 2) * 8 + (i % 2) * 4 + i // 64).astype(F32).astype(BF)
@@ -154,23 +192,25 @@
         rows = jnp.dot(order, inbound[b * 256 : (b + 1) * 256, :], preferred_element_type=F32).astype(BF)
         for g in range(4):
             x[b * 64 : (b + 1) * 64, g * 1024 : (g + 1) * 1024] = rows[g * 64 : (g + 1) * 64]
-    gated = jnp.dot(x[...], gate[0], preferred_element_type=F32)
-    upped = jnp.dot(x[...], up[0], preferred_element_type=F32)
+    gated, upped = jnp.zeros((256, 256), F32), jnp.zeros((256, 256), F32)
+    for g in range(4):
+        lo, hi = g * 1024, (g + 1) * 1024
+        copies[2 * g].wait()
+        gated = gated + jnp.dot(x[:, lo:hi], gate_up[0, lo:hi], preferred_element_type=F32)
+        copies[2 * g + 1].wait()
+        upped = upped + jnp.dot(x[:, lo:hi], gate_up[1, lo:hi], preferred_element_type=F32)
+    copies[-1].wait()
     hidden = (silu(gated) * upped).astype(BF)
     for g in range(4):
-        part = jnp.dot(hidden, down[0, :, g * 1024 : (g + 1) * 1024], preferred_element_type=F32)
+        part = jnp.dot(hidden, down_copy[:, g * 1024 : (g + 1) * 1024], preferred_element_type=F32)
         x[:, g * 1024 : (g + 1) * 1024] = part.astype(BF)
     for b in range(4):
         rows = jnp.concatenate([x[b * 64 : (b + 1) * 64, g * 1024 : (g + 1) * 1024] for g in range(4)], axis=0)
         out[b * 256 : (b + 1) * 256, :] = jnp.dot(back, rows, preferred_element_type=F32).astype(BF)
 
 
-def combine_kernel(returned, target, weight, stream, s0, s1, s2, s3, out):
-    column = lax.broadcasted_iota(jnp.int32, (128, 1024), 1)
-    mix = jnp.zeros((128, 1024), F32)
-    for k in range(4):
-        mix = mix + jnp.where(column == target[:, k : k + 1], weight[:, k : k + 1], 0.0)
-    routed = jnp.dot(mix.astype(BF), returned[...], preferred_element_type=F32)
+def combine_kernel(returned, mix, stream, s0, s1, s2, s3, out):
+    routed = jnp.dot(mix[...], returned[...], preferred_element_type=F32)
     for g in range(4):
         lo, hi = g * 1024, (g + 1) * 1024
         total = stream[:, lo:hi] + routed[g * 32 : (g + 1) * 32]
@@ -192,23 +232,16 @@
     for n, own_block in counts:
         tiles.append((take(n), take(1)[0], own_block))
         if first and not own_block:
-            planes += tiles[-1][0]
+            planes.append(tiles[-1][0][0])
     if not first:
         m_in, l_in, an_in, ab_in = take(4)
-    if first:
-        weights_in = take(2)
     if last:
         own_out, send_out = take(2)
     else:
         m_out, l_out, an_out, ab_out = take(4)
-    if first:
-        weights_out, sems = take(2), take(1)[0]
-        copies = [pltpu.make_async_copy(weights_in[i], weights_out[i], sems.at[i]) for i in range(2)]
-        for copy in copies:
-            copy.start()
 
     def keys(ref, lo, hi):
-        value = ref[1:, :, lo:hi] if any(ref is p for p in planes) else ref[..., lo:hi]
+        value = ref[1, :, lo:hi] if any(ref is p for p in planes) else ref[..., lo:hi]
         return value.reshape(-1, hi - lo)
 
     results = {}
@@ -273,12 +306,9 @@
             for h in range(6):
                 stats = jnp.where(lane == h, results[(side, h)], stats)
             out[:, 1024:1152] = stats
-    if first:
-        for copy in copies:
-            copy.wait()
-
-
-def attend(q_own, q_other, core, tiles, state, last, weights=None):
+
+
+def attend(q_own, q_other, core, tiles, state, last):
     counts = tuple((len(arrays), own_block) for arrays, _, own_block in tiles)
     operands = [q_own, q_other, core]
     n_keys = 0
@@ -290,9 +320,6 @@
     if state is not None:
         operands += list(state)
         specs += [VMEM] * 4
-    else:
-        operands += list(weights)
-        specs += [HBM] * 2
     if last:
         shapes = [jax.ShapeDtypeStruct((128, 1152), F32)] * 2
     else:
@@ -302,14 +329,11 @@
             jax.ShapeDtypeStruct((1024, 128), F32),
             jax.ShapeDtypeStruct((512, 256), F32),
         ]
-    if state is None:
-        shapes += [jax.ShapeDtypeStruct(w.shape, w.dtype) for w in weights]
     return pl.pallas_call(
         functools.partial(attend_kernel, counts, state is None, last),
         out_shape=shapes,
         in_specs=specs,
         out_specs=[VMEM] * len(shapes),
-        scratch_shapes=[pltpu.SemaphoreType.DMA((2,))] if state is None else [],
         compiler_params=pltpu.CompilerParams(vmem_limit_bytes=24 * 1024 * 1024),
         cost_estimate=pl.CostEstimate(
             flops=4 * n_keys * 256 * 1024, transcendentals=n_keys * 1536, bytes_accessed=4 * 1024 * 1024
@@ -347,48 +371,58 @@
         [shaped((128, 768), BF), shaped((128, 1024), BF)],
         hbm=range(6),
         scratch=[pltpu.SemaphoreType.DMA((6,))],
-    )
+        moved=0,
+    )
+    target, mix = call(
+        route_kernel,
+        (route_ids.T, route_weight.T),
+        [shaped((4, 128), jnp.int32), shaped((128, 1024), BF)],
+    )
+    place = jnp.stack([z, y, c, t])
     line = [turn(own_kv, k, 0) for k in ORDER[1:]]
     q_other = swap_core(q_own)
-    (plane,) = call(stack_kernel, [own_kv] + line, [shaped((4, 128, 768), BF)])
-    back, ahead, far = (turn(plane, k, 1) for k in ORDER[1:])
+    low, high = call(stack_kernel, [own_kv] + line + [target], [shaped((2, 128, 768), BF)] * 2)
+    low_back, high_ahead = turn(low, 1, 1), turn(high, 3, 1)
+    low_ahead, high_back = turn(low, 3, 1), turn(high, 1, 1)
+    low_far, high_far = turn(low_back, 1, 1), turn(high_ahead, 3, 1)
 
     own_bias, bias_1, bias_2, bias_3 = call(
         bias_kernel,
-        (jnp.stack([z, y, c]), gates_narrow.T, gates_broad.T),
+        (place, gates_narrow.T, gates_broad.T),
         [shaped((8, n), F32) for n in (128, 384, 1024, 512)],
         smem=(0,),
     )
     core = c.reshape(1)
-    first_tiles = [((own_kv,), own_bias, True), ((plane,), bias_1, False)]
-    *state, narrow, broad = attend(
-        q_own, q_other, core, first_tiles, None, False, (project_narrow, project_broad)
-    )
-    state = attend(q_own, q_other, core, [((back, ahead), bias_2, False)], state, False)
-    own_part, send_part = attend(q_own, q_other, core, [((far,), bias_3, False)], state, True)
+    first_tiles = [((own_kv,), own_bias, True), ((low, high), bias_1, False)]
+    state = attend(q_own, q_other, core, first_tiles, None, False)
+    second_tiles = [((low_back, low_ahead, high_back, high_ahead), bias_2, False)]
+    state = attend(q_own, q_other, core, second_tiles, state, False)
+    own_part, send_part = attend(q_own, q_other, core, [((low_far, high_far), bias_3, False)], state, True)
     other_part = swap_core(send_part)
 
     p0, p1, p2, p3 = call(
         project_kernel,
-        (t.reshape(1), own_part, other_part, narrow, broad),
+        (place, own_part, other_part, project_narrow, project_broad),
         [shaped((32, 4096), BF)] * 4,
         smem=(0,),
-        scratch=[pltpu.VMEM((128, 4096), F32), pltpu.VMEM((128, 1024), BF)],
+        hbm=(3, 4),
+        scratch=[
+            pltpu.VMEM((128, 4096), F32),
+            pltpu.VMEM((128, 1024), BF),
+            pltpu.VMEM((2, 512, 4096), BF),
+            pltpu.SemaphoreType.DMA((8,)),
+        ],
+        mib=20,
+        moved=0,
         flops=2 * 128 * 1024 * 4096,
     )
     p1, p2, p3 = shift(p1, "tp", 1), shift(p2, "tp", 2), shift(p3, "tp", 3)
 
-    flat = route_ids.reshape(-1)
-    earlier = jnp.arange(128)[:, None] // 4 > jnp.arange(128)[None, :] // 4
-    slot = jnp.sum((earlier & (flat[:, None] == flat[None, :])).astype(jnp.int32), axis=1).reshape(32, 4)
-    target = jnp.tile(route_ids * 8 + slot * 4, (4, 1)) + jnp.arange(128, dtype=jnp.int32)[:, None] // 32
-    weight = jnp.tile(route_weight.astype(BF).astype(F32), (4, 1))
-
-    own_rows = lax.dynamic_slice_in_dim(residual, t * 32, 32, 0)
     stream, normed, outbound = call(
         dispatch_kernel,
-        (p0, p1, p2, p3, own_rows, norm_gain.reshape(1, -1), target.T),
+        (place, p0, p1, p2, p3, residual, norm_gain.reshape(1, -1), target),
         [shaped((32, 4096), F32), shaped((32, 4096), BF), shaped((1024, 1024), BF)],
+        smem=(0,),
         flops=2 * 1024 * 128 * 1024,
     )
     every = SP + ("tp",)
@@ -411,13 +445,21 @@
         expert_kernel,
         (inbound.reshape(1024, 1024), expert_gate, expert_up, expert_down),
         [shaped((1024, 1024), BF)],
-        scratch=[pltpu.VMEM((256, 4096), BF)],
+        hbm=(1, 2, 3),
+        scratch=[
+            pltpu.VMEM((256, 4096), BF),
+            pltpu.VMEM((2, 4096, 256), BF),
+            pltpu.VMEM((256, 4096), BF),
+            pltpu.SemaphoreType.DMA((9,)),
+        ],
+        mib=20,
+        moved=0,
         flops=2 * 256 * 4096 * 768,
     )
     returned = lax.all_to_all(result.reshape(128, 8, 1024), every, 0, 0, tiled=True)
     (out,) = call(
         combine_kernel,
-        (returned.reshape(1024, 1024), target, weight, stream, s0, s1, s2, s3),
+        (returned.reshape(1024, 1024), mix, stream, s0, s1, s2, s3),
         [shaped((32, 4096), BF)],
         flops=2 * 128 * 1024 * 1024,
     )

time: 186 us -> 176 us (0.946)
  local copies, waits for them, and re-layouts: 24.7 us -> 16.1 us
  waiting for transfers between devices: 66.1 us -> 62.6 us
  starting transfers between devices: 29.9 us -> 33 us
  blocking collectives: 39.1 us -> 36.1 us
  Pallas kernels: 24 us -> 26.6 us
    unnamed x57 -> x48, local copies, waits for them, and re-layouts: 24.1 us -> 16.1 us
    pallas_call x8 -> x9, Pallas kernels: 12.4 us -> 16.7 us  [call(): pl.pallas_call(kernel, out_shape=shapes, in_specs=[SMEM if i in smem else...]
    ppermute x6 -> x9, starting transfers between devices: 11.5 us -> 14.8 us  [turn(): return lax.ppermute(x, SP, pairs)]
    ppermute x6 -> x9, waiting for transfers between devices: 10.4 us -> 7.11 us  [turn(): return lax.ppermute(x, SP, pairs)]
    all_to_all x1, blocking collectives: 39.1 us -> 36.1 us  [local(): lax.all_to_all(outbound.reshape(128, 8, 1024), every, 0, 0, tiled=True)]
  transfers between devices with their start and end apart: 18 -> 21, of which waited for: 12 -> 11; matrix products, arithmetic and copies ran while one was open for 1% -> 0% of each run, Pallas kernels for 6% -> 5%
where the time goes in v4:
time: 176 us; the launch traced here: 175 us
  waiting for transfers between devices  62.6 us (36%)
  blocking collectives  36.1 us (21%)
  starting transfers between devices  33 us (19%)
  Pallas kernels  26.6 us (15%)
  local copies, waits for them, and re-layouts  16.1 us (9%)
    ppermute x9, waiting for transfers between devices, shift(): return lax.ppermute(x, axis, [(i, (i + k) % 4) for i in range(4)])  53.5 us
    all_to_all x1, blocking collectives, local(): lax.all_to_all(outbound.reshape(128, 8, 1024), every, 0, 0, tiled=True)  36.1 us
    pallas_call x9, Pallas kernels, call(): pl.pallas_call(kernel, out_shape=shapes, in_specs=[SMEM if i in smem else...  16.7 us
    unnamed x48, local copies, waits for them, and re-layouts  16.1 us
    ppermute x9, starting transfers between devices, turn(): return lax.ppermute(x, SP, pairs)  14.8 us
    ppermute x9, starting transfers between devices, shift(): return lax.ppermute(x, axis, [(i, (i + k) % 4) for i in range(4)])  13.4 us
    pallas_call x3, Pallas kernels, attend(): pl.pallas_call(functools.partial(attend_kernel, counts, state is None, la...  9.84 us
    ppermute x9, waiting for transfers between devices, turn(): return lax.ppermute(x, SP, pairs)  7.11 us
  transfers between devices with their start and end apart: 21, of which 11 were waited for; matrix products, arithmetic and copies ran while one was open for 0% of the time, Pallas kernels for 5%

profile of v4, /device:TPU:0, one launch (start us, length us, event | category | flops | bytes accessed | tf_op | source)
XLA Modules:
  0.0 174.6 jit_solution(15847161197820120508)
XLA Ops:
  0.0 0.9 copy-done.13
  0.9 0.9 copy-done.14
  1.8 0.8 copy-done.15
  2.7 0.8 copy-done.16
  3.5 0.8 copy-done.18
  4.3 0.8 copy-done.19
  5.1 1.8 %collective-permute-start.1 = (bf16[128,768]{1,0:T(8,128)(2,1)S(1)}, bf16[128,768]{1,0:T(8,128)(2,1)S(1)}, u32[]{:S(2)}, u32[]{:S(2)}) collective-permute-start(bf16[128,768]{1,0:T(8,128)(2,1)S(1)} %get-tuple-element.37.a.refs_3_), channel_id=1, source_target_pairs={{0,8},{4,36},{8,16},{12,44},{16,24},{20,52},{24,0},{28,60},{32,40}... | collective-permute-start | bytes 589832 | tf_op jit(solution)/shard_map/ppermute | solution.py:41
  6.9 1.5 collective-permute-start.2
  8.4 2.1 %collective-permute-start.3 = (bf16[128,768]{1,0:T(8,128)(2,1)S(1)}, bf16[128,768]{1,0:T(8,128)(2,1)S(1)}, u32[]{:S(2)}, u32[]{:S(2)}) collective-permute-start(bf16[128,768]{1,0:T(8,128)(2,1)S(1)} %get-tuple-element.37.a.refs_3_), channel_id=1, source_target_pairs={{0,16},{4,68},{8,24},{12,76},{16,0},{20,84},{24,8},{28,92},{32,48}... | collective-permute-start | bytes 589832 | tf_op jit(solution)/shard_map/ppermute | solution.py:41
  12.6 3.1 %collective-permute-done.3.d = bf16[128,768]{1,0:T(8,128)(2,1)S(1)} collective-permute-done((bf16[128,768]{1,0:T(8,128)(2,1)S(1)}, bf16[128,768]{1,0:T(8,128)(2,1)S(1)}, u32[]{:S(2)}, u32[]{:S(2)}) %collective-permute-start.3) | collective-permute-done | bytes 196640 | tf_op jit(solution)/shard_map/ppermute | solution.py:41
  15.6 1.0 shard_map.192
  16.6 2.0 %collective-permute-start.4 = (bf16[2,128,768]{2,1,0:T(8,128)(2,1)}, bf16[2,128,768]{2,1,0:T(8,128)(2,1)S(1)}, u32[]{:S(2)}, u32[]{:S(2)}) collective-permute-start(bf16[2,128,768]{2,1,0:T(8,128)(2,1)} %get-tuple-element.39.refs_5_), channel_id=1, source_target_pairs={{0,32},{4,12},{8,40},{12,20},{16,48},{20,28},{24,56},{28,4},{32,64... | collective-permute-start | bytes 1179656 | tf_op jit(solution)/shard_map/ppermute | solution.py:41
  18.6 2.1 %collective-permute-start.6 = (bf16[2,128,768]{2,1,0:T(8,128)(2,1)}, bf16[2,128,768]{2,1,0:T(8,128)(2,1)S(1)}, u32[]{:S(2)}, u32[]{:S(2)}) collective-permute-start(bf16[2,128,768]{2,1,0:T(8,128)(2,1)} %get-tuple-element.40.refs_6_), channel_id=1, source_target_pairs={{0,96},{4,28},{8,104},{12,4},{16,112},{20,12},{24,120},{28,20},{32... | collective-permute-start | bytes 1179656 | tf_op jit(solution)/shard_map/ppermute | solution.py:41
  20.7 2.0 %collective-permute-start.8 = (bf16[2,128,768]{2,1,0:T(8,128)(2,1)}, bf16[2,128,768]{2,1,0:T(8,128)(2,1)S(1)}, u32[]{:S(2)}, u32[]{:S(2)}) collective-permute-start(bf16[2,128,768]{2,1,0:T(8,128)(2,1)} %get-tuple-element.39.refs_5_), channel_id=1, source_target_pairs={{0,96},{4,28},{8,104},{12,4},{16,112},{20,12},{24,120},{28,20},{32... | collective-permute-start | bytes 1179656 | tf_op jit(solution)/shard_map/ppermute | solution.py:41
  22.8 3.9 %collective-permute-done.4.refs_3_ = bf16[2,128,768]{2,1,0:T(8,128)(2,1)S(1)} collective-permute-done((bf16[2,128,768]{2,1,0:T(8,128)(2,1)}, bf16[2,128,768]{2,1,0:T(8,128)(2,1)S(1)}, u32[]{:S(2)}, u32[]{:S(2)}) %collective-permute-start.4) | collective-permute-done | bytes 393248 | tf_op jit(solution)/shard_map/ppermute | solution.py:41
  26.7 3.2 %collective-permute-start.7 = (bf16[2,128,768]{2,1,0:T(8,128)(2,1)S(1)}, bf16[2,128,768]{2,1,0:T(8,128)(2,1)S(1)}, u32[]{:S(2)}, u32[]{:S(2)}) collective-permute-start(bf16[2,128,768]{2,1,0:T(8,128)(2,1)S(1)} %collective-permute-done.6.refs_6_), channel_id=1, source_target_pairs={{0,96},{4,28},{8,104},{12,4},{16,112},{20,12},{24,120},{28,20},{32... | collective-permute-start | bytes 1179656 | tf_op jit(solution)/shard_map/ppermute | solution.py:41
  30.0 0.8 copy-done.17
  30.8 0.8 copy-done.20
  32.3 3.3 %shard_map.194 = (f32[1536,128]{1,0:T(8,128)S(1)}, f32[1536,128]{1,0:T(8,128)S(1)}, f32[1024,128]{1,0:T(8,128)S(1)}, f32[512,256]{1,0:T(8,128)S(1)}) custom-call(bf16[128,1024]{1,0:T(8,128)(2,1)S(1)} %get-tuple-element.36.refs_0_, bf16[128,1024]{1,0:T(8,128)(2,1)S(1)} %collective-permute-done.refs_1_, s32[1]{0:T(128)} %bitcast.2.refs_2_, ...), custom_call_target="tpu_custom_call" | custom-call | flops 536870912 | bytes 4194304 | tf_op jit(solution)/shard_map/pallas_call | solution.py:332
  35.7 3.9 %shard_map.195 = (f32[1536,128]{1,0:T(8,128)S(1)}, f32[1536,128]{1,0:T(8,128)S(1)}, f32[1024,128]{1,0:T(8,128)S(1)}, f32[512,256]{1,0:T(8,128)S(1)}) custom-call(bf16[128,1024]{1,0:T(8,128)(2,1)S(1)} %get-tuple-element.36.refs_0_, bf16[128,1024]{1,0:T(8,128)(2,1)S(1)} %collective-permute-done.refs_1_, s32[1]{0:T(128)} %bitcast.2.refs_2_, ...), custom_call_target="tpu_custom_call" | custom-call | flops 1073741824 | bytes 4194304 | tf_op jit(solution)/shard_map/pallas_call | solution.py:332
  39.6 2.6 %shard_map.196 = (f32[128,1152]{1,0:T(8,128)S(1)}, f32[128,1152]{1,0:T(8,128)S(1)}) custom-call(bf16[128,1024]{1,0:T(8,128)(2,1)S(1)} %get-tuple-element.36.refs_0_, bf16[128,1024]{1,0:T(8,128)(2,1)S(1)} %collective-permute-done.refs_1_, s32[1]{0:T(128)} %bitcast.2.refs_2_, bf16[2,128,768]{2,1,0:T(8,128)(2,1)S(1)} %collective-permute-done.5.refs_3_, ...), custom_call_target="tpu_custom_call" | custom-call | flops 536870912 | bytes 4194304 | tf_op jit(solution)/shard_map/pallas_call | solution.py:332
  42.3 2.0 %collective-permute-done.10.other = f32[128,1152]{1,0:T(8,128)S(1)} collective-permute-done((f32[128,1152]{1,0:T(8,128)S(1)}, f32[128,1152]{1,0:T(8,128)S(1)}, u32[]{:S(2)}, u32[]{:S(2)}) %collective-permute-start.10) | collective-permute-done | bytes 589856 | tf_op jit(solution)/shard_map/ppermute | solution.py:31
  44.3 4.0 %shard_map.197 = (bf16[32,4096]{1,0:T(8,128)(2,1)S(1)}, bf16[32,4096]{1,0:T(8,128)(2,1)S(1)}, bf16[32,4096]{1,0:T(8,128)(2,1)S(1)}, bf16[32,4096]{1,0:T(8,128)(2,1)S(1)}) custom-call(s32[4]{0:T(128)S(1)} %pad_add_fusion.place, f32[128,1152]{1,0:T(8,128)S(1)} %get-tuple-element.53.own, f32[128,1152]{1,0:T(8,128)S(1)} %collective-permute-done.10.other, ...), custom_call_target="tpu_custom_call" | custom-call | flops 1073741824 | tf_op jit(solution)/shard_map/pallas_call | solution.py:45
  48.3 1.6 collective-permute-start.11
  49.9 2.7 %collective-permute-start.12 = (bf16[32,4096]{1,0:T(8,128)(2,1)S(1)}, bf16[32,4096]{1,0:T(8,128)(2,1)S(1)}, u32[]{:S(2)}, u32[]{:S(2)}) collective-permute-start(bf16[32,4096]{1,0:T(8,128)(2,1)S(1)} %get-tuple-element.57), channel_id=1, source_target_pairs={{0,2},{1,3},{2,0},{3,1},{4,6},{5,7},{6,4},{7,5},{8,10},{9,11},{10,... | collective-permute-start | bytes 786440 | tf_op jit(solution)/shard_map/ppermute | solution.py:27
  52.6 1.4 collective-permute-start.13
  54.0 3.9 %collective-permute-done.11.p1 = bf16[32,4096]{1,0:T(8,128)(2,1)S(1)} collective-permute-done((bf16[32,4096]{1,0:T(8,128)(2,1)S(1)}, bf16[32,4096]{1,0:T(8,128)(2,1)S(1)}, u32[]{:S(2)}, u32[]{:S(2)}) %collective-permute-start.11) | collective-permute-done | bytes 262176 | tf_op jit(solution)/shard_map/ppermute | solution.py:27
  57.9 6.6 %collective-permute-done.12.p2 = bf16[32,4096]{1,0:T(8,128)(2,1)S(1)} collective-permute-done((bf16[32,4096]{1,0:T(8,128)(2,1)S(1)}, bf16[32,4096]{1,0:T(8,128)(2,1)S(1)}, u32[]{:S(2)}, u32[]{:S(2)}) %collective-permute-start.12) | collective-permute-done | bytes 262176 | tf_op jit(solution)/shard_map/ppermute | solution.py:27
  64.5 1.6 shard_map.198
  66.1 36.1 %all_to_all.10 = bf16[128,8,1024]{2,1,0:T(8,128)(2,1)S(1)} all-to-all(bf16[128,8,1024]{2,1,0:T(8,128)(2,1)S(1)} %bitcast.15), channel_id=1, replica_groups=mesh['z'=4,'y'=4,'c'=2,'tp'=4] {'z','y','c','tp'}, dimensions={0} | all-to-all | bytes 4194304 | tf_op jit(solution)/shard_map/all_to_all | solution.py:429
  102.2 6.5 %shard_map.199 = bf16[1024,1024]{1,0:T(8,128)(2,1)} custom-call(bf16[1024,1024]{1,0:T(8,128)(2,1)S(1)} %bitcast.13, bf16[1,4096,256]{2,1,0:T(8,128)(2,1)S(1)} %copy-done.2, bf16[1,4096,256]{2,1,0:T(8,128)(2,1)S(1)} %copy-done.3, bf16[1,256,4096]{2,1,0:T(8,128)(2,1)S(1)} %copy-done.4), custom_call_target="tpu_custom_call" | custom-call | flops 1610612736 | tf_op jit(solution)/shard_map/pallas_call | solution.py:45
  108.8 4.7 %all-to-all-start.1 = ((bf16[128,8,1024]{2,1,0:T(8,128)(2,1)}), bf16[128,8,1024]{2,1,0:T(8,128)(2,1)S(1)}, u32[]{:S(2)}, u32[]{:S(2)}) async-start(bf16[128,8,1024]{2,1,0:T(8,128)(2,1)} %bitcast.11), calls=%async_computation.1 | async-start | bytes 4194304 | tf_op jit(solution)/shard_map/all_to_all | solution.py:459
  113.4 0.9 collective-permute-start.14
  114.3 2.7 %collective-permute-start.15 = (bf16[32,4096]{1,0:T(8,128)(2,1)S(1)}, bf16[32,4096]{1,0:T(8,128)(2,1)S(1)}, u32[]{:S(2)}, u32[]{:S(2)}) collective-permute-start(bf16[32,4096]{1,0:T(8,128)(2,1)S(1)} %get-tuple-element.62.n0), channel_id=1, source_target_pairs={{0,2},{1,3},{2,0},{3,1},{4,6},{5,7},{6,4},{7,5},{8,10},{9,11},{10,... | collective-permute-start | bytes 786440 | tf_op jit(solution)/shard_map/ppermute | solution.py:27
  117.1 1.4 collective-permute-start.16
  118.5 25.7 %collective-permute-done.14.n1 = bf16[32,4096]{1,0:T(8,128)(2,1)S(1)} collective-permute-done((bf16[32,4096]{1,0:T(8,128)(2,1)S(1)}, bf16[32,4096]{1,0:T(8,128)(2,1)S(1)}, u32[]{:S(2)}, u32[]{:S(2)}) %collective-permute-start.14) | collective-permute-done | bytes 262176 | tf_op jit(solution)/shard_map/ppermute | solution.py:27
  144.2 5.6 %collective-permute-done.15.n2 = bf16[32,4096]{1,0:T(8,128)(2,1)S(1)} collective-permute-done((bf16[32,4096]{1,0:T(8,128)(2,1)S(1)}, bf16[32,4096]{1,0:T(8,128)(2,1)S(1)}, u32[]{:S(2)}, u32[]{:S(2)}) %collective-permute-start.15) | collective-permute-done | bytes 262176 | tf_op jit(solution)/shard_map/ppermute | solution.py:27
  149.8 1.6 copy-done.5
  151.4 1.6 copy-done.6
  153.0 1.6 copy-done.7
  154.6 1.1 shard_map.200
  155.9 2.0 %collective-permute-start.18 = (bf16[32,4096]{1,0:T(8,128)(2,1)S(1)}, bf16[32,4096]{1,0:T(8,128)(2,1)S(1)}, u32[]{:S(2)}, u32[]{:S(2)}) collective-permute-start(bf16[32,4096]{1,0:T(8,128)(2,1)S(1)} %get-tuple-element.65), channel_id=1, source_target_pairs={{0,2},{1,3},{2,0},{3,1},{4,6},{5,7},{6,4},{7,5},{8,10},{9,11},{10,... | collective-permute-start | bytes 786440 | tf_op jit(solution)/shard_map/ppermute | solution.py:27
  158.4 6.6 %collective-permute-done.17.s1 = bf16[32,4096]{1,0:T(8,128)(2,1)S(1)} collective-permute-done((bf16[32,4096]{1,0:T(8,128)(2,1)S(1)}, bf16[32,4096]{1,0:T(8,128)(2,1)S(1)}, u32[]{:S(2)}, u32[]{:S(2)}) %collective-permute-start.17) | collective-permute-done | bytes 262176 | tf_op jit(solution)/shard_map/ppermute | solution.py:27
  165.0 1.6 collective-permute-done.18.s2
  167.3 3.4 %collective-permute-done.19.s3 = bf16[32,4096]{1,0:T(8,128)(2,1)S(1)} collective-permute-done((bf16[32,4096]{1,0:T(8,128)(2,1)S(1)}, bf16[32,4096]{1,0:T(8,128)(2,1)S(1)}, u32[]{:S(2)}, u32[]{:S(2)}) %collective-permute-start.19) | collective-permute-done | bytes 262176 | tf_op jit(solution)/shard_map/ppermute | solution.py:27
  171.5 0.9 copy-done.10
  172.4 0.9 copy-done.12
  173.4 1.2 shard_map.201
  (56 shorter events, 5.2 us)
Async XLA Ops:
  0.0 0.9 copy-start.13
  0.9 0.9 copy-start.14
  1.8 0.8 copy-start.15
  2.6 0.8 copy-start.16
  3.5 0.8 copy-start.18
  4.2 0.8 copy-start.19
  5.1 7.3 %collective-permute-start.1 = (bf16[128,768]{1,0:T(8,128)(2,1)S(1)}, bf16[128,768]{1,0:T(8,128)(2,1)S(1)}, u32[]{:S(2)}, u32[]{:S(2)}) collective-permute-start(bf16[128,768]{1,0:T(8,128)(2,1)S(1)} %get-tuple-element.37.a.refs_3_), channel_id=1, source_target_pairs={{0,8},{4,36},{8,16},{12,44},{16,24},{20,52},{24,0},{28,60},{32,40}... | collective-permute-start | bytes 589832 | tf_op jit(solution)/shard_map/ppermute | solution.py:41
  6.9 5.7 %collective-permute-start.2 = (bf16[128,768]{1,0:T(8,128)(2,1)S(1)}, bf16[128,768]{1,0:T(8,128)(2,1)S(1)}, u32[]{:S(2)}, u32[]{:S(2)}) collective-permute-start(bf16[128,768]{1,0:T(8,128)(2,1)S(1)} %get-tuple-element.37.a.refs_3_), channel_id=1, source_target_pairs={{0,24},{4,100},{8,0},{12,108},{16,8},{20,116},{24,16},{28,124},{32... | collective-permute-start | bytes 589832 | tf_op jit(solution)/shard_map/ppermute | solution.py:41
  8.4 7.2 %collective-permute-start.3 = (bf16[128,768]{1,0:T(8,128)(2,1)S(1)}, bf16[128,768]{1,0:T(8,128)(2,1)S(1)}, u32[]{:S(2)}, u32[]{:S(2)}) collective-permute-start(bf16[128,768]{1,0:T(8,128)(2,1)S(1)} %get-tuple-element.37.a.refs_3_), channel_id=1, source_target_pairs={{0,16},{4,68},{8,24},{12,76},{16,0},{20,84},{24,8},{28,92},{32,48}... | collective-permute-start | bytes 589832 | tf_op jit(solution)/shard_map/ppermute | solution.py:41
  10.5 0.7 copy-start.22
  11.2 0.7 copy-start.23
  16.6 10.1 %collective-permute-start.4 = (bf16[2,128,768]{2,1,0:T(8,128)(2,1)}, bf16[2,128,768]{2,1,0:T(8,128)(2,1)S(1)}, u32[]{:S(2)}, u32[]{:S(2)}) collective-permute-start(bf16[2,128,768]{2,1,0:T(8,128)(2,1)} %get-tuple-element.39.refs_5_), channel_id=1, source_target_pairs={{0,32},{4,12},{8,40},{12,20},{16,48},{20,28},{24,56},{28,4},{32,64... | collective-permute-start | bytes 1179656 | tf_op jit(solution)/shard_map/ppermute | solution.py:41
  18.6 8.1 %collective-permute-start.6 = (bf16[2,128,768]{2,1,0:T(8,128)(2,1)}, bf16[2,128,768]{2,1,0:T(8,128)(2,1)S(1)}, u32[]{:S(2)}, u32[]{:S(2)}) collective-permute-start(bf16[2,128,768]{2,1,0:T(8,128)(2,1)} %get-tuple-element.40.refs_6_), channel_id=1, source_target_pairs={{0,96},{4,28},{8,104},{12,4},{16,112},{20,12},{24,120},{28,20},{32... | collective-permute-start | bytes 1179656 | tf_op jit(solution)/shard_map/ppermute | solution.py:41
  20.7 14.9 %collective-permute-start.8 = (bf16[2,128,768]{2,1,0:T(8,128)(2,1)}, bf16[2,128,768]{2,1,0:T(8,128)(2,1)S(1)}, u32[]{:S(2)}, u32[]{:S(2)}) collective-permute-start(bf16[2,128,768]{2,1,0:T(8,128)(2,1)} %get-tuple-element.39.refs_5_), channel_id=1, source_target_pairs={{0,96},{4,28},{8,104},{12,4},{16,112},{20,12},{24,120},{28,20},{32... | collective-permute-start | bytes 1179656 | tf_op jit(solution)/shard_map/ppermute | solution.py:41
  22.7 12.9 %collective-permute-start.9 = (bf16[2,128,768]{2,1,0:T(8,128)(2,1)}, bf16[2,128,768]{2,1,0:T(8,128)(2,1)S(1)}, u32[]{:S(2)}, u32[]{:S(2)}) collective-permute-start(bf16[2,128,768]{2,1,0:T(8,128)(2,1)} %get-tuple-element.40.refs_6_), channel_id=1, source_target_pairs={{0,32},{4,12},{8,40},{12,20},{16,48},{20,28},{24,56},{28,4},{32,64... | collective-permute-start | bytes 1179656 | tf_op jit(solution)/shard_map/ppermute | solution.py:41
  22.7 9.6 %collective-permute-start = (bf16[128,1024]{1,0:T(8,128)(2,1)S(1)}, bf16[128,1024]{1,0:T(8,128)(2,1)S(1)}, u32[]{:S(2)}, u32[]{:S(2)}) collective-permute-start(bf16[128,1024]{1,0:T(8,128)(2,1)S(1)} %get-tuple-element.36.refs_0_), channel_id=1, source_target_pairs={{0,4},{4,0},{1,5},{5,1},{2,6},{6,2},{3,7},{7,3},{8,12},{12,8},{9,1... | collective-permute-start | bytes 786440 | tf_op jit(solution)/shard_map/ppermute | solution.py:31
  26.7 12.9 %collective-permute-start.5 = (bf16[2,128,768]{2,1,0:T(8,128)(2,1)S(1)}, bf16[2,128,768]{2,1,0:T(8,128)(2,1)S(1)}, u32[]{:S(2)}, u32[]{:S(2)}) collective-permute-start(bf16[2,128,768]{2,1,0:T(8,128)(2,1)S(1)} %collective-permute-done.4.refs_3_), channel_id=1, source_target_pairs={{0,32},{4,12},{8,40},{12,20},{16,48},{20,28},{24,56},{28,4},{32,64... | collective-permute-start | bytes 1179656 | tf_op jit(solution)/shard_map/ppermute | solution.py:41
  26.7 12.9 %collective-permute-start.7 = (bf16[2,128,768]{2,1,0:T(8,128)(2,1)S(1)}, bf16[2,128,768]{2,1,0:T(8,128)(2,1)S(1)}, u32[]{:S(2)}, u32[]{:S(2)}) collective-permute-start(bf16[2,128,768]{2,1,0:T(8,128)(2,1)S(1)} %collective-permute-done.6.refs_6_), channel_id=1, source_target_pairs={{0,96},{4,28},{8,104},{12,4},{16,112},{20,12},{24,120},{28,20},{32... | collective-permute-start | bytes 1179656 | tf_op jit(solution)/shard_map/ppermute | solution.py:41
  30.0 0.8 copy-start.17
  30.8 0.8 copy-start.20
  35.7 8.6 %copy-start = (bf16[512,4096]{1,0:T(8,128)(2,1)S(1)}, bf16[512,4096]{1,0:T(8,128)(2,1)}, u32[]{:S(2)}) copy-start(bf16[512,4096]{1,0:T(8,128)(2,1)} %narrow.1) | copy-start | bytes 12582916
  35.7 8.6 %copy-start.1 = (bf16[512,4096]{1,0:T(8,128)(2,1)S(1)}, bf16[512,4096]{1,0:T(8,128)(2,1)}, u32[]{:S(2)}) copy-start(bf16[512,4096]{1,0:T(8,128)(2,1)} %broad.1) | copy-start | bytes 12582916
  42.2 2.1 %collective-permute-start.10 = (f32[128,1152]{1,0:T(8,128)S(1)}, f32[128,1152]{1,0:T(8,128)S(1)}, u32[]{:S(2)}, u32[]{:S(2)}) collective-permute-start(f32[128,1152]{1,0:T(8,128)S(1)} %get-tuple-element.54), channel_id=1, source_target_pairs={{0,4},{4,0},{1,5},{5,1},{2,6},{6,2},{3,7},{7,3},{8,12},{12,8},{9,1... | collective-permute-start | bytes 1769480 | tf_op jit(solution)/shard_map/ppermute | solution.py:31
  44.3 20.2 %copy-start.8 = (bf16[128,4096]{1,0:T(8,128)(2,1)S(1)}, bf16[128,4096]{1,0:T(8,128)(2,1)}, u32[]{:S(2)}) copy-start(bf16[128,4096]{1,0:T(8,128)(2,1)} %residual.1) | copy-start | bytes 3145732
  44.3 20.2 %copy-start.21 = (f32[4096]{0:T(1024)S(1)}, f32[4096]{0:T(1024)}, u32[]{:S(2)}) copy-start(f32[4096]{0:T(1024)} %param.31) | copy-start | bytes 49156
  48.3 9.6 %collective-permute-start.11 = (bf16[32,4096]{1,0:T(8,128)(2,1)S(1)}, bf16[32,4096]{1,0:T(8,128)(2,1)S(1)}, u32[]{:S(2)}, u32[]{:S(2)}) collective-permute-start(bf16[32,4096]{1,0:T(8,128)(2,1)S(1)} %get-tuple-element.56), channel_id=1, source_target_pairs={{0,1},{1,2},{2,3},{3,0},{4,5},{5,6},{6,7},{7,4},{8,9},{9,10},{10,1... | collective-permute-start | bytes 786440 | tf_op jit(solution)/shard_map/ppermute | solution.py:27
  49.9 14.6 %collective-permute-start.12 = (bf16[32,4096]{1,0:T(8,128)(2,1)S(1)}, bf16[32,4096]{1,0:T(8,128)(2,1)S(1)}, u32[]{:S(2)}, u32[]{:S(2)}) collective-permute-start(bf16[32,4096]{1,0:T(8,128)(2,1)S(1)} %get-tuple-element.57), channel_id=1, source_target_pairs={{0,2},{1,3},{2,0},{3,1},{4,6},{5,7},{6,4},{7,5},{8,10},{9,11},{10,... | collective-permute-start | bytes 786440 | tf_op jit(solution)/shard_map/ppermute | solution.py:27
  52.6 11.9 %collective-permute-start.13 = (bf16[32,4096]{1,0:T(8,128)(2,1)S(1)}, bf16[32,4096]{1,0:T(8,128)(2,1)S(1)}, u32[]{:S(2)}, u32[]{:S(2)}) collective-permute-start(bf16[32,4096]{1,0:T(8,128)(2,1)S(1)} %get-tuple-element.58), channel_id=1, source_target_pairs={{0,3},{1,0},{2,1},{3,2},{4,7},{5,4},{6,5},{7,6},{8,11},{9,8},{10,9... | collective-permute-start | bytes 786440 | tf_op jit(solution)/shard_map/ppermute | solution.py:27
  64.5 37.7 %copy-start.4 = (bf16[1,256,4096]{2,1,0:T(8,128)(2,1)S(1)}, bf16[1,256,4096]{2,1,0:T(8,128)(2,1)}, u32[]{:S(2)}) copy-start(bf16[1,256,4096]{2,1,0:T(8,128)(2,1)} %down.2) | copy-start | bytes 6291460
  66.1 36.1 %copy-start.2 = (bf16[1,4096,256]{2,1,0:T(8,128)(2,1)S(1)}, bf16[1,4096,256]{2,1,0:T(8,128)(2,1)}, u32[]{:S(2)}) copy-start(bf16[1,4096,256]{2,1,0:T(8,128)(2,1)} %gate.2) | copy-start | bytes 6291460
  66.1 36.1 %copy-start.3 = (bf16[1,4096,256]{2,1,0:T(8,128)(2,1)S(1)}, bf16[1,4096,256]{2,1,0:T(8,128)(2,1)}, u32[]{:S(2)}) copy-start(bf16[1,4096,256]{2,1,0:T(8,128)(2,1)} %up.2) | copy-start | bytes 6291460
  108.8 62.7 %all-to-all-start.1 = ((bf16[128,8,1024]{2,1,0:T(8,128)(2,1)}), bf16[128,8,1024]{2,1,0:T(8,128)(2,1)S(1)}, u32[]{:S(2)}, u32[]{:S(2)}) async-start(bf16[128,8,1024]{2,1,0:T(8,128)(2,1)} %bitcast.11), calls=%async_computation.1 | async-start | bytes 4194304 | tf_op jit(solution)/shard_map/all_to_all | solution.py:459
  113.4 30.8 %collective-permute-start.14 = (bf16[32,4096]{1,0:T(8,128)(2,1)S(1)}, bf16[32,4096]{1,0:T(8,128)(2,1)S(1)}, u32[]{:S(2)}, u32[]{:S(2)}) collective-permute-start(bf16[32,4096]{1,0:T(8,128)(2,1)S(1)} %get-tuple-element.62.n0), channel_id=1, source_target_pairs={{0,1},{1,2},{2,3},{3,0},{4,5},{5,6},{6,7},{7,4},{8,9},{9,10},{10,1... | collective-permute-start | bytes 786440 | tf_op jit(solution)/shard_map/ppermute | solution.py:27
  114.3 35.5 %collective-permute-start.15 = (bf16[32,4096]{1,0:T(8,128)(2,1)S(1)}, bf16[32,4096]{1,0:T(8,128)(2,1)S(1)}, u32[]{:S(2)}, u32[]{:S(2)}) collective-permute-start(bf16[32,4096]{1,0:T(8,128)(2,1)S(1)} %get-tuple-element.62.n0), channel_id=1, source_target_pairs={{0,2},{1,3},{2,0},{3,1},{4,6},{5,7},{6,4},{7,5},{8,10},{9,11},{10,... | collective-permute-start | bytes 786440 | tf_op jit(solution)/shard_map/ppermute | solution.py:27
  117.1 32.8 %collective-permute-start.16 = (bf16[32,4096]{1,0:T(8,128)(2,1)S(1)}, bf16[32,4096]{1,0:T(8,128)(2,1)S(1)}, u32[]{:S(2)}, u32[]{:S(2)}) collective-permute-start(bf16[32,4096]{1,0:T(8,128)(2,1)S(1)} %get-tuple-element.62.n0), channel_id=1, source_target_pairs={{0,3},{1,0},{2,1},{3,2},{4,7},{5,4},{6,5},{7,6},{8,11},{9,8},{10,9... | collective-permute-start | bytes 786440 | tf_op jit(solution)/shard_map/ppermute | solution.py:27
  149.8 1.6 copy-start.5
  151.4 1.6 copy-start.6
  153.0 1.6 copy-start.7
  155.7 9.2 %collective-permute-start.17 = (bf16[32,4096]{1,0:T(8,128)(2,1)S(1)}, bf16[32,4096]{1,0:T(8,128)(2,1)S(1)}, u32[]{:S(2)}, u32[]{:S(2)}) collective-permute-start(bf16[32,4096]{1,0:T(8,128)(2,1)S(1)} %get-tuple-element.64), channel_id=1, source_target_pairs={{0,3},{1,0},{2,1},{3,2},{4,7},{5,4},{6,5},{7,6},{8,11},{9,8},{10,9... | collective-permute-start | bytes 786440 | tf_op jit(solution)/shard_map/ppermute | solution.py:27
  155.9 10.8 %collective-permute-start.18 = (bf16[32,4096]{1,0:T(8,128)(2,1)S(1)}, bf16[32,4096]{1,0:T(8,128)(2,1)S(1)}, u32[]{:S(2)}, u32[]{:S(2)}) collective-permute-start(bf16[32,4096]{1,0:T(8,128)(2,1)S(1)} %get-tuple-element.65), channel_id=1, source_target_pairs={{0,2},{1,3},{2,0},{3,1},{4,6},{5,7},{6,4},{7,5},{8,10},{9,11},{10,... | collective-permute-start | bytes 786440 | tf_op jit(solution)/shard_map/ppermute | solution.py:27
  157.8 13.0 %collective-permute-start.19 = (bf16[32,4096]{1,0:T(8,128)(2,1)S(1)}, bf16[32,4096]{1,0:T(8,128)(2,1)S(1)}, u32[]{:S(2)}, u32[]{:S(2)}) collective-permute-start(bf16[32,4096]{1,0:T(8,128)(2,1)S(1)} %get-tuple-element.66), channel_id=1, source_target_pairs={{0,1},{1,2},{2,3},{3,0},{4,5},{5,6},{6,7},{7,4},{8,9},{9,10},{10,1... | collective-permute-start | bytes 786440 | tf_op jit(solution)/shard_map/ppermute | solution.py:27
  166.6 0.7 copy-start.9
  170.8 0.7 copy-start.11
  171.5 1.0 copy-start.10
  172.4 0.9 copy-start.12

commit v5 on v4

--- a/solution.py
+++ b/solution.py
@@ -41,12 +41,15 @@
     return lax.ppermute(x, SP, pairs)
 
 
-def call(kernel, operands, shapes, smem=(), hbm=(), scratch=(), mib=16, flops=0, moved=2**21):
+def call(kernel, operands, shapes, smem=(), hbm=(), hbm_out=(), scratch=(), mib=16, flops=0, moved=2**21):
+    operands = [
+        pltpu.with_memory_space_constraint(x, pltpu.HBM) if i in hbm else x for i, x in enumerate(operands)
+    ]
     return pl.pallas_call(
         kernel,
         out_shape=shapes,
         in_specs=[SMEM if i in smem else HBM if i in hbm else VMEM for i in range(len(operands))],
-        out_specs=[VMEM] * len(shapes),
+        out_specs=[HBM if i in hbm_out else VMEM for i in range(len(shapes))],
         scratch_shapes=list(scratch),
         compiler_params=pltpu.CompilerParams(vmem_limit_bytes=mib * 1024 * 1024),
         cost_estimate=pl.CostEstimate(flops=flops, transcendentals=0, bytes_accessed=moved),
@@ -68,7 +71,7 @@
         copy.wait()
 
 
-def stack_kernel(a, b, c, d, ready, low, high):
+def stack_kernel(a, b, c, d, routed, biased, low, high):
     for out, i, ref in ((low, 0, a), (low, 1, b), (high, 0, c), (high, 1, d)):
         out[i] = ref[...]
 
@@ -117,14 +120,7 @@
 
 
 def project_kernel(place, own, other, narrow, broad, *refs):
-    outs, total, attn, weights, sems = refs[:4], *refs[4:]
-    copies = []
-    for at in range(0, 4096, 1024):
-        for i, ref in enumerate((narrow, broad)):
-            source, target = ref.at[:, at : at + 1024], weights.at[i, :, at : at + 1024]
-            copies.append(pltpu.make_async_copy(source, target, sems.at[len(copies)]))
-    for copy in copies:
-        copy.start()
+    outs, total, attn = refs[:4], *refs[4:]
     a, b = own[:, 1024:], other[:, 1024:]
     top = jnp.maximum(a, b)
     wa, wb = jnp.exp2(a - top), jnp.exp2(b - top)
@@ -135,16 +131,14 @@
         value = own[:, lo : lo + size] * wa[:, h : h + 1] + other[:, lo : lo + size] * wb[:, h : h + 1]
         attn[:, lo : lo + size] = value.astype(BF)
     for at in range(0, 4096, 1024):
-        copies[at // 512].wait()
-        copies[at // 512 + 1].wait()
-        part = jnp.dot(attn[:, :512], weights[0, :, at : at + 1024], preferred_element_type=F32)
-        part = part + jnp.dot(attn[:, 512:], weights[1, :, at : at + 1024], preferred_element_type=F32)
+        part = jnp.dot(attn[:, :512], narrow[:, at : at + 1024], preferred_element_type=F32)
+        part = part + jnp.dot(attn[:, 512:], broad[:, at : at + 1024], preferred_element_type=F32)
         total[:, at : at + 1024] = part
     for k in range(4):
         outs[k][...] = total[pl.ds(((place[3] + k) % 4) * 32, 32), :].astype(BF)
 
 
-def dispatch_kernel(place, p0, p1, p2, p3, residual, gain, target, stream_out, normed_out, out):
+def dispatch_kernel(place, p0, p1, p2, p3, residual, gain, target, stream_out, normed_out, out, rows, sems):
     mixture = p0[...].astype(F32) + p1[...].astype(F32) + p2[...].astype(F32) + p3[...].astype(F32)
     stream = residual[pl.ds(place[3] * 32, 32), :].astype(F32) + mixture
     stream_out[...] = stream
@@ -153,11 +147,17 @@
     normed_out[...] = normed
     cut = jnp.concatenate([normed[:, g * 1024 : (g + 1) * 1024] for g in range(4)], axis=0)
     row = lax.broadcasted_iota(jnp.int32, (256, 128), 0)
+    copies = []
     for at in range(0, 1024, 256):
         pick = row + at == target[0:1, :]
         for k in range(1, 4):
             pick = pick | (row + at == target[k : k + 1, :])
-        out[at : at + 256, :] = jnp.dot(pick.astype(F32).astype(BF), cut, preferred_element_type=F32).astype(BF)
+        rows[at : at + 256, :] = jnp.dot(pick.astype(F32).astype(BF), cut, preferred_element_type=F32).astype(BF)
+        part = pl.ds(at, 256)
+        copies.append(pltpu.make_async_copy(rows.at[part], out.at[part], sems.at[at // 256]))
+        copies[-1].start()
+    for copy in copies:
+        copy.wait()
 
 
 def silu(v):
@@ -175,7 +175,7 @@
             out[:, at : at + 1024] = part[k * 32 : (k + 1) * 32]
 
 
-def expert_kernel(inbound, gate, up, down, out, x, gate_up, down_copy, sems):
+def expert_kernel(inbound, gate, up, down, stream, s0, s1, s2, s3, out, base, x, gate_up, down_copy, sems):
     copies = []
     for g in range(4):
         for i, ref in enumerate((gate, up)):
@@ -184,6 +184,10 @@
     copies.append(pltpu.make_async_copy(down.at[0], down_copy, sems.at[len(copies)]))
     for copy in copies:
         copy.start()
+    total = stream[...]
+    for s in (s0, s1, s2, s3):
+        total = total + s[...].astype(F32)
+    base[...] = total
     i = lax.broadcasted_iota(jnp.int32, (256, 256), 0)
     j = lax.broadcasted_iota(jnp.int32, (256, 256), 1)
     order = (j == ((i % 64) // 2) * 8 + (i % 2) * 4 + i // 64).astype(F32).astype(BF)
@@ -209,14 +213,12 @@
         out[b * 256 : (b + 1) * 256, :] = jnp.dot(back, rows, preferred_element_type=F32).astype(BF)
 
 
-def combine_kernel(returned, mix, stream, s0, s1, s2, s3, out):
-    routed = jnp.dot(mix[...], returned[...], preferred_element_type=F32)
+def combine_kernel(returned, mix, base, out):
     for g in range(4):
         lo, hi = g * 1024, (g + 1) * 1024
-        total = stream[:, lo:hi] + routed[g * 32 : (g + 1) * 32]
-        for s in (s0, s1, s2, s3):
-            total = total + s[:, lo:hi].astype(F32)
-        out[:, lo:hi] = total.astype(BF)
+        rows = mix[g * 32 : (g + 1) * 32, :]
+        routed = jnp.dot(rows, returned[...], preferred_element_type=F32)
+        out[:, lo:hi] = (base[:, lo:hi] + routed).astype(BF)
 
 
 def attend_kernel(counts, first, last, *refs):
@@ -379,19 +381,28 @@
         [shaped((4, 128), jnp.int32), shaped((128, 1024), BF)],
     )
     place = jnp.stack([z, y, c, t])
-    line = [turn(own_kv, k, 0) for k in ORDER[1:]]
     q_other = swap_core(q_own)
-    low, high = call(stack_kernel, [own_kv] + line + [target], [shaped((2, 128, 768), BF)] * 2)
-    low_back, high_ahead = turn(low, 1, 1), turn(high, 3, 1)
-    low_ahead, high_back = turn(low, 3, 1), turn(high, 1, 1)
-    low_far, high_far = turn(low_back, 1, 1), turn(high_ahead, 3, 1)
-
+    line = {}
+    for k in (2, 1, 3):
+        line[k] = turn(own_kv, k, 0)
     own_bias, bias_1, bias_2, bias_3 = call(
         bias_kernel,
         (place, gates_narrow.T, gates_broad.T),
         [shaped((8, n), F32) for n in (128, 384, 1024, 512)],
         smem=(0,),
     )
+    low, high = call(
+        stack_kernel,
+        [own_kv] + [line[k] for k in ORDER[1:]] + [target, own_bias],
+        [shaped((2, 128, 768), BF)] * 2,
+    )
+    low_back = turn(low, 1, 1)
+    high_ahead = turn(high, 3, 1)
+    low_ahead = turn(low, 3, 1)
+    high_back = turn(high, 1, 1)
+    low_far = turn(low_back, 1, 1)
+    high_far = turn(high_ahead, 3, 1)
+
     core = c.reshape(1)
     first_tiles = [((own_kv,), own_bias, True), ((low, high), bias_1, False)]
     state = attend(q_own, q_other, core, first_tiles, None, False)
@@ -405,24 +416,20 @@
         (place, own_part, other_part, project_narrow, project_broad),
         [shaped((32, 4096), BF)] * 4,
         smem=(0,),
-        hbm=(3, 4),
-        scratch=[
-            pltpu.VMEM((128, 4096), F32),
-            pltpu.VMEM((128, 1024), BF),
-            pltpu.VMEM((2, 512, 4096), BF),
-            pltpu.SemaphoreType.DMA((8,)),
-        ],
-        mib=20,
-        moved=0,
+        scratch=[pltpu.VMEM((128, 4096), F32), pltpu.VMEM((128, 1024), BF)],
         flops=2 * 128 * 1024 * 4096,
     )
-    p1, p2, p3 = shift(p1, "tp", 1), shift(p2, "tp", 2), shift(p3, "tp", 3)
+    p2 = shift(p2, "tp", 2)
+    p1 = shift(p1, "tp", 1)
+    p3 = shift(p3, "tp", 3)
 
     stream, normed, outbound = call(
         dispatch_kernel,
         (place, p0, p1, p2, p3, residual, norm_gain.reshape(1, -1), target),
-        [shaped((32, 4096), F32), shaped((32, 4096), BF), shaped((1024, 1024), BF)],
+        [shaped((32, 4096), F32), shaped((32, 4096), BF), pltpu.HBM((1024, 1024), BF)],
         smem=(0,),
+        hbm_out=(2,),
+        scratch=[pltpu.VMEM((1024, 1024), BF), pltpu.SemaphoreType.DMA((4,))],
         flops=2 * 1024 * 128 * 1024,
     )
     every = SP + ("tp",)
@@ -441,10 +448,10 @@
     s2 = shift(s2, "tp", 2)
     s3 = shift(s3, "tp", 1)
 
-    (result,) = call(
+    result, base = call(
         expert_kernel,
-        (inbound.reshape(1024, 1024), expert_gate, expert_up, expert_down),
-        [shaped((1024, 1024), BF)],
+        (inbound.reshape(1024, 1024), expert_gate, expert_up, expert_down, stream, s0, s1, s2, s3),
+        [shaped((1024, 1024), BF), shaped((32, 4096), F32)],
         hbm=(1, 2, 3),
         scratch=[
             pltpu.VMEM((256, 4096), BF),
@@ -459,7 +466,7 @@
     returned = lax.all_to_all(result.reshape(128, 8, 1024), every, 0, 0, tiled=True)
     (out,) = call(
         combine_kernel,
-        (returned.reshape(1024, 1024), mix, stream, s0, s1, s2, s3),
+        (returned.reshape(1024, 1024), mix, base),
         [shaped((32, 4096), BF)],
         flops=2 * 128 * 1024 * 1024,
     )

time: 176 us -> 174 us (0.989)
  local copies, waits for them, and re-layouts: 16.1 us -> 11.1 us
  starting transfers between devices: 33 us -> 36.7 us
  blocking collectives: 36.1 us -> 38.9 us
  waiting for transfers between devices: 62.6 us -> 59.9 us
    unnamed x48 -> x30, local copies, waits for them, and re-layouts: 16.1 us -> 11.1 us
    all_to_all x1, starting transfers between devices: 4.67 us -> 8.03 us  [local(): lax.all_to_all(outbound.reshape(128, 8, 1024), every, 0, 0, tiled=True)]
    all_to_all x1, blocking collectives: 36.1 us -> 38.9 us  [local(): lax.all_to_all(result.reshape(128, 8, 1024), every, 0, 0, tiled=True)]
    ppermute x9, waiting for transfers between devices: 7.11 us -> 4.43 us  [turn(): return lax.ppermute(x, SP, pairs)]
  transfers between devices with their start and end apart: 21 -> 21, of which waited for: 11 -> 10; matrix products, arithmetic and copies ran while one was open for 0% -> 0% of each run, Pallas kernels for 5% -> 5%
where the time goes in v5:
time: 174 us; the launch traced here: 172 us
  waiting for transfers between devices  59.9 us (34%)
  blocking collectives  38.9 us (22%)
  starting transfers between devices  36.7 us (21%)
  Pallas kernels  25.1 us (14%)
  local copies, waits for them, and re-layouts  11.1 us (6%)
    ppermute x9, waiting for transfers between devices, shift(): return lax.ppermute(x, axis, [(i, (i + k) % 4) for i in range(4)])  53.5 us
    all_to_all x1, blocking collectives, local(): lax.all_to_all(result.reshape(128, 8, 1024), every, 0, 0, tiled=True)  38.9 us
    pallas_call x9, Pallas kernels, call(): pl.pallas_call(kernel, out_shape=shapes, in_specs=[SMEM if i in smem else...  16.2 us
    ppermute x9, starting transfers between devices, turn(): return lax.ppermute(x, SP, pairs)  15 us
    ppermute x9, starting transfers between devices, shift(): return lax.ppermute(x, axis, [(i, (i + k) % 4) for i in range(4)])  13.5 us
    unnamed x30, local copies, waits for them, and re-layouts  11.1 us
    pallas_call x3, Pallas kernels, attend(): pl.pallas_call(functools.partial(attend_kernel, counts, state is None, la...  8.92 us
    all_to_all x1, starting transfers between devices, local(): lax.all_to_all(outbound.reshape(128, 8, 1024), every, 0, 0, tiled=True)  8.03 us
  transfers between devices with their start and end apart: 21, of which 10 were waited for; matrix products, arithmetic and copies ran while one was open for 0% of the time, Pallas kernels for 5%

profile of v5, /device:TPU:0, one launch (start us, length us, event | category | flops | bytes accessed | tf_op | source)
XLA Modules:
  0.0 172.0 jit_solution(240670156954284107)
XLA Ops:
  0.0 1.1 shard_map.190
  1.1 1.8 %collective-permute-start.1 = (bf16[128,768]{1,0:T(8,128)(2,1)S(1)}, bf16[128,768]{1,0:T(8,128)(2,1)S(1)}, u32[]{:S(2)}, u32[]{:S(2)}) collective-permute-start(bf16[128,768]{1,0:T(8,128)(2,1)S(1)} %get-tuple-element.39.a.refs_3_), channel_id=1, source_target_pairs={{0,8},{4,36},{8,16},{12,44},{16,24},{20,52},{24,0},{28,60},{32,40}... | collective-permute-start | bytes 589832 | tf_op jit(solution)/shard_map/ppermute | solution.py:41
  2.9 1.5 collective-permute-start.2
  4.4 2.1 %collective-permute-start.3 = (bf16[128,768]{1,0:T(8,128)(2,1)S(1)}, bf16[128,768]{1,0:T(8,128)(2,1)S(1)}, u32[]{:S(2)}, u32[]{:S(2)}) collective-permute-start(bf16[128,768]{1,0:T(8,128)(2,1)S(1)} %get-tuple-element.39.a.refs_3_), channel_id=1, source_target_pairs={{0,16},{4,68},{8,24},{12,76},{16,0},{20,84},{24,8},{28,92},{32,48}... | collective-permute-start | bytes 589832 | tf_op jit(solution)/shard_map/ppermute | solution.py:41
  6.5 0.7 copy-done.13
  7.2 0.7 copy-done.14
  8.5 0.8 copy-done.10
  9.4 0.8 copy-done.11
  10.1 0.7 shard_map.192
  10.8 0.8 collective-permute-done.3.d
  11.7 2.1 %collective-permute-start.4 = (bf16[2,128,768]{2,1,0:T(8,128)(2,1)S(1)}, bf16[2,128,768]{2,1,0:T(8,128)(2,1)S(1)}, u32[]{:S(2)}, u32[]{:S(2)}) collective-permute-start(bf16[2,128,768]{2,1,0:T(8,128)(2,1)S(1)} %get-tuple-element.42.refs_5_), channel_id=1, source_target_pairs={{0,32},{4,12},{8,40},{12,20},{16,48},{20,28},{24,56},{28,4},{32,64... | collective-permute-start | bytes 1179656 | tf_op jit(solution)/shard_map/ppermute | solution.py:41
  13.8 2.2 %collective-permute-start.6 = (bf16[2,128,768]{2,1,0:T(8,128)(2,1)S(1)}, bf16[2,128,768]{2,1,0:T(8,128)(2,1)S(1)}, u32[]{:S(2)}, u32[]{:S(2)}) collective-permute-start(bf16[2,128,768]{2,1,0:T(8,128)(2,1)S(1)} %get-tuple-element.43.refs_6_), channel_id=1, source_target_pairs={{0,96},{4,28},{8,104},{12,4},{16,112},{20,12},{24,120},{28,20},{32... | collective-permute-start | bytes 1179656 | tf_op jit(solution)/shard_map/ppermute | solution.py:41
  16.0 1.9 %collective-permute-start.8 = (bf16[2,128,768]{2,1,0:T(8,128)(2,1)S(1)}, bf16[2,128,768]{2,1,0:T(8,128)(2,1)S(1)}, u32[]{:S(2)}, u32[]{:S(2)}) collective-permute-start(bf16[2,128,768]{2,1,0:T(8,128)(2,1)S(1)} %get-tuple-element.42.refs_5_), channel_id=1, source_target_pairs={{0,96},{4,28},{8,104},{12,4},{16,112},{20,12},{24,120},{28,20},{32... | collective-permute-start | bytes 1179656 | tf_op jit(solution)/shard_map/ppermute | solution.py:41
  18.0 3.6 %collective-permute-done.4.refs_3_ = bf16[2,128,768]{2,1,0:T(8,128)(2,1)S(1)} collective-permute-done((bf16[2,128,768]{2,1,0:T(8,128)(2,1)S(1)}, bf16[2,128,768]{2,1,0:T(8,128)(2,1)S(1)}, u32[]{:S(2)}, u32[]{:S(2)}) %collective-permute-start.4) | collective-permute-done | bytes 393248 | tf_op jit(solution)/shard_map/ppermute | solution.py:41
  21.6 3.3 %collective-permute-start.7 = (bf16[2,128,768]{2,1,0:T(8,128)(2,1)S(1)}, bf16[2,128,768]{2,1,0:T(8,128)(2,1)S(1)}, u32[]{:S(2)}, u32[]{:S(2)}) collective-permute-start(bf16[2,128,768]{2,1,0:T(8,128)(2,1)S(1)} %collective-permute-done.6.refs_6_), channel_id=1, source_target_pairs={{0,96},{4,28},{8,104},{12,4},{16,112},{20,12},{24,120},{28,20},{32... | collective-permute-start | bytes 1179656 | tf_op jit(solution)/shard_map/ppermute | solution.py:41
  25.0 2.3 %shard_map.194 = (f32[1536,128]{1,0:T(8,128)S(1)}, f32[1536,128]{1,0:T(8,128)S(1)}, f32[1024,128]{1,0:T(8,128)S(1)}, f32[512,256]{1,0:T(8,128)S(1)}) custom-call(bf16[128,1024]{1,0:T(8,128)(2,1)S(1)} %get-tuple-element.38.refs_0_, bf16[128,1024]{1,0:T(8,128)(2,1)S(1)} %collective-permute-done.refs_1_, s32[1]{0:T(128)} %bitcast.2.refs_2_, ...), custom_call_target="tpu_custom_call" | custom-call | flops 536870912 | bytes 4194304 | tf_op jit(solution)/shard_map/pallas_call | solution.py:334
  27.3 4.1 %shard_map.195 = (f32[1536,128]{1,0:T(8,128)S(1)}, f32[1536,128]{1,0:T(8,128)S(1)}, f32[1024,128]{1,0:T(8,128)S(1)}, f32[512,256]{1,0:T(8,128)S(1)}) custom-call(bf16[128,1024]{1,0:T(8,128)(2,1)S(1)} %get-tuple-element.38.refs_0_, bf16[128,1024]{1,0:T(8,128)(2,1)S(1)} %collective-permute-done.refs_1_, s32[1]{0:T(128)} %bitcast.2.refs_2_, ...), custom_call_target="tpu_custom_call" | custom-call | flops 1073741824 | bytes 4194304 | tf_op jit(solution)/shard_map/pallas_call | solution.py:334
  31.4 2.6 %shard_map.196 = (f32[128,1152]{1,0:T(8,128)S(1)}, f32[128,1152]{1,0:T(8,128)S(1)}) custom-call(bf16[128,1024]{1,0:T(8,128)(2,1)S(1)} %get-tuple-element.38.refs_0_, bf16[128,1024]{1,0:T(8,128)(2,1)S(1)} %collective-permute-done.refs_1_, s32[1]{0:T(128)} %bitcast.2.refs_2_, bf16[2,128,768]{2,1,0:T(8,128)(2,1)S(1)} %collective-permute-done.5.refs_3_, ...), custom_call_target="tpu_custom_call" | custom-call | flops 536870912 | bytes 4194304 | tf_op jit(solution)/shard_map/pallas_call | solution.py:334
  34.0 2.0 %collective-permute-done.10.other = f32[128,1152]{1,0:T(8,128)S(1)} collective-permute-done((f32[128,1152]{1,0:T(8,128)S(1)}, f32[128,1152]{1,0:T(8,128)S(1)}, u32[]{:S(2)}, u32[]{:S(2)}) %collective-permute-start.10) | collective-permute-done | bytes 589856 | tf_op jit(solution)/shard_map/ppermute | solution.py:31
  36.1 2.1 %shard_map.197 = (bf16[32,4096]{1,0:T(8,128)(2,1)S(1)}, bf16[32,4096]{1,0:T(8,128)(2,1)S(1)}, bf16[32,4096]{1,0:T(8,128)(2,1)S(1)}, bf16[32,4096]{1,0:T(8,128)(2,1)S(1)}) custom-call(s32[4]{0:T(128)S(1)} %pad_add_fusion.place, f32[128,1152]{1,0:T(8,128)S(1)} %get-tuple-element.55.own, f32[128,1152]{1,0:T(8,128)S(1)} %collective-permute-done.10.other, ...), custom_call_target="tpu_custom_call" | custom-call | flops 1073741824 | bytes 2097152 | tf_op jit(solution)/shard_map/pallas_call | solution.py:48
  38.2 1.6 collective-permute-start.11
  39.7 2.7 %collective-permute-start.12 = (bf16[32,4096]{1,0:T(8,128)(2,1)S(1)}, bf16[32,4096]{1,0:T(8,128)(2,1)S(1)}, u32[]{:S(2)}, u32[]{:S(2)}) collective-permute-start(bf16[32,4096]{1,0:T(8,128)(2,1)S(1)} %get-tuple-element.59), channel_id=1, source_target_pairs={{0,2},{1,3},{2,0},{3,1},{4,6},{5,7},{6,4},{7,5},{8,10},{9,11},{10,... | collective-permute-start | bytes 786440 | tf_op jit(solution)/shard_map/ppermute | solution.py:27
  42.4 1.4 collective-permute-start.13
  43.9 3.9 %collective-permute-done.11.p1 = bf16[32,4096]{1,0:T(8,128)(2,1)S(1)} collective-permute-done((bf16[32,4096]{1,0:T(8,128)(2,1)S(1)}, bf16[32,4096]{1,0:T(8,128)(2,1)S(1)}, u32[]{:S(2)}, u32[]{:S(2)}) %collective-permute-start.11) | collective-permute-done | bytes 262176 | tf_op jit(solution)/shard_map/ppermute | solution.py:27
  47.8 6.6 %collective-permute-done.12.p2 = bf16[32,4096]{1,0:T(8,128)(2,1)S(1)} collective-permute-done((bf16[32,4096]{1,0:T(8,128)(2,1)S(1)}, bf16[32,4096]{1,0:T(8,128)(2,1)S(1)}, u32[]{:S(2)}, u32[]{:S(2)}) %collective-permute-start.12) | collective-permute-done | bytes 262176 | tf_op jit(solution)/shard_map/ppermute | solution.py:27
  54.4 2.5 %shard_map.198 = (f32[32,4096]{1,0:T(8,128)S(1)}, bf16[32,4096]{1,0:T(8,128)(2,1)S(1)}, bf16[1024,1024]{1,0:T(8,128)(2,1)}) custom-call(s32[4]{0:T(128)S(1)} %pad_add_fusion.place, bf16[32,4096]{1,0:T(8,128)(2,1)S(1)} %get-tuple-element.57.p0, bf16[32,4096]{1,0:T(8,128)(2,1)S(1)} %collective-permute-done.11.p1, ...), custom_call_target="tpu_custom_call" | custom-call | flops 268435456 | bytes 2097152 | tf_op jit(solution)/shard_map/pallas_call | solution.py:48
  56.9 8.0 %all-to-all-start = ((bf16[128,8,1024]{2,1,0:T(8,128)(2,1)}), bf16[128,8,1024]{2,1,0:T(8,128)(2,1)S(1)}, u32[]{:S(2)}, u32[]{:S(2)}) async-start(bf16[128,8,1024]{2,1,0:T(8,128)(2,1)} %bitcast.21), calls=%async_computation | async-start | bytes 4194304 | tf_op jit(solution)/shard_map/all_to_all | solution.py:436
  65.0 1.0 collective-permute-start.14
  66.0 2.7 %collective-permute-start.15 = (bf16[32,4096]{1,0:T(8,128)(2,1)S(1)}, bf16[32,4096]{1,0:T(8,128)(2,1)S(1)}, u32[]{:S(2)}, u32[]{:S(2)}) collective-permute-start(bf16[32,4096]{1,0:T(8,128)(2,1)S(1)} %get-tuple-element.63.n0), channel_id=1, source_target_pairs={{0,2},{1,3},{2,0},{3,1},{4,6},{5,7},{6,4},{7,5},{8,10},{9,11},{10,... | collective-permute-start | bytes 786440 | tf_op jit(solution)/shard_map/ppermute | solution.py:27
  68.7 1.5 collective-permute-start.16
  70.1 25.7 %collective-permute-done.14.n1 = bf16[32,4096]{1,0:T(8,128)(2,1)S(1)} collective-permute-done((bf16[32,4096]{1,0:T(8,128)(2,1)S(1)}, bf16[32,4096]{1,0:T(8,128)(2,1)S(1)}, u32[]{:S(2)}, u32[]{:S(2)}) %collective-permute-start.14) | collective-permute-done | bytes 262176 | tf_op jit(solution)/shard_map/ppermute | solution.py:27
  95.8 5.6 %collective-permute-done.15.n2 = bf16[32,4096]{1,0:T(8,128)(2,1)S(1)} collective-permute-done((bf16[32,4096]{1,0:T(8,128)(2,1)S(1)}, bf16[32,4096]{1,0:T(8,128)(2,1)S(1)}, u32[]{:S(2)}, u32[]{:S(2)}) %collective-permute-start.15) | collective-permute-done | bytes 262176 | tf_op jit(solution)/shard_map/ppermute | solution.py:27
  101.4 1.6 copy-done.2
  103.0 1.6 copy-done.3
  104.6 1.6 copy-done.4
  106.2 1.1 shard_map.199
  107.5 1.9 %collective-permute-start.18 = (bf16[32,4096]{1,0:T(8,128)(2,1)S(1)}, bf16[32,4096]{1,0:T(8,128)(2,1)S(1)}, u32[]{:S(2)}, u32[]{:S(2)}) collective-permute-start(bf16[32,4096]{1,0:T(8,128)(2,1)S(1)} %get-tuple-element.66), channel_id=1, source_target_pairs={{0,2},{1,3},{2,0},{3,1},{4,6},{5,7},{6,4},{7,5},{8,10},{9,11},{10,... | collective-permute-start | bytes 786440 | tf_op jit(solution)/shard_map/ppermute | solution.py:27
  109.4 0.6 collective-permute-start.19
  110.0 6.6 %collective-permute-done.17.s1 = bf16[32,4096]{1,0:T(8,128)(2,1)S(1)} collective-permute-done((bf16[32,4096]{1,0:T(8,128)(2,1)S(1)}, bf16[32,4096]{1,0:T(8,128)(2,1)S(1)}, u32[]{:S(2)}, u32[]{:S(2)}) %collective-permute-start.17) | collective-permute-done | bytes 262176 | tf_op jit(solution)/shard_map/ppermute | solution.py:27
  116.6 1.6 collective-permute-done.18.s2
  118.2 0.7 copy-done.6
  118.9 3.4 %collective-permute-done.19.s3 = bf16[32,4096]{1,0:T(8,128)(2,1)S(1)} collective-permute-done((bf16[32,4096]{1,0:T(8,128)(2,1)S(1)}, bf16[32,4096]{1,0:T(8,128)(2,1)S(1)}, u32[]{:S(2)}, u32[]{:S(2)}) %collective-permute-start.19) | collective-permute-done | bytes 262176 | tf_op jit(solution)/shard_map/ppermute | solution.py:27
  122.4 0.7 copy-done.8
  123.1 0.9 copy-done.7
  124.0 0.9 copy-done.9
  125.0 5.8 %shard_map.200 = (bf16[1024,1024]{1,0:T(8,128)(2,1)S(1)}, f32[32,4096]{1,0:T(8,128)S(1)}) custom-call(bf16[1024,1024]{1,0:T(8,128)(2,1)S(1)} %bitcast.13, bf16[1,4096,256]{2,1,0:T(8,128)(2,1)} %gate.3, bf16[1,4096,256]{2,1,0:T(8,128)(2,1)} %up.3, bf16[1,256,4096]{2,1,0:T(8,128)(2,1)} %down.3, f32[32,4096]{1,0:T(8,128)S(1)} %get-tuple-element.62.stream, ...), custom_call_target="tpu_custom_call" | custom-call | flops 1610612736 | tf_op jit(solution)/shard_map/pallas_call | solution.py:48
  130.8 38.9 %all_to_all.10 = bf16[128,8,1024]{2,1,0:T(8,128)(2,1)S(1)} all-to-all(bf16[128,8,1024]{2,1,0:T(8,128)(2,1)S(1)} %bitcast.15), channel_id=1, replica_groups=mesh['z'=4,'y'=4,'c'=2,'tp'=4] {'z','y','c','tp'}, dimensions={0} | all-to-all | bytes 4194304 | tf_op jit(solution)/shard_map/all_to_all | solution.py:466
  169.8 2.3 %shard_map.201 = bf16[32,4096]{1,0:T(8,128)(2,1)} custom-call(bf16[1024,1024]{1,0:T(8,128)(2,1)S(1)} %bitcast.14, bf16[128,1024]{1,0:T(8,128)(2,1)S(1)} %get-tuple-element.69.mix, f32[32,4096]{1,0:T(8,128)S(1)} %get-tuple-element.70.base), custom_call_target="tpu_custom_call" | custom-call | flops 268435456 | bytes 2097152 | tf_op jit(solution)/shard_map/pallas_call | solution.py:48
  (38 shorter events, 1.1 us)
Async XLA Ops:
  1.1 9.7 %collective-permute-start.1 = (bf16[128,768]{1,0:T(8,128)(2,1)S(1)}, bf16[128,768]{1,0:T(8,128)(2,1)S(1)}, u32[]{:S(2)}, u32[]{:S(2)}) collective-permute-start(bf16[128,768]{1,0:T(8,128)(2,1)S(1)} %get-tuple-element.39.a.refs_3_), channel_id=1, source_target_pairs={{0,8},{4,36},{8,16},{12,44},{16,24},{20,52},{24,0},{28,60},{32,40}... | collective-permute-start | bytes 589832 | tf_op jit(solution)/shard_map/ppermute | solution.py:41
  2.9 7.9 %collective-permute-start.2 = (bf16[128,768]{1,0:T(8,128)(2,1)S(1)}, bf16[128,768]{1,0:T(8,128)(2,1)S(1)}, u32[]{:S(2)}, u32[]{:S(2)}) collective-permute-start(bf16[128,768]{1,0:T(8,128)(2,1)S(1)} %get-tuple-element.39.a.refs_3_), channel_id=1, source_target_pairs={{0,24},{4,100},{8,0},{12,108},{16,8},{20,116},{24,16},{28,124},{32... | collective-permute-start | bytes 589832 | tf_op jit(solution)/shard_map/ppermute | solution.py:41
  4.4 7.2 %collective-permute-start.3 = (bf16[128,768]{1,0:T(8,128)(2,1)S(1)}, bf16[128,768]{1,0:T(8,128)(2,1)S(1)}, u32[]{:S(2)}, u32[]{:S(2)}) collective-permute-start(bf16[128,768]{1,0:T(8,128)(2,1)S(1)} %get-tuple-element.39.a.refs_3_), channel_id=1, source_target_pairs={{0,16},{4,68},{8,24},{12,76},{16,0},{20,84},{24,8},{28,92},{32,48}... | collective-permute-start | bytes 589832 | tf_op jit(solution)/shard_map/ppermute | solution.py:41
  6.5 0.7 copy-start.13
  7.2 0.7 copy-start.14
  8.5 0.8 copy-start.10
  9.4 0.8 copy-start.11
  11.7 10.0 %collective-permute-start.4 = (bf16[2,128,768]{2,1,0:T(8,128)(2,1)S(1)}, bf16[2,128,768]{2,1,0:T(8,128)(2,1)S(1)}, u32[]{:S(2)}, u32[]{:S(2)}) collective-permute-start(bf16[2,128,768]{2,1,0:T(8,128)(2,1)S(1)} %get-tuple-element.42.refs_5_), channel_id=1, source_target_pairs={{0,32},{4,12},{8,40},{12,20},{16,48},{20,28},{24,56},{28,4},{32,64... | collective-permute-start | bytes 1179656 | tf_op jit(solution)/shard_map/ppermute | solution.py:41
  13.8 7.9 %collective-permute-start.6 = (bf16[2,128,768]{2,1,0:T(8,128)(2,1)S(1)}, bf16[2,128,768]{2,1,0:T(8,128)(2,1)S(1)}, u32[]{:S(2)}, u32[]{:S(2)}) collective-permute-start(bf16[2,128,768]{2,1,0:T(8,128)(2,1)S(1)} %get-tuple-element.43.refs_6_), channel_id=1, source_target_pairs={{0,96},{4,28},{8,104},{12,4},{16,112},{20,12},{24,120},{28,20},{32... | collective-permute-start | bytes 1179656 | tf_op jit(solution)/shard_map/ppermute | solution.py:41
  16.0 11.3 %collective-permute-start.8 = (bf16[2,128,768]{2,1,0:T(8,128)(2,1)S(1)}, bf16[2,128,768]{2,1,0:T(8,128)(2,1)S(1)}, u32[]{:S(2)}, u32[]{:S(2)}) collective-permute-start(bf16[2,128,768]{2,1,0:T(8,128)(2,1)S(1)} %get-tuple-element.42.refs_5_), channel_id=1, source_target_pairs={{0,96},{4,28},{8,104},{12,4},{16,112},{20,12},{24,120},{28,20},{32... | collective-permute-start | bytes 1179656 | tf_op jit(solution)/shard_map/ppermute | solution.py:41
  17.9 9.3 %collective-permute-start.9 = (bf16[2,128,768]{2,1,0:T(8,128)(2,1)S(1)}, bf16[2,128,768]{2,1,0:T(8,128)(2,1)S(1)}, u32[]{:S(2)}, u32[]{:S(2)}) collective-permute-start(bf16[2,128,768]{2,1,0:T(8,128)(2,1)S(1)} %get-tuple-element.43.refs_6_), channel_id=1, source_target_pairs={{0,32},{4,12},{8,40},{12,20},{16,48},{20,28},{24,56},{28,4},{32,64... | collective-permute-start | bytes 1179656 | tf_op jit(solution)/shard_map/ppermute | solution.py:41
  18.0 7.0 %collective-permute-start = (bf16[128,1024]{1,0:T(8,128)(2,1)S(1)}, bf16[128,1024]{1,0:T(8,128)(2,1)S(1)}, u32[]{:S(2)}, u32[]{:S(2)}) collective-permute-start(bf16[128,1024]{1,0:T(8,128)(2,1)S(1)} %get-tuple-element.38.refs_0_), channel_id=1, source_target_pairs={{0,4},{4,0},{1,5},{5,1},{2,6},{6,2},{3,7},{7,3},{8,12},{12,8},{9,1... | collective-permute-start | bytes 786440 | tf_op jit(solution)/shard_map/ppermute | solution.py:31
  21.6 9.7 %collective-permute-start.5 = (bf16[2,128,768]{2,1,0:T(8,128)(2,1)S(1)}, bf16[2,128,768]{2,1,0:T(8,128)(2,1)S(1)}, u32[]{:S(2)}, u32[]{:S(2)}) collective-permute-start(bf16[2,128,768]{2,1,0:T(8,128)(2,1)S(1)} %collective-permute-done.4.refs_3_), channel_id=1, source_target_pairs={{0,32},{4,12},{8,40},{12,20},{16,48},{20,28},{24,56},{28,4},{32,64... | collective-permute-start | bytes 1179656 | tf_op jit(solution)/shard_map/ppermute | solution.py:41
  21.6 9.7 %collective-permute-start.7 = (bf16[2,128,768]{2,1,0:T(8,128)(2,1)S(1)}, bf16[2,128,768]{2,1,0:T(8,128)(2,1)S(1)}, u32[]{:S(2)}, u32[]{:S(2)}) collective-permute-start(bf16[2,128,768]{2,1,0:T(8,128)(2,1)S(1)} %collective-permute-done.6.refs_6_), channel_id=1, source_target_pairs={{0,96},{4,28},{8,104},{12,4},{16,112},{20,12},{24,120},{28,20},{32... | collective-permute-start | bytes 1179656 | tf_op jit(solution)/shard_map/ppermute | solution.py:41
  27.2 8.8 %copy-start = (bf16[512,4096]{1,0:T(8,128)(2,1)S(1)}, bf16[512,4096]{1,0:T(8,128)(2,1)}, u32[]{:S(2)}) copy-start(bf16[512,4096]{1,0:T(8,128)(2,1)} %narrow.1) | copy-start | bytes 12582916
  27.3 8.8 %copy-start.1 = (bf16[512,4096]{1,0:T(8,128)(2,1)S(1)}, bf16[512,4096]{1,0:T(8,128)(2,1)}, u32[]{:S(2)}) copy-start(bf16[512,4096]{1,0:T(8,128)(2,1)} %broad.1) | copy-start | bytes 12582916
  34.0 2.1 %collective-permute-start.10 = (f32[128,1152]{1,0:T(8,128)S(1)}, f32[128,1152]{1,0:T(8,128)S(1)}, u32[]{:S(2)}, u32[]{:S(2)}) collective-permute-start(f32[128,1152]{1,0:T(8,128)S(1)} %get-tuple-element.56), channel_id=1, source_target_pairs={{0,4},{4,0},{1,5},{5,1},{2,6},{6,2},{3,7},{7,3},{8,12},{12,8},{9,1... | collective-permute-start | bytes 1769480 | tf_op jit(solution)/shard_map/ppermute | solution.py:31
  36.0 18.3 %copy-start.5 = (bf16[128,4096]{1,0:T(8,128)(2,1)S(1)}, bf16[128,4096]{1,0:T(8,128)(2,1)}, u32[]{:S(2)}) copy-start(bf16[128,4096]{1,0:T(8,128)(2,1)} %residual.1) | copy-start | bytes 3145732
  36.0 18.3 %copy-start.12 = (f32[4096]{0:T(1024)S(1)}, f32[4096]{0:T(1024)}, u32[]{:S(2)}) copy-start(f32[4096]{0:T(1024)} %param.31) | copy-start | bytes 49156
  38.2 9.6 %collective-permute-start.11 = (bf16[32,4096]{1,0:T(8,128)(2,1)S(1)}, bf16[32,4096]{1,0:T(8,128)(2,1)S(1)}, u32[]{:S(2)}, u32[]{:S(2)}) collective-permute-start(bf16[32,4096]{1,0:T(8,128)(2,1)S(1)} %get-tuple-element.58), channel_id=1, source_target_pairs={{0,1},{1,2},{2,3},{3,0},{4,5},{5,6},{6,7},{7,4},{8,9},{9,10},{10,1... | collective-permute-start | bytes 786440 | tf_op jit(solution)/shard_map/ppermute | solution.py:27
  39.7 14.7 %collective-permute-start.12 = (bf16[32,4096]{1,0:T(8,128)(2,1)S(1)}, bf16[32,4096]{1,0:T(8,128)(2,1)S(1)}, u32[]{:S(2)}, u32[]{:S(2)}) collective-permute-start(bf16[32,4096]{1,0:T(8,128)(2,1)S(1)} %get-tuple-element.59), channel_id=1, source_target_pairs={{0,2},{1,3},{2,0},{3,1},{4,6},{5,7},{6,4},{7,5},{8,10},{9,11},{10,... | collective-permute-start | bytes 786440 | tf_op jit(solution)/shard_map/ppermute | solution.py:27
  42.4 11.9 %collective-permute-start.13 = (bf16[32,4096]{1,0:T(8,128)(2,1)S(1)}, bf16[32,4096]{1,0:T(8,128)(2,1)S(1)}, u32[]{:S(2)}, u32[]{:S(2)}) collective-permute-start(bf16[32,4096]{1,0:T(8,128)(2,1)S(1)} %get-tuple-element.60), channel_id=1, source_target_pairs={{0,3},{1,0},{2,1},{3,2},{4,7},{5,4},{6,5},{7,6},{8,11},{9,8},{10,9... | collective-permute-start | bytes 786440 | tf_op jit(solution)/shard_map/ppermute | solution.py:27
  56.9 66.2 %all-to-all-start = ((bf16[128,8,1024]{2,1,0:T(8,128)(2,1)}), bf16[128,8,1024]{2,1,0:T(8,128)(2,1)S(1)}, u32[]{:S(2)}, u32[]{:S(2)}) async-start(bf16[128,8,1024]{2,1,0:T(8,128)(2,1)} %bitcast.21), calls=%async_computation | async-start | bytes 4194304 | tf_op jit(solution)/shard_map/all_to_all | solution.py:436
  65.0 30.8 %collective-permute-start.14 = (bf16[32,4096]{1,0:T(8,128)(2,1)S(1)}, bf16[32,4096]{1,0:T(8,128)(2,1)S(1)}, u32[]{:S(2)}, u32[]{:S(2)}) collective-permute-start(bf16[32,4096]{1,0:T(8,128)(2,1)S(1)} %get-tuple-element.63.n0), channel_id=1, source_target_pairs={{0,1},{1,2},{2,3},{3,0},{4,5},{5,6},{6,7},{7,4},{8,9},{9,10},{10,1... | collective-permute-start | bytes 786440 | tf_op jit(solution)/shard_map/ppermute | solution.py:27
  66.0 35.4 %collective-permute-start.15 = (bf16[32,4096]{1,0:T(8,128)(2,1)S(1)}, bf16[32,4096]{1,0:T(8,128)(2,1)S(1)}, u32[]{:S(2)}, u32[]{:S(2)}) collective-permute-start(bf16[32,4096]{1,0:T(8,128)(2,1)S(1)} %get-tuple-element.63.n0), channel_id=1, source_target_pairs={{0,2},{1,3},{2,0},{3,1},{4,6},{5,7},{6,4},{7,5},{8,10},{9,11},{10,... | collective-permute-start | bytes 786440 | tf_op jit(solution)/shard_map/ppermute | solution.py:27
  68.7 32.8 %collective-permute-start.16 = (bf16[32,4096]{1,0:T(8,128)(2,1)S(1)}, bf16[32,4096]{1,0:T(8,128)(2,1)S(1)}, u32[]{:S(2)}, u32[]{:S(2)}) collective-permute-start(bf16[32,4096]{1,0:T(8,128)(2,1)S(1)} %get-tuple-element.63.n0), channel_id=1, source_target_pairs={{0,3},{1,0},{2,1},{3,2},{4,7},{5,4},{6,5},{7,6},{8,11},{9,8},{10,9... | collective-permute-start | bytes 786440 | tf_op jit(solution)/shard_map/ppermute | solution.py:27
  101.4 1.6 copy-start.2
  103.0 1.6 copy-start.3
  104.6 1.6 copy-start.4
  107.3 9.2 %collective-permute-start.17 = (bf16[32,4096]{1,0:T(8,128)(2,1)S(1)}, bf16[32,4096]{1,0:T(8,128)(2,1)S(1)}, u32[]{:S(2)}, u32[]{:S(2)}) collective-permute-start(bf16[32,4096]{1,0:T(8,128)(2,1)S(1)} %get-tuple-element.65), channel_id=1, source_target_pairs={{0,3},{1,0},{2,1},{3,2},{4,7},{5,4},{6,5},{7,6},{8,11},{9,8},{10,9... | collective-permute-start | bytes 786440 | tf_op jit(solution)/shard_map/ppermute | solution.py:27
  107.5 10.7 %collective-permute-start.18 = (bf16[32,4096]{1,0:T(8,128)(2,1)S(1)}, bf16[32,4096]{1,0:T(8,128)(2,1)S(1)}, u32[]{:S(2)}, u32[]{:S(2)}) collective-permute-start(bf16[32,4096]{1,0:T(8,128)(2,1)S(1)} %get-tuple-element.66), channel_id=1, source_target_pairs={{0,2},{1,3},{2,0},{3,1},{4,6},{5,7},{6,4},{7,5},{8,10},{9,11},{10,... | collective-permute-start | bytes 786440 | tf_op jit(solution)/shard_map/ppermute | solution.py:27
  109.4 12.9 %collective-permute-start.19 = (bf16[32,4096]{1,0:T(8,128)(2,1)S(1)}, bf16[32,4096]{1,0:T(8,128)(2,1)S(1)}, u32[]{:S(2)}, u32[]{:S(2)}) collective-permute-start(bf16[32,4096]{1,0:T(8,128)(2,1)S(1)} %get-tuple-element.67), channel_id=1, source_target_pairs={{0,1},{1,2},{2,3},{3,0},{4,5},{5,6},{6,7},{7,4},{8,9},{9,10},{10,1... | collective-permute-start | bytes 786440 | tf_op jit(solution)/shard_map/ppermute | solution.py:27
  118.2 0.7 copy-start.6
  122.4 0.7 copy-start.8
  123.1 1.0 copy-start.7
  124.0 0.9 copy-start.9

commit v6 on v5

--- a/solution.py
+++ b/solution.py
@@ -76,7 +76,15 @@
         out[i] = ref[...]
 
 
-def route_kernel(ids_in, weight_in, target, mix):
+def tables_kernel(place, ids_hbm, weight_hbm, narrow_hbm, broad_hbm, target, mix, own, first, second, third, *scratch):
+    ids_in, weight_in, narrow, broad, sems = scratch
+    copies = []
+    for ref, held in ((narrow_hbm, narrow), (broad_hbm, broad), (ids_hbm, ids_in), (weight_hbm, weight_in)):
+        copies.append(pltpu.make_async_copy(ref, held, sems.at[len(copies)]))
+    for copy in copies:
+        copy.start()
+    for copy in copies:
+        copy.wait()
     ids = jnp.concatenate([ids_in[...]] * 4, axis=1)
     weight = jnp.concatenate([weight_in[...].astype(BF).astype(F32)] * 4, axis=1)
     expert = lax.broadcasted_iota(jnp.int32, (128, 128), 0)
@@ -96,7 +104,6 @@
     mix[...] = total.T.astype(BF)
 
 
-def bias_kernel(place, narrow, broad, own, first, second, third):
     z, y, c = place[0], place[1], place[2]
     here = z * 4 + y
 
@@ -160,14 +167,25 @@
         copy.wait()
 
 
+def fetch(pairs, sems):
+    copies = [pltpu.make_async_copy(ref, held, sems.at[i]) for i, (ref, held) in enumerate(pairs)]
+    for copy in copies:
+        copy.start()
+    return copies
+
+
 def silu(v):
     return v / (1.0 + jnp.exp(-v))
 
 
-def shared_kernel(n0, n1, n2, n3, gate, up, down, o0, o1, o2, o3):
+def shared_kernel(n0, n1, n2, n3, gate_hbm, up_hbm, down_hbm, o0, o1, o2, o3, gate, up, down, sems):
+    fetched = fetch(((gate_hbm, gate), (up_hbm, up), (down_hbm, down)), sems)
     x = jnp.concatenate([n0[...], n1[...], n2[...], n3[...]], axis=0)
+    fetched[0].wait()
     g = jnp.dot(x, gate[...], preferred_element_type=F32)
+    fetched[1].wait()
     u = jnp.dot(x, up[...], preferred_element_type=F32)
+    fetched[2].wait()
     hidden = (silu(g) * u).astype(BF)
     for at in range(0, 4096, 1024):
         part = jnp.dot(hidden, down[:, at : at + 1024], preferred_element_type=F32).astype(BF)
@@ -175,19 +193,9 @@
             out[:, at : at + 1024] = part[k * 32 : (k + 1) * 32]
 
 
-def expert_kernel(inbound, gate, up, down, stream, s0, s1, s2, s3, out, base, x, gate_up, down_copy, sems):
-    copies = []
-    for g in range(4):
-        for i, ref in enumerate((gate, up)):
-            part = pl.ds(g * 1024, 1024)
-            copies.append(pltpu.make_async_copy(ref.at[0, part], gate_up.at[i, part], sems.at[len(copies)]))
-    copies.append(pltpu.make_async_copy(down.at[0], down_copy, sems.at[len(copies)]))
-    for copy in copies:
-        copy.start()
-    total = stream[...]
-    for s in (s0, s1, s2, s3):
-        total = total + s[...].astype(F32)
-    base[...] = total
+def expert_kernel(inbound, gate_hbm, up_hbm, down_hbm, out, x, rows_out, gate, up, down, weight_sems, sems):
+    pairs = [(ref.at[0], held) for ref, held in ((gate_hbm, gate), (up_hbm, up), (down_hbm, down))]
+    fetched = fetch(pairs, weight_sems)
     i = lax.broadcasted_iota(jnp.int32, (256, 256), 0)
     j = lax.broadcasted_iota(jnp.int32, (256, 256), 1)
     order = (j == ((i % 64) // 2) * 8 + (i % 2) * 4 + i // 64).astype(F32).astype(BF)
@@ -196,29 +204,34 @@
         rows = jnp.dot(order, inbound[b * 256 : (b + 1) * 256, :], preferred_element_type=F32).astype(BF)
         for g in range(4):
             x[b * 64 : (b + 1) * 64, g * 1024 : (g + 1) * 1024] = rows[g * 64 : (g + 1) * 64]
-    gated, upped = jnp.zeros((256, 256), F32), jnp.zeros((256, 256), F32)
+    fetched[0].wait()
+    gated = jnp.dot(x[...], gate[...], preferred_element_type=F32)
+    fetched[1].wait()
+    upped = jnp.dot(x[...], up[...], preferred_element_type=F32)
+    fetched[2].wait()
+    hidden = (silu(gated) * upped).astype(BF)
+    for g in range(4):
+        part = jnp.dot(hidden, down[:, g * 1024 : (g + 1) * 1024], preferred_element_type=F32)
+        x[:, g * 1024 : (g + 1) * 1024] = part.astype(BF)
+    copies = []
+    for b in range(4):
+        rows = jnp.concatenate([x[b * 64 : (b + 1) * 64, g * 1024 : (g + 1) * 1024] for g in range(4)], axis=0)
+        part = pl.ds(b * 256, 256)
+        rows_out[part, :] = jnp.dot(back, rows, preferred_element_type=F32).astype(BF)
+        copies.append(pltpu.make_async_copy(rows_out.at[part], out.at[part], sems.at[b]))
+        copies[-1].start()
+    for copy in copies:
+        copy.wait()
+
+
+def combine_kernel(returned, mix, stream, s0, s1, s2, s3, out):
+    routed = jnp.dot(mix[...], returned[...], preferred_element_type=F32)
     for g in range(4):
         lo, hi = g * 1024, (g + 1) * 1024
-        copies[2 * g].wait()
-        gated = gated + jnp.dot(x[:, lo:hi], gate_up[0, lo:hi], preferred_element_type=F32)
-        copies[2 * g + 1].wait()
-        upped = upped + jnp.dot(x[:, lo:hi], gate_up[1, lo:hi], preferred_element_type=F32)
-    copies[-1].wait()
-    hidden = (silu(gated) * upped).astype(BF)
-    for g in range(4):
-        part = jnp.dot(hidden, down_copy[:, g * 1024 : (g + 1) * 1024], preferred_element_type=F32)
-        x[:, g * 1024 : (g + 1) * 1024] = part.astype(BF)
-    for b in range(4):
-        rows = jnp.concatenate([x[b * 64 : (b + 1) * 64, g * 1024 : (g + 1) * 1024] for g in range(4)], axis=0)
-        out[b * 256 : (b + 1) * 256, :] = jnp.dot(back, rows, preferred_element_type=F32).astype(BF)
-
-
-def combine_kernel(returned, mix, base, out):
-    for g in range(4):
-        lo, hi = g * 1024, (g + 1) * 1024
-        rows = mix[g * 32 : (g + 1) * 32, :]
-        routed = jnp.dot(rows, returned[...], preferred_element_type=F32)
-        out[:, lo:hi] = (base[:, lo:hi] + routed).astype(BF)
+        total = stream[:, lo:hi] + routed[g * 32 : (g + 1) * 32]
+        for s in (s0, s1, s2, s3):
+            total = total + s[:, lo:hi].astype(F32)
+        out[:, lo:hi] = total.astype(BF)
 
 
 def attend_kernel(counts, first, last, *refs):
@@ -375,21 +388,24 @@
         scratch=[pltpu.SemaphoreType.DMA((6,))],
         moved=0,
     )
-    target, mix = call(
-        route_kernel,
-        (route_ids.T, route_weight.T),
-        [shaped((4, 128), jnp.int32), shaped((128, 1024), BF)],
-    )
     place = jnp.stack([z, y, c, t])
     q_other = swap_core(q_own)
     line = {}
     for k in (2, 1, 3):
         line[k] = turn(own_kv, k, 0)
-    own_bias, bias_1, bias_2, bias_3 = call(
-        bias_kernel,
-        (place, gates_narrow.T, gates_broad.T),
-        [shaped((8, n), F32) for n in (128, 384, 1024, 512)],
+    target, mix, own_bias, bias_1, bias_2, bias_3 = call(
+        tables_kernel,
+        (place, route_ids.T, route_weight.T, gates_narrow.T, gates_broad.T),
+        [shaped((4, 128), jnp.int32), shaped((128, 1024), BF)] + [shaped((8, n), F32) for n in (128, 384, 1024, 512)],
         smem=(0,),
+        hbm=(1, 2, 3, 4),
+        scratch=[
+            pltpu.VMEM((4, 32), jnp.int32),
+            pltpu.VMEM((4, 32), F32),
+            pltpu.VMEM((4, 4096), F32),
+            pltpu.VMEM((2, 4096), F32),
+            pltpu.SemaphoreType.DMA((4,)),
+        ],
     )
     low, high = call(
         stack_kernel,
@@ -442,31 +458,42 @@
         shared_kernel,
         (normed, n1, n2, n3, shared_gate, shared_up, shared_down),
         [shaped((32, 4096), BF)] * 4,
+        hbm=(4, 5, 6),
+        scratch=[
+            pltpu.VMEM((4096, 256), BF),
+            pltpu.VMEM((4096, 256), BF),
+            pltpu.VMEM((256, 4096), BF),
+            pltpu.SemaphoreType.DMA((3,)),
+        ],
+        mib=20,
         flops=2 * 128 * 4096 * 768,
     )
     s1 = shift(s1, "tp", 3)
     s2 = shift(s2, "tp", 2)
     s3 = shift(s3, "tp", 1)
 
-    result, base = call(
+    (result,) = call(
         expert_kernel,
-        (inbound.reshape(1024, 1024), expert_gate, expert_up, expert_down, stream, s0, s1, s2, s3),
-        [shaped((1024, 1024), BF), shaped((32, 4096), F32)],
+        (inbound.reshape(1024, 1024), expert_gate, expert_up, expert_down),
+        [pltpu.HBM((1024, 1024), BF)],
         hbm=(1, 2, 3),
+        hbm_out=(0,),
         scratch=[
             pltpu.VMEM((256, 4096), BF),
-            pltpu.VMEM((2, 4096, 256), BF),
+            pltpu.VMEM((1024, 1024), BF),
+            pltpu.VMEM((4096, 256), BF),
+            pltpu.VMEM((4096, 256), BF),
             pltpu.VMEM((256, 4096), BF),
-            pltpu.SemaphoreType.DMA((9,)),
+            pltpu.SemaphoreType.DMA((3,)),
+            pltpu.SemaphoreType.DMA((4,)),
         ],
         mib=20,
-        moved=0,
         flops=2 * 256 * 4096 * 768,
     )
     returned = lax.all_to_all(result.reshape(128, 8, 1024), every, 0, 0, tiled=True)
     (out,) = call(
         combine_kernel,
-        (returned.reshape(1024, 1024), mix, base),
+        (returned.reshape(1024, 1024), mix, stream, s0, s1, s2, s3),
         [shaped((32, 4096), BF)],
         flops=2 * 128 * 1024 * 1024,
     )

time: 174 us -> 167 us (0.960)
  local copies, waits for them, and re-layouts: 11.1 us -> 3.32 us
  starting transfers between devices: 36.7 us -> 33.2 us
  Pallas kernels: 25.1 us -> 28.2 us
  waiting for transfers between devices: 59.9 us -> 62.1 us
    unnamed x30 -> x16, local copies, waits for them, and re-layouts: 11.1 us -> 3.32 us
    all_to_all x1, starting transfers between devices: 8.03 us -> 4.67 us  [local(): lax.all_to_all(result.reshape(128, 8, 1024), every, 0, 0, tiled=True)]
    pallas_call x9 -> x8, Pallas kernels: 16.2 us -> 19.3 us  [call(): pl.pallas_call(kernel, out_shape=shapes, in_specs=[SMEM if i in smem else...]
    ppermute x9, waiting for transfers between devices: 4.43 us -> 6.68 us  [turn(): return lax.ppermute(x, SP, pairs)]
  transfers between devices with their start and end apart: 21 -> 21, of which waited for: 10 -> 10; matrix products, arithmetic and copies ran while one was open for 0% -> 0% of each run, Pallas kernels for 5% -> 7%
where the time goes in v6:
time: 167 us; the launch traced here: 165 us
  waiting for transfers between devices  62.1 us (37%)
  blocking collectives  38.1 us (23%)
  starting transfers between devices  33.2 us (20%)
  Pallas kernels  28.2 us (17%)
  local copies, waits for them, and re-layouts  3.32 us (2%)
    ppermute x9, waiting for transfers between devices, shift(): return lax.ppermute(x, axis, [(i, (i + k) % 4) for i in range(4)])  53.5 us
    all_to_all x1, blocking collectives, local(): lax.all_to_all(outbound.reshape(128, 8, 1024), every, 0, 0, tiled=True)  38.1 us
    pallas_call x8, Pallas kernels, call(): pl.pallas_call(kernel, out_shape=shapes, in_specs=[SMEM if i in smem else...  19.3 us
    ppermute x9, starting transfers between devices, turn(): return lax.ppermute(x, SP, pairs)  15 us
    ppermute x9, starting transfers between devices, shift(): return lax.ppermute(x, axis, [(i, (i + k) % 4) for i in range(4)])  13.4 us
    pallas_call x3, Pallas kernels, attend(): pl.pallas_call(functools.partial(attend_kernel, counts, state is None, la...  8.92 us
    ppermute x9, waiting for transfers between devices, turn(): return lax.ppermute(x, SP, pairs)  6.68 us
    all_to_all x1, starting transfers between devices, local(): lax.all_to_all(result.reshape(128, 8, 1024), every, 0, 0, tiled=True)  4.67 us
  transfers between devices with their start and end apart: 21, of which 10 were waited for; matrix products, arithmetic and copies ran while one was open for 0% of the time, Pallas kernels for 7%

profile of v6, /device:TPU:0, one launch (start us, length us, event | category | flops | bytes accessed | tf_op | source)
XLA Modules:
  0.0 165.3 jit_solution(16162531348768741919)
XLA Ops:
  0.0 1.1 shard_map.190
  1.1 1.8 %collective-permute-start.1 = (bf16[128,768]{1,0:T(8,128)(2,1)S(1)}, bf16[128,768]{1,0:T(8,128)(2,1)S(1)}, u32[]{:S(2)}, u32[]{:S(2)}) collective-permute-start(bf16[128,768]{1,0:T(8,128)(2,1)S(1)} %get-tuple-element.37.a.refs_3_), channel_id=1, source_target_pairs={{0,8},{4,36},{8,16},{12,44},{16,24},{20,52},{24,0},{28,60},{32,40}... | collective-permute-start | bytes 589832 | tf_op jit(solution)/shard_map/ppermute | solution.py:41
  2.9 1.5 collective-permute-start.2
  4.4 2.1 %collective-permute-start.3 = (bf16[128,768]{1,0:T(8,128)(2,1)S(1)}, bf16[128,768]{1,0:T(8,128)(2,1)S(1)}, u32[]{:S(2)}, u32[]{:S(2)}) collective-permute-start(bf16[128,768]{1,0:T(8,128)(2,1)S(1)} %get-tuple-element.37.a.refs_3_), channel_id=1, source_target_pairs={{0,16},{4,68},{8,24},{12,76},{16,0},{20,84},{24,8},{28,92},{32,48}... | collective-permute-start | bytes 589832 | tf_op jit(solution)/shard_map/ppermute | solution.py:41
  6.5 0.1 pad_add_fusion.place
  6.6 2.0 %shard_map.191 = (s32[4,128]{1,0:T(4,128)S(1)}, bf16[128,1024]{1,0:T(8,128)(2,1)S(1)}, f32[8,128]{1,0:T(8,128)S(1)}, f32[8,384]{1,0:T(8,128)S(1)}, f32[8,1024]{1,0:T(8,128)S(1)}, /*index=5*/f32[8,512]{1,0:T(8,128)S(1)}) custom-call(s32[4]{0:T(128)S(1)} %pad_add_fusion.place, s32[4,32]{1,0:T(4,128)} %bitcast.20, f32[4,32]{1,0:T(4,128)} %bitcast.21, ...), custom_call_target="tpu_custom_call" | custom-call | bytes 2097152 | tf_op jit(solution)/shard_map/pallas_call | solution.py:48
  8.6 3.0 %collective-permute-done.3.d = bf16[128,768]{1,0:T(8,128)(2,1)S(1)} collective-permute-done((bf16[128,768]{1,0:T(8,128)(2,1)S(1)}, bf16[128,768]{1,0:T(8,128)(2,1)S(1)}, u32[]{:S(2)}, u32[]{:S(2)}) %collective-permute-start.3) | collective-permute-done | bytes 196640 | tf_op jit(solution)/shard_map/ppermute | solution.py:41
  11.6 0.1 shard_map.192
  11.7 2.1 %collective-permute-start.4 = (bf16[2,128,768]{2,1,0:T(8,128)(2,1)S(1)}, bf16[2,128,768]{2,1,0:T(8,128)(2,1)S(1)}, u32[]{:S(2)}, u32[]{:S(2)}) collective-permute-start(bf16[2,128,768]{2,1,0:T(8,128)(2,1)S(1)} %get-tuple-element.40.refs_5_), channel_id=1, source_target_pairs={{0,32},{4,12},{8,40},{12,20},{16,48},{20,28},{24,56},{28,4},{32,64... | collective-permute-start | bytes 1179656 | tf_op jit(solution)/shard_map/ppermute | solution.py:41
  13.8 2.2 %collective-permute-start.6 = (bf16[2,128,768]{2,1,0:T(8,128)(2,1)S(1)}, bf16[2,128,768]{2,1,0:T(8,128)(2,1)S(1)}, u32[]{:S(2)}, u32[]{:S(2)}) collective-permute-start(bf16[2,128,768]{2,1,0:T(8,128)(2,1)S(1)} %get-tuple-element.41.refs_6_), channel_id=1, source_target_pairs={{0,96},{4,28},{8,104},{12,4},{16,112},{20,12},{24,120},{28,20},{32... | collective-permute-start | bytes 1179656 | tf_op jit(solution)/shard_map/ppermute | solution.py:41
  16.0 1.9 %collective-permute-start.8 = (bf16[2,128,768]{2,1,0:T(8,128)(2,1)S(1)}, bf16[2,128,768]{2,1,0:T(8,128)(2,1)S(1)}, u32[]{:S(2)}, u32[]{:S(2)}) collective-permute-start(bf16[2,128,768]{2,1,0:T(8,128)(2,1)S(1)} %get-tuple-element.40.refs_5_), channel_id=1, source_target_pairs={{0,96},{4,28},{8,104},{12,4},{16,112},{20,12},{24,120},{28,20},{32... | collective-permute-start | bytes 1179656 | tf_op jit(solution)/shard_map/ppermute | solution.py:41
  17.9 0.1 collective-permute-start.9
  18.0 3.6 %collective-permute-done.4.refs_3_ = bf16[2,128,768]{2,1,0:T(8,128)(2,1)S(1)} collective-permute-done((bf16[2,128,768]{2,1,0:T(8,128)(2,1)S(1)}, bf16[2,128,768]{2,1,0:T(8,128)(2,1)S(1)}, u32[]{:S(2)}, u32[]{:S(2)}) %collective-permute-start.4) | collective-permute-done | bytes 393248 | tf_op jit(solution)/shard_map/ppermute | solution.py:41
  21.6 3.3 %collective-permute-start.7 = (bf16[2,128,768]{2,1,0:T(8,128)(2,1)S(1)}, bf16[2,128,768]{2,1,0:T(8,128)(2,1)S(1)}, u32[]{:S(2)}, u32[]{:S(2)}) collective-permute-start(bf16[2,128,768]{2,1,0:T(8,128)(2,1)S(1)} %collective-permute-done.6.refs_6_), channel_id=1, source_target_pairs={{0,96},{4,28},{8,104},{12,4},{16,112},{20,12},{24,120},{28,20},{32... | collective-permute-start | bytes 1179656 | tf_op jit(solution)/shard_map/ppermute | solution.py:41
  25.0 2.3 %shard_map.193 = (f32[1536,128]{1,0:T(8,128)S(1)}, f32[1536,128]{1,0:T(8,128)S(1)}, f32[1024,128]{1,0:T(8,128)S(1)}, f32[512,256]{1,0:T(8,128)S(1)}) custom-call(bf16[128,1024]{1,0:T(8,128)(2,1)S(1)} %get-tuple-element.36.refs_0_, bf16[128,1024]{1,0:T(8,128)(2,1)S(1)} %collective-permute-done.refs_1_, s32[1]{0:T(128)} %bitcast.2.refs_2_, ...), custom_call_target="tpu_custom_call" | custom-call | flops 536870912 | bytes 4194304 | tf_op jit(solution)/shard_map/pallas_call | solution.py:347
  27.2 0.0 copy-start
  27.3 0.0 copy-start.1
  27.3 4.1 %shard_map.194 = (f32[1536,128]{1,0:T(8,128)S(1)}, f32[1536,128]{1,0:T(8,128)S(1)}, f32[1024,128]{1,0:T(8,128)S(1)}, f32[512,256]{1,0:T(8,128)S(1)}) custom-call(bf16[128,1024]{1,0:T(8,128)(2,1)S(1)} %get-tuple-element.36.refs_0_, bf16[128,1024]{1,0:T(8,128)(2,1)S(1)} %collective-permute-done.refs_1_, s32[1]{0:T(128)} %bitcast.2.refs_2_, ...), custom_call_target="tpu_custom_call" | custom-call | flops 1073741824 | bytes 4194304 | tf_op jit(solution)/shard_map/pallas_call | solution.py:347
  31.4 2.6 %shard_map.195 = (f32[128,1152]{1,0:T(8,128)S(1)}, f32[128,1152]{1,0:T(8,128)S(1)}) custom-call(bf16[128,1024]{1,0:T(8,128)(2,1)S(1)} %get-tuple-element.36.refs_0_, bf16[128,1024]{1,0:T(8,128)(2,1)S(1)} %collective-permute-done.refs_1_, s32[1]{0:T(128)} %bitcast.2.refs_2_, bf16[2,128,768]{2,1,0:T(8,128)(2,1)S(1)} %collective-permute-done.5.refs_3_, ...), custom_call_target="tpu_custom_call" | custom-call | flops 536870912 | bytes 4194304 | tf_op jit(solution)/shard_map/pallas_call | solution.py:347
  34.0 0.1 collective-permute-start.10
  34.0 2.0 %collective-permute-done.10.other = f32[128,1152]{1,0:T(8,128)S(1)} collective-permute-done((f32[128,1152]{1,0:T(8,128)S(1)}, f32[128,1152]{1,0:T(8,128)S(1)}, u32[]{:S(2)}, u32[]{:S(2)}) %collective-permute-start.10) | collective-permute-done | bytes 589856 | tf_op jit(solution)/shard_map/ppermute | solution.py:31
  36.1 2.1 %shard_map.196 = (bf16[32,4096]{1,0:T(8,128)(2,1)S(1)}, bf16[32,4096]{1,0:T(8,128)(2,1)S(1)}, bf16[32,4096]{1,0:T(8,128)(2,1)S(1)}, bf16[32,4096]{1,0:T(8,128)(2,1)S(1)}) custom-call(s32[4]{0:T(128)S(1)} %pad_add_fusion.place, f32[128,1152]{1,0:T(8,128)S(1)} %get-tuple-element.53.own, f32[128,1152]{1,0:T(8,128)S(1)} %collective-permute-done.10.other, ...), custom_call_target="tpu_custom_call" | custom-call | flops 1073741824 | bytes 2097152 | tf_op jit(solution)/shard_map/pallas_call | solution.py:48
  38.2 1.6 collective-permute-start.11
  39.7 2.7 %collective-permute-start.12 = (bf16[32,4096]{1,0:T(8,128)(2,1)S(1)}, bf16[32,4096]{1,0:T(8,128)(2,1)S(1)}, u32[]{:S(2)}, u32[]{:S(2)}) collective-permute-start(bf16[32,4096]{1,0:T(8,128)(2,1)S(1)} %get-tuple-element.57), channel_id=1, source_target_pairs={{0,2},{1,3},{2,0},{3,1},{4,6},{5,7},{6,4},{7,5},{8,10},{9,11},{10,... | collective-permute-start | bytes 786440 | tf_op jit(solution)/shard_map/ppermute | solution.py:27
  42.4 1.4 collective-permute-start.13
  43.9 3.9 %collective-permute-done.11.p1 = bf16[32,4096]{1,0:T(8,128)(2,1)S(1)} collective-permute-done((bf16[32,4096]{1,0:T(8,128)(2,1)S(1)}, bf16[32,4096]{1,0:T(8,128)(2,1)S(1)}, u32[]{:S(2)}, u32[]{:S(2)}) %collective-permute-start.11) | collective-permute-done | bytes 262176 | tf_op jit(solution)/shard_map/ppermute | solution.py:27
  47.8 6.6 %collective-permute-done.12.p2 = bf16[32,4096]{1,0:T(8,128)(2,1)S(1)} collective-permute-done((bf16[32,4096]{1,0:T(8,128)(2,1)S(1)}, bf16[32,4096]{1,0:T(8,128)(2,1)S(1)}, u32[]{:S(2)}, u32[]{:S(2)}) %collective-permute-start.12) | collective-permute-done | bytes 262176 | tf_op jit(solution)/shard_map/ppermute | solution.py:27
  54.4 2.6 %shard_map.197 = (f32[32,4096]{1,0:T(8,128)S(1)}, bf16[32,4096]{1,0:T(8,128)(2,1)S(1)}, bf16[1024,1024]{1,0:T(8,128)(2,1)}) custom-call(s32[4]{0:T(128)S(1)} %pad_add_fusion.place, bf16[32,4096]{1,0:T(8,128)(2,1)S(1)} %get-tuple-element.55.p0, bf16[32,4096]{1,0:T(8,128)(2,1)S(1)} %collective-permute-done.11.p1, ...), custom_call_target="tpu_custom_call" | custom-call | flops 268435456 | bytes 2097152 | tf_op jit(solution)/shard_map/pallas_call | solution.py:48
  57.0 38.1 %all_to_all.10 = bf16[128,8,1024]{2,1,0:T(8,128)(2,1)S(1)} all-to-all(bf16[128,8,1024]{2,1,0:T(8,128)(2,1)} %bitcast.17), channel_id=1, replica_groups=mesh['z'=4,'y'=4,'c'=2,'tp'=4] {'z','y','c','tp'}, dimensions={0} | all-to-all | bytes 4194304 | tf_op jit(solution)/shard_map/all_to_all | solution.py:452
  95.0 6.8 %shard_map.198 = bf16[1024,1024]{1,0:T(8,128)(2,1)} custom-call(bf16[1024,1024]{1,0:T(8,128)(2,1)S(1)} %bitcast.13, bf16[1,4096,256]{2,1,0:T(8,128)(2,1)} %gate_hbm.2, bf16[1,4096,256]{2,1,0:T(8,128)(2,1)} %up_hbm.2, bf16[1,256,4096]{2,1,0:T(8,128)(2,1)} %down_hbm.2), custom_call_target="tpu_custom_call" | custom-call | flops 1610612736 | bytes 2097152 | tf_op jit(solution)/shard_map/pallas_call | solution.py:48
  101.9 4.7 %all-to-all-start.1 = ((bf16[128,8,1024]{2,1,0:T(8,128)(2,1)}), bf16[128,8,1024]{2,1,0:T(8,128)(2,1)S(1)}, u32[]{:S(2)}, u32[]{:S(2)}) async-start(bf16[128,8,1024]{2,1,0:T(8,128)(2,1)} %bitcast.16), calls=%async_computation.1 | async-start | bytes 4194304 | tf_op jit(solution)/shard_map/all_to_all | solution.py:493
  106.6 0.9 collective-permute-start.14
  107.5 2.7 %collective-permute-start.15 = (bf16[32,4096]{1,0:T(8,128)(2,1)S(1)}, bf16[32,4096]{1,0:T(8,128)(2,1)S(1)}, u32[]{:S(2)}, u32[]{:S(2)}) collective-permute-start(bf16[32,4096]{1,0:T(8,128)(2,1)S(1)} %get-tuple-element.62.n0), channel_id=1, source_target_pairs={{0,2},{1,3},{2,0},{3,1},{4,6},{5,7},{6,4},{7,5},{8,10},{9,11},{10,... | collective-permute-start | bytes 786440 | tf_op jit(solution)/shard_map/ppermute | solution.py:27
  110.2 1.4 collective-permute-start.16
  111.6 25.7 %collective-permute-done.14.n1 = bf16[32,4096]{1,0:T(8,128)(2,1)S(1)} collective-permute-done((bf16[32,4096]{1,0:T(8,128)(2,1)S(1)}, bf16[32,4096]{1,0:T(8,128)(2,1)S(1)}, u32[]{:S(2)}, u32[]{:S(2)}) %collective-permute-start.14) | collective-permute-done | bytes 262176 | tf_op jit(solution)/shard_map/ppermute | solution.py:27
  137.3 5.6 %collective-permute-done.15.n2 = bf16[32,4096]{1,0:T(8,128)(2,1)S(1)} collective-permute-done((bf16[32,4096]{1,0:T(8,128)(2,1)S(1)}, bf16[32,4096]{1,0:T(8,128)(2,1)S(1)}, u32[]{:S(2)}, u32[]{:S(2)}) %collective-permute-start.15) | collective-permute-done | bytes 262176 | tf_op jit(solution)/shard_map/ppermute | solution.py:27
  142.9 3.4 %shard_map.199 = (bf16[32,4096]{1,0:T(8,128)(2,1)S(1)}, bf16[32,4096]{1,0:T(8,128)(2,1)S(1)}, bf16[32,4096]{1,0:T(8,128)(2,1)S(1)}, bf16[32,4096]{1,0:T(8,128)(2,1)S(1)}) custom-call(bf16[32,4096]{1,0:T(8,128)(2,1)S(1)} %get-tuple-element.62.n0, bf16[32,4096]{1,0:T(8,128)(2,1)S(1)} %collective-permute-done.14.n1, ...), custom_call_target="tpu_custom_call" | custom-call | flops 805306368 | bytes 2097152 | tf_op jit(solution)/shard_map/pallas_call | solution.py:48
  146.4 0.1 collective-permute-start.17
  146.5 2.0 %collective-permute-start.18 = (bf16[32,4096]{1,0:T(8,128)(2,1)S(1)}, bf16[32,4096]{1,0:T(8,128)(2,1)S(1)}, u32[]{:S(2)}, u32[]{:S(2)}) collective-permute-start(bf16[32,4096]{1,0:T(8,128)(2,1)S(1)} %get-tuple-element.65), channel_id=1, source_target_pairs={{0,2},{1,3},{2,0},{3,1},{4,6},{5,7},{6,4},{7,5},{8,10},{9,11},{10,... | collective-permute-start | bytes 786440 | tf_op jit(solution)/shard_map/ppermute | solution.py:27
  148.5 0.6 collective-permute-start.19
  149.1 6.6 %collective-permute-done.17.s1 = bf16[32,4096]{1,0:T(8,128)(2,1)S(1)} collective-permute-done((bf16[32,4096]{1,0:T(8,128)(2,1)S(1)}, bf16[32,4096]{1,0:T(8,128)(2,1)S(1)}, u32[]{:S(2)}, u32[]{:S(2)}) %collective-permute-start.17) | collective-permute-done | bytes 262176 | tf_op jit(solution)/shard_map/ppermute | solution.py:27
  155.6 1.6 collective-permute-done.18.s2
  157.3 0.7 copy-done.3
  158.0 3.4 %collective-permute-done.19.s3 = bf16[32,4096]{1,0:T(8,128)(2,1)S(1)} collective-permute-done((bf16[32,4096]{1,0:T(8,128)(2,1)S(1)}, bf16[32,4096]{1,0:T(8,128)(2,1)S(1)}, u32[]{:S(2)}, u32[]{:S(2)}) %collective-permute-start.19) | collective-permute-done | bytes 262176 | tf_op jit(solution)/shard_map/ppermute | solution.py:27
  161.4 0.7 copy-done.5
  162.1 0.9 copy-done.4
  163.1 0.9 copy-done.6
  164.0 1.2 shard_map.200
  (23 shorter events, 0.1 us)
Async XLA Ops:
  1.1 7.4 %collective-permute-start.1 = (bf16[128,768]{1,0:T(8,128)(2,1)S(1)}, bf16[128,768]{1,0:T(8,128)(2,1)S(1)}, u32[]{:S(2)}, u32[]{:S(2)}) collective-permute-start(bf16[128,768]{1,0:T(8,128)(2,1)S(1)} %get-tuple-element.37.a.refs_3_), channel_id=1, source_target_pairs={{0,8},{4,36},{8,16},{12,44},{16,24},{20,52},{24,0},{28,60},{32,40}... | collective-permute-start | bytes 589832 | tf_op jit(solution)/shard_map/ppermute | solution.py:41
  2.9 5.7 %collective-permute-start.2 = (bf16[128,768]{1,0:T(8,128)(2,1)S(1)}, bf16[128,768]{1,0:T(8,128)(2,1)S(1)}, u32[]{:S(2)}, u32[]{:S(2)}) collective-permute-start(bf16[128,768]{1,0:T(8,128)(2,1)S(1)} %get-tuple-element.37.a.refs_3_), channel_id=1, source_target_pairs={{0,24},{4,100},{8,0},{12,108},{16,8},{20,116},{24,16},{28,124},{32... | collective-permute-start | bytes 589832 | tf_op jit(solution)/shard_map/ppermute | solution.py:41
  4.4 7.2 %collective-permute-start.3 = (bf16[128,768]{1,0:T(8,128)(2,1)S(1)}, bf16[128,768]{1,0:T(8,128)(2,1)S(1)}, u32[]{:S(2)}, u32[]{:S(2)}) collective-permute-start(bf16[128,768]{1,0:T(8,128)(2,1)S(1)} %get-tuple-element.37.a.refs_3_), channel_id=1, source_target_pairs={{0,16},{4,68},{8,24},{12,76},{16,0},{20,84},{24,8},{28,92},{32,48}... | collective-permute-start | bytes 589832 | tf_op jit(solution)/shard_map/ppermute | solution.py:41
  11.7 10.0 %collective-permute-start.4 = (bf16[2,128,768]{2,1,0:T(8,128)(2,1)S(1)}, bf16[2,128,768]{2,1,0:T(8,128)(2,1)S(1)}, u32[]{:S(2)}, u32[]{:S(2)}) collective-permute-start(bf16[2,128,768]{2,1,0:T(8,128)(2,1)S(1)} %get-tuple-element.40.refs_5_), channel_id=1, source_target_pairs={{0,32},{4,12},{8,40},{12,20},{16,48},{20,28},{24,56},{28,4},{32,64... | collective-permute-start | bytes 1179656 | tf_op jit(solution)/shard_map/ppermute | solution.py:41
  13.8 7.9 %collective-permute-start.6 = (bf16[2,128,768]{2,1,0:T(8,128)(2,1)S(1)}, bf16[2,128,768]{2,1,0:T(8,128)(2,1)S(1)}, u32[]{:S(2)}, u32[]{:S(2)}) collective-permute-start(bf16[2,128,768]{2,1,0:T(8,128)(2,1)S(1)} %get-tuple-element.41.refs_6_), channel_id=1, source_target_pairs={{0,96},{4,28},{8,104},{12,4},{16,112},{20,12},{24,120},{28,20},{32... | collective-permute-start | bytes 1179656 | tf_op jit(solution)/shard_map/ppermute | solution.py:41
  16.0 11.3 %collective-permute-start.8 = (bf16[2,128,768]{2,1,0:T(8,128)(2,1)S(1)}, bf16[2,128,768]{2,1,0:T(8,128)(2,1)S(1)}, u32[]{:S(2)}, u32[]{:S(2)}) collective-permute-start(bf16[2,128,768]{2,1,0:T(8,128)(2,1)S(1)} %get-tuple-element.40.refs_5_), channel_id=1, source_target_pairs={{0,96},{4,28},{8,104},{12,4},{16,112},{20,12},{24,120},{28,20},{32... | collective-permute-start | bytes 1179656 | tf_op jit(solution)/shard_map/ppermute | solution.py:41
  17.9 9.3 %collective-permute-start.9 = (bf16[2,128,768]{2,1,0:T(8,128)(2,1)S(1)}, bf16[2,128,768]{2,1,0:T(8,128)(2,1)S(1)}, u32[]{:S(2)}, u32[]{:S(2)}) collective-permute-start(bf16[2,128,768]{2,1,0:T(8,128)(2,1)S(1)} %get-tuple-element.41.refs_6_), channel_id=1, source_target_pairs={{0,32},{4,12},{8,40},{12,20},{16,48},{20,28},{24,56},{28,4},{32,64... | collective-permute-start | bytes 1179656 | tf_op jit(solution)/shard_map/ppermute | solution.py:41
  18.0 7.0 %collective-permute-start = (bf16[128,1024]{1,0:T(8,128)(2,1)S(1)}, bf16[128,1024]{1,0:T(8,128)(2,1)S(1)}, u32[]{:S(2)}, u32[]{:S(2)}) collective-permute-start(bf16[128,1024]{1,0:T(8,128)(2,1)S(1)} %get-tuple-element.36.refs_0_), channel_id=1, source_target_pairs={{0,4},{4,0},{1,5},{5,1},{2,6},{6,2},{3,7},{7,3},{8,12},{12,8},{9,1... | collective-permute-start | bytes 786440 | tf_op jit(solution)/shard_map/ppermute | solution.py:31
  21.6 9.7 %collective-permute-start.5 = (bf16[2,128,768]{2,1,0:T(8,128)(2,1)S(1)}, bf16[2,128,768]{2,1,0:T(8,128)(2,1)S(1)}, u32[]{:S(2)}, u32[]{:S(2)}) collective-permute-start(bf16[2,128,768]{2,1,0:T(8,128)(2,1)S(1)} %collective-permute-done.4.refs_3_), channel_id=1, source_target_pairs={{0,32},{4,12},{8,40},{12,20},{16,48},{20,28},{24,56},{28,4},{32,64... | collective-permute-start | bytes 1179656 | tf_op jit(solution)/shard_map/ppermute | solution.py:41
  21.6 9.7 %collective-permute-start.7 = (bf16[2,128,768]{2,1,0:T(8,128)(2,1)S(1)}, bf16[2,128,768]{2,1,0:T(8,128)(2,1)S(1)}, u32[]{:S(2)}, u32[]{:S(2)}) collective-permute-start(bf16[2,128,768]{2,1,0:T(8,128)(2,1)S(1)} %collective-permute-done.6.refs_6_), channel_id=1, source_target_pairs={{0,96},{4,28},{8,104},{12,4},{16,112},{20,12},{24,120},{28,20},{32... | collective-permute-start | bytes 1179656 | tf_op jit(solution)/shard_map/ppermute | solution.py:41
  27.2 8.8 %copy-start = (bf16[512,4096]{1,0:T(8,128)(2,1)S(1)}, bf16[512,4096]{1,0:T(8,128)(2,1)}, u32[]{:S(2)}) copy-start(bf16[512,4096]{1,0:T(8,128)(2,1)} %narrow.1) | copy-start | bytes 12582916
  27.3 8.8 %copy-start.1 = (bf16[512,4096]{1,0:T(8,128)(2,1)S(1)}, bf16[512,4096]{1,0:T(8,128)(2,1)}, u32[]{:S(2)}) copy-start(bf16[512,4096]{1,0:T(8,128)(2,1)} %broad.1) | copy-start | bytes 12582916
  34.0 2.1 %collective-permute-start.10 = (f32[128,1152]{1,0:T(8,128)S(1)}, f32[128,1152]{1,0:T(8,128)S(1)}, u32[]{:S(2)}, u32[]{:S(2)}) collective-permute-start(f32[128,1152]{1,0:T(8,128)S(1)} %get-tuple-element.54), channel_id=1, source_target_pairs={{0,4},{4,0},{1,5},{5,1},{2,6},{6,2},{3,7},{7,3},{8,12},{12,8},{9,1... | collective-permute-start | bytes 1769480 | tf_op jit(solution)/shard_map/ppermute | solution.py:31
  36.0 18.3 %copy-start.2 = (bf16[128,4096]{1,0:T(8,128)(2,1)S(1)}, bf16[128,4096]{1,0:T(8,128)(2,1)}, u32[]{:S(2)}) copy-start(bf16[128,4096]{1,0:T(8,128)(2,1)} %residual.1) | copy-start | bytes 3145732
  36.0 18.3 %copy-start.7 = (f32[4096]{0:T(1024)S(1)}, f32[4096]{0:T(1024)}, u32[]{:S(2)}) copy-start(f32[4096]{0:T(1024)} %param.31) | copy-start | bytes 49156
  38.2 9.6 %collective-permute-start.11 = (bf16[32,4096]{1,0:T(8,128)(2,1)S(1)}, bf16[32,4096]{1,0:T(8,128)(2,1)S(1)}, u32[]{:S(2)}, u32[]{:S(2)}) collective-permute-start(bf16[32,4096]{1,0:T(8,128)(2,1)S(1)} %get-tuple-element.56), channel_id=1, source_target_pairs={{0,1},{1,2},{2,3},{3,0},{4,5},{5,6},{6,7},{7,4},{8,9},{9,10},{10,1... | collective-permute-start | bytes 786440 | tf_op jit(solution)/shard_map/ppermute | solution.py:27
  39.7 14.7 %collective-permute-start.12 = (bf16[32,4096]{1,0:T(8,128)(2,1)S(1)}, bf16[32,4096]{1,0:T(8,128)(2,1)S(1)}, u32[]{:S(2)}, u32[]{:S(2)}) collective-permute-start(bf16[32,4096]{1,0:T(8,128)(2,1)S(1)} %get-tuple-element.57), channel_id=1, source_target_pairs={{0,2},{1,3},{2,0},{3,1},{4,6},{5,7},{6,4},{7,5},{8,10},{9,11},{10,... | collective-permute-start | bytes 786440 | tf_op jit(solution)/shard_map/ppermute | solution.py:27
  42.4 11.9 %collective-permute-start.13 = (bf16[32,4096]{1,0:T(8,128)(2,1)S(1)}, bf16[32,4096]{1,0:T(8,128)(2,1)S(1)}, u32[]{:S(2)}, u32[]{:S(2)}) collective-permute-start(bf16[32,4096]{1,0:T(8,128)(2,1)S(1)} %get-tuple-element.58), channel_id=1, source_target_pairs={{0,3},{1,0},{2,1},{3,2},{4,7},{5,4},{6,5},{7,6},{8,11},{9,8},{10,9... | collective-permute-start | bytes 786440 | tf_op jit(solution)/shard_map/ppermute | solution.py:27
  101.9 60.2 %all-to-all-start.1 = ((bf16[128,8,1024]{2,1,0:T(8,128)(2,1)}), bf16[128,8,1024]{2,1,0:T(8,128)(2,1)S(1)}, u32[]{:S(2)}, u32[]{:S(2)}) async-start(bf16[128,8,1024]{2,1,0:T(8,128)(2,1)} %bitcast.16), calls=%async_computation.1 | async-start | bytes 4194304 | tf_op jit(solution)/shard_map/all_to_all | solution.py:493
  106.6 30.8 %collective-permute-start.14 = (bf16[32,4096]{1,0:T(8,128)(2,1)S(1)}, bf16[32,4096]{1,0:T(8,128)(2,1)S(1)}, u32[]{:S(2)}, u32[]{:S(2)}) collective-permute-start(bf16[32,4096]{1,0:T(8,128)(2,1)S(1)} %get-tuple-element.62.n0), channel_id=1, source_target_pairs={{0,1},{1,2},{2,3},{3,0},{4,5},{5,6},{6,7},{7,4},{8,9},{9,10},{10,1... | collective-permute-start | bytes 786440 | tf_op jit(solution)/shard_map/ppermute | solution.py:27
  107.5 35.5 %collective-permute-start.15 = (bf16[32,4096]{1,0:T(8,128)(2,1)S(1)}, bf16[32,4096]{1,0:T(8,128)(2,1)S(1)}, u32[]{:S(2)}, u32[]{:S(2)}) collective-permute-start(bf16[32,4096]{1,0:T(8,128)(2,1)S(1)} %get-tuple-element.62.n0), channel_id=1, source_target_pairs={{0,2},{1,3},{2,0},{3,1},{4,6},{5,7},{6,4},{7,5},{8,10},{9,11},{10,... | collective-permute-start | bytes 786440 | tf_op jit(solution)/shard_map/ppermute | solution.py:27
  110.2 32.8 %collective-permute-start.16 = (bf16[32,4096]{1,0:T(8,128)(2,1)S(1)}, bf16[32,4096]{1,0:T(8,128)(2,1)S(1)}, u32[]{:S(2)}, u32[]{:S(2)}) collective-permute-start(bf16[32,4096]{1,0:T(8,128)(2,1)S(1)} %get-tuple-element.62.n0), channel_id=1, source_target_pairs={{0,3},{1,0},{2,1},{3,2},{4,7},{5,4},{6,5},{7,6},{8,11},{9,8},{10,9... | collective-permute-start | bytes 786440 | tf_op jit(solution)/shard_map/ppermute | solution.py:27
  146.4 9.2 %collective-permute-start.17 = (bf16[32,4096]{1,0:T(8,128)(2,1)S(1)}, bf16[32,4096]{1,0:T(8,128)(2,1)S(1)}, u32[]{:S(2)}, u32[]{:S(2)}) collective-permute-start(bf16[32,4096]{1,0:T(8,128)(2,1)S(1)} %get-tuple-element.64), channel_id=1, source_target_pairs={{0,3},{1,0},{2,1},{3,2},{4,7},{5,4},{6,5},{7,6},{8,11},{9,8},{10,9... | collective-permute-start | bytes 786440 | tf_op jit(solution)/shard_map/ppermute | solution.py:27
  146.5 10.8 %collective-permute-start.18 = (bf16[32,4096]{1,0:T(8,128)(2,1)S(1)}, bf16[32,4096]{1,0:T(8,128)(2,1)S(1)}, u32[]{:S(2)}, u32[]{:S(2)}) collective-permute-start(bf16[32,4096]{1,0:T(8,128)(2,1)S(1)} %get-tuple-element.65), channel_id=1, source_target_pairs={{0,2},{1,3},{2,0},{3,1},{4,6},{5,7},{6,4},{7,5},{8,10},{9,11},{10,... | collective-permute-start | bytes 786440 | tf_op jit(solution)/shard_map/ppermute | solution.py:27
  148.5 12.9 %collective-permute-start.19 = (bf16[32,4096]{1,0:T(8,128)(2,1)S(1)}, bf16[32,4096]{1,0:T(8,128)(2,1)S(1)}, u32[]{:S(2)}, u32[]{:S(2)}) collective-permute-start(bf16[32,4096]{1,0:T(8,128)(2,1)S(1)} %get-tuple-element.66), channel_id=1, source_target_pairs={{0,1},{1,2},{2,3},{3,0},{4,5},{5,6},{6,7},{7,4},{8,9},{9,10},{10,1... | collective-permute-start | bytes 786440 | tf_op jit(solution)/shard_map/ppermute | solution.py:27
  157.3 0.7 copy-start.3
  161.4 0.7 copy-start.5
  162.1 1.0 copy-start.4
  163.1 0.9 copy-start.6

commit v7 on v6

--- a/solution.py
+++ b/solution.py
@@ -194,8 +194,11 @@
 
 
 def expert_kernel(inbound, gate_hbm, up_hbm, down_hbm, out, x, rows_out, gate, up, down, weight_sems, sems):
-    pairs = [(ref.at[0], held) for ref, held in ((gate_hbm, gate), (up_hbm, up), (down_hbm, down))]
-    fetched = fetch(pairs, weight_sems)
+    pairs = []
+    for g in range(4):
+        part = pl.ds(g * 1024, 1024)
+        pairs += [(ref.at[0, part], held.at[part]) for ref, held in ((gate_hbm, gate), (up_hbm, up))]
+    fetched = fetch(pairs + [(down_hbm.at[0], down)], weight_sems)
     i = lax.broadcasted_iota(jnp.int32, (256, 256), 0)
     j = lax.broadcasted_iota(jnp.int32, (256, 256), 1)
     order = (j == ((i % 64) // 2) * 8 + (i % 2) * 4 + i // 64).astype(F32).astype(BF)
@@ -204,11 +207,14 @@
         rows = jnp.dot(order, inbound[b * 256 : (b + 1) * 256, :], preferred_element_type=F32).astype(BF)
         for g in range(4):
             x[b * 64 : (b + 1) * 64, g * 1024 : (g + 1) * 1024] = rows[g * 64 : (g + 1) * 64]
-    fetched[0].wait()
-    gated = jnp.dot(x[...], gate[...], preferred_element_type=F32)
-    fetched[1].wait()
-    upped = jnp.dot(x[...], up[...], preferred_element_type=F32)
-    fetched[2].wait()
+    gated, upped = jnp.zeros((256, 256), F32), jnp.zeros((256, 256), F32)
+    for g in range(4):
+        lo, hi = g * 1024, (g + 1) * 1024
+        fetched[2 * g].wait()
+        fetched[2 * g + 1].wait()
+        gated = gated + jnp.dot(x[:, lo:hi], gate[lo:hi], preferred_element_type=F32)
+        upped = upped + jnp.dot(x[:, lo:hi], up[lo:hi], preferred_element_type=F32)
+    fetched[8].wait()
     hidden = (silu(gated) * upped).astype(BF)
     for g in range(4):
         part = jnp.dot(hidden, down[:, g * 1024 : (g + 1) * 1024], preferred_element_type=F32)
@@ -260,7 +266,8 @@
         return value.reshape(-1, hi - lo)
 
     results = {}
-    for group, size, heads, lo in (("n", NARROW_SIZE, 4, 0), ("b", BROAD_SIZE, 2, 256)):
+    for group, size, heads, lo, per in (("n", NARROW_SIZE, 4, 0, 2 if last else 4), ("b", BROAD_SIZE, 2, 256, 2)):
+        count = per * 128
         scale = size**-0.5 * LOG2E
         base = 0 if group == "n" else 4
         row_base = 0 if group == "n" else 1024
@@ -270,29 +277,29 @@
             v = jnp.concatenate([keys(r, lo + size, lo + 2 * size) for r in arrays], axis=0)
             loaded.append((k, v, bias, own_block))
         for side, q_ref in ((0, q_own), (1, q_other)):
-            for h0 in range(0, heads, 2):
+            for h0 in range(0, heads, per):
                 col = (0 if group == "n" else 512) + h0 * size
-                q = jnp.concatenate([q_ref[:, col + i * size : col + (i + 1) * size] for i in range(2)], axis=0)
+                q = jnp.concatenate([q_ref[:, col + i * size : col + (i + 1) * size] for i in range(per)], axis=0)
                 rows = row_base + side * heads * 128 + h0 * 128
                 arow = rows - row_base
                 scores = []
                 for k, v, bias, own_block in loaded:
                     s = lax.dot_general(q, k, (((1,), (1,)), ((), ())), preferred_element_type=F32) * scale
                     n = k.shape[0]
-                    b = bias[base + h0 : base + h0 + 2, :]
-                    s = (s.reshape(2, 128, n) + b[:, None, :]).reshape(256, n)
+                    b = bias[base + h0 : base + h0 + per, :]
+                    s = (s.reshape(per, 128, n) + b[:, None, :]).reshape(count, n)
                     if own_block:
-                        qi = lax.broadcasted_iota(jnp.int32, (256, n), 0) % 128
-                        ki = lax.broadcasted_iota(jnp.int32, (256, n), 1)
+                        qi = lax.broadcasted_iota(jnp.int32, (count, n), 0) % 128
+                        ki = lax.broadcasted_iota(jnp.int32, (count, n), 1)
                         offset = 0 if side == 0 else 128 * (1 - 2 * core[0])
                         s = jnp.where(ki <= qi + offset, s, MASKED)
                     scores.append(s)
                 m = functools.reduce(jnp.maximum, [jnp.max(s, axis=1, keepdims=True) for s in scores])
                 if not first:
-                    m_old = m_in[pl.ds(rows, 256), :][:, :1]
+                    m_old = m_in[pl.ds(rows, count), :][:, :1]
                     m = jnp.maximum(m, m_old)
-                l = jnp.zeros((256, 1), F32)
-                acc = jnp.zeros((256, size), F32)
+                l = jnp.zeros((count, 1), F32)
+                acc = jnp.zeros((count, size), F32)
                 for s, (k, v, bias, own_block) in zip(scores, loaded):
                     p = jnp.exp2(s - m)
                     l = l + jnp.sum(p, axis=1, keepdims=True)
@@ -300,20 +307,20 @@
                 if not first:
                     a_in = an_in if group == "n" else ab_in
                     factor = jnp.exp2(m_old - m)
-                    l = l + l_in[pl.ds(rows, 256), :][:, :1] * factor
-                    acc = acc + a_in[pl.ds(arow, 256), :] * factor
+                    l = l + l_in[pl.ds(rows, count), :][:, :1] * factor
+                    acc = acc + a_in[pl.ds(arow, count), :] * factor
                 if last:
                     out = own_out if side == 0 else send_out
                     o = acc / l
                     lse = m + jnp.log2(l)
-                    for i in range(2):
+                    for i in range(per):
                         out[:, col + i * size : col + (i + 1) * size] = o[i * 128 : (i + 1) * 128]
                         results[(side, base + h0 + i)] = lse[i * 128 : (i + 1) * 128]
                 else:
                     a_out = an_out if group == "n" else ab_out
-                    m_out[pl.ds(rows, 256), :] = jnp.broadcast_to(m, (256, 128))
-                    l_out[pl.ds(rows, 256), :] = jnp.broadcast_to(l, (256, 128))
-                    a_out[pl.ds(arow, 256), :] = acc
+                    m_out[pl.ds(rows, count), :] = jnp.broadcast_to(m, (count, 128))
+                    l_out[pl.ds(rows, count), :] = jnp.broadcast_to(l, (count, 128))
+                    a_out[pl.ds(arow, count), :] = acc
     if last:
         lane = lax.broadcasted_iota(jnp.int32, (128, 128), 1)
         for side, out in ((0, own_out), (1, send_out)):
@@ -484,7 +491,7 @@
             pltpu.VMEM((4096, 256), BF),
             pltpu.VMEM((4096, 256), BF),
             pltpu.VMEM((256, 4096), BF),
-            pltpu.SemaphoreType.DMA((3,)),
+            pltpu.SemaphoreType.DMA((9,)),
             pltpu.SemaphoreType.DMA((4,)),
         ],
         mib=20,

time: 167 us -> 166 us (level)
  Pallas kernels: 28.2 us -> 26.2 us
  transfers between devices with their start and end apart: 21 -> 21, of which waited for: 10 -> 12; matrix products, arithmetic and copies ran while one was open for 0% -> 0% of each run, Pallas kernels for 7% -> 7%
where the time goes in v7:
time: 166 us; the launch traced here: 164 us
  waiting for transfers between devices  62.9 us (38%)
  blocking collectives  38.3 us (23%)
  starting transfers between devices  33.4 us (20%)
  Pallas kernels  26.2 us (16%)
  local copies, waits for them, and re-layouts  3.32 us (2%)
    ppermute x9, waiting for transfers between devices, shift(): return lax.ppermute(x, axis, [(i, (i + k) % 4) for i in range(4)])  53.5 us
    all_to_all x1, blocking collectives, local(): lax.all_to_all(outbound.reshape(128, 8, 1024), every, 0, 0, tiled=True)  38.3 us
    pallas_call x8, Pallas kernels, call(): pl.pallas_call(kernel, out_shape=shapes, in_specs=[SMEM if i in smem else...  18.2 us
    ppermute x9, starting transfers between devices, turn(): return lax.ppermute(x, SP, pairs)  15 us
    ppermute x9, starting transfers between devices, shift(): return lax.ppermute(x, axis, [(i, (i + k) % 4) for i in range(4)])  13.4 us
    pallas_call x3, Pallas kernels, attend(): pl.pallas_call(functools.partial(attend_kernel, counts, state is None, la...  8.01 us
    ppermute x9, waiting for transfers between devices, turn(): return lax.ppermute(x, SP, pairs)  7.39 us
    all_to_all x1, starting transfers between devices, local(): lax.all_to_all(result.reshape(128, 8, 1024), every, 0, 0, tiled=True)  4.67 us
  transfers between devices with their start and end apart: 21, of which 12 were waited for; matrix products, arithmetic and copies ran while one was open for 0% of the time, Pallas kernels for 7%

profile of v7, /device:TPU:0, one launch (start us, length us, event | category | flops | bytes accessed | tf_op | source)
XLA Modules:
  0.0 164.4 jit_solution(567783032776971665)
XLA Ops:
  0.0 1.1 shard_map.190
  1.1 1.8 %collective-permute-start.1 = (bf16[128,768]{1,0:T(8,128)(2,1)S(1)}, bf16[128,768]{1,0:T(8,128)(2,1)S(1)}, u32[]{:S(2)}, u32[]{:S(2)}) collective-permute-start(bf16[128,768]{1,0:T(8,128)(2,1)S(1)} %get-tuple-element.37.a.refs_3_), channel_id=1, source_target_pairs={{0,8},{4,36},{8,16},{12,44},{16,24},{20,52},{24,0},{28,60},{32,40}... | collective-permute-start | bytes 589832 | tf_op jit(solution)/shard_map/ppermute | solution.py:41
  2.9 1.5 collective-permute-start.2
  4.4 2.1 %collective-permute-start.3 = (bf16[128,768]{1,0:T(8,128)(2,1)S(1)}, bf16[128,768]{1,0:T(8,128)(2,1)S(1)}, u32[]{:S(2)}, u32[]{:S(2)}) collective-permute-start(bf16[128,768]{1,0:T(8,128)(2,1)S(1)} %get-tuple-element.37.a.refs_3_), channel_id=1, source_target_pairs={{0,16},{4,68},{8,24},{12,76},{16,0},{20,84},{24,8},{28,92},{32,48}... | collective-permute-start | bytes 589832 | tf_op jit(solution)/shard_map/ppermute | solution.py:41
  6.5 0.1 pad_add_fusion.place
  6.6 2.0 %shard_map.191 = (s32[4,128]{1,0:T(4,128)S(1)}, bf16[128,1024]{1,0:T(8,128)(2,1)S(1)}, f32[8,128]{1,0:T(8,128)S(1)}, f32[8,384]{1,0:T(8,128)S(1)}, f32[8,1024]{1,0:T(8,128)S(1)}, /*index=5*/f32[8,512]{1,0:T(8,128)S(1)}) custom-call(s32[4]{0:T(128)S(1)} %pad_add_fusion.place, s32[4,32]{1,0:T(4,128)} %bitcast.20, f32[4,32]{1,0:T(4,128)} %bitcast.21, ...), custom_call_target="tpu_custom_call" | custom-call | bytes 2097152 | tf_op jit(solution)/shard_map/pallas_call | solution.py:48
  8.6 3.0 %collective-permute-done.3.d = bf16[128,768]{1,0:T(8,128)(2,1)S(1)} collective-permute-done((bf16[128,768]{1,0:T(8,128)(2,1)S(1)}, bf16[128,768]{1,0:T(8,128)(2,1)S(1)}, u32[]{:S(2)}, u32[]{:S(2)}) %collective-permute-start.3) | collective-permute-done | bytes 196640 | tf_op jit(solution)/shard_map/ppermute | solution.py:41
  11.6 0.1 shard_map.192
  11.7 2.1 %collective-permute-start.4 = (bf16[2,128,768]{2,1,0:T(8,128)(2,1)S(1)}, bf16[2,128,768]{2,1,0:T(8,128)(2,1)S(1)}, u32[]{:S(2)}, u32[]{:S(2)}) collective-permute-start(bf16[2,128,768]{2,1,0:T(8,128)(2,1)S(1)} %get-tuple-element.40.refs_5_), channel_id=1, source_target_pairs={{0,32},{4,12},{8,40},{12,20},{16,48},{20,28},{24,56},{28,4},{32,64... | collective-permute-start | bytes 1179656 | tf_op jit(solution)/shard_map/ppermute | solution.py:41
  13.8 2.2 %collective-permute-start.6 = (bf16[2,128,768]{2,1,0:T(8,128)(2,1)S(1)}, bf16[2,128,768]{2,1,0:T(8,128)(2,1)S(1)}, u32[]{:S(2)}, u32[]{:S(2)}) collective-permute-start(bf16[2,128,768]{2,1,0:T(8,128)(2,1)S(1)} %get-tuple-element.41.refs_6_), channel_id=1, source_target_pairs={{0,96},{4,28},{8,104},{12,4},{16,112},{20,12},{24,120},{28,20},{32... | collective-permute-start | bytes 1179656 | tf_op jit(solution)/shard_map/ppermute | solution.py:41
  16.0 1.9 %collective-permute-start.8 = (bf16[2,128,768]{2,1,0:T(8,128)(2,1)S(1)}, bf16[2,128,768]{2,1,0:T(8,128)(2,1)S(1)}, u32[]{:S(2)}, u32[]{:S(2)}) collective-permute-start(bf16[2,128,768]{2,1,0:T(8,128)(2,1)S(1)} %get-tuple-element.40.refs_5_), channel_id=1, source_target_pairs={{0,96},{4,28},{8,104},{12,4},{16,112},{20,12},{24,120},{28,20},{32... | collective-permute-start | bytes 1179656 | tf_op jit(solution)/shard_map/ppermute | solution.py:41
  17.9 0.1 collective-permute-start.9
  18.0 3.6 %collective-permute-done.4.refs_3_ = bf16[2,128,768]{2,1,0:T(8,128)(2,1)S(1)} collective-permute-done((bf16[2,128,768]{2,1,0:T(8,128)(2,1)S(1)}, bf16[2,128,768]{2,1,0:T(8,128)(2,1)S(1)}, u32[]{:S(2)}, u32[]{:S(2)}) %collective-permute-start.4) | collective-permute-done | bytes 393248 | tf_op jit(solution)/shard_map/ppermute | solution.py:41
  21.6 3.3 %collective-permute-start.7 = (bf16[2,128,768]{2,1,0:T(8,128)(2,1)S(1)}, bf16[2,128,768]{2,1,0:T(8,128)(2,1)S(1)}, u32[]{:S(2)}, u32[]{:S(2)}) collective-permute-start(bf16[2,128,768]{2,1,0:T(8,128)(2,1)S(1)} %collective-permute-done.6.refs_6_), channel_id=1, source_target_pairs={{0,96},{4,28},{8,104},{12,4},{16,112},{20,12},{24,120},{28,20},{32... | collective-permute-start | bytes 1179656 | tf_op jit(solution)/shard_map/ppermute | solution.py:41
  25.0 1.9 %shard_map.193 = (f32[1536,128]{1,0:T(8,128)S(1)}, f32[1536,128]{1,0:T(8,128)S(1)}, f32[1024,128]{1,0:T(8,128)S(1)}, f32[512,256]{1,0:T(8,128)S(1)}) custom-call(bf16[128,1024]{1,0:T(8,128)(2,1)S(1)} %get-tuple-element.36.refs_0_, bf16[128,1024]{1,0:T(8,128)(2,1)S(1)} %collective-permute-done.refs_1_, s32[1]{0:T(128)} %bitcast.2.refs_2_, ...), custom_call_target="tpu_custom_call" | custom-call | flops 536870912 | bytes 4194304 | tf_op jit(solution)/shard_map/pallas_call | solution.py:354
  26.8 0.1 collective-permute-done.9.refs_5_
  26.9 3.6 %shard_map.194 = (f32[1536,128]{1,0:T(8,128)S(1)}, f32[1536,128]{1,0:T(8,128)S(1)}, f32[1024,128]{1,0:T(8,128)S(1)}, f32[512,256]{1,0:T(8,128)S(1)}) custom-call(bf16[128,1024]{1,0:T(8,128)(2,1)S(1)} %get-tuple-element.36.refs_0_, bf16[128,1024]{1,0:T(8,128)(2,1)S(1)} %collective-permute-done.refs_1_, s32[1]{0:T(128)} %bitcast.2.refs_2_, ...), custom_call_target="tpu_custom_call" | custom-call | flops 1073741824 | bytes 4194304 | tf_op jit(solution)/shard_map/pallas_call | solution.py:354
  30.5 0.6 collective-permute-done.5.refs_3_
  31.1 2.6 %shard_map.195 = (f32[128,1152]{1,0:T(8,128)S(1)}, f32[128,1152]{1,0:T(8,128)S(1)}) custom-call(bf16[128,1024]{1,0:T(8,128)(2,1)S(1)} %get-tuple-element.36.refs_0_, bf16[128,1024]{1,0:T(8,128)(2,1)S(1)} %collective-permute-done.refs_1_, s32[1]{0:T(128)} %bitcast.2.refs_2_, bf16[2,128,768]{2,1,0:T(8,128)(2,1)S(1)} %collective-permute-done.5.refs_3_, ...), custom_call_target="tpu_custom_call" | custom-call | flops 536870912 | bytes 4194304 | tf_op jit(solution)/shard_map/pallas_call | solution.py:354
  33.7 0.3 collective-permute-start.10
  34.0 2.0 %collective-permute-done.10.other = f32[128,1152]{1,0:T(8,128)S(1)} collective-permute-done((f32[128,1152]{1,0:T(8,128)S(1)}, f32[128,1152]{1,0:T(8,128)S(1)}, u32[]{:S(2)}, u32[]{:S(2)}) %collective-permute-start.10) | collective-permute-done | bytes 589856 | tf_op jit(solution)/shard_map/ppermute | solution.py:31
  36.0 2.1 %shard_map.196 = (bf16[32,4096]{1,0:T(8,128)(2,1)S(1)}, bf16[32,4096]{1,0:T(8,128)(2,1)S(1)}, bf16[32,4096]{1,0:T(8,128)(2,1)S(1)}, bf16[32,4096]{1,0:T(8,128)(2,1)S(1)}) custom-call(s32[4]{0:T(128)S(1)} %pad_add_fusion.place, f32[128,1152]{1,0:T(8,128)S(1)} %get-tuple-element.53.own, f32[128,1152]{1,0:T(8,128)S(1)} %collective-permute-done.10.other, ...), custom_call_target="tpu_custom_call" | custom-call | flops 1073741824 | bytes 2097152 | tf_op jit(solution)/shard_map/pallas_call | solution.py:48
  38.1 1.6 collective-permute-start.11
  39.7 2.7 %collective-permute-start.12 = (bf16[32,4096]{1,0:T(8,128)(2,1)S(1)}, bf16[32,4096]{1,0:T(8,128)(2,1)S(1)}, u32[]{:S(2)}, u32[]{:S(2)}) collective-permute-start(bf16[32,4096]{1,0:T(8,128)(2,1)S(1)} %get-tuple-element.57), channel_id=1, source_target_pairs={{0,2},{1,3},{2,0},{3,1},{4,6},{5,7},{6,4},{7,5},{8,10},{9,11},{10,... | collective-permute-start | bytes 786440 | tf_op jit(solution)/shard_map/ppermute | solution.py:27
  42.4 1.4 collective-permute-start.13
  43.8 3.9 %collective-permute-done.11.p1 = bf16[32,4096]{1,0:T(8,128)(2,1)S(1)} collective-permute-done((bf16[32,4096]{1,0:T(8,128)(2,1)S(1)}, bf16[32,4096]{1,0:T(8,128)(2,1)S(1)}, u32[]{:S(2)}, u32[]{:S(2)}) %collective-permute-start.11) | collective-permute-done | bytes 262176 | tf_op jit(solution)/shard_map/ppermute | solution.py:27
  47.7 6.6 %collective-permute-done.12.p2 = bf16[32,4096]{1,0:T(8,128)(2,1)S(1)} collective-permute-done((bf16[32,4096]{1,0:T(8,128)(2,1)S(1)}, bf16[32,4096]{1,0:T(8,128)(2,1)S(1)}, u32[]{:S(2)}, u32[]{:S(2)}) %collective-permute-start.12) | collective-permute-done | bytes 262176 | tf_op jit(solution)/shard_map/ppermute | solution.py:27
  54.3 2.6 %shard_map.197 = (f32[32,4096]{1,0:T(8,128)S(1)}, bf16[32,4096]{1,0:T(8,128)(2,1)S(1)}, bf16[1024,1024]{1,0:T(8,128)(2,1)}) custom-call(s32[4]{0:T(128)S(1)} %pad_add_fusion.place, bf16[32,4096]{1,0:T(8,128)(2,1)S(1)} %get-tuple-element.55.p0, bf16[32,4096]{1,0:T(8,128)(2,1)S(1)} %collective-permute-done.11.p1, ...), custom_call_target="tpu_custom_call" | custom-call | flops 268435456 | bytes 2097152 | tf_op jit(solution)/shard_map/pallas_call | solution.py:48
  56.9 38.3 %all_to_all.10 = bf16[128,8,1024]{2,1,0:T(8,128)(2,1)S(1)} all-to-all(bf16[128,8,1024]{2,1,0:T(8,128)(2,1)} %bitcast.17), channel_id=1, replica_groups=mesh['z'=4,'y'=4,'c'=2,'tp'=4] {'z','y','c','tp'}, dimensions={0} | all-to-all | bytes 4194304 | tf_op jit(solution)/shard_map/all_to_all | solution.py:459
  95.2 5.7 %shard_map.198 = bf16[1024,1024]{1,0:T(8,128)(2,1)} custom-call(bf16[1024,1024]{1,0:T(8,128)(2,1)S(1)} %bitcast.13, bf16[1,4096,256]{2,1,0:T(8,128)(2,1)} %gate_hbm.2, bf16[1,4096,256]{2,1,0:T(8,128)(2,1)} %up_hbm.2, bf16[1,256,4096]{2,1,0:T(8,128)(2,1)} %down_hbm.2), custom_call_target="tpu_custom_call" | custom-call | flops 1610612736 | bytes 2097152 | tf_op jit(solution)/shard_map/pallas_call | solution.py:48
  101.0 4.7 %all-to-all-start.1 = ((bf16[128,8,1024]{2,1,0:T(8,128)(2,1)}), bf16[128,8,1024]{2,1,0:T(8,128)(2,1)S(1)}, u32[]{:S(2)}, u32[]{:S(2)}) async-start(bf16[128,8,1024]{2,1,0:T(8,128)(2,1)} %bitcast.16), calls=%async_computation.1 | async-start | bytes 4194304 | tf_op jit(solution)/shard_map/all_to_all | solution.py:500
  105.7 0.9 collective-permute-start.14
  106.5 2.7 %collective-permute-start.15 = (bf16[32,4096]{1,0:T(8,128)(2,1)S(1)}, bf16[32,4096]{1,0:T(8,128)(2,1)S(1)}, u32[]{:S(2)}, u32[]{:S(2)}) collective-permute-start(bf16[32,4096]{1,0:T(8,128)(2,1)S(1)} %get-tuple-element.62.n0), channel_id=1, source_target_pairs={{0,2},{1,3},{2,0},{3,1},{4,6},{5,7},{6,4},{7,5},{8,10},{9,11},{10,... | collective-permute-start | bytes 786440 | tf_op jit(solution)/shard_map/ppermute | solution.py:27
  109.3 1.4 collective-permute-start.16
  110.7 25.7 %collective-permute-done.14.n1 = bf16[32,4096]{1,0:T(8,128)(2,1)S(1)} collective-permute-done((bf16[32,4096]{1,0:T(8,128)(2,1)S(1)}, bf16[32,4096]{1,0:T(8,128)(2,1)S(1)}, u32[]{:S(2)}, u32[]{:S(2)}) %collective-permute-start.14) | collective-permute-done | bytes 262176 | tf_op jit(solution)/shard_map/ppermute | solution.py:27
  136.4 5.6 %collective-permute-done.15.n2 = bf16[32,4096]{1,0:T(8,128)(2,1)S(1)} collective-permute-done((bf16[32,4096]{1,0:T(8,128)(2,1)S(1)}, bf16[32,4096]{1,0:T(8,128)(2,1)S(1)}, u32[]{:S(2)}, u32[]{:S(2)}) %collective-permute-start.15) | collective-permute-done | bytes 262176 | tf_op jit(solution)/shard_map/ppermute | solution.py:27
  142.0 3.4 %shard_map.199 = (bf16[32,4096]{1,0:T(8,128)(2,1)S(1)}, bf16[32,4096]{1,0:T(8,128)(2,1)S(1)}, bf16[32,4096]{1,0:T(8,128)(2,1)S(1)}, bf16[32,4096]{1,0:T(8,128)(2,1)S(1)}) custom-call(bf16[32,4096]{1,0:T(8,128)(2,1)S(1)} %get-tuple-element.62.n0, bf16[32,4096]{1,0:T(8,128)(2,1)S(1)} %collective-permute-done.14.n1, ...), custom_call_target="tpu_custom_call" | custom-call | flops 805306368 | bytes 2097152 | tf_op jit(solution)/shard_map/pallas_call | solution.py:48
  145.5 0.1 collective-permute-start.17
  145.6 2.0 %collective-permute-start.18 = (bf16[32,4096]{1,0:T(8,128)(2,1)S(1)}, bf16[32,4096]{1,0:T(8,128)(2,1)S(1)}, u32[]{:S(2)}, u32[]{:S(2)}) collective-permute-start(bf16[32,4096]{1,0:T(8,128)(2,1)S(1)} %get-tuple-element.65), channel_id=1, source_target_pairs={{0,2},{1,3},{2,0},{3,1},{4,6},{5,7},{6,4},{7,5},{8,10},{9,11},{10,... | collective-permute-start | bytes 786440 | tf_op jit(solution)/shard_map/ppermute | solution.py:27
  147.6 0.6 collective-permute-start.19
  148.1 6.6 %collective-permute-done.17.s1 = bf16[32,4096]{1,0:T(8,128)(2,1)S(1)} collective-permute-done((bf16[32,4096]{1,0:T(8,128)(2,1)S(1)}, bf16[32,4096]{1,0:T(8,128)(2,1)S(1)}, u32[]{:S(2)}, u32[]{:S(2)}) %collective-permute-start.17) | collective-permute-done | bytes 262176 | tf_op jit(solution)/shard_map/ppermute | solution.py:27
  154.7 1.6 collective-permute-done.18.s2
  156.4 0.7 copy-done.3
  157.1 3.4 %collective-permute-done.19.s3 = bf16[32,4096]{1,0:T(8,128)(2,1)S(1)} collective-permute-done((bf16[32,4096]{1,0:T(8,128)(2,1)S(1)}, bf16[32,4096]{1,0:T(8,128)(2,1)S(1)}, u32[]{:S(2)}, u32[]{:S(2)}) %collective-permute-start.19) | collective-permute-done | bytes 262176 | tf_op jit(solution)/shard_map/ppermute | solution.py:27
  160.5 0.7 copy-done.5
  161.2 0.9 copy-done.4
  162.2 0.9 copy-done.6
  163.1 1.2 shard_map.200
  (23 shorter events, 0.1 us)
Async XLA Ops:
  1.1 7.4 %collective-permute-start.1 = (bf16[128,768]{1,0:T(8,128)(2,1)S(1)}, bf16[128,768]{1,0:T(8,128)(2,1)S(1)}, u32[]{:S(2)}, u32[]{:S(2)}) collective-permute-start(bf16[128,768]{1,0:T(8,128)(2,1)S(1)} %get-tuple-element.37.a.refs_3_), channel_id=1, source_target_pairs={{0,8},{4,36},{8,16},{12,44},{16,24},{20,52},{24,0},{28,60},{32,40}... | collective-permute-start | bytes 589832 | tf_op jit(solution)/shard_map/ppermute | solution.py:41
  2.9 5.7 %collective-permute-start.2 = (bf16[128,768]{1,0:T(8,128)(2,1)S(1)}, bf16[128,768]{1,0:T(8,128)(2,1)S(1)}, u32[]{:S(2)}, u32[]{:S(2)}) collective-permute-start(bf16[128,768]{1,0:T(8,128)(2,1)S(1)} %get-tuple-element.37.a.refs_3_), channel_id=1, source_target_pairs={{0,24},{4,100},{8,0},{12,108},{16,8},{20,116},{24,16},{28,124},{32... | collective-permute-start | bytes 589832 | tf_op jit(solution)/shard_map/ppermute | solution.py:41
  4.4 7.2 %collective-permute-start.3 = (bf16[128,768]{1,0:T(8,128)(2,1)S(1)}, bf16[128,768]{1,0:T(8,128)(2,1)S(1)}, u32[]{:S(2)}, u32[]{:S(2)}) collective-permute-start(bf16[128,768]{1,0:T(8,128)(2,1)S(1)} %get-tuple-element.37.a.refs_3_), channel_id=1, source_target_pairs={{0,16},{4,68},{8,24},{12,76},{16,0},{20,84},{24,8},{28,92},{32,48}... | collective-permute-start | bytes 589832 | tf_op jit(solution)/shard_map/ppermute | solution.py:41
  11.7 10.0 %collective-permute-start.4 = (bf16[2,128,768]{2,1,0:T(8,128)(2,1)S(1)}, bf16[2,128,768]{2,1,0:T(8,128)(2,1)S(1)}, u32[]{:S(2)}, u32[]{:S(2)}) collective-permute-start(bf16[2,128,768]{2,1,0:T(8,128)(2,1)S(1)} %get-tuple-element.40.refs_5_), channel_id=1, source_target_pairs={{0,32},{4,12},{8,40},{12,20},{16,48},{20,28},{24,56},{28,4},{32,64... | collective-permute-start | bytes 1179656 | tf_op jit(solution)/shard_map/ppermute | solution.py:41
  13.8 7.9 %collective-permute-start.6 = (bf16[2,128,768]{2,1,0:T(8,128)(2,1)S(1)}, bf16[2,128,768]{2,1,0:T(8,128)(2,1)S(1)}, u32[]{:S(2)}, u32[]{:S(2)}) collective-permute-start(bf16[2,128,768]{2,1,0:T(8,128)(2,1)S(1)} %get-tuple-element.41.refs_6_), channel_id=1, source_target_pairs={{0,96},{4,28},{8,104},{12,4},{16,112},{20,12},{24,120},{28,20},{32... | collective-permute-start | bytes 1179656 | tf_op jit(solution)/shard_map/ppermute | solution.py:41
  16.0 10.9 %collective-permute-start.8 = (bf16[2,128,768]{2,1,0:T(8,128)(2,1)S(1)}, bf16[2,128,768]{2,1,0:T(8,128)(2,1)S(1)}, u32[]{:S(2)}, u32[]{:S(2)}) collective-permute-start(bf16[2,128,768]{2,1,0:T(8,128)(2,1)S(1)} %get-tuple-element.40.refs_5_), channel_id=1, source_target_pairs={{0,96},{4,28},{8,104},{12,4},{16,112},{20,12},{24,120},{28,20},{32... | collective-permute-start | bytes 1179656 | tf_op jit(solution)/shard_map/ppermute | solution.py:41
  17.9 9.0 %collective-permute-start.9 = (bf16[2,128,768]{2,1,0:T(8,128)(2,1)S(1)}, bf16[2,128,768]{2,1,0:T(8,128)(2,1)S(1)}, u32[]{:S(2)}, u32[]{:S(2)}) collective-permute-start(bf16[2,128,768]{2,1,0:T(8,128)(2,1)S(1)} %get-tuple-element.41.refs_6_), channel_id=1, source_target_pairs={{0,32},{4,12},{8,40},{12,20},{16,48},{20,28},{24,56},{28,4},{32,64... | collective-permute-start | bytes 1179656 | tf_op jit(solution)/shard_map/ppermute | solution.py:41
  18.0 7.0 %collective-permute-start = (bf16[128,1024]{1,0:T(8,128)(2,1)S(1)}, bf16[128,1024]{1,0:T(8,128)(2,1)S(1)}, u32[]{:S(2)}, u32[]{:S(2)}) collective-permute-start(bf16[128,1024]{1,0:T(8,128)(2,1)S(1)} %get-tuple-element.36.refs_0_), channel_id=1, source_target_pairs={{0,4},{4,0},{1,5},{5,1},{2,6},{6,2},{3,7},{7,3},{8,12},{12,8},{9,1... | collective-permute-start | bytes 786440 | tf_op jit(solution)/shard_map/ppermute | solution.py:31
  21.6 9.5 %collective-permute-start.5 = (bf16[2,128,768]{2,1,0:T(8,128)(2,1)S(1)}, bf16[2,128,768]{2,1,0:T(8,128)(2,1)S(1)}, u32[]{:S(2)}, u32[]{:S(2)}) collective-permute-start(bf16[2,128,768]{2,1,0:T(8,128)(2,1)S(1)} %collective-permute-done.4.refs_3_), channel_id=1, source_target_pairs={{0,32},{4,12},{8,40},{12,20},{16,48},{20,28},{24,56},{28,4},{32,64... | collective-permute-start | bytes 1179656 | tf_op jit(solution)/shard_map/ppermute | solution.py:41
  21.6 9.5 %collective-permute-start.7 = (bf16[2,128,768]{2,1,0:T(8,128)(2,1)S(1)}, bf16[2,128,768]{2,1,0:T(8,128)(2,1)S(1)}, u32[]{:S(2)}, u32[]{:S(2)}) collective-permute-start(bf16[2,128,768]{2,1,0:T(8,128)(2,1)S(1)} %collective-permute-done.6.refs_6_), channel_id=1, source_target_pairs={{0,96},{4,28},{8,104},{12,4},{16,112},{20,12},{24,120},{28,20},{32... | collective-permute-start | bytes 1179656 | tf_op jit(solution)/shard_map/ppermute | solution.py:41
  26.9 9.1 %copy-start = (bf16[512,4096]{1,0:T(8,128)(2,1)S(1)}, bf16[512,4096]{1,0:T(8,128)(2,1)}, u32[]{:S(2)}) copy-start(bf16[512,4096]{1,0:T(8,128)(2,1)} %narrow.1) | copy-start | bytes 12582916
  26.9 9.1 %copy-start.1 = (bf16[512,4096]{1,0:T(8,128)(2,1)S(1)}, bf16[512,4096]{1,0:T(8,128)(2,1)}, u32[]{:S(2)}) copy-start(bf16[512,4096]{1,0:T(8,128)(2,1)} %broad.1) | copy-start | bytes 12582916
  33.7 2.3 %collective-permute-start.10 = (f32[128,1152]{1,0:T(8,128)S(1)}, f32[128,1152]{1,0:T(8,128)S(1)}, u32[]{:S(2)}, u32[]{:S(2)}) collective-permute-start(f32[128,1152]{1,0:T(8,128)S(1)} %get-tuple-element.54), channel_id=1, source_target_pairs={{0,4},{4,0},{1,5},{5,1},{2,6},{6,2},{3,7},{7,3},{8,12},{12,8},{9,1... | collective-permute-start | bytes 1769480 | tf_op jit(solution)/shard_map/ppermute | solution.py:31
  36.0 18.4 %copy-start.2 = (bf16[128,4096]{1,0:T(8,128)(2,1)S(1)}, bf16[128,4096]{1,0:T(8,128)(2,1)}, u32[]{:S(2)}) copy-start(bf16[128,4096]{1,0:T(8,128)(2,1)} %residual.1) | copy-start | bytes 3145732
  36.0 18.4 %copy-start.7 = (f32[4096]{0:T(1024)S(1)}, f32[4096]{0:T(1024)}, u32[]{:S(2)}) copy-start(f32[4096]{0:T(1024)} %param.31) | copy-start | bytes 49156
  38.1 9.6 %collective-permute-start.11 = (bf16[32,4096]{1,0:T(8,128)(2,1)S(1)}, bf16[32,4096]{1,0:T(8,128)(2,1)S(1)}, u32[]{:S(2)}, u32[]{:S(2)}) collective-permute-start(bf16[32,4096]{1,0:T(8,128)(2,1)S(1)} %get-tuple-element.56), channel_id=1, source_target_pairs={{0,1},{1,2},{2,3},{3,0},{4,5},{5,6},{6,7},{7,4},{8,9},{9,10},{10,1... | collective-permute-start | bytes 786440 | tf_op jit(solution)/shard_map/ppermute | solution.py:27
  39.7 14.7 %collective-permute-start.12 = (bf16[32,4096]{1,0:T(8,128)(2,1)S(1)}, bf16[32,4096]{1,0:T(8,128)(2,1)S(1)}, u32[]{:S(2)}, u32[]{:S(2)}) collective-permute-start(bf16[32,4096]{1,0:T(8,128)(2,1)S(1)} %get-tuple-element.57), channel_id=1, source_target_pairs={{0,2},{1,3},{2,0},{3,1},{4,6},{5,7},{6,4},{7,5},{8,10},{9,11},{10,... | collective-permute-start | bytes 786440 | tf_op jit(solution)/shard_map/ppermute | solution.py:27
  42.4 12.0 %collective-permute-start.13 = (bf16[32,4096]{1,0:T(8,128)(2,1)S(1)}, bf16[32,4096]{1,0:T(8,128)(2,1)S(1)}, u32[]{:S(2)}, u32[]{:S(2)}) collective-permute-start(bf16[32,4096]{1,0:T(8,128)(2,1)S(1)} %get-tuple-element.58), channel_id=1, source_target_pairs={{0,3},{1,0},{2,1},{3,2},{4,7},{5,4},{6,5},{7,6},{8,11},{9,8},{10,9... | collective-permute-start | bytes 786440 | tf_op jit(solution)/shard_map/ppermute | solution.py:27
  101.0 60.2 %all-to-all-start.1 = ((bf16[128,8,1024]{2,1,0:T(8,128)(2,1)}), bf16[128,8,1024]{2,1,0:T(8,128)(2,1)S(1)}, u32[]{:S(2)}, u32[]{:S(2)}) async-start(bf16[128,8,1024]{2,1,0:T(8,128)(2,1)} %bitcast.16), calls=%async_computation.1 | async-start | bytes 4194304 | tf_op jit(solution)/shard_map/all_to_all | solution.py:500
  105.7 30.8 %collective-permute-start.14 = (bf16[32,4096]{1,0:T(8,128)(2,1)S(1)}, bf16[32,4096]{1,0:T(8,128)(2,1)S(1)}, u32[]{:S(2)}, u32[]{:S(2)}) collective-permute-start(bf16[32,4096]{1,0:T(8,128)(2,1)S(1)} %get-tuple-element.62.n0), channel_id=1, source_target_pairs={{0,1},{1,2},{2,3},{3,0},{4,5},{5,6},{6,7},{7,4},{8,9},{9,10},{10,1... | collective-permute-start | bytes 786440 | tf_op jit(solution)/shard_map/ppermute | solution.py:27
  106.5 35.5 %collective-permute-start.15 = (bf16[32,4096]{1,0:T(8,128)(2,1)S(1)}, bf16[32,4096]{1,0:T(8,128)(2,1)S(1)}, u32[]{:S(2)}, u32[]{:S(2)}) collective-permute-start(bf16[32,4096]{1,0:T(8,128)(2,1)S(1)} %get-tuple-element.62.n0), channel_id=1, source_target_pairs={{0,2},{1,3},{2,0},{3,1},{4,6},{5,7},{6,4},{7,5},{8,10},{9,11},{10,... | collective-permute-start | bytes 786440 | tf_op jit(solution)/shard_map/ppermute | solution.py:27
  109.3 32.8 %collective-permute-start.16 = (bf16[32,4096]{1,0:T(8,128)(2,1)S(1)}, bf16[32,4096]{1,0:T(8,128)(2,1)S(1)}, u32[]{:S(2)}, u32[]{:S(2)}) collective-permute-start(bf16[32,4096]{1,0:T(8,128)(2,1)S(1)} %get-tuple-element.62.n0), channel_id=1, source_target_pairs={{0,3},{1,0},{2,1},{3,2},{4,7},{5,4},{6,5},{7,6},{8,11},{9,8},{10,9... | collective-permute-start | bytes 786440 | tf_op jit(solution)/shard_map/ppermute | solution.py:27
  145.5 9.2 %collective-permute-start.17 = (bf16[32,4096]{1,0:T(8,128)(2,1)S(1)}, bf16[32,4096]{1,0:T(8,128)(2,1)S(1)}, u32[]{:S(2)}, u32[]{:S(2)}) collective-permute-start(bf16[32,4096]{1,0:T(8,128)(2,1)S(1)} %get-tuple-element.64), channel_id=1, source_target_pairs={{0,3},{1,0},{2,1},{3,2},{4,7},{5,4},{6,5},{7,6},{8,11},{9,8},{10,9... | collective-permute-start | bytes 786440 | tf_op jit(solution)/shard_map/ppermute | solution.py:27
  145.6 10.8 %collective-permute-start.18 = (bf16[32,4096]{1,0:T(8,128)(2,1)S(1)}, bf16[32,4096]{1,0:T(8,128)(2,1)S(1)}, u32[]{:S(2)}, u32[]{:S(2)}) collective-permute-start(bf16[32,4096]{1,0:T(8,128)(2,1)S(1)} %get-tuple-element.65), channel_id=1, source_target_pairs={{0,2},{1,3},{2,0},{3,1},{4,6},{5,7},{6,4},{7,5},{8,10},{9,11},{10,... | collective-permute-start | bytes 786440 | tf_op jit(solution)/shard_map/ppermute | solution.py:27
  147.6 13.0 %collective-permute-start.19 = (bf16[32,4096]{1,0:T(8,128)(2,1)S(1)}, bf16[32,4096]{1,0:T(8,128)(2,1)S(1)}, u32[]{:S(2)}, u32[]{:S(2)}) collective-permute-start(bf16[32,4096]{1,0:T(8,128)(2,1)S(1)} %get-tuple-element.66), channel_id=1, source_target_pairs={{0,1},{1,2},{2,3},{3,0},{4,5},{5,6},{6,7},{7,4},{8,9},{9,10},{10,1... | collective-permute-start | bytes 786440 | tf_op jit(solution)/shard_map/ppermute | solution.py:27
  156.4 0.7 copy-start.3
  160.5 0.7 copy-start.5
  161.2 1.0 copy-start.4
  162.2 0.9 copy-start.6

commit v8 on v7

--- a/solution.py
+++ b/solution.py
@@ -178,14 +178,16 @@
     return v / (1.0 + jnp.exp(-v))
 
 
-def shared_kernel(n0, n1, n2, n3, gate_hbm, up_hbm, down_hbm, o0, o1, o2, o3, gate, up, down, sems):
-    fetched = fetch(((gate_hbm, gate), (up_hbm, up), (down_hbm, down)), sems)
-    x = jnp.concatenate([n0[...], n1[...], n2[...], n3[...]], axis=0)
-    fetched[0].wait()
+def shared_kernel(n0, n1, n2, n3, gate_hbm, up_hbm, down_hbm, o0, o1, o2, o3, x, gate, up, down, sems):
+    pairs = [(n, x.at[pl.ds(k * 32, 32)]) for k, n in enumerate((n0, n1, n2, n3))]
+    fetched = fetch(pairs + [(gate_hbm, gate), (up_hbm, up), (down_hbm, down)], sems)
+    for copy in fetched[:5]:
+        copy.wait()
+    x = x[...]
     g = jnp.dot(x, gate[...], preferred_element_type=F32)
-    fetched[1].wait()
+    fetched[5].wait()
     u = jnp.dot(x, up[...], preferred_element_type=F32)
-    fetched[2].wait()
+    fetched[6].wait()
     hidden = (silu(g) * u).astype(BF)
     for at in range(0, 4096, 1024):
         part = jnp.dot(hidden, down[:, at : at + 1024], preferred_element_type=F32).astype(BF)
@@ -193,7 +195,11 @@
             out[:, at : at + 1024] = part[k * 32 : (k + 1) * 32]
 
 
-def expert_kernel(inbound, gate_hbm, up_hbm, down_hbm, out, x, rows_out, gate, up, down, weight_sems, sems):
+def mark_kernel(value, out):
+    out[...] = value[...]
+
+
+def expert_kernel(mark, inbound, gate_hbm, up_hbm, down_hbm, out, x, rows_out, gate, up, down, weight_sems, sems):
     pairs = []
     for g in range(4):
         part = pl.ds(g * 1024, 1024)
@@ -230,13 +236,17 @@
         copy.wait()
 
 
-def combine_kernel(returned, mix, stream, s0, s1, s2, s3, out):
+def combine_kernel(returned, mix, stream_hbm, s0, s1, s2, s3, out, stream, shared, sems):
+    pairs = [(s, shared.at[k]) for k, s in enumerate((s0, s1, s2, s3))]
+    fetched = fetch(pairs + [(stream_hbm, stream)], sems)
     routed = jnp.dot(mix[...], returned[...], preferred_element_type=F32)
+    for copy in fetched:
+        copy.wait()
     for g in range(4):
         lo, hi = g * 1024, (g + 1) * 1024
         total = stream[:, lo:hi] + routed[g * 32 : (g + 1) * 32]
-        for s in (s0, s1, s2, s3):
-            total = total + s[:, lo:hi].astype(F32)
+        for k in range(4):
+            total = total + shared[k, :, lo:hi].astype(F32)
         out[:, lo:hi] = total.astype(BF)
 
 
@@ -465,12 +475,13 @@
         shared_kernel,
         (normed, n1, n2, n3, shared_gate, shared_up, shared_down),
         [shaped((32, 4096), BF)] * 4,
-        hbm=(4, 5, 6),
+        hbm=range(7),
         scratch=[
+            pltpu.VMEM((128, 4096), BF),
             pltpu.VMEM((4096, 256), BF),
             pltpu.VMEM((4096, 256), BF),
             pltpu.VMEM((256, 4096), BF),
-            pltpu.SemaphoreType.DMA((3,)),
+            pltpu.SemaphoreType.DMA((7,)),
         ],
         mib=20,
         flops=2 * 128 * 4096 * 768,
@@ -479,11 +490,12 @@
     s2 = shift(s2, "tp", 2)
     s3 = shift(s3, "tp", 1)
 
+    (mark,) = call(mark_kernel, (target,), [shaped((4, 128), jnp.int32)])
     (result,) = call(
         expert_kernel,
-        (inbound.reshape(1024, 1024), expert_gate, expert_up, expert_down),
+        (mark, inbound.reshape(1024, 1024), expert_gate, expert_up, expert_down),
         [pltpu.HBM((1024, 1024), BF)],
-        hbm=(1, 2, 3),
+        hbm=(2, 3, 4),
         hbm_out=(0,),
         scratch=[
             pltpu.VMEM((256, 4096), BF),
@@ -502,6 +514,8 @@
         combine_kernel,
         (returned.reshape(1024, 1024), mix, stream, s0, s1, s2, s3),
         [shaped((32, 4096), BF)],
+        hbm=(2, 3, 4, 5, 6),
+        scratch=[pltpu.VMEM((32, 4096), F32), pltpu.VMEM((4, 32, 4096), BF), pltpu.SemaphoreType.DMA((5,))],
         flops=2 * 128 * 1024 * 1024,
     )
     return out

time: 166 us -> 168 us (1.012)
  blocking collectives: 38.3 us -> 0 us
  waiting for transfers between devices: 62.9 us -> 94.1 us
  starting transfers between devices: 33.4 us -> 41.1 us
    all_to_all x1 -> x0, blocking collectives: 38.3 us -> none  [local(): lax.all_to_all(outbound.reshape(128, 8, 1024), every, 0, 0, tiled=True)]
    all_to_all x0 -> x1, waiting for transfers between devices: none -> 30 us  [local(): lax.all_to_all(outbound.reshape(128, 8, 1024), every, 0, 0, tiled=True)]
    all_to_all x0 -> x1, starting transfers between devices: none -> 8.26 us  [local(): lax.all_to_all(outbound.reshape(128, 8, 1024), every, 0, 0, tiled=True)]
    pallas_call x8 -> x9, Pallas kernels: 18.2 us -> 19.9 us  [call(): pl.pallas_call(kernel, out_shape=shapes, in_specs=[SMEM if i in smem else...]
    unnamed x16 -> x26, local copies, waits for them, and re-layouts: 3.32 us -> 3.6 us
  transfers between devices with their start and end apart: 21 -> 22, of which waited for: 12 -> 13; matrix products, arithmetic and copies ran while one was open for 0% -> 0% of each run, Pallas kernels for 7% -> 7%
where the time goes in v8:
time: 168 us; the launch traced here: 167 us
  waiting for transfers between devices  94.1 us (56%)
  starting transfers between devices  41.1 us (24%)
  Pallas kernels  27.8 us (17%)
  local copies, waits for them, and re-layouts  3.6 us (2%)
    ppermute x9, waiting for transfers between devices, shift(): return lax.ppermute(x, axis, [(i, (i + k) % 4) for i in range(4)])  54.6 us
    all_to_all x1, waiting for transfers between devices, local(): lax.all_to_all(outbound.reshape(128, 8, 1024), every, 0, 0, tiled=True)  30 us
    pallas_call x9, Pallas kernels, call(): pl.pallas_call(kernel, out_shape=shapes, in_specs=[SMEM if i in smem else...  19.9 us
    ppermute x9, starting transfers between devices, turn(): return lax.ppermute(x, SP, pairs)  15 us
    ppermute x9, starting transfers between devices, shift(): return lax.ppermute(x, axis, [(i, (i + k) % 4) for i in range(4)])  12.9 us
    all_to_all x1, starting transfers between devices, local(): lax.all_to_all(outbound.reshape(128, 8, 1024), every, 0, 0, tiled=True)  8.26 us
    pallas_call x3, Pallas kernels, attend(): pl.pallas_call(functools.partial(attend_kernel, counts, state is None, la...  7.92 us
    ppermute x9, waiting for transfers between devices, turn(): return lax.ppermute(x, SP, pairs)  7.44 us
  transfers between devices with their start and end apart: 22, of which 13 were waited for; matrix products, arithmetic and copies ran while one was open for 0% of the time, Pallas kernels for 7%

profile of v8, /device:TPU:0, one launch (start us, length us, event | category | flops | bytes accessed | tf_op | source)
XLA Modules:
  0.0 167.0 jit_solution(3828266954388177326)
XLA Ops:
  0.0 1.1 shard_map.192
  1.1 1.8 %collective-permute-start.1 = (bf16[128,768]{1,0:T(8,128)(2,1)S(1)}, bf16[128,768]{1,0:T(8,128)(2,1)S(1)}, u32[]{:S(2)}, u32[]{:S(2)}) collective-permute-start(bf16[128,768]{1,0:T(8,128)(2,1)S(1)} %get-tuple-element.38.a.refs_3_), channel_id=1, source_target_pairs={{0,8},{4,36},{8,16},{12,44},{16,24},{20,52},{24,0},{28,60},{32,40}... | collective-permute-start | bytes 589832 | tf_op jit(solution)/shard_map/ppermute | solution.py:41
  2.9 1.5 collective-permute-start.2
  4.4 2.1 %collective-permute-start.3 = (bf16[128,768]{1,0:T(8,128)(2,1)S(1)}, bf16[128,768]{1,0:T(8,128)(2,1)S(1)}, u32[]{:S(2)}, u32[]{:S(2)}) collective-permute-start(bf16[128,768]{1,0:T(8,128)(2,1)S(1)} %get-tuple-element.38.a.refs_3_), channel_id=1, source_target_pairs={{0,16},{4,68},{8,24},{12,76},{16,0},{20,84},{24,8},{28,92},{32,48}... | collective-permute-start | bytes 589832 | tf_op jit(solution)/shard_map/ppermute | solution.py:41
  6.5 0.1 pad_add_fusion.place
  6.6 2.0 %shard_map.190 = (s32[4,128]{1,0:T(4,128)S(1)}, bf16[128,1024]{1,0:T(8,128)(2,1)S(1)}, f32[8,128]{1,0:T(8,128)S(1)}, f32[8,384]{1,0:T(8,128)S(1)}, f32[8,1024]{1,0:T(8,128)S(1)}, /*index=5*/f32[8,512]{1,0:T(8,128)S(1)}) custom-call(s32[4]{0:T(128)S(1)} %pad_add_fusion.place, s32[4,32]{1,0:T(4,128)} %bitcast.20, f32[4,32]{1,0:T(4,128)} %bitcast.21, ...), custom_call_target="tpu_custom_call" | custom-call | bytes 2097152 | tf_op jit(solution)/shard_map/pallas_call | solution.py:48
  8.6 3.0 %collective-permute-done.3.d = bf16[128,768]{1,0:T(8,128)(2,1)S(1)} collective-permute-done((bf16[128,768]{1,0:T(8,128)(2,1)S(1)}, bf16[128,768]{1,0:T(8,128)(2,1)S(1)}, u32[]{:S(2)}, u32[]{:S(2)}) %collective-permute-start.3) | collective-permute-done | bytes 196640 | tf_op jit(solution)/shard_map/ppermute | solution.py:41
  11.7 2.1 %collective-permute-start.4 = (bf16[2,128,768]{2,1,0:T(8,128)(2,1)S(1)}, bf16[2,128,768]{2,1,0:T(8,128)(2,1)S(1)}, u32[]{:S(2)}, u32[]{:S(2)}) collective-permute-start(bf16[2,128,768]{2,1,0:T(8,128)(2,1)S(1)} %get-tuple-element.40.refs_5_), channel_id=1, source_target_pairs={{0,32},{4,12},{8,40},{12,20},{16,48},{20,28},{24,56},{28,4},{32,64... | collective-permute-start | bytes 1179656 | tf_op jit(solution)/shard_map/ppermute | solution.py:41
  13.8 2.2 %collective-permute-start.6 = (bf16[2,128,768]{2,1,0:T(8,128)(2,1)S(1)}, bf16[2,128,768]{2,1,0:T(8,128)(2,1)S(1)}, u32[]{:S(2)}, u32[]{:S(2)}) collective-permute-start(bf16[2,128,768]{2,1,0:T(8,128)(2,1)S(1)} %get-tuple-element.41.refs_6_), channel_id=1, source_target_pairs={{0,96},{4,28},{8,104},{12,4},{16,112},{20,12},{24,120},{28,20},{32... | collective-permute-start | bytes 1179656 | tf_op jit(solution)/shard_map/ppermute | solution.py:41
  16.0 1.9 %collective-permute-start.8 = (bf16[2,128,768]{2,1,0:T(8,128)(2,1)S(1)}, bf16[2,128,768]{2,1,0:T(8,128)(2,1)S(1)}, u32[]{:S(2)}, u32[]{:S(2)}) collective-permute-start(bf16[2,128,768]{2,1,0:T(8,128)(2,1)S(1)} %get-tuple-element.40.refs_5_), channel_id=1, source_target_pairs={{0,96},{4,28},{8,104},{12,4},{16,112},{20,12},{24,120},{28,20},{32... | collective-permute-start | bytes 1179656 | tf_op jit(solution)/shard_map/ppermute | solution.py:41
  17.9 0.1 collective-permute-start.9
  18.0 3.6 %collective-permute-done.4.refs_3_ = bf16[2,128,768]{2,1,0:T(8,128)(2,1)S(1)} collective-permute-done((bf16[2,128,768]{2,1,0:T(8,128)(2,1)S(1)}, bf16[2,128,768]{2,1,0:T(8,128)(2,1)S(1)}, u32[]{:S(2)}, u32[]{:S(2)}) %collective-permute-start.4) | collective-permute-done | bytes 393248 | tf_op jit(solution)/shard_map/ppermute | solution.py:41
  21.6 3.3 %collective-permute-start.7 = (bf16[2,128,768]{2,1,0:T(8,128)(2,1)S(1)}, bf16[2,128,768]{2,1,0:T(8,128)(2,1)S(1)}, u32[]{:S(2)}, u32[]{:S(2)}) collective-permute-start(bf16[2,128,768]{2,1,0:T(8,128)(2,1)S(1)} %collective-permute-done.6.refs_6_), channel_id=1, source_target_pairs={{0,96},{4,28},{8,104},{12,4},{16,112},{20,12},{24,120},{28,20},{32... | collective-permute-start | bytes 1179656 | tf_op jit(solution)/shard_map/ppermute | solution.py:41
  25.0 1.8 %shard_map.194 = (f32[1536,128]{1,0:T(8,128)S(1)}, f32[1536,128]{1,0:T(8,128)S(1)}, f32[1024,128]{1,0:T(8,128)S(1)}, f32[512,256]{1,0:T(8,128)S(1)}) custom-call(bf16[128,1024]{1,0:T(8,128)(2,1)S(1)} %get-tuple-element.37.refs_0_, bf16[128,1024]{1,0:T(8,128)(2,1)S(1)} %collective-permute-done.refs_1_, s32[1]{0:T(128)} %bitcast.2.refs_2_, ...), custom_call_target="tpu_custom_call" | custom-call | flops 536870912 | bytes 4194304 | tf_op jit(solution)/shard_map/pallas_call | solution.py:364
  26.8 0.1 collective-permute-done.9.refs_5_
  26.9 3.5 %shard_map.195 = (f32[1536,128]{1,0:T(8,128)S(1)}, f32[1536,128]{1,0:T(8,128)S(1)}, f32[1024,128]{1,0:T(8,128)S(1)}, f32[512,256]{1,0:T(8,128)S(1)}) custom-call(bf16[128,1024]{1,0:T(8,128)(2,1)S(1)} %get-tuple-element.37.refs_0_, bf16[128,1024]{1,0:T(8,128)(2,1)S(1)} %collective-permute-done.refs_1_, s32[1]{0:T(128)} %bitcast.2.refs_2_, ...), custom_call_target="tpu_custom_call" | custom-call | flops 1073741824 | bytes 4194304 | tf_op jit(solution)/shard_map/pallas_call | solution.py:364
  30.4 0.7 collective-permute-done.5.refs_3_
  31.1 2.6 %shard_map.196 = (f32[128,1152]{1,0:T(8,128)S(1)}, f32[128,1152]{1,0:T(8,128)S(1)}) custom-call(bf16[128,1024]{1,0:T(8,128)(2,1)S(1)} %get-tuple-element.37.refs_0_, bf16[128,1024]{1,0:T(8,128)(2,1)S(1)} %collective-permute-done.refs_1_, s32[1]{0:T(128)} %bitcast.2.refs_2_, bf16[2,128,768]{2,1,0:T(8,128)(2,1)S(1)} %collective-permute-done.5.refs_3_, ...), custom_call_target="tpu_custom_call" | custom-call | flops 536870912 | bytes 4194304 | tf_op jit(solution)/shard_map/pallas_call | solution.py:364
  33.7 0.3 collective-permute-start.10
  34.0 2.0 %collective-permute-done.10.other = f32[128,1152]{1,0:T(8,128)S(1)} collective-permute-done((f32[128,1152]{1,0:T(8,128)S(1)}, f32[128,1152]{1,0:T(8,128)S(1)}, u32[]{:S(2)}, u32[]{:S(2)}) %collective-permute-start.10) | collective-permute-done | bytes 589856 | tf_op jit(solution)/shard_map/ppermute | solution.py:31
  36.0 2.1 %shard_map.197 = (bf16[32,4096]{1,0:T(8,128)(2,1)S(1)}, bf16[32,4096]{1,0:T(8,128)(2,1)S(1)}, bf16[32,4096]{1,0:T(8,128)(2,1)S(1)}, bf16[32,4096]{1,0:T(8,128)(2,1)S(1)}) custom-call(s32[4]{0:T(128)S(1)} %pad_add_fusion.place, f32[128,1152]{1,0:T(8,128)S(1)} %get-tuple-element.53.own, f32[128,1152]{1,0:T(8,128)S(1)} %collective-permute-done.10.other, ...), custom_call_target="tpu_custom_call" | custom-call | flops 1073741824 | bytes 2097152 | tf_op jit(solution)/shard_map/pallas_call | solution.py:48
  38.1 1.6 collective-permute-start.11
  39.6 2.7 %collective-permute-start.12 = (bf16[32,4096]{1,0:T(8,128)(2,1)S(1)}, bf16[32,4096]{1,0:T(8,128)(2,1)S(1)}, u32[]{:S(2)}, u32[]{:S(2)}) collective-permute-start(bf16[32,4096]{1,0:T(8,128)(2,1)S(1)} %get-tuple-element.57), channel_id=1, source_target_pairs={{0,2},{1,3},{2,0},{3,1},{4,6},{5,7},{6,4},{7,5},{8,10},{9,11},{10,... | collective-permute-start | bytes 786440 | tf_op jit(solution)/shard_map/ppermute | solution.py:27
  42.4 1.4 collective-permute-start.13
  43.8 3.9 %collective-permute-done.11.p1 = bf16[32,4096]{1,0:T(8,128)(2,1)S(1)} collective-permute-done((bf16[32,4096]{1,0:T(8,128)(2,1)S(1)}, bf16[32,4096]{1,0:T(8,128)(2,1)S(1)}, u32[]{:S(2)}, u32[]{:S(2)}) %collective-permute-start.11) | collective-permute-done | bytes 262176 | tf_op jit(solution)/shard_map/ppermute | solution.py:27
  47.7 6.6 %collective-permute-done.12.p2 = bf16[32,4096]{1,0:T(8,128)(2,1)S(1)} collective-permute-done((bf16[32,4096]{1,0:T(8,128)(2,1)S(1)}, bf16[32,4096]{1,0:T(8,128)(2,1)S(1)}, u32[]{:S(2)}, u32[]{:S(2)}) %collective-permute-start.12) | collective-permute-done | bytes 262176 | tf_op jit(solution)/shard_map/ppermute | solution.py:27
  54.3 2.6 %shard_map.198 = (f32[32,4096]{1,0:T(8,128)S(1)}, bf16[32,4096]{1,0:T(8,128)(2,1)S(1)}, bf16[1024,1024]{1,0:T(8,128)(2,1)}) custom-call(s32[4]{0:T(128)S(1)} %pad_add_fusion.place, bf16[32,4096]{1,0:T(8,128)(2,1)S(1)} %get-tuple-element.55.p0, bf16[32,4096]{1,0:T(8,128)(2,1)S(1)} %collective-permute-done.11.p1, ...), custom_call_target="tpu_custom_call" | custom-call | flops 268435456 | bytes 2097152 | tf_op jit(solution)/shard_map/pallas_call | solution.py:48
  56.9 0.8 copy-done.3
  57.7 8.3 %all-to-all-start = ((bf16[128,8,1024]{2,1,0:T(8,128)(2,1)}), bf16[128,8,1024]{2,1,0:T(8,128)(2,1)S(1)}, u32[]{:S(2)}, u32[]{:S(2)}) async-start(bf16[128,8,1024]{2,1,0:T(8,128)(2,1)} %bitcast.17), calls=%async_computation | async-start | bytes 4194304 | tf_op jit(solution)/shard_map/all_to_all | solution.py:469
  66.0 30.0 %all-to-all-done = bf16[128,8,1024]{2,1,0:T(8,128)(2,1)S(1)} async-done(((bf16[128,8,1024]{2,1,0:T(8,128)(2,1)}), bf16[128,8,1024]{2,1,0:T(8,128)(2,1)S(1)}, u32[]{:S(2)}, u32[]{:S(2)}) %all-to-all-start) | async-done | bytes 2097184 | tf_op jit(solution)/shard_map/all_to_all | solution.py:469
  96.0 5.7 %shard_map.199 = bf16[1024,1024]{1,0:T(8,128)(2,1)} custom-call(s32[4,128]{1,0:T(4,128)S(1)} %shard_map.191.mark, bf16[1024,1024]{1,0:T(8,128)(2,1)S(1)} %bitcast.14, bf16[1,4096,256]{2,1,0:T(8,128)(2,1)} %gate_hbm.2, bf16[1,4096,256]{2,1,0:T(8,128)(2,1)} %up_hbm.2, bf16[1,256,4096]{2,1,0:T(8,128)(2,1)} %down_hbm.2), custom_call_target="tpu_custom_call" | custom-call | flops 1610612736 | bytes 2097152 | tf_op jit(solution)/shard_map/pallas_call | solution.py:48
  101.7 4.7 %all-to-all-start.1 = ((bf16[128,8,1024]{2,1,0:T(8,128)(2,1)}), bf16[128,8,1024]{2,1,0:T(8,128)(2,1)S(1)}, u32[]{:S(2)}, u32[]{:S(2)}) async-start(bf16[128,8,1024]{2,1,0:T(8,128)(2,1)} %bitcast.16), calls=%async_computation.1 | async-start | bytes 4194304 | tf_op jit(solution)/shard_map/all_to_all | solution.py:512
  106.4 0.9 collective-permute-start.14
  107.3 2.7 %collective-permute-start.15 = (bf16[32,4096]{1,0:T(8,128)(2,1)S(1)}, bf16[32,4096]{1,0:T(8,128)(2,1)S(1)}, u32[]{:S(2)}, u32[]{:S(2)}) collective-permute-start(bf16[32,4096]{1,0:T(8,128)(2,1)S(1)} %get-tuple-element.62.n0), channel_id=1, source_target_pairs={{0,2},{1,3},{2,0},{3,1},{4,6},{5,7},{6,4},{7,5},{8,10},{9,11},{10,... | collective-permute-start | bytes 786440 | tf_op jit(solution)/shard_map/ppermute | solution.py:27
  110.0 1.4 collective-permute-start.16
  111.5 25.7 %collective-permute-done.14.n1 = bf16[32,4096]{1,0:T(8,128)(2,1)S(1)} collective-permute-done((bf16[32,4096]{1,0:T(8,128)(2,1)S(1)}, bf16[32,4096]{1,0:T(8,128)(2,1)S(1)}, u32[]{:S(2)}, u32[]{:S(2)}) %collective-permute-start.14) | collective-permute-done | bytes 262176 | tf_op jit(solution)/shard_map/ppermute | solution.py:27
  137.2 5.6 %collective-permute-done.15.n2 = bf16[32,4096]{1,0:T(8,128)(2,1)S(1)} collective-permute-done((bf16[32,4096]{1,0:T(8,128)(2,1)S(1)}, bf16[32,4096]{1,0:T(8,128)(2,1)S(1)}, u32[]{:S(2)}, u32[]{:S(2)}) %collective-permute-start.15) | collective-permute-done | bytes 262176 | tf_op jit(solution)/shard_map/ppermute | solution.py:27
  142.8 0.7 copy-done.11
  143.5 0.7 copy-done.12
  144.2 3.8 %shard_map.200 = (bf16[32,4096]{1,0:T(8,128)(2,1)S(1)}, bf16[32,4096]{1,0:T(8,128)(2,1)S(1)}, bf16[32,4096]{1,0:T(8,128)(2,1)S(1)}, bf16[32,4096]{1,0:T(8,128)(2,1)S(1)}) custom-call(bf16[32,4096]{1,0:T(8,128)(2,1)} %copy-done.4, bf16[32,4096]{1,0:T(8,128)(2,1)} %copy-done.10, bf16[32,4096]{1,0:T(8,128)(2,1)} %copy-done.11, bf16[32,4096]{1,0:T(8,128)(2,1)} %copy-done.12, ...), custom_call_target="tpu_custom_call" | custom-call | flops 805306368 | bytes 2097152 | tf_op jit(solution)/shard_map/pallas_call | solution.py:48
  148.0 0.7 copy-done.5
  148.7 1.3 collective-permute-start.18
  150.1 0.7 collective-permute-start.19
  150.8 7.1 %collective-permute-done.17.s1 = bf16[32,4096]{1,0:T(8,128)(2,1)S(1)} collective-permute-done((bf16[32,4096]{1,0:T(8,128)(2,1)S(1)}, bf16[32,4096]{1,0:T(8,128)(2,1)S(1)}, u32[]{:S(2)}, u32[]{:S(2)}) %collective-permute-start.17) | collective-permute-done | bytes 262176 | tf_op jit(solution)/shard_map/ppermute | solution.py:27
  157.9 1.5 collective-permute-done.18.s2
  159.5 4.1 %collective-permute-done.19.s3 = bf16[32,4096]{1,0:T(8,128)(2,1)S(1)} collective-permute-done((bf16[32,4096]{1,0:T(8,128)(2,1)S(1)}, bf16[32,4096]{1,0:T(8,128)(2,1)S(1)}, u32[]{:S(2)}, u32[]{:S(2)}) %collective-permute-start.19) | collective-permute-done | bytes 262176 | tf_op jit(solution)/shard_map/ppermute | solution.py:27
  163.6 0.7 copy-done.9
  164.3 2.6 %shard_map.201 = bf16[32,4096]{1,0:T(8,128)(2,1)} custom-call(bf16[1024,1024]{1,0:T(8,128)(2,1)S(1)} %bitcast.13, bf16[128,1024]{1,0:T(8,128)(2,1)S(1)} %get-tuple-element.60.mix, f32[32,4096]{1,0:T(8,128)} %copy-done.3, bf16[32,4096]{1,0:T(8,128)(2,1)} %copy-done.5, bf16[32,4096]{1,0:T(8,128)(2,1)} %copy-done.7, bf16[32,4096]{1,0:T(8,128)(2,1)} %copy-done.8, ...), custom_call_target="tpu_custom_call" | custom-call | flops 268435456 | bytes 2097152 | tf_op jit(solution)/shard_map/pallas_call | solution.py:48
  (35 shorter events, 0.1 us)
Async XLA Ops:
  1.1 7.4 %collective-permute-start.1 = (bf16[128,768]{1,0:T(8,128)(2,1)S(1)}, bf16[128,768]{1,0:T(8,128)(2,1)S(1)}, u32[]{:S(2)}, u32[]{:S(2)}) collective-permute-start(bf16[128,768]{1,0:T(8,128)(2,1)S(1)} %get-tuple-element.38.a.refs_3_), channel_id=1, source_target_pairs={{0,8},{4,36},{8,16},{12,44},{16,24},{20,52},{24,0},{28,60},{32,40}... | collective-permute-start | bytes 589832 | tf_op jit(solution)/shard_map/ppermute | solution.py:41
  2.9 5.7 %collective-permute-start.2 = (bf16[128,768]{1,0:T(8,128)(2,1)S(1)}, bf16[128,768]{1,0:T(8,128)(2,1)S(1)}, u32[]{:S(2)}, u32[]{:S(2)}) collective-permute-start(bf16[128,768]{1,0:T(8,128)(2,1)S(1)} %get-tuple-element.38.a.refs_3_), channel_id=1, source_target_pairs={{0,24},{4,100},{8,0},{12,108},{16,8},{20,116},{24,16},{28,124},{32... | collective-permute-start | bytes 589832 | tf_op jit(solution)/shard_map/ppermute | solution.py:41
  4.4 7.2 %collective-permute-start.3 = (bf16[128,768]{1,0:T(8,128)(2,1)S(1)}, bf16[128,768]{1,0:T(8,128)(2,1)S(1)}, u32[]{:S(2)}, u32[]{:S(2)}) collective-permute-start(bf16[128,768]{1,0:T(8,128)(2,1)S(1)} %get-tuple-element.38.a.refs_3_), channel_id=1, source_target_pairs={{0,16},{4,68},{8,24},{12,76},{16,0},{20,84},{24,8},{28,92},{32,48}... | collective-permute-start | bytes 589832 | tf_op jit(solution)/shard_map/ppermute | solution.py:41
  11.7 10.0 %collective-permute-start.4 = (bf16[2,128,768]{2,1,0:T(8,128)(2,1)S(1)}, bf16[2,128,768]{2,1,0:T(8,128)(2,1)S(1)}, u32[]{:S(2)}, u32[]{:S(2)}) collective-permute-start(bf16[2,128,768]{2,1,0:T(8,128)(2,1)S(1)} %get-tuple-element.40.refs_5_), channel_id=1, source_target_pairs={{0,32},{4,12},{8,40},{12,20},{16,48},{20,28},{24,56},{28,4},{32,64... | collective-permute-start | bytes 1179656 | tf_op jit(solution)/shard_map/ppermute | solution.py:41
  13.8 7.9 %collective-permute-start.6 = (bf16[2,128,768]{2,1,0:T(8,128)(2,1)S(1)}, bf16[2,128,768]{2,1,0:T(8,128)(2,1)S(1)}, u32[]{:S(2)}, u32[]{:S(2)}) collective-permute-start(bf16[2,128,768]{2,1,0:T(8,128)(2,1)S(1)} %get-tuple-element.41.refs_6_), channel_id=1, source_target_pairs={{0,96},{4,28},{8,104},{12,4},{16,112},{20,12},{24,120},{28,20},{32... | collective-permute-start | bytes 1179656 | tf_op jit(solution)/shard_map/ppermute | solution.py:41
  16.0 10.8 %collective-permute-start.8 = (bf16[2,128,768]{2,1,0:T(8,128)(2,1)S(1)}, bf16[2,128,768]{2,1,0:T(8,128)(2,1)S(1)}, u32[]{:S(2)}, u32[]{:S(2)}) collective-permute-start(bf16[2,128,768]{2,1,0:T(8,128)(2,1)S(1)} %get-tuple-element.40.refs_5_), channel_id=1, source_target_pairs={{0,96},{4,28},{8,104},{12,4},{16,112},{20,12},{24,120},{28,20},{32... | collective-permute-start | bytes 1179656 | tf_op jit(solution)/shard_map/ppermute | solution.py:41
  17.9 9.0 %collective-permute-start.9 = (bf16[2,128,768]{2,1,0:T(8,128)(2,1)S(1)}, bf16[2,128,768]{2,1,0:T(8,128)(2,1)S(1)}, u32[]{:S(2)}, u32[]{:S(2)}) collective-permute-start(bf16[2,128,768]{2,1,0:T(8,128)(2,1)S(1)} %get-tuple-element.41.refs_6_), channel_id=1, source_target_pairs={{0,32},{4,12},{8,40},{12,20},{16,48},{20,28},{24,56},{28,4},{32,64... | collective-permute-start | bytes 1179656 | tf_op jit(solution)/shard_map/ppermute | solution.py:41
  18.0 7.0 %collective-permute-start = (bf16[128,1024]{1,0:T(8,128)(2,1)S(1)}, bf16[128,1024]{1,0:T(8,128)(2,1)S(1)}, u32[]{:S(2)}, u32[]{:S(2)}) collective-permute-start(bf16[128,1024]{1,0:T(8,128)(2,1)S(1)} %get-tuple-element.37.refs_0_), channel_id=1, source_target_pairs={{0,4},{4,0},{1,5},{5,1},{2,6},{6,2},{3,7},{7,3},{8,12},{12,8},{9,1... | collective-permute-start | bytes 786440 | tf_op jit(solution)/shard_map/ppermute | solution.py:31
  21.6 9.5 %collective-permute-start.5 = (bf16[2,128,768]{2,1,0:T(8,128)(2,1)S(1)}, bf16[2,128,768]{2,1,0:T(8,128)(2,1)S(1)}, u32[]{:S(2)}, u32[]{:S(2)}) collective-permute-start(bf16[2,128,768]{2,1,0:T(8,128)(2,1)S(1)} %collective-permute-done.4.refs_3_), channel_id=1, source_target_pairs={{0,32},{4,12},{8,40},{12,20},{16,48},{20,28},{24,56},{28,4},{32,64... | collective-permute-start | bytes 1179656 | tf_op jit(solution)/shard_map/ppermute | solution.py:41
  21.6 9.5 %collective-permute-start.7 = (bf16[2,128,768]{2,1,0:T(8,128)(2,1)S(1)}, bf16[2,128,768]{2,1,0:T(8,128)(2,1)S(1)}, u32[]{:S(2)}, u32[]{:S(2)}) collective-permute-start(bf16[2,128,768]{2,1,0:T(8,128)(2,1)S(1)} %collective-permute-done.6.refs_6_), channel_id=1, source_target_pairs={{0,96},{4,28},{8,104},{12,4},{16,112},{20,12},{24,120},{28,20},{32... | collective-permute-start | bytes 1179656 | tf_op jit(solution)/shard_map/ppermute | solution.py:41
  26.9 9.1 %copy-start = (bf16[512,4096]{1,0:T(8,128)(2,1)S(1)}, bf16[512,4096]{1,0:T(8,128)(2,1)}, u32[]{:S(2)}) copy-start(bf16[512,4096]{1,0:T(8,128)(2,1)} %narrow.1) | copy-start | bytes 12582916
  26.9 9.1 %copy-start.1 = (bf16[512,4096]{1,0:T(8,128)(2,1)S(1)}, bf16[512,4096]{1,0:T(8,128)(2,1)}, u32[]{:S(2)}) copy-start(bf16[512,4096]{1,0:T(8,128)(2,1)} %broad.1) | copy-start | bytes 12582916
  33.7 2.3 %collective-permute-start.10 = (f32[128,1152]{1,0:T(8,128)S(1)}, f32[128,1152]{1,0:T(8,128)S(1)}, u32[]{:S(2)}, u32[]{:S(2)}) collective-permute-start(f32[128,1152]{1,0:T(8,128)S(1)} %get-tuple-element.54), channel_id=1, source_target_pairs={{0,4},{4,0},{1,5},{5,1},{2,6},{6,2},{3,7},{7,3},{8,12},{12,8},{9,1... | collective-permute-start | bytes 1769480 | tf_op jit(solution)/shard_map/ppermute | solution.py:31
  36.0 18.4 %copy-start.2 = (bf16[128,4096]{1,0:T(8,128)(2,1)S(1)}, bf16[128,4096]{1,0:T(8,128)(2,1)}, u32[]{:S(2)}) copy-start(bf16[128,4096]{1,0:T(8,128)(2,1)} %residual.1) | copy-start | bytes 3145732
  36.0 18.4 %copy-start.6 = (f32[4096]{0:T(1024)S(1)}, f32[4096]{0:T(1024)}, u32[]{:S(2)}) copy-start(f32[4096]{0:T(1024)} %param.31) | copy-start | bytes 49156
  38.1 9.6 %collective-permute-start.11 = (bf16[32,4096]{1,0:T(8,128)(2,1)S(1)}, bf16[32,4096]{1,0:T(8,128)(2,1)S(1)}, u32[]{:S(2)}, u32[]{:S(2)}) collective-permute-start(bf16[32,4096]{1,0:T(8,128)(2,1)S(1)} %get-tuple-element.56), channel_id=1, source_target_pairs={{0,1},{1,2},{2,3},{3,0},{4,5},{5,6},{6,7},{7,4},{8,9},{9,10},{10,1... | collective-permute-start | bytes 786440 | tf_op jit(solution)/shard_map/ppermute | solution.py:27
  39.6 14.7 %collective-permute-start.12 = (bf16[32,4096]{1,0:T(8,128)(2,1)S(1)}, bf16[32,4096]{1,0:T(8,128)(2,1)S(1)}, u32[]{:S(2)}, u32[]{:S(2)}) collective-permute-start(bf16[32,4096]{1,0:T(8,128)(2,1)S(1)} %get-tuple-element.57), channel_id=1, source_target_pairs={{0,2},{1,3},{2,0},{3,1},{4,6},{5,7},{6,4},{7,5},{8,10},{9,11},{10,... | collective-permute-start | bytes 786440 | tf_op jit(solution)/shard_map/ppermute | solution.py:27
  42.4 11.9 %collective-permute-start.13 = (bf16[32,4096]{1,0:T(8,128)(2,1)S(1)}, bf16[32,4096]{1,0:T(8,128)(2,1)S(1)}, u32[]{:S(2)}, u32[]{:S(2)}) collective-permute-start(bf16[32,4096]{1,0:T(8,128)(2,1)S(1)} %get-tuple-element.58), channel_id=1, source_target_pairs={{0,3},{1,0},{2,1},{3,2},{4,7},{5,4},{6,5},{7,6},{8,11},{9,8},{10,9... | collective-permute-start | bytes 786440 | tf_op jit(solution)/shard_map/ppermute | solution.py:27
  56.9 0.8 copy-start.3
  57.7 52.3 %copy-start.4 = (bf16[32,4096]{1,0:T(8,128)(2,1)}, bf16[32,4096]{1,0:T(8,128)(2,1)S(1)}, u32[]{:S(2)}) copy-start(bf16[32,4096]{1,0:T(8,128)(2,1)S(1)} %get-tuple-element.62.n0) | copy-start | bytes 786436
  57.7 38.3 %all-to-all-start = ((bf16[128,8,1024]{2,1,0:T(8,128)(2,1)}), bf16[128,8,1024]{2,1,0:T(8,128)(2,1)S(1)}, u32[]{:S(2)}, u32[]{:S(2)}) async-start(bf16[128,8,1024]{2,1,0:T(8,128)(2,1)} %bitcast.17), calls=%async_computation | async-start | bytes 4194304 | tf_op jit(solution)/shard_map/all_to_all | solution.py:469
  101.7 61.9 %all-to-all-start.1 = ((bf16[128,8,1024]{2,1,0:T(8,128)(2,1)}), bf16[128,8,1024]{2,1,0:T(8,128)(2,1)S(1)}, u32[]{:S(2)}, u32[]{:S(2)}) async-start(bf16[128,8,1024]{2,1,0:T(8,128)(2,1)} %bitcast.16), calls=%async_computation.1 | async-start | bytes 4194304 | tf_op jit(solution)/shard_map/all_to_all | solution.py:512
  106.4 30.8 %collective-permute-start.14 = (bf16[32,4096]{1,0:T(8,128)(2,1)S(1)}, bf16[32,4096]{1,0:T(8,128)(2,1)S(1)}, u32[]{:S(2)}, u32[]{:S(2)}) collective-permute-start(bf16[32,4096]{1,0:T(8,128)(2,1)S(1)} %get-tuple-element.62.n0), channel_id=1, source_target_pairs={{0,1},{1,2},{2,3},{3,0},{4,5},{5,6},{6,7},{7,4},{8,9},{9,10},{10,1... | collective-permute-start | bytes 786440 | tf_op jit(solution)/shard_map/ppermute | solution.py:27
  107.3 35.5 %collective-permute-start.15 = (bf16[32,4096]{1,0:T(8,128)(2,1)S(1)}, bf16[32,4096]{1,0:T(8,128)(2,1)S(1)}, u32[]{:S(2)}, u32[]{:S(2)}) collective-permute-start(bf16[32,4096]{1,0:T(8,128)(2,1)S(1)} %get-tuple-element.62.n0), channel_id=1, source_target_pairs={{0,2},{1,3},{2,0},{3,1},{4,6},{5,7},{6,4},{7,5},{8,10},{9,11},{10,... | collective-permute-start | bytes 786440 | tf_op jit(solution)/shard_map/ppermute | solution.py:27
  110.0 32.8 %collective-permute-start.16 = (bf16[32,4096]{1,0:T(8,128)(2,1)S(1)}, bf16[32,4096]{1,0:T(8,128)(2,1)S(1)}, u32[]{:S(2)}, u32[]{:S(2)}) collective-permute-start(bf16[32,4096]{1,0:T(8,128)(2,1)S(1)} %get-tuple-element.62.n0), channel_id=1, source_target_pairs={{0,3},{1,0},{2,1},{3,2},{4,7},{5,4},{6,5},{7,6},{8,11},{9,8},{10,9... | collective-permute-start | bytes 786440 | tf_op jit(solution)/shard_map/ppermute | solution.py:27
  137.2 5.6 %copy-start.10 = (bf16[32,4096]{1,0:T(8,128)(2,1)}, bf16[32,4096]{1,0:T(8,128)(2,1)S(1)}, u32[]{:S(2)}) copy-start(bf16[32,4096]{1,0:T(8,128)(2,1)S(1)} %collective-permute-done.14.n1) | copy-start | bytes 786436
  142.8 0.7 copy-start.11
  143.5 0.7 copy-start.12
  148.0 0.7 copy-start.5
  148.7 9.2 %collective-permute-start.17 = (bf16[32,4096]{1,0:T(8,128)(2,1)S(1)}, bf16[32,4096]{1,0:T(8,128)(2,1)S(1)}, u32[]{:S(2)}, u32[]{:S(2)}) collective-permute-start(bf16[32,4096]{1,0:T(8,128)(2,1)S(1)} %get-tuple-element.64), channel_id=1, source_target_pairs={{0,3},{1,0},{2,1},{3,2},{4,7},{5,4},{6,5},{7,6},{8,11},{9,8},{10,9... | collective-permute-start | bytes 786440 | tf_op jit(solution)/shard_map/ppermute | solution.py:27
  148.7 10.7 %collective-permute-start.18 = (bf16[32,4096]{1,0:T(8,128)(2,1)S(1)}, bf16[32,4096]{1,0:T(8,128)(2,1)S(1)}, u32[]{:S(2)}, u32[]{:S(2)}) collective-permute-start(bf16[32,4096]{1,0:T(8,128)(2,1)S(1)} %get-tuple-element.65), channel_id=1, source_target_pairs={{0,2},{1,3},{2,0},{3,1},{4,6},{5,7},{6,4},{7,5},{8,10},{9,11},{10,... | collective-permute-start | bytes 786440 | tf_op jit(solution)/shard_map/ppermute | solution.py:27
  150.1 13.6 %collective-permute-start.19 = (bf16[32,4096]{1,0:T(8,128)(2,1)S(1)}, bf16[32,4096]{1,0:T(8,128)(2,1)S(1)}, u32[]{:S(2)}, u32[]{:S(2)}) collective-permute-start(bf16[32,4096]{1,0:T(8,128)(2,1)S(1)} %get-tuple-element.66), channel_id=1, source_target_pairs={{0,1},{1,2},{2,3},{3,0},{4,5},{5,6},{6,7},{7,4},{8,9},{9,10},{10,1... | collective-permute-start | bytes 786440 | tf_op jit(solution)/shard_map/ppermute | solution.py:27
  157.9 5.7 %copy-start.7 = (bf16[32,4096]{1,0:T(8,128)(2,1)}, bf16[32,4096]{1,0:T(8,128)(2,1)S(1)}, u32[]{:S(2)}) copy-start(bf16[32,4096]{1,0:T(8,128)(2,1)S(1)} %collective-permute-done.17.s1) | copy-start | bytes 786436
  159.5 4.2 %copy-start.8 = (bf16[32,4096]{1,0:T(8,128)(2,1)}, bf16[32,4096]{1,0:T(8,128)(2,1)S(1)}, u32[]{:S(2)}) copy-start(bf16[32,4096]{1,0:T(8,128)(2,1)S(1)} %collective-permute-done.18.s2) | copy-start | bytes 786436
  163.6 0.7 copy-start.9

commit v9 on v8

--- a/solution.py
+++ b/solution.py
@@ -128,14 +128,15 @@
 
 def project_kernel(place, own, other, narrow, broad, *refs):
     outs, total, attn = refs[:4], *refs[4:]
-    a, b = own[:, 1024:], other[:, 1024:]
+    a, b = own[:, 1024:], other[:, 1024:].astype(F32)
+    b = b + pltpu.roll(b, 120, 1) + pltpu.roll(b, 112, 1)
     top = jnp.maximum(a, b)
     wa, wb = jnp.exp2(a - top), jnp.exp2(b - top)
     joined = wa + wb
     wa, wb = wa / joined, wb / joined
     for h in range(6):
         lo, size = (h * 128, 128) if h < 4 else (512 + (h - 4) * 256, 256)
-        value = own[:, lo : lo + size] * wa[:, h : h + 1] + other[:, lo : lo + size] * wb[:, h : h + 1]
+        value = own[:, lo : lo + size] * wa[:, h : h + 1] + other[:, lo : lo + size].astype(F32) * wb[:, h : h + 1]
         attn[:, lo : lo + size] = value.astype(BF)
     for at in range(0, 4096, 1024):
         part = jnp.dot(attn[:, :512], narrow[:, at : at + 1024], preferred_element_type=F32)
@@ -145,16 +146,17 @@
         outs[k][...] = total[pl.ds(((place[3] + k) % 4) * 32, 32), :].astype(BF)
 
 
-def dispatch_kernel(place, p0, p1, p2, p3, residual, gain, target, stream_out, normed_out, out, rows, sems):
+def dispatch_kernel(place, p0, p1, p2, p3, residual, gain, target, stream_out, normed_out, out, stream_held, rows, sems):
     mixture = p0[...].astype(F32) + p1[...].astype(F32) + p2[...].astype(F32) + p3[...].astype(F32)
     stream = residual[pl.ds(place[3] * 32, 32), :].astype(F32) + mixture
-    stream_out[...] = stream
+    stream_held[...] = stream
+    copies = [pltpu.make_async_copy(stream_held, stream_out, sems.at[4])]
+    copies[0].start()
     scale = lax.rsqrt(jnp.mean(stream * stream, axis=1, keepdims=True) + EPSILON)
     normed = (stream * scale * gain[...]).astype(BF)
     normed_out[...] = normed
     cut = jnp.concatenate([normed[:, g * 1024 : (g + 1) * 1024] for g in range(4)], axis=0)
     row = lax.broadcasted_iota(jnp.int32, (256, 128), 0)
-    copies = []
     for at in range(0, 1024, 256):
         pick = row + at == target[0:1, :]
         for k in range(1, 4):
@@ -195,11 +197,7 @@
             out[:, at : at + 1024] = part[k * 32 : (k + 1) * 32]
 
 
-def mark_kernel(value, out):
-    out[...] = value[...]
-
-
-def expert_kernel(mark, inbound, gate_hbm, up_hbm, down_hbm, out, x, rows_out, gate, up, down, weight_sems, sems):
+def expert_kernel(inbound, gate_hbm, up_hbm, down_hbm, out, x, rows_out, gate, up, down, weight_sems, sems):
     pairs = []
     for g in range(4):
         part = pl.ds(g * 1024, 1024)
@@ -236,18 +234,22 @@
         copy.wait()
 
 
-def combine_kernel(returned, mix, stream_hbm, s0, s1, s2, s3, out, stream, shared, sems):
+def fold_kernel(stream_hbm, s0, s1, s2, s3, out, stream, shared, sems):
     pairs = [(s, shared.at[k]) for k, s in enumerate((s0, s1, s2, s3))]
-    fetched = fetch(pairs + [(stream_hbm, stream)], sems)
-    routed = jnp.dot(mix[...], returned[...], preferred_element_type=F32)
+    fetched = fetch([(stream_hbm, stream)] + pairs, sems)
     for copy in fetched:
         copy.wait()
+    total = stream[...]
+    for k in range(4):
+        total = total + shared[k].astype(F32)
+    out[...] = total
+
+
+def combine_kernel(returned, mix, base, out):
+    routed = jnp.dot(mix[...], returned[...], preferred_element_type=F32)
     for g in range(4):
         lo, hi = g * 1024, (g + 1) * 1024
-        total = stream[:, lo:hi] + routed[g * 32 : (g + 1) * 32]
-        for k in range(4):
-            total = total + shared[k, :, lo:hi].astype(F32)
-        out[:, lo:hi] = total.astype(BF)
+        out[:, lo:hi] = (base[:, lo:hi] + routed[g * 32 : (g + 1) * 32]).astype(BF)
 
 
 def attend_kernel(counts, first, last, *refs):
@@ -324,7 +326,7 @@
                     o = acc / l
                     lse = m + jnp.log2(l)
                     for i in range(per):
-                        out[:, col + i * size : col + (i + 1) * size] = o[i * 128 : (i + 1) * 128]
+                        out[:, col + i * size : col + (i + 1) * size] = o[i * 128 : (i + 1) * 128].astype(out.dtype)
                         results[(side, base + h0 + i)] = lse[i * 128 : (i + 1) * 128]
                 else:
                     a_out = an_out if group == "n" else ab_out
@@ -336,8 +338,12 @@
         for side, out in ((0, own_out), (1, send_out)):
             stats = jnp.zeros((128, 128), F32)
             for h in range(6):
-                stats = jnp.where(lane == h, results[(side, h)], stats)
-            out[:, 1024:1152] = stats
+                stats = jnp.where(lane % 8 == h, results[(side, h)], stats)
+            if side == 1:
+                high = stats.astype(BF).astype(F32)
+                middle = (stats - high).astype(BF).astype(F32)
+                stats = jnp.where(lane < 8, high, jnp.where(lane < 16, middle, stats - high - middle))
+            out[:, 1024:1152] = stats.astype(out.dtype)
 
 
 def attend(q_own, q_other, core, tiles, state, last):
@@ -353,7 +359,7 @@
         operands += list(state)
         specs += [VMEM] * 4
     if last:
-        shapes = [jax.ShapeDtypeStruct((128, 1152), F32)] * 2
+        shapes = [jax.ShapeDtypeStruct((128, 1152), F32), jax.ShapeDtypeStruct((128, 1152), BF)]
     else:
         shapes = [
             jax.ShapeDtypeStruct((1536, 128), F32),
@@ -459,10 +465,10 @@
     stream, normed, outbound = call(
         dispatch_kernel,
         (place, p0, p1, p2, p3, residual, norm_gain.reshape(1, -1), target),
-        [shaped((32, 4096), F32), shaped((32, 4096), BF), pltpu.HBM((1024, 1024), BF)],
+        [pltpu.HBM((32, 4096), F32), shaped((32, 4096), BF), pltpu.HBM((1024, 1024), BF)],
         smem=(0,),
-        hbm_out=(2,),
-        scratch=[pltpu.VMEM((1024, 1024), BF), pltpu.SemaphoreType.DMA((4,))],
+        hbm_out=(0, 2),
+        scratch=[pltpu.VMEM((32, 4096), F32), pltpu.VMEM((1024, 1024), BF), pltpu.SemaphoreType.DMA((5,))],
         flops=2 * 1024 * 128 * 1024,
     )
     every = SP + ("tp",)
@@ -490,12 +496,11 @@
     s2 = shift(s2, "tp", 2)
     s3 = shift(s3, "tp", 1)
 
-    (mark,) = call(mark_kernel, (target,), [shaped((4, 128), jnp.int32)])
     (result,) = call(
         expert_kernel,
-        (mark, inbound.reshape(1024, 1024), expert_gate, expert_up, expert_down),
+        (inbound.reshape(1024, 1024), expert_gate, expert_up, expert_down),
         [pltpu.HBM((1024, 1024), BF)],
-        hbm=(2, 3, 4),
+        hbm=(1, 2, 3),
         hbm_out=(0,),
         scratch=[
             pltpu.VMEM((256, 4096), BF),
@@ -510,12 +515,17 @@
         flops=2 * 256 * 4096 * 768,
     )
     returned = lax.all_to_all(result.reshape(128, 8, 1024), every, 0, 0, tiled=True)
+    (base,) = call(
+        fold_kernel,
+        (stream, s0, s1, s2, s3),
+        [shaped((32, 4096), F32)],
+        hbm=range(5),
+        scratch=[pltpu.VMEM((32, 4096), F32), pltpu.VMEM((4, 32, 4096), BF), pltpu.SemaphoreType.DMA((5,))],
+    )
     (out,) = call(
         combine_kernel,
-        (returned.reshape(1024, 1024), mix, stream, s0, s1, s2, s3),
+        (returned.reshape(1024, 1024), mix, base),
         [shaped((32, 4096), BF)],
-        hbm=(2, 3, 4, 5, 6),
-        scratch=[pltpu.VMEM((32, 4096), F32), pltpu.VMEM((4, 32, 4096), BF), pltpu.SemaphoreType.DMA((5,))],
         flops=2 * 128 * 1024 * 1024,
     )
     return out

time: 168 us -> 167 us (level)
  blocking collectives: 0 us -> 38.3 us
  waiting for transfers between devices: 94.1 us -> 63.6 us
  starting transfers between devices: 41.1 us -> 32.8 us
    all_to_all x0 -> x1, blocking collectives: none -> 38.3 us  [local(): lax.all_to_all(outbound.reshape(128, 8, 1024), every, 0, 0, tiled=True)]
    all_to_all x1 -> x0, waiting for transfers between devices: 30 us -> none  [local(): lax.all_to_all(outbound.reshape(128, 8, 1024), every, 0, 0, tiled=True)]
    all_to_all x1 -> x0, starting transfers between devices: 8.26 us -> none  [local(): lax.all_to_all(outbound.reshape(128, 8, 1024), every, 0, 0, tiled=True)]
    unnamed x26 -> x24, local copies, waits for them, and re-layouts: 3.6 us -> 2.85 us
  transfers between devices with their start and end apart: 22 -> 21, of which waited for: 13 -> 12; matrix products, arithmetic and copies ran while one was open for 0% -> 0% of each run, Pallas kernels for 7% -> 8%
where the time goes in v9:
time: 167 us; the launch traced here: 166 us
  waiting for transfers between devices  63.6 us (38%)
  blocking collectives  38.3 us (23%)
  starting transfers between devices  32.8 us (20%)
  Pallas kernels  28.1 us (17%)
  local copies, waits for them, and re-layouts  2.85 us (2%)
    ppermute x9, waiting for transfers between devices, shift(): return lax.ppermute(x, axis, [(i, (i + k) % 4) for i in range(4)])  54.6 us
    all_to_all x1, blocking collectives, local(): lax.all_to_all(outbound.reshape(128, 8, 1024), every, 0, 0, tiled=True)  38.3 us
    pallas_call x9, Pallas kernels, call(): pl.pallas_call(kernel, out_shape=shapes, in_specs=[SMEM if i in smem else...  20.1 us
    ppermute x9, starting transfers between devices, turn(): return lax.ppermute(x, SP, pairs)  15 us
    ppermute x9, starting transfers between devices, shift(): return lax.ppermute(x, axis, [(i, (i + k) % 4) for i in range(4)])  12.8 us
    pallas_call x3, Pallas kernels, attend(): pl.pallas_call(functools.partial(attend_kernel, counts, state is None, la...  8.01 us
    ppermute x9, waiting for transfers between devices, turn(): return lax.ppermute(x, SP, pairs)  7.39 us
    all_to_all x1, starting transfers between devices, local(): lax.all_to_all(result.reshape(128, 8, 1024), every, 0, 0, tiled=True)  4.67 us
  transfers between devices with their start and end apart: 21, of which 12 were waited for; matrix products, arithmetic and copies ran while one was open for 0% of the time, Pallas kernels for 8%

profile of v9, /device:TPU:0, one launch (start us, length us, event | category | flops | bytes accessed | tf_op | source)
XLA Modules:
  0.0 165.9 jit_solution(2042265072700599949)
XLA Ops:
  0.0 1.1 shard_map.190
  1.1 1.8 %collective-permute-start.1 = (bf16[128,768]{1,0:T(8,128)(2,1)S(1)}, bf16[128,768]{1,0:T(8,128)(2,1)S(1)}, u32[]{:S(2)}, u32[]{:S(2)}) collective-permute-start(bf16[128,768]{1,0:T(8,128)(2,1)S(1)} %get-tuple-element.37.a.refs_3_), channel_id=1, source_target_pairs={{0,8},{4,36},{8,16},{12,44},{16,24},{20,52},{24,0},{28,60},{32,40}... | collective-permute-start | bytes 589832 | tf_op jit(solution)/shard_map/ppermute | solution.py:41
  2.9 1.5 collective-permute-start.2
  4.4 2.1 %collective-permute-start.3 = (bf16[128,768]{1,0:T(8,128)(2,1)S(1)}, bf16[128,768]{1,0:T(8,128)(2,1)S(1)}, u32[]{:S(2)}, u32[]{:S(2)}) collective-permute-start(bf16[128,768]{1,0:T(8,128)(2,1)S(1)} %get-tuple-element.37.a.refs_3_), channel_id=1, source_target_pairs={{0,16},{4,68},{8,24},{12,76},{16,0},{20,84},{24,8},{28,92},{32,48}... | collective-permute-start | bytes 589832 | tf_op jit(solution)/shard_map/ppermute | solution.py:41
  6.5 0.1 pad_add_fusion.place
  6.6 2.0 %shard_map.191 = (s32[4,128]{1,0:T(4,128)S(1)}, bf16[128,1024]{1,0:T(8,128)(2,1)S(1)}, f32[8,128]{1,0:T(8,128)S(1)}, f32[8,384]{1,0:T(8,128)S(1)}, f32[8,1024]{1,0:T(8,128)S(1)}, /*index=5*/f32[8,512]{1,0:T(8,128)S(1)}) custom-call(s32[4]{0:T(128)S(1)} %pad_add_fusion.place, s32[4,32]{1,0:T(4,128)} %bitcast.20, f32[4,32]{1,0:T(4,128)} %bitcast.21, ...), custom_call_target="tpu_custom_call" | custom-call | bytes 2097152 | tf_op jit(solution)/shard_map/pallas_call | solution.py:48
  8.6 3.0 %collective-permute-done.3.d = bf16[128,768]{1,0:T(8,128)(2,1)S(1)} collective-permute-done((bf16[128,768]{1,0:T(8,128)(2,1)S(1)}, bf16[128,768]{1,0:T(8,128)(2,1)S(1)}, u32[]{:S(2)}, u32[]{:S(2)}) %collective-permute-start.3) | collective-permute-done | bytes 196640 | tf_op jit(solution)/shard_map/ppermute | solution.py:41
  11.6 0.1 shard_map.192
  11.7 2.1 %collective-permute-start.4 = (bf16[2,128,768]{2,1,0:T(8,128)(2,1)S(1)}, bf16[2,128,768]{2,1,0:T(8,128)(2,1)S(1)}, u32[]{:S(2)}, u32[]{:S(2)}) collective-permute-start(bf16[2,128,768]{2,1,0:T(8,128)(2,1)S(1)} %get-tuple-element.40.refs_5_), channel_id=1, source_target_pairs={{0,32},{4,12},{8,40},{12,20},{16,48},{20,28},{24,56},{28,4},{32,64... | collective-permute-start | bytes 1179656 | tf_op jit(solution)/shard_map/ppermute | solution.py:41
  13.8 2.2 %collective-permute-start.6 = (bf16[2,128,768]{2,1,0:T(8,128)(2,1)S(1)}, bf16[2,128,768]{2,1,0:T(8,128)(2,1)S(1)}, u32[]{:S(2)}, u32[]{:S(2)}) collective-permute-start(bf16[2,128,768]{2,1,0:T(8,128)(2,1)S(1)} %get-tuple-element.41.refs_6_), channel_id=1, source_target_pairs={{0,96},{4,28},{8,104},{12,4},{16,112},{20,12},{24,120},{28,20},{32... | collective-permute-start | bytes 1179656 | tf_op jit(solution)/shard_map/ppermute | solution.py:41
  16.0 1.9 %collective-permute-start.8 = (bf16[2,128,768]{2,1,0:T(8,128)(2,1)S(1)}, bf16[2,128,768]{2,1,0:T(8,128)(2,1)S(1)}, u32[]{:S(2)}, u32[]{:S(2)}) collective-permute-start(bf16[2,128,768]{2,1,0:T(8,128)(2,1)S(1)} %get-tuple-element.40.refs_5_), channel_id=1, source_target_pairs={{0,96},{4,28},{8,104},{12,4},{16,112},{20,12},{24,120},{28,20},{32... | collective-permute-start | bytes 1179656 | tf_op jit(solution)/shard_map/ppermute | solution.py:41
  17.9 0.1 collective-permute-start.9
  18.0 3.6 %collective-permute-done.4.refs_3_ = bf16[2,128,768]{2,1,0:T(8,128)(2,1)S(1)} collective-permute-done((bf16[2,128,768]{2,1,0:T(8,128)(2,1)S(1)}, bf16[2,128,768]{2,1,0:T(8,128)(2,1)S(1)}, u32[]{:S(2)}, u32[]{:S(2)}) %collective-permute-start.4) | collective-permute-done | bytes 393248 | tf_op jit(solution)/shard_map/ppermute | solution.py:41
  21.6 3.3 %collective-permute-start.7 = (bf16[2,128,768]{2,1,0:T(8,128)(2,1)S(1)}, bf16[2,128,768]{2,1,0:T(8,128)(2,1)S(1)}, u32[]{:S(2)}, u32[]{:S(2)}) collective-permute-start(bf16[2,128,768]{2,1,0:T(8,128)(2,1)S(1)} %collective-permute-done.6.refs_6_), channel_id=1, source_target_pairs={{0,96},{4,28},{8,104},{12,4},{16,112},{20,12},{24,120},{28,20},{32... | collective-permute-start | bytes 1179656 | tf_op jit(solution)/shard_map/ppermute | solution.py:41
  25.0 1.9 %shard_map.193 = (f32[1536,128]{1,0:T(8,128)S(1)}, f32[1536,128]{1,0:T(8,128)S(1)}, f32[1024,128]{1,0:T(8,128)S(1)}, f32[512,256]{1,0:T(8,128)S(1)}) custom-call(bf16[128,1024]{1,0:T(8,128)(2,1)S(1)} %get-tuple-element.36.refs_0_, bf16[128,1024]{1,0:T(8,128)(2,1)S(1)} %collective-permute-done.refs_1_, s32[1]{0:T(128)} %bitcast.2.refs_2_, ...), custom_call_target="tpu_custom_call" | custom-call | flops 536870912 | bytes 4194304 | tf_op jit(solution)/shard_map/pallas_call | solution.py:370
  26.8 0.1 collective-permute-done.9.refs_5_
  26.9 3.6 %shard_map.194 = (f32[1536,128]{1,0:T(8,128)S(1)}, f32[1536,128]{1,0:T(8,128)S(1)}, f32[1024,128]{1,0:T(8,128)S(1)}, f32[512,256]{1,0:T(8,128)S(1)}) custom-call(bf16[128,1024]{1,0:T(8,128)(2,1)S(1)} %get-tuple-element.36.refs_0_, bf16[128,1024]{1,0:T(8,128)(2,1)S(1)} %collective-permute-done.refs_1_, s32[1]{0:T(128)} %bitcast.2.refs_2_, ...), custom_call_target="tpu_custom_call" | custom-call | flops 1073741824 | bytes 4194304 | tf_op jit(solution)/shard_map/pallas_call | solution.py:370
  30.5 0.6 collective-permute-done.5.refs_3_
  31.1 2.6 %shard_map.195 = (f32[128,1152]{1,0:T(8,128)S(1)}, bf16[128,1152]{1,0:T(8,128)(2,1)S(1)}) custom-call(bf16[128,1024]{1,0:T(8,128)(2,1)S(1)} %get-tuple-element.36.refs_0_, bf16[128,1024]{1,0:T(8,128)(2,1)S(1)} %collective-permute-done.refs_1_, s32[1]{0:T(128)} %bitcast.2.refs_2_, bf16[2,128,768]{2,1,0:T(8,128)(2,1)S(1)} %collective-permute-done.5.refs_3_, ...), custom_call_target="tpu_custom_call" | custom-call | flops 536870912 | bytes 4194304 | tf_op jit(solution)/shard_map/pallas_call | solution.py:370
  33.7 0.3 collective-permute-start.10
  34.0 1.6 collective-permute-done.10.other
  35.6 2.2 %shard_map.196 = (bf16[32,4096]{1,0:T(8,128)(2,1)S(1)}, bf16[32,4096]{1,0:T(8,128)(2,1)S(1)}, bf16[32,4096]{1,0:T(8,128)(2,1)S(1)}, bf16[32,4096]{1,0:T(8,128)(2,1)S(1)}) custom-call(s32[4]{0:T(128)S(1)} %pad_add_fusion.place, f32[128,1152]{1,0:T(8,128)S(1)} %get-tuple-element.53.own, bf16[128,1152]{1,0:T(8,128)(2,1)S(1)} %collective-permute-done.10.other, ...), custom_call_target="tpu_custom_call" | custom-call | flops 1073741824 | bytes 2097152 | tf_op jit(solution)/shard_map/pallas_call | solution.py:48
  37.8 1.6 collective-permute-start.11
  39.3 2.7 %collective-permute-start.12 = (bf16[32,4096]{1,0:T(8,128)(2,1)S(1)}, bf16[32,4096]{1,0:T(8,128)(2,1)S(1)}, u32[]{:S(2)}, u32[]{:S(2)}) collective-permute-start(bf16[32,4096]{1,0:T(8,128)(2,1)S(1)} %get-tuple-element.57), channel_id=1, source_target_pairs={{0,2},{1,3},{2,0},{3,1},{4,6},{5,7},{6,4},{7,5},{8,10},{9,11},{10,... | collective-permute-start | bytes 786440 | tf_op jit(solution)/shard_map/ppermute | solution.py:27
  42.0 1.4 collective-permute-start.13
  43.5 3.9 %collective-permute-done.11.p1 = bf16[32,4096]{1,0:T(8,128)(2,1)S(1)} collective-permute-done((bf16[32,4096]{1,0:T(8,128)(2,1)S(1)}, bf16[32,4096]{1,0:T(8,128)(2,1)S(1)}, u32[]{:S(2)}, u32[]{:S(2)}) %collective-permute-start.11) | collective-permute-done | bytes 262176 | tf_op jit(solution)/shard_map/ppermute | solution.py:27
  47.4 6.6 %collective-permute-done.12.p2 = bf16[32,4096]{1,0:T(8,128)(2,1)S(1)} collective-permute-done((bf16[32,4096]{1,0:T(8,128)(2,1)S(1)}, bf16[32,4096]{1,0:T(8,128)(2,1)S(1)}, u32[]{:S(2)}, u32[]{:S(2)}) %collective-permute-start.12) | collective-permute-done | bytes 262176 | tf_op jit(solution)/shard_map/ppermute | solution.py:27
  54.0 2.6 %shard_map.197 = (f32[32,4096]{1,0:T(8,128)}, bf16[32,4096]{1,0:T(8,128)(2,1)S(1)}, bf16[1024,1024]{1,0:T(8,128)(2,1)}) custom-call(s32[4]{0:T(128)S(1)} %pad_add_fusion.place, bf16[32,4096]{1,0:T(8,128)(2,1)S(1)} %get-tuple-element.55.p0, bf16[32,4096]{1,0:T(8,128)(2,1)S(1)} %collective-permute-done.11.p1, bf16[32,4096]{1,0:T(8,128)(2,1)S(1)} %collective-permute-done.12.p2, ...), custom_call_target="tpu_custom_call" | custom-call | flops 268435456 | bytes 2097152 | tf_op jit(solution)/shard_map/pallas_call | solution.py:48
  56.6 38.3 %all_to_all.10 = bf16[128,8,1024]{2,1,0:T(8,128)(2,1)S(1)} all-to-all(bf16[128,8,1024]{2,1,0:T(8,128)(2,1)} %bitcast.17), channel_id=1, replica_groups=mesh['z'=4,'y'=4,'c'=2,'tp'=4] {'z','y','c','tp'}, dimensions={0} | all-to-all | bytes 4194304 | tf_op jit(solution)/shard_map/all_to_all | solution.py:475
  94.9 5.7 %shard_map.198 = bf16[1024,1024]{1,0:T(8,128)(2,1)} custom-call(bf16[1024,1024]{1,0:T(8,128)(2,1)S(1)} %bitcast.13, bf16[1,4096,256]{2,1,0:T(8,128)(2,1)} %gate_hbm.2, bf16[1,4096,256]{2,1,0:T(8,128)(2,1)} %up_hbm.2, bf16[1,256,4096]{2,1,0:T(8,128)(2,1)} %down_hbm.2), custom_call_target="tpu_custom_call" | custom-call | flops 1610612736 | bytes 2097152 | tf_op jit(solution)/shard_map/pallas_call | solution.py:48
  100.6 4.7 %all-to-all-start.1 = ((bf16[128,8,1024]{2,1,0:T(8,128)(2,1)}), bf16[128,8,1024]{2,1,0:T(8,128)(2,1)S(1)}, u32[]{:S(2)}, u32[]{:S(2)}) async-start(bf16[128,8,1024]{2,1,0:T(8,128)(2,1)} %bitcast.16), calls=%async_computation.1 | async-start | bytes 4194304 | tf_op jit(solution)/shard_map/all_to_all | solution.py:517
  105.3 0.9 collective-permute-start.14
  106.2 2.7 %collective-permute-start.15 = (bf16[32,4096]{1,0:T(8,128)(2,1)S(1)}, bf16[32,4096]{1,0:T(8,128)(2,1)S(1)}, u32[]{:S(2)}, u32[]{:S(2)}) collective-permute-start(bf16[32,4096]{1,0:T(8,128)(2,1)S(1)} %get-tuple-element.62.n0), channel_id=1, source_target_pairs={{0,2},{1,3},{2,0},{3,1},{4,6},{5,7},{6,4},{7,5},{8,10},{9,11},{10,... | collective-permute-start | bytes 786440 | tf_op jit(solution)/shard_map/ppermute | solution.py:27
  108.9 1.4 collective-permute-start.16
  110.4 25.7 %collective-permute-done.14.n1 = bf16[32,4096]{1,0:T(8,128)(2,1)S(1)} collective-permute-done((bf16[32,4096]{1,0:T(8,128)(2,1)S(1)}, bf16[32,4096]{1,0:T(8,128)(2,1)S(1)}, u32[]{:S(2)}, u32[]{:S(2)}) %collective-permute-start.14) | collective-permute-done | bytes 262176 | tf_op jit(solution)/shard_map/ppermute | solution.py:27
  136.1 5.6 %collective-permute-done.15.n2 = bf16[32,4096]{1,0:T(8,128)(2,1)S(1)} collective-permute-done((bf16[32,4096]{1,0:T(8,128)(2,1)S(1)}, bf16[32,4096]{1,0:T(8,128)(2,1)S(1)}, u32[]{:S(2)}, u32[]{:S(2)}) %collective-permute-start.15) | collective-permute-done | bytes 262176 | tf_op jit(solution)/shard_map/ppermute | solution.py:27
  141.7 0.7 copy-done.7
  142.4 0.7 copy-done.8
  143.1 3.8 %shard_map.199 = (bf16[32,4096]{1,0:T(8,128)(2,1)S(1)}, bf16[32,4096]{1,0:T(8,128)(2,1)S(1)}, bf16[32,4096]{1,0:T(8,128)(2,1)S(1)}, bf16[32,4096]{1,0:T(8,128)(2,1)S(1)}) custom-call(bf16[32,4096]{1,0:T(8,128)(2,1)} %copy-done.3, bf16[32,4096]{1,0:T(8,128)(2,1)} %copy-done.6, bf16[32,4096]{1,0:T(8,128)(2,1)} %copy-done.7, bf16[32,4096]{1,0:T(8,128)(2,1)} %copy-done.8, ...), custom_call_target="tpu_custom_call" | custom-call | flops 805306368 | bytes 2097152 | tf_op jit(solution)/shard_map/pallas_call | solution.py:48
  146.9 0.7 copy-done.4
  147.6 1.3 collective-permute-start.18
  149.0 0.7 collective-permute-start.19
  149.7 7.1 %collective-permute-done.17.s1 = bf16[32,4096]{1,0:T(8,128)(2,1)S(1)} collective-permute-done((bf16[32,4096]{1,0:T(8,128)(2,1)S(1)}, bf16[32,4096]{1,0:T(8,128)(2,1)S(1)}, u32[]{:S(2)}, u32[]{:S(2)}) %collective-permute-start.17) | collective-permute-done | bytes 262176 | tf_op jit(solution)/shard_map/ppermute | solution.py:27
  156.8 1.5 collective-permute-done.18.s2
  158.4 4.1 %collective-permute-done.19.s3 = bf16[32,4096]{1,0:T(8,128)(2,1)S(1)} collective-permute-done((bf16[32,4096]{1,0:T(8,128)(2,1)S(1)}, bf16[32,4096]{1,0:T(8,128)(2,1)S(1)}, u32[]{:S(2)}, u32[]{:S(2)}) %collective-permute-start.19) | collective-permute-done | bytes 262176 | tf_op jit(solution)/shard_map/ppermute | solution.py:27
  162.5 0.7 copy-done.11
  163.2 1.5 shard_map.200.base
  164.8 1.2 shard_map.201
  (32 shorter events, 0.1 us)
Async XLA Ops:
  1.1 7.4 %collective-permute-start.1 = (bf16[128,768]{1,0:T(8,128)(2,1)S(1)}, bf16[128,768]{1,0:T(8,128)(2,1)S(1)}, u32[]{:S(2)}, u32[]{:S(2)}) collective-permute-start(bf16[128,768]{1,0:T(8,128)(2,1)S(1)} %get-tuple-element.37.a.refs_3_), channel_id=1, source_target_pairs={{0,8},{4,36},{8,16},{12,44},{16,24},{20,52},{24,0},{28,60},{32,40}... | collective-permute-start | bytes 589832 | tf_op jit(solution)/shard_map/ppermute | solution.py:41
  2.9 5.7 %collective-permute-start.2 = (bf16[128,768]{1,0:T(8,128)(2,1)S(1)}, bf16[128,768]{1,0:T(8,128)(2,1)S(1)}, u32[]{:S(2)}, u32[]{:S(2)}) collective-permute-start(bf16[128,768]{1,0:T(8,128)(2,1)S(1)} %get-tuple-element.37.a.refs_3_), channel_id=1, source_target_pairs={{0,24},{4,100},{8,0},{12,108},{16,8},{20,116},{24,16},{28,124},{32... | collective-permute-start | bytes 589832 | tf_op jit(solution)/shard_map/ppermute | solution.py:41
  4.4 7.2 %collective-permute-start.3 = (bf16[128,768]{1,0:T(8,128)(2,1)S(1)}, bf16[128,768]{1,0:T(8,128)(2,1)S(1)}, u32[]{:S(2)}, u32[]{:S(2)}) collective-permute-start(bf16[128,768]{1,0:T(8,128)(2,1)S(1)} %get-tuple-element.37.a.refs_3_), channel_id=1, source_target_pairs={{0,16},{4,68},{8,24},{12,76},{16,0},{20,84},{24,8},{28,92},{32,48}... | collective-permute-start | bytes 589832 | tf_op jit(solution)/shard_map/ppermute | solution.py:41
  11.7 10.0 %collective-permute-start.4 = (bf16[2,128,768]{2,1,0:T(8,128)(2,1)S(1)}, bf16[2,128,768]{2,1,0:T(8,128)(2,1)S(1)}, u32[]{:S(2)}, u32[]{:S(2)}) collective-permute-start(bf16[2,128,768]{2,1,0:T(8,128)(2,1)S(1)} %get-tuple-element.40.refs_5_), channel_id=1, source_target_pairs={{0,32},{4,12},{8,40},{12,20},{16,48},{20,28},{24,56},{28,4},{32,64... | collective-permute-start | bytes 1179656 | tf_op jit(solution)/shard_map/ppermute | solution.py:41
  13.8 7.9 %collective-permute-start.6 = (bf16[2,128,768]{2,1,0:T(8,128)(2,1)S(1)}, bf16[2,128,768]{2,1,0:T(8,128)(2,1)S(1)}, u32[]{:S(2)}, u32[]{:S(2)}) collective-permute-start(bf16[2,128,768]{2,1,0:T(8,128)(2,1)S(1)} %get-tuple-element.41.refs_6_), channel_id=1, source_target_pairs={{0,96},{4,28},{8,104},{12,4},{16,112},{20,12},{24,120},{28,20},{32... | collective-permute-start | bytes 1179656 | tf_op jit(solution)/shard_map/ppermute | solution.py:41
  16.0 10.9 %collective-permute-start.8 = (bf16[2,128,768]{2,1,0:T(8,128)(2,1)S(1)}, bf16[2,128,768]{2,1,0:T(8,128)(2,1)S(1)}, u32[]{:S(2)}, u32[]{:S(2)}) collective-permute-start(bf16[2,128,768]{2,1,0:T(8,128)(2,1)S(1)} %get-tuple-element.40.refs_5_), channel_id=1, source_target_pairs={{0,96},{4,28},{8,104},{12,4},{16,112},{20,12},{24,120},{28,20},{32... | collective-permute-start | bytes 1179656 | tf_op jit(solution)/shard_map/ppermute | solution.py:41
  17.9 9.0 %collective-permute-start.9 = (bf16[2,128,768]{2,1,0:T(8,128)(2,1)S(1)}, bf16[2,128,768]{2,1,0:T(8,128)(2,1)S(1)}, u32[]{:S(2)}, u32[]{:S(2)}) collective-permute-start(bf16[2,128,768]{2,1,0:T(8,128)(2,1)S(1)} %get-tuple-element.41.refs_6_), channel_id=1, source_target_pairs={{0,32},{4,12},{8,40},{12,20},{16,48},{20,28},{24,56},{28,4},{32,64... | collective-permute-start | bytes 1179656 | tf_op jit(solution)/shard_map/ppermute | solution.py:41
  18.0 7.0 %collective-permute-start = (bf16[128,1024]{1,0:T(8,128)(2,1)S(1)}, bf16[128,1024]{1,0:T(8,128)(2,1)S(1)}, u32[]{:S(2)}, u32[]{:S(2)}) collective-permute-start(bf16[128,1024]{1,0:T(8,128)(2,1)S(1)} %get-tuple-element.36.refs_0_), channel_id=1, source_target_pairs={{0,4},{4,0},{1,5},{5,1},{2,6},{6,2},{3,7},{7,3},{8,12},{12,8},{9,1... | collective-permute-start | bytes 786440 | tf_op jit(solution)/shard_map/ppermute | solution.py:31
  21.6 9.5 %collective-permute-start.5 = (bf16[2,128,768]{2,1,0:T(8,128)(2,1)S(1)}, bf16[2,128,768]{2,1,0:T(8,128)(2,1)S(1)}, u32[]{:S(2)}, u32[]{:S(2)}) collective-permute-start(bf16[2,128,768]{2,1,0:T(8,128)(2,1)S(1)} %collective-permute-done.4.refs_3_), channel_id=1, source_target_pairs={{0,32},{4,12},{8,40},{12,20},{16,48},{20,28},{24,56},{28,4},{32,64... | collective-permute-start | bytes 1179656 | tf_op jit(solution)/shard_map/ppermute | solution.py:41
  21.6 9.5 %collective-permute-start.7 = (bf16[2,128,768]{2,1,0:T(8,128)(2,1)S(1)}, bf16[2,128,768]{2,1,0:T(8,128)(2,1)S(1)}, u32[]{:S(2)}, u32[]{:S(2)}) collective-permute-start(bf16[2,128,768]{2,1,0:T(8,128)(2,1)S(1)} %collective-permute-done.6.refs_6_), channel_id=1, source_target_pairs={{0,96},{4,28},{8,104},{12,4},{16,112},{20,12},{24,120},{28,20},{32... | collective-permute-start | bytes 1179656 | tf_op jit(solution)/shard_map/ppermute | solution.py:41
  26.9 8.7 %copy-start = (bf16[512,4096]{1,0:T(8,128)(2,1)S(1)}, bf16[512,4096]{1,0:T(8,128)(2,1)}, u32[]{:S(2)}) copy-start(bf16[512,4096]{1,0:T(8,128)(2,1)} %narrow.1) | copy-start | bytes 12582916
  26.9 8.7 %copy-start.1 = (bf16[512,4096]{1,0:T(8,128)(2,1)S(1)}, bf16[512,4096]{1,0:T(8,128)(2,1)}, u32[]{:S(2)}) copy-start(bf16[512,4096]{1,0:T(8,128)(2,1)} %broad.1) | copy-start | bytes 12582916
  33.7 1.8 %collective-permute-start.10 = (bf16[128,1152]{1,0:T(8,128)(2,1)S(1)}, bf16[128,1152]{1,0:T(8,128)(2,1)S(1)}, u32[]{:S(2)}, u32[]{:S(2)}) collective-permute-start(bf16[128,1152]{1,0:T(8,128)(2,1)S(1)} %get-tuple-element.54), channel_id=1, source_target_pairs={{0,4},{4,0},{1,5},{5,1},{2,6},{6,2},{3,7},{7,3},{8,12},{12,8},{9,1... | collective-permute-start | bytes 884744 | tf_op jit(solution)/shard_map/ppermute | solution.py:31
  35.6 18.4 %copy-start.2 = (bf16[128,4096]{1,0:T(8,128)(2,1)S(1)}, bf16[128,4096]{1,0:T(8,128)(2,1)}, u32[]{:S(2)}) copy-start(bf16[128,4096]{1,0:T(8,128)(2,1)} %residual.1) | copy-start | bytes 3145732
  35.6 18.4 %copy-start.5 = (f32[4096]{0:T(1024)S(1)}, f32[4096]{0:T(1024)}, u32[]{:S(2)}) copy-start(f32[4096]{0:T(1024)} %param.31) | copy-start | bytes 49156
  37.8 9.6 %collective-permute-start.11 = (bf16[32,4096]{1,0:T(8,128)(2,1)S(1)}, bf16[32,4096]{1,0:T(8,128)(2,1)S(1)}, u32[]{:S(2)}, u32[]{:S(2)}) collective-permute-start(bf16[32,4096]{1,0:T(8,128)(2,1)S(1)} %get-tuple-element.56), channel_id=1, source_target_pairs={{0,1},{1,2},{2,3},{3,0},{4,5},{5,6},{6,7},{7,4},{8,9},{9,10},{10,1... | collective-permute-start | bytes 786440 | tf_op jit(solution)/shard_map/ppermute | solution.py:27
  39.3 14.7 %collective-permute-start.12 = (bf16[32,4096]{1,0:T(8,128)(2,1)S(1)}, bf16[32,4096]{1,0:T(8,128)(2,1)S(1)}, u32[]{:S(2)}, u32[]{:S(2)}) collective-permute-start(bf16[32,4096]{1,0:T(8,128)(2,1)S(1)} %get-tuple-element.57), channel_id=1, source_target_pairs={{0,2},{1,3},{2,0},{3,1},{4,6},{5,7},{6,4},{7,5},{8,10},{9,11},{10,... | collective-permute-start | bytes 786440 | tf_op jit(solution)/shard_map/ppermute | solution.py:27
  42.0 11.9 %collective-permute-start.13 = (bf16[32,4096]{1,0:T(8,128)(2,1)S(1)}, bf16[32,4096]{1,0:T(8,128)(2,1)S(1)}, u32[]{:S(2)}, u32[]{:S(2)}) collective-permute-start(bf16[32,4096]{1,0:T(8,128)(2,1)S(1)} %get-tuple-element.58), channel_id=1, source_target_pairs={{0,3},{1,0},{2,1},{3,2},{4,7},{5,4},{6,5},{7,6},{8,11},{9,8},{10,9... | collective-permute-start | bytes 786440 | tf_op jit(solution)/shard_map/ppermute | solution.py:27
  56.6 52.4 %copy-start.3 = (bf16[32,4096]{1,0:T(8,128)(2,1)}, bf16[32,4096]{1,0:T(8,128)(2,1)S(1)}, u32[]{:S(2)}) copy-start(bf16[32,4096]{1,0:T(8,128)(2,1)S(1)} %get-tuple-element.62.n0) | copy-start | bytes 786436
  100.6 64.1 %all-to-all-start.1 = ((bf16[128,8,1024]{2,1,0:T(8,128)(2,1)}), bf16[128,8,1024]{2,1,0:T(8,128)(2,1)S(1)}, u32[]{:S(2)}, u32[]{:S(2)}) async-start(bf16[128,8,1024]{2,1,0:T(8,128)(2,1)} %bitcast.16), calls=%async_computation.1 | async-start | bytes 4194304 | tf_op jit(solution)/shard_map/all_to_all | solution.py:517
  105.3 30.8 %collective-permute-start.14 = (bf16[32,4096]{1,0:T(8,128)(2,1)S(1)}, bf16[32,4096]{1,0:T(8,128)(2,1)S(1)}, u32[]{:S(2)}, u32[]{:S(2)}) collective-permute-start(bf16[32,4096]{1,0:T(8,128)(2,1)S(1)} %get-tuple-element.62.n0), channel_id=1, source_target_pairs={{0,1},{1,2},{2,3},{3,0},{4,5},{5,6},{6,7},{7,4},{8,9},{9,10},{10,1... | collective-permute-start | bytes 786440 | tf_op jit(solution)/shard_map/ppermute | solution.py:27
  106.2 35.5 %collective-permute-start.15 = (bf16[32,4096]{1,0:T(8,128)(2,1)S(1)}, bf16[32,4096]{1,0:T(8,128)(2,1)S(1)}, u32[]{:S(2)}, u32[]{:S(2)}) collective-permute-start(bf16[32,4096]{1,0:T(8,128)(2,1)S(1)} %get-tuple-element.62.n0), channel_id=1, source_target_pairs={{0,2},{1,3},{2,0},{3,1},{4,6},{5,7},{6,4},{7,5},{8,10},{9,11},{10,... | collective-permute-start | bytes 786440 | tf_op jit(solution)/shard_map/ppermute | solution.py:27
  108.9 32.8 %collective-permute-start.16 = (bf16[32,4096]{1,0:T(8,128)(2,1)S(1)}, bf16[32,4096]{1,0:T(8,128)(2,1)S(1)}, u32[]{:S(2)}, u32[]{:S(2)}) collective-permute-start(bf16[32,4096]{1,0:T(8,128)(2,1)S(1)} %get-tuple-element.62.n0), channel_id=1, source_target_pairs={{0,3},{1,0},{2,1},{3,2},{4,7},{5,4},{6,5},{7,6},{8,11},{9,8},{10,9... | collective-permute-start | bytes 786440 | tf_op jit(solution)/shard_map/ppermute | solution.py:27
  136.1 5.6 %copy-start.6 = (bf16[32,4096]{1,0:T(8,128)(2,1)}, bf16[32,4096]{1,0:T(8,128)(2,1)S(1)}, u32[]{:S(2)}) copy-start(bf16[32,4096]{1,0:T(8,128)(2,1)S(1)} %collective-permute-done.14.n1) | copy-start | bytes 786436
  141.7 0.7 copy-start.7
  142.4 0.7 copy-start.8
  146.9 0.7 copy-start.4
  147.6 9.2 %collective-permute-start.17 = (bf16[32,4096]{1,0:T(8,128)(2,1)S(1)}, bf16[32,4096]{1,0:T(8,128)(2,1)S(1)}, u32[]{:S(2)}, u32[]{:S(2)}) collective-permute-start(bf16[32,4096]{1,0:T(8,128)(2,1)S(1)} %get-tuple-element.64), channel_id=1, source_target_pairs={{0,3},{1,0},{2,1},{3,2},{4,7},{5,4},{6,5},{7,6},{8,11},{9,8},{10,9... | collective-permute-start | bytes 786440 | tf_op jit(solution)/shard_map/ppermute | solution.py:27
  147.6 10.7 %collective-permute-start.18 = (bf16[32,4096]{1,0:T(8,128)(2,1)S(1)}, bf16[32,4096]{1,0:T(8,128)(2,1)S(1)}, u32[]{:S(2)}, u32[]{:S(2)}) collective-permute-start(bf16[32,4096]{1,0:T(8,128)(2,1)S(1)} %get-tuple-element.65), channel_id=1, source_target_pairs={{0,2},{1,3},{2,0},{3,1},{4,6},{5,7},{6,4},{7,5},{8,10},{9,11},{10,... | collective-permute-start | bytes 786440 | tf_op jit(solution)/shard_map/ppermute | solution.py:27
  149.0 13.6 %collective-permute-start.19 = (bf16[32,4096]{1,0:T(8,128)(2,1)S(1)}, bf16[32,4096]{1,0:T(8,128)(2,1)S(1)}, u32[]{:S(2)}, u32[]{:S(2)}) collective-permute-start(bf16[32,4096]{1,0:T(8,128)(2,1)S(1)} %get-tuple-element.66), channel_id=1, source_target_pairs={{0,1},{1,2},{2,3},{3,0},{4,5},{5,6},{6,7},{7,4},{8,9},{9,10},{10,1... | collective-permute-start | bytes 786440 | tf_op jit(solution)/shard_map/ppermute | solution.py:27
  156.8 5.7 %copy-start.9 = (bf16[32,4096]{1,0:T(8,128)(2,1)}, bf16[32,4096]{1,0:T(8,128)(2,1)S(1)}, u32[]{:S(2)}) copy-start(bf16[32,4096]{1,0:T(8,128)(2,1)S(1)} %collective-permute-done.17.s1) | copy-start | bytes 786436
  158.4 4.2 %copy-start.10 = (bf16[32,4096]{1,0:T(8,128)(2,1)}, bf16[32,4096]{1,0:T(8,128)(2,1)S(1)}, u32[]{:S(2)}) copy-start(bf16[32,4096]{1,0:T(8,128)(2,1)S(1)} %collective-permute-done.18.s2) | copy-start | bytes 786436
  162.5 0.7 copy-start.11

commit v10 on v9

--- a/solution.py
+++ b/solution.py
@@ -76,7 +76,7 @@
         out[i] = ref[...]
 
 
-def tables_kernel(place, ids_hbm, weight_hbm, narrow_hbm, broad_hbm, target, mix, own, first, second, third, *scratch):
+def tables_kernel(place, ids_hbm, weight_hbm, narrow_hbm, broad_hbm, target, mix, own, first, second, third, fourth, *scratch):
     ids_in, weight_in, narrow, broad, sems = scratch
     copies = []
     for ref, held in ((narrow_hbm, narrow), (broad_hbm, broad), (ids_hbm, ids_in), (weight_hbm, weight_in)):
@@ -121,9 +121,9 @@
     for i in range(1, 4):
         put(first, (i - 1) * 128, ORDER[i], 0)
     for i in range(4):
-        put(second, i * 128, ORDER[i % 2], 1 if i < 2 else 3)
-        put(second, 512 + i * 128, ORDER[2 + i % 2], 1 if i < 2 else 3)
-        put(third, i * 128, ORDER[i], 2)
+        put(second, i * 128, ORDER[i], 1 if i < 2 else 3)
+        put(third, i * 128, ORDER[i], 3 if i < 2 else 1)
+        put(fourth, i * 128, ORDER[i], 2)
 
 
 def project_kernel(place, own, other, narrow, broad, *refs):
@@ -278,7 +278,7 @@
         return value.reshape(-1, hi - lo)
 
     results = {}
-    for group, size, heads, lo, per in (("n", NARROW_SIZE, 4, 0, 2 if last else 4), ("b", BROAD_SIZE, 2, 256, 2)):
+    for group, size, heads, lo, per in (("n", NARROW_SIZE, 4, 0, 4 if first else 2), ("b", BROAD_SIZE, 2, 256, 2)):
         count = per * 128
         scale = size**-0.5 * LOG2E
         base = 0 if group == "n" else 4
@@ -416,10 +416,10 @@
     line = {}
     for k in (2, 1, 3):
         line[k] = turn(own_kv, k, 0)
-    target, mix, own_bias, bias_1, bias_2, bias_3 = call(
+    target, mix, own_bias, bias_1, bias_2, bias_3, bias_4 = call(
         tables_kernel,
         (place, route_ids.T, route_weight.T, gates_narrow.T, gates_broad.T),
-        [shaped((4, 128), jnp.int32), shaped((128, 1024), BF)] + [shaped((8, n), F32) for n in (128, 384, 1024, 512)],
+        [shaped((4, 128), jnp.int32), shaped((128, 1024), BF)] + [shaped((8, n), F32) for n in (128, 384, 512, 512, 512)],
         smem=(0,),
         hbm=(1, 2, 3, 4),
         scratch=[
@@ -445,9 +445,9 @@
     core = c.reshape(1)
     first_tiles = [((own_kv,), own_bias, True), ((low, high), bias_1, False)]
     state = attend(q_own, q_other, core, first_tiles, None, False)
-    second_tiles = [((low_back, low_ahead, high_back, high_ahead), bias_2, False)]
-    state = attend(q_own, q_other, core, second_tiles, state, False)
-    own_part, send_part = attend(q_own, q_other, core, [((low_far, high_far), bias_3, False)], state, True)
+    state = attend(q_own, q_other, core, [((low_back, high_ahead), bias_2, False)], state, False)
+    state = attend(q_own, q_other, core, [((low_ahead, high_back), bias_3, False)], state, False)
+    own_part, send_part = attend(q_own, q_other, core, [((low_far, high_far), bias_4, False)], state, True)
     other_part = swap_core(send_part)
 
     p0, p1, p2, p3 = call(

time: 167 us -> 167 us (level)
  Pallas kernels: 28.1 us -> 29.8 us
    pallas_call x3 -> x4, Pallas kernels: 8.01 us -> 9.75 us  [attend(): pl.pallas_call(functools.partial(attend_kernel, counts, state is None, la...]
  transfers between devices with their start and end apart: 21 -> 21, of which waited for: 12 -> 10; matrix products, arithmetic and copies ran while one was open for 0% -> 0% of each run, Pallas kernels for 8% -> 9%
where the time goes in v10:
time: 167 us; the launch traced here: 166 us
  waiting for transfers between devices  62.9 us (38%)
  blocking collectives  37.2 us (22%)
  starting transfers between devices  32.6 us (20%)
  Pallas kernels  29.8 us (18%)
  local copies, waits for them, and re-layouts  2.86 us (2%)
    ppermute x9, waiting for transfers between devices, shift(): return lax.ppermute(x, axis, [(i, (i + k) % 4) for i in range(4)])  54.6 us
    all_to_all x1, blocking collectives, local(): lax.all_to_all(outbound.reshape(128, 8, 1024), every, 0, 0, tiled=True)  37.2 us
    pallas_call x9, Pallas kernels, call(): pl.pallas_call(kernel, out_shape=shapes, in_specs=[SMEM if i in smem else...  20.1 us
    ppermute x9, starting transfers between devices, turn(): return lax.ppermute(x, SP, pairs)  15 us
    ppermute x9, starting transfers between devices, shift(): return lax.ppermute(x, axis, [(i, (i + k) % 4) for i in range(4)])  12.8 us
    pallas_call x4, Pallas kernels, attend(): pl.pallas_call(functools.partial(attend_kernel, counts, state is None, la...  9.75 us
    ppermute x9, waiting for transfers between devices, turn(): return lax.ppermute(x, SP, pairs)  6.68 us
    all_to_all x1, starting transfers between devices, local(): lax.all_to_all(result.reshape(128, 8, 1024), every, 0, 0, tiled=True)  4.67 us
  transfers between devices with their start and end apart: 21, of which 10 were waited for; matrix products, arithmetic and copies ran while one was open for 0% of the time, Pallas kernels for 9%

profile of v10, /device:TPU:0, one launch (start us, length us, event | category | flops | bytes accessed | tf_op | source)
XLA Modules:
  0.0 165.7 jit_solution(11806802325304725067)
XLA Ops:
  0.0 1.1 shard_map.190
  1.1 1.8 %collective-permute-start.1 = (bf16[128,768]{1,0:T(8,128)(2,1)S(1)}, bf16[128,768]{1,0:T(8,128)(2,1)S(1)}, u32[]{:S(2)}, u32[]{:S(2)}) collective-permute-start(bf16[128,768]{1,0:T(8,128)(2,1)S(1)} %get-tuple-element.42.a.refs_3_), channel_id=1, source_target_pairs={{0,8},{4,36},{8,16},{12,44},{16,24},{20,52},{24,0},{28,60},{32,40}... | collective-permute-start | bytes 589832 | tf_op jit(solution)/shard_map/ppermute | solution.py:41
  2.9 1.5 collective-permute-start.2
  4.4 2.1 %collective-permute-start.3 = (bf16[128,768]{1,0:T(8,128)(2,1)S(1)}, bf16[128,768]{1,0:T(8,128)(2,1)S(1)}, u32[]{:S(2)}, u32[]{:S(2)}) collective-permute-start(bf16[128,768]{1,0:T(8,128)(2,1)S(1)} %get-tuple-element.42.a.refs_3_), channel_id=1, source_target_pairs={{0,16},{4,68},{8,24},{12,76},{16,0},{20,84},{24,8},{28,92},{32,48}... | collective-permute-start | bytes 589832 | tf_op jit(solution)/shard_map/ppermute | solution.py:41
  6.5 0.1 pad_add_fusion.place
  6.6 2.0 %shard_map.191 = (s32[4,128]{1,0:T(4,128)S(1)}, bf16[128,1024]{1,0:T(8,128)(2,1)S(1)}, f32[8,128]{1,0:T(8,128)S(1)}, f32[8,384]{1,0:T(8,128)S(1)}, f32[8,512]{1,...) custom-call(s32[4]{0:T(128)S(1)} %pad_add_fusion.place, s32[4,32]{1,0:T(4,128)} %bitcast.20, ...), custom_call_target="tpu_custom_call" | custom-call | bytes 2097152 | tf_op jit(solution)/shard_map/pallas_call | solution.py:48
  8.6 3.0 %collective-permute-done.3.d = bf16[128,768]{1,0:T(8,128)(2,1)S(1)} collective-permute-done((bf16[128,768]{1,0:T(8,128)(2,1)S(1)}, bf16[128,768]{1,0:T(8,128)(2,1)S(1)}, u32[]{:S(2)}, u32[]{:S(2)}) %collective-permute-start.3) | collective-permute-done | bytes 196640 | tf_op jit(solution)/shard_map/ppermute | solution.py:41
  11.6 0.1 shard_map.192
  11.7 2.1 %collective-permute-start.4 = (bf16[2,128,768]{2,1,0:T(8,128)(2,1)S(1)}, bf16[2,128,768]{2,1,0:T(8,128)(2,1)S(1)}, u32[]{:S(2)}, u32[]{:S(2)}) collective-permute-start(bf16[2,128,768]{2,1,0:T(8,128)(2,1)S(1)} %get-tuple-element.45.refs_5_), channel_id=1, source_target_pairs={{0,32},{4,12},{8,40},{12,20},{16,48},{20,28},{24,56},{28,4},{32,64... | collective-permute-start | bytes 1179656 | tf_op jit(solution)/shard_map/ppermute | solution.py:41
  13.8 2.2 %collective-permute-start.6 = (bf16[2,128,768]{2,1,0:T(8,128)(2,1)S(1)}, bf16[2,128,768]{2,1,0:T(8,128)(2,1)S(1)}, u32[]{:S(2)}, u32[]{:S(2)}) collective-permute-start(bf16[2,128,768]{2,1,0:T(8,128)(2,1)S(1)} %get-tuple-element.46.refs_6_), channel_id=1, source_target_pairs={{0,96},{4,28},{8,104},{12,4},{16,112},{20,12},{24,120},{28,20},{32... | collective-permute-start | bytes 1179656 | tf_op jit(solution)/shard_map/ppermute | solution.py:41
  16.0 1.9 %collective-permute-start.8 = (bf16[2,128,768]{2,1,0:T(8,128)(2,1)S(1)}, bf16[2,128,768]{2,1,0:T(8,128)(2,1)S(1)}, u32[]{:S(2)}, u32[]{:S(2)}) collective-permute-start(bf16[2,128,768]{2,1,0:T(8,128)(2,1)S(1)} %get-tuple-element.45.refs_5_), channel_id=1, source_target_pairs={{0,96},{4,28},{8,104},{12,4},{16,112},{20,12},{24,120},{28,20},{32... | collective-permute-start | bytes 1179656 | tf_op jit(solution)/shard_map/ppermute | solution.py:41
  17.9 0.1 collective-permute-start.9
  18.0 3.6 %collective-permute-done.4.refs_3_ = bf16[2,128,768]{2,1,0:T(8,128)(2,1)S(1)} collective-permute-done((bf16[2,128,768]{2,1,0:T(8,128)(2,1)S(1)}, bf16[2,128,768]{2,1,0:T(8,128)(2,1)S(1)}, u32[]{:S(2)}, u32[]{:S(2)}) %collective-permute-start.4) | collective-permute-done | bytes 393248 | tf_op jit(solution)/shard_map/ppermute | solution.py:41
  21.6 3.3 %collective-permute-start.7 = (bf16[2,128,768]{2,1,0:T(8,128)(2,1)S(1)}, bf16[2,128,768]{2,1,0:T(8,128)(2,1)S(1)}, u32[]{:S(2)}, u32[]{:S(2)}) collective-permute-start(bf16[2,128,768]{2,1,0:T(8,128)(2,1)S(1)} %collective-permute-done.6.refs_4_), channel_id=1, source_target_pairs={{0,96},{4,28},{8,104},{12,4},{16,112},{20,12},{24,120},{28,20},{32... | collective-permute-start | bytes 1179656 | tf_op jit(solution)/shard_map/ppermute | solution.py:41
  25.0 1.9 %shard_map.193 = (f32[1536,128]{1,0:T(8,128)S(1)}, f32[1536,128]{1,0:T(8,128)S(1)}, f32[1024,128]{1,0:T(8,128)S(1)}, f32[512,256]{1,0:T(8,128)S(1)}) custom-call(bf16[128,1024]{1,0:T(8,128)(2,1)S(1)} %get-tuple-element.41.refs_0_, bf16[128,1024]{1,0:T(8,128)(2,1)S(1)} %collective-permute-done.refs_1_, s32[1]{0:T(128)} %bitcast.2.refs_2_, ...), custom_call_target="tpu_custom_call" | custom-call | flops 536870912 | bytes 4194304 | tf_op jit(solution)/shard_map/pallas_call | solution.py:370
  26.8 0.0 copy-start.1
  26.8 2.6 %shard_map.194 = (f32[1536,128]{1,0:T(8,128)S(1)}, f32[1536,128]{1,0:T(8,128)S(1)}, f32[1024,128]{1,0:T(8,128)S(1)}, f32[512,256]{1,0:T(8,128)S(1)}) custom-call(bf16[128,1024]{1,0:T(8,128)(2,1)S(1)} %get-tuple-element.41.refs_0_, bf16[128,1024]{1,0:T(8,128)(2,1)S(1)} %collective-permute-done.refs_1_, s32[1]{0:T(128)} %bitcast.2.refs_2_, ...), custom_call_target="tpu_custom_call" | custom-call | flops 536870912 | bytes 4194304 | tf_op jit(solution)/shard_map/pallas_call | solution.py:370
  29.5 2.6 %shard_map.195 = (f32[1536,128]{1,0:T(8,128)S(1)}, f32[1536,128]{1,0:T(8,128)S(1)}, f32[1024,128]{1,0:T(8,128)S(1)}, f32[512,256]{1,0:T(8,128)S(1)}) custom-call(bf16[128,1024]{1,0:T(8,128)(2,1)S(1)} %get-tuple-element.41.refs_0_, bf16[128,1024]{1,0:T(8,128)(2,1)S(1)} %collective-permute-done.refs_1_, s32[1]{0:T(128)} %bitcast.2.refs_2_, ...), custom_call_target="tpu_custom_call" | custom-call | flops 536870912 | bytes 4194304 | tf_op jit(solution)/shard_map/pallas_call | solution.py:370
  32.2 2.6 %shard_map.196 = (f32[128,1152]{1,0:T(8,128)S(1)}, bf16[128,1152]{1,0:T(8,128)(2,1)S(1)}) custom-call(bf16[128,1024]{1,0:T(8,128)(2,1)S(1)} %get-tuple-element.41.refs_0_, bf16[128,1024]{1,0:T(8,128)(2,1)S(1)} %collective-permute-done.refs_1_, s32[1]{0:T(128)} %bitcast.2.refs_2_, bf16[2,128,768]{2,1,0:T(8,128)(2,1)S(1)} %collective-permute-done.5.refs_3_, ...), custom_call_target="tpu_custom_call" | custom-call | flops 536870912 | bytes 4194304 | tf_op jit(solution)/shard_map/pallas_call | solution.py:370
  34.8 0.1 collective-permute-start.10
  34.9 1.6 collective-permute-done.10.other
  36.5 2.2 %shard_map.197 = (bf16[32,4096]{1,0:T(8,128)(2,1)S(1)}, bf16[32,4096]{1,0:T(8,128)(2,1)S(1)}, bf16[32,4096]{1,0:T(8,128)(2,1)S(1)}, bf16[32,4096]{1,0:T(8,128)(2,1)S(1)}) custom-call(s32[4]{0:T(128)S(1)} %pad_add_fusion.place, f32[128,1152]{1,0:T(8,128)S(1)} %get-tuple-element.63.own, bf16[128,1152]{1,0:T(8,128)(2,1)S(1)} %collective-permute-done.10.other, ...), custom_call_target="tpu_custom_call" | custom-call | flops 1073741824 | bytes 2097152 | tf_op jit(solution)/shard_map/pallas_call | solution.py:48
  38.7 1.6 collective-permute-start.11
  40.2 2.7 %collective-permute-start.12 = (bf16[32,4096]{1,0:T(8,128)(2,1)S(1)}, bf16[32,4096]{1,0:T(8,128)(2,1)S(1)}, u32[]{:S(2)}, u32[]{:S(2)}) collective-permute-start(bf16[32,4096]{1,0:T(8,128)(2,1)S(1)} %get-tuple-element.67), channel_id=1, source_target_pairs={{0,2},{1,3},{2,0},{3,1},{4,6},{5,7},{6,4},{7,5},{8,10},{9,11},{10,... | collective-permute-start | bytes 786440 | tf_op jit(solution)/shard_map/ppermute | solution.py:27
  42.9 1.4 collective-permute-start.13
  44.4 3.9 %collective-permute-done.11.p1 = bf16[32,4096]{1,0:T(8,128)(2,1)S(1)} collective-permute-done((bf16[32,4096]{1,0:T(8,128)(2,1)S(1)}, bf16[32,4096]{1,0:T(8,128)(2,1)S(1)}, u32[]{:S(2)}, u32[]{:S(2)}) %collective-permute-start.11) | collective-permute-done | bytes 262176 | tf_op jit(solution)/shard_map/ppermute | solution.py:27
  48.3 6.6 %collective-permute-done.12.p2 = bf16[32,4096]{1,0:T(8,128)(2,1)S(1)} collective-permute-done((bf16[32,4096]{1,0:T(8,128)(2,1)S(1)}, bf16[32,4096]{1,0:T(8,128)(2,1)S(1)}, u32[]{:S(2)}, u32[]{:S(2)}) %collective-permute-start.12) | collective-permute-done | bytes 262176 | tf_op jit(solution)/shard_map/ppermute | solution.py:27
  54.9 2.6 %shard_map.198 = (f32[32,4096]{1,0:T(8,128)}, bf16[32,4096]{1,0:T(8,128)(2,1)S(1)}, bf16[1024,1024]{1,0:T(8,128)(2,1)}) custom-call(s32[4]{0:T(128)S(1)} %pad_add_fusion.place, bf16[32,4096]{1,0:T(8,128)(2,1)S(1)} %get-tuple-element.65.p0, bf16[32,4096]{1,0:T(8,128)(2,1)S(1)} %collective-permute-done.11.p1, bf16[32,4096]{1,0:T(8,128)(2,1)S(1)} %collective-permute-done.12.p2, ...), custom_call_target="tpu_custom_call" | custom-call | flops 268435456 | bytes 2097152 | tf_op jit(solution)/shard_map/pallas_call | solution.py:48
  57.5 37.2 %all_to_all.10 = bf16[128,8,1024]{2,1,0:T(8,128)(2,1)S(1)} all-to-all(bf16[128,8,1024]{2,1,0:T(8,128)(2,1)} %bitcast.17), channel_id=1, replica_groups=mesh['z'=4,'y'=4,'c'=2,'tp'=4] {'z','y','c','tp'}, dimensions={0} | all-to-all | bytes 4194304 | tf_op jit(solution)/shard_map/all_to_all | solution.py:475
  94.7 5.7 %shard_map.199 = bf16[1024,1024]{1,0:T(8,128)(2,1)} custom-call(bf16[1024,1024]{1,0:T(8,128)(2,1)S(1)} %bitcast.13, bf16[1,4096,256]{2,1,0:T(8,128)(2,1)} %gate_hbm.2, bf16[1,4096,256]{2,1,0:T(8,128)(2,1)} %up_hbm.2, bf16[1,256,4096]{2,1,0:T(8,128)(2,1)} %down_hbm.2), custom_call_target="tpu_custom_call" | custom-call | flops 1610612736 | bytes 2097152 | tf_op jit(solution)/shard_map/pallas_call | solution.py:48
  100.4 4.7 %all-to-all-start.1 = ((bf16[128,8,1024]{2,1,0:T(8,128)(2,1)}), bf16[128,8,1024]{2,1,0:T(8,128)(2,1)S(1)}, u32[]{:S(2)}, u32[]{:S(2)}) async-start(bf16[128,8,1024]{2,1,0:T(8,128)(2,1)} %bitcast.16), calls=%async_computation.1 | async-start | bytes 4194304 | tf_op jit(solution)/shard_map/all_to_all | solution.py:517
  105.1 0.9 collective-permute-start.14
  106.0 2.7 %collective-permute-start.15 = (bf16[32,4096]{1,0:T(8,128)(2,1)S(1)}, bf16[32,4096]{1,0:T(8,128)(2,1)S(1)}, u32[]{:S(2)}, u32[]{:S(2)}) collective-permute-start(bf16[32,4096]{1,0:T(8,128)(2,1)S(1)} %get-tuple-element.72.n0), channel_id=1, source_target_pairs={{0,2},{1,3},{2,0},{3,1},{4,6},{5,7},{6,4},{7,5},{8,10},{9,11},{10,... | collective-permute-start | bytes 786440 | tf_op jit(solution)/shard_map/ppermute | solution.py:27
  108.7 1.4 collective-permute-start.16
  110.2 25.7 %collective-permute-done.14.n1 = bf16[32,4096]{1,0:T(8,128)(2,1)S(1)} collective-permute-done((bf16[32,4096]{1,0:T(8,128)(2,1)S(1)}, bf16[32,4096]{1,0:T(8,128)(2,1)S(1)}, u32[]{:S(2)}, u32[]{:S(2)}) %collective-permute-start.14) | collective-permute-done | bytes 262176 | tf_op jit(solution)/shard_map/ppermute | solution.py:27
  135.9 5.6 %collective-permute-done.15.n2 = bf16[32,4096]{1,0:T(8,128)(2,1)S(1)} collective-permute-done((bf16[32,4096]{1,0:T(8,128)(2,1)S(1)}, bf16[32,4096]{1,0:T(8,128)(2,1)S(1)}, u32[]{:S(2)}, u32[]{:S(2)}) %collective-permute-start.15) | collective-permute-done | bytes 262176 | tf_op jit(solution)/shard_map/ppermute | solution.py:27
  141.5 0.7 copy-done.7
  142.2 0.7 copy-done.8
  142.9 3.8 %shard_map.200 = (bf16[32,4096]{1,0:T(8,128)(2,1)S(1)}, bf16[32,4096]{1,0:T(8,128)(2,1)S(1)}, bf16[32,4096]{1,0:T(8,128)(2,1)S(1)}, bf16[32,4096]{1,0:T(8,128)(2,1)S(1)}) custom-call(bf16[32,4096]{1,0:T(8,128)(2,1)} %copy-done.3, bf16[32,4096]{1,0:T(8,128)(2,1)} %copy-done.6, bf16[32,4096]{1,0:T(8,128)(2,1)} %copy-done.7, bf16[32,4096]{1,0:T(8,128)(2,1)} %copy-done.8, ...), custom_call_target="tpu_custom_call" | custom-call | flops 805306368 | bytes 2097152 | tf_op jit(solution)/shard_map/pallas_call | solution.py:48
  146.7 0.7 copy-done.4
  147.4 1.3 collective-permute-start.18
  148.8 0.8 collective-permute-start.19
  149.5 7.1 %collective-permute-done.17.s1 = bf16[32,4096]{1,0:T(8,128)(2,1)S(1)} collective-permute-done((bf16[32,4096]{1,0:T(8,128)(2,1)S(1)}, bf16[32,4096]{1,0:T(8,128)(2,1)S(1)}, u32[]{:S(2)}, u32[]{:S(2)}) %collective-permute-start.17) | collective-permute-done | bytes 262176 | tf_op jit(solution)/shard_map/ppermute | solution.py:27
  156.6 1.5 collective-permute-done.18.s2
  158.2 4.1 %collective-permute-done.19.s3 = bf16[32,4096]{1,0:T(8,128)(2,1)S(1)} collective-permute-done((bf16[32,4096]{1,0:T(8,128)(2,1)S(1)}, bf16[32,4096]{1,0:T(8,128)(2,1)S(1)}, u32[]{:S(2)}, u32[]{:S(2)}) %collective-permute-start.19) | collective-permute-done | bytes 262176 | tf_op jit(solution)/shard_map/ppermute | solution.py:27
  162.3 0.7 copy-done.11
  163.0 1.5 shard_map.201.base
  164.6 1.2 shard_map.202
  (33 shorter events, 0.1 us)
Async XLA Ops:
  1.1 7.4 %collective-permute-start.1 = (bf16[128,768]{1,0:T(8,128)(2,1)S(1)}, bf16[128,768]{1,0:T(8,128)(2,1)S(1)}, u32[]{:S(2)}, u32[]{:S(2)}) collective-permute-start(bf16[128,768]{1,0:T(8,128)(2,1)S(1)} %get-tuple-element.42.a.refs_3_), channel_id=1, source_target_pairs={{0,8},{4,36},{8,16},{12,44},{16,24},{20,52},{24,0},{28,60},{32,40}... | collective-permute-start | bytes 589832 | tf_op jit(solution)/shard_map/ppermute | solution.py:41
  2.9 5.7 %collective-permute-start.2 = (bf16[128,768]{1,0:T(8,128)(2,1)S(1)}, bf16[128,768]{1,0:T(8,128)(2,1)S(1)}, u32[]{:S(2)}, u32[]{:S(2)}) collective-permute-start(bf16[128,768]{1,0:T(8,128)(2,1)S(1)} %get-tuple-element.42.a.refs_3_), channel_id=1, source_target_pairs={{0,24},{4,100},{8,0},{12,108},{16,8},{20,116},{24,16},{28,124},{32... | collective-permute-start | bytes 589832 | tf_op jit(solution)/shard_map/ppermute | solution.py:41
  4.4 7.2 %collective-permute-start.3 = (bf16[128,768]{1,0:T(8,128)(2,1)S(1)}, bf16[128,768]{1,0:T(8,128)(2,1)S(1)}, u32[]{:S(2)}, u32[]{:S(2)}) collective-permute-start(bf16[128,768]{1,0:T(8,128)(2,1)S(1)} %get-tuple-element.42.a.refs_3_), channel_id=1, source_target_pairs={{0,16},{4,68},{8,24},{12,76},{16,0},{20,84},{24,8},{28,92},{32,48}... | collective-permute-start | bytes 589832 | tf_op jit(solution)/shard_map/ppermute | solution.py:41
  11.7 10.0 %collective-permute-start.4 = (bf16[2,128,768]{2,1,0:T(8,128)(2,1)S(1)}, bf16[2,128,768]{2,1,0:T(8,128)(2,1)S(1)}, u32[]{:S(2)}, u32[]{:S(2)}) collective-permute-start(bf16[2,128,768]{2,1,0:T(8,128)(2,1)S(1)} %get-tuple-element.45.refs_5_), channel_id=1, source_target_pairs={{0,32},{4,12},{8,40},{12,20},{16,48},{20,28},{24,56},{28,4},{32,64... | collective-permute-start | bytes 1179656 | tf_op jit(solution)/shard_map/ppermute | solution.py:41
  13.8 7.9 %collective-permute-start.6 = (bf16[2,128,768]{2,1,0:T(8,128)(2,1)S(1)}, bf16[2,128,768]{2,1,0:T(8,128)(2,1)S(1)}, u32[]{:S(2)}, u32[]{:S(2)}) collective-permute-start(bf16[2,128,768]{2,1,0:T(8,128)(2,1)S(1)} %get-tuple-element.46.refs_6_), channel_id=1, source_target_pairs={{0,96},{4,28},{8,104},{12,4},{16,112},{20,12},{24,120},{28,20},{32... | collective-permute-start | bytes 1179656 | tf_op jit(solution)/shard_map/ppermute | solution.py:41
  16.0 13.5 %collective-permute-start.8 = (bf16[2,128,768]{2,1,0:T(8,128)(2,1)S(1)}, bf16[2,128,768]{2,1,0:T(8,128)(2,1)S(1)}, u32[]{:S(2)}, u32[]{:S(2)}) collective-permute-start(bf16[2,128,768]{2,1,0:T(8,128)(2,1)S(1)} %get-tuple-element.45.refs_5_), channel_id=1, source_target_pairs={{0,96},{4,28},{8,104},{12,4},{16,112},{20,12},{24,120},{28,20},{32... | collective-permute-start | bytes 1179656 | tf_op jit(solution)/shard_map/ppermute | solution.py:41
  17.9 11.6 %collective-permute-start.9 = (bf16[2,128,768]{2,1,0:T(8,128)(2,1)S(1)}, bf16[2,128,768]{2,1,0:T(8,128)(2,1)S(1)}, u32[]{:S(2)}, u32[]{:S(2)}) collective-permute-start(bf16[2,128,768]{2,1,0:T(8,128)(2,1)S(1)} %get-tuple-element.46.refs_6_), channel_id=1, source_target_pairs={{0,32},{4,12},{8,40},{12,20},{16,48},{20,28},{24,56},{28,4},{32,64... | collective-permute-start | bytes 1179656 | tf_op jit(solution)/shard_map/ppermute | solution.py:41
  18.0 7.0 %collective-permute-start = (bf16[128,1024]{1,0:T(8,128)(2,1)S(1)}, bf16[128,1024]{1,0:T(8,128)(2,1)S(1)}, u32[]{:S(2)}, u32[]{:S(2)}) collective-permute-start(bf16[128,1024]{1,0:T(8,128)(2,1)S(1)} %get-tuple-element.41.refs_0_), channel_id=1, source_target_pairs={{0,4},{4,0},{1,5},{5,1},{2,6},{6,2},{3,7},{7,3},{8,12},{12,8},{9,1... | collective-permute-start | bytes 786440 | tf_op jit(solution)/shard_map/ppermute | solution.py:31
  21.6 10.5 %collective-permute-start.5 = (bf16[2,128,768]{2,1,0:T(8,128)(2,1)S(1)}, bf16[2,128,768]{2,1,0:T(8,128)(2,1)S(1)}, u32[]{:S(2)}, u32[]{:S(2)}) collective-permute-start(bf16[2,128,768]{2,1,0:T(8,128)(2,1)S(1)} %collective-permute-done.4.refs_3_), channel_id=1, source_target_pairs={{0,32},{4,12},{8,40},{12,20},{16,48},{20,28},{24,56},{28,4},{32,64... | collective-permute-start | bytes 1179656 | tf_op jit(solution)/shard_map/ppermute | solution.py:41
  21.6 10.5 %collective-permute-start.7 = (bf16[2,128,768]{2,1,0:T(8,128)(2,1)S(1)}, bf16[2,128,768]{2,1,0:T(8,128)(2,1)S(1)}, u32[]{:S(2)}, u32[]{:S(2)}) collective-permute-start(bf16[2,128,768]{2,1,0:T(8,128)(2,1)S(1)} %collective-permute-done.6.refs_4_), channel_id=1, source_target_pairs={{0,96},{4,28},{8,104},{12,4},{16,112},{20,12},{24,120},{28,20},{32... | collective-permute-start | bytes 1179656 | tf_op jit(solution)/shard_map/ppermute | solution.py:41
  26.8 9.6 %copy-start.1 = (bf16[512,4096]{1,0:T(8,128)(2,1)S(1)}, bf16[512,4096]{1,0:T(8,128)(2,1)}, u32[]{:S(2)}) copy-start(bf16[512,4096]{1,0:T(8,128)(2,1)} %broad.1) | copy-start | bytes 12582916
  29.5 7.0 %copy-start = (bf16[512,4096]{1,0:T(8,128)(2,1)S(1)}, bf16[512,4096]{1,0:T(8,128)(2,1)}, u32[]{:S(2)}) copy-start(bf16[512,4096]{1,0:T(8,128)(2,1)} %narrow.1) | copy-start | bytes 12582916
  34.8 1.7 %collective-permute-start.10 = (bf16[128,1152]{1,0:T(8,128)(2,1)S(1)}, bf16[128,1152]{1,0:T(8,128)(2,1)S(1)}, u32[]{:S(2)}, u32[]{:S(2)}) collective-permute-start(bf16[128,1152]{1,0:T(8,128)(2,1)S(1)} %get-tuple-element.64), channel_id=1, source_target_pairs={{0,4},{4,0},{1,5},{5,1},{2,6},{6,2},{3,7},{7,3},{8,12},{12,8},{9,1... | collective-permute-start | bytes 884744 | tf_op jit(solution)/shard_map/ppermute | solution.py:31
  36.5 18.4 %copy-start.2 = (bf16[128,4096]{1,0:T(8,128)(2,1)S(1)}, bf16[128,4096]{1,0:T(8,128)(2,1)}, u32[]{:S(2)}) copy-start(bf16[128,4096]{1,0:T(8,128)(2,1)} %residual.1) | copy-start | bytes 3145732
  36.5 18.4 %copy-start.5 = (f32[4096]{0:T(1024)S(1)}, f32[4096]{0:T(1024)}, u32[]{:S(2)}) copy-start(f32[4096]{0:T(1024)} %param.31) | copy-start | bytes 49156
  38.7 9.6 %collective-permute-start.11 = (bf16[32,4096]{1,0:T(8,128)(2,1)S(1)}, bf16[32,4096]{1,0:T(8,128)(2,1)S(1)}, u32[]{:S(2)}, u32[]{:S(2)}) collective-permute-start(bf16[32,4096]{1,0:T(8,128)(2,1)S(1)} %get-tuple-element.66), channel_id=1, source_target_pairs={{0,1},{1,2},{2,3},{3,0},{4,5},{5,6},{6,7},{7,4},{8,9},{9,10},{10,1... | collective-permute-start | bytes 786440 | tf_op jit(solution)/shard_map/ppermute | solution.py:27
  40.2 14.7 %collective-permute-start.12 = (bf16[32,4096]{1,0:T(8,128)(2,1)S(1)}, bf16[32,4096]{1,0:T(8,128)(2,1)S(1)}, u32[]{:S(2)}, u32[]{:S(2)}) collective-permute-start(bf16[32,4096]{1,0:T(8,128)(2,1)S(1)} %get-tuple-element.67), channel_id=1, source_target_pairs={{0,2},{1,3},{2,0},{3,1},{4,6},{5,7},{6,4},{7,5},{8,10},{9,11},{10,... | collective-permute-start | bytes 786440 | tf_op jit(solution)/shard_map/ppermute | solution.py:27
  42.9 11.9 %collective-permute-start.13 = (bf16[32,4096]{1,0:T(8,128)(2,1)S(1)}, bf16[32,4096]{1,0:T(8,128)(2,1)S(1)}, u32[]{:S(2)}, u32[]{:S(2)}) collective-permute-start(bf16[32,4096]{1,0:T(8,128)(2,1)S(1)} %get-tuple-element.68), channel_id=1, source_target_pairs={{0,3},{1,0},{2,1},{3,2},{4,7},{5,4},{6,5},{7,6},{8,11},{9,8},{10,9... | collective-permute-start | bytes 786440 | tf_op jit(solution)/shard_map/ppermute | solution.py:27
  57.5 51.3 %copy-start.3 = (bf16[32,4096]{1,0:T(8,128)(2,1)}, bf16[32,4096]{1,0:T(8,128)(2,1)S(1)}, u32[]{:S(2)}) copy-start(bf16[32,4096]{1,0:T(8,128)(2,1)S(1)} %get-tuple-element.72.n0) | copy-start | bytes 786436
  100.4 64.1 %all-to-all-start.1 = ((bf16[128,8,1024]{2,1,0:T(8,128)(2,1)}), bf16[128,8,1024]{2,1,0:T(8,128)(2,1)S(1)}, u32[]{:S(2)}, u32[]{:S(2)}) async-start(bf16[128,8,1024]{2,1,0:T(8,128)(2,1)} %bitcast.16), calls=%async_computation.1 | async-start | bytes 4194304 | tf_op jit(solution)/shard_map/all_to_all | solution.py:517
  105.1 30.8 %collective-permute-start.14 = (bf16[32,4096]{1,0:T(8,128)(2,1)S(1)}, bf16[32,4096]{1,0:T(8,128)(2,1)S(1)}, u32[]{:S(2)}, u32[]{:S(2)}) collective-permute-start(bf16[32,4096]{1,0:T(8,128)(2,1)S(1)} %get-tuple-element.72.n0), channel_id=1, source_target_pairs={{0,1},{1,2},{2,3},{3,0},{4,5},{5,6},{6,7},{7,4},{8,9},{9,10},{10,1... | collective-permute-start | bytes 786440 | tf_op jit(solution)/shard_map/ppermute | solution.py:27
  106.0 35.5 %collective-permute-start.15 = (bf16[32,4096]{1,0:T(8,128)(2,1)S(1)}, bf16[32,4096]{1,0:T(8,128)(2,1)S(1)}, u32[]{:S(2)}, u32[]{:S(2)}) collective-permute-start(bf16[32,4096]{1,0:T(8,128)(2,1)S(1)} %get-tuple-element.72.n0), channel_id=1, source_target_pairs={{0,2},{1,3},{2,0},{3,1},{4,6},{5,7},{6,4},{7,5},{8,10},{9,11},{10,... | collective-permute-start | bytes 786440 | tf_op jit(solution)/shard_map/ppermute | solution.py:27
  108.7 32.8 %collective-permute-start.16 = (bf16[32,4096]{1,0:T(8,128)(2,1)S(1)}, bf16[32,4096]{1,0:T(8,128)(2,1)S(1)}, u32[]{:S(2)}, u32[]{:S(2)}) collective-permute-start(bf16[32,4096]{1,0:T(8,128)(2,1)S(1)} %get-tuple-element.72.n0), channel_id=1, source_target_pairs={{0,3},{1,0},{2,1},{3,2},{4,7},{5,4},{6,5},{7,6},{8,11},{9,8},{10,9... | collective-permute-start | bytes 786440 | tf_op jit(solution)/shard_map/ppermute | solution.py:27
  135.9 5.6 %copy-start.6 = (bf16[32,4096]{1,0:T(8,128)(2,1)}, bf16[32,4096]{1,0:T(8,128)(2,1)S(1)}, u32[]{:S(2)}) copy-start(bf16[32,4096]{1,0:T(8,128)(2,1)S(1)} %collective-permute-done.14.n1) | copy-start | bytes 786436
  141.5 0.7 copy-start.7
  142.2 0.7 copy-start.8
  146.7 0.7 copy-start.4
  147.4 9.2 %collective-permute-start.17 = (bf16[32,4096]{1,0:T(8,128)(2,1)S(1)}, bf16[32,4096]{1,0:T(8,128)(2,1)S(1)}, u32[]{:S(2)}, u32[]{:S(2)}) collective-permute-start(bf16[32,4096]{1,0:T(8,128)(2,1)S(1)} %get-tuple-element.74), channel_id=1, source_target_pairs={{0,3},{1,0},{2,1},{3,2},{4,7},{5,4},{6,5},{7,6},{8,11},{9,8},{10,9... | collective-permute-start | bytes 786440 | tf_op jit(solution)/shard_map/ppermute | solution.py:27
  147.4 10.7 %collective-permute-start.18 = (bf16[32,4096]{1,0:T(8,128)(2,1)S(1)}, bf16[32,4096]{1,0:T(8,128)(2,1)S(1)}, u32[]{:S(2)}, u32[]{:S(2)}) collective-permute-start(bf16[32,4096]{1,0:T(8,128)(2,1)S(1)} %get-tuple-element.75), channel_id=1, source_target_pairs={{0,2},{1,3},{2,0},{3,1},{4,6},{5,7},{6,4},{7,5},{8,10},{9,11},{10,... | collective-permute-start | bytes 786440 | tf_op jit(solution)/shard_map/ppermute | solution.py:27
  148.8 13.6 %collective-permute-start.19 = (bf16[32,4096]{1,0:T(8,128)(2,1)S(1)}, bf16[32,4096]{1,0:T(8,128)(2,1)S(1)}, u32[]{:S(2)}, u32[]{:S(2)}) collective-permute-start(bf16[32,4096]{1,0:T(8,128)(2,1)S(1)} %get-tuple-element.76), channel_id=1, source_target_pairs={{0,1},{1,2},{2,3},{3,0},{4,5},{5,6},{6,7},{7,4},{8,9},{9,10},{10,1... | collective-permute-start | bytes 786440 | tf_op jit(solution)/shard_map/ppermute | solution.py:27
  156.6 5.7 %copy-start.9 = (bf16[32,4096]{1,0:T(8,128)(2,1)}, bf16[32,4096]{1,0:T(8,128)(2,1)S(1)}, u32[]{:S(2)}) copy-start(bf16[32,4096]{1,0:T(8,128)(2,1)S(1)} %collective-permute-done.17.s1) | copy-start | bytes 786436
  158.2 4.2 %copy-start.10 = (bf16[32,4096]{1,0:T(8,128)(2,1)}, bf16[32,4096]{1,0:T(8,128)(2,1)S(1)}, u32[]{:S(2)}) copy-start(bf16[32,4096]{1,0:T(8,128)(2,1)S(1)} %collective-permute-done.18.s2) | copy-start | bytes 786436
  162.3 0.7 copy-start.11

commit v11 on v10

--- a/solution.py
+++ b/solution.py
@@ -156,14 +156,14 @@
     normed = (stream * scale * gain[...]).astype(BF)
     normed_out[...] = normed
     cut = jnp.concatenate([normed[:, g * 1024 : (g + 1) * 1024] for g in range(4)], axis=0)
-    row = lax.broadcasted_iota(jnp.int32, (256, 128), 0)
-    for at in range(0, 1024, 256):
+    row = lax.broadcasted_iota(jnp.int32, (512, 128), 0)
+    for at in range(0, 1024, 512):
         pick = row + at == target[0:1, :]
         for k in range(1, 4):
             pick = pick | (row + at == target[k : k + 1, :])
-        rows[at : at + 256, :] = jnp.dot(pick.astype(F32).astype(BF), cut, preferred_element_type=F32).astype(BF)
-        part = pl.ds(at, 256)
-        copies.append(pltpu.make_async_copy(rows.at[part], out.at[part], sems.at[at // 256]))
+        rows[at : at + 512, :] = jnp.dot(pick.astype(F32).astype(BF), cut, preferred_element_type=F32).astype(BF)
+        part = pl.ds(at, 512)
+        copies.append(pltpu.make_async_copy(rows.at[part], out.at[part], sems.at[at // 512]))
         copies[-1].start()
     for copy in copies:
         copy.wait()

time: 167 us -> 167 us (level)
  no operation moved by 1% of the time
where the time goes in v11:
time: 167 us; the launch traced here: 166 us
  waiting for transfers between devices  62.9 us (38%)
  blocking collectives  37.2 us (22%)
  starting transfers between devices  32.6 us (20%)
  Pallas kernels  30 us (18%)
  local copies, waits for them, and re-layouts  2.86 us (2%)
    ppermute x9, waiting for transfers between devices, shift(): return lax.ppermute(x, axis, [(i, (i + k) % 4) for i in range(4)])  54.6 us
    all_to_all x1, blocking collectives, local(): lax.all_to_all(outbound.reshape(128, 8, 1024), every, 0, 0, tiled=True)  37.2 us
    pallas_call x9, Pallas kernels, call(): pl.pallas_call(kernel, out_shape=shapes, in_specs=[SMEM if i in smem else...  20.2 us
    ppermute x9, starting transfers between devices, turn(): return lax.ppermute(x, SP, pairs)  15 us
    ppermute x9, starting transfers between devices, shift(): return lax.ppermute(x, axis, [(i, (i + k) % 4) for i in range(4)])  12.8 us
    pallas_call x4, Pallas kernels, attend(): pl.pallas_call(functools.partial(attend_kernel, counts, state is None, la...  9.75 us
    ppermute x9, waiting for transfers between devices, turn(): return lax.ppermute(x, SP, pairs)  6.68 us
    all_to_all x1, starting transfers between devices, local(): lax.all_to_all(result.reshape(128, 8, 1024), every, 0, 0, tiled=True)  4.67 us
  transfers between devices with their start and end apart: 21, of which 10 were waited for; matrix products, arithmetic and copies ran while one was open for 0% of the time, Pallas kernels for 9%

profile of v11, /device:TPU:0, one launch (start us, length us, event | category | flops | bytes accessed | tf_op | source)
XLA Modules:
  0.0 165.9 jit_solution(18235340647235010838)
XLA Ops:
  0.0 1.1 shard_map.190
  1.1 1.8 %collective-permute-start.1 = (bf16[128,768]{1,0:T(8,128)(2,1)S(1)}, bf16[128,768]{1,0:T(8,128)(2,1)S(1)}, u32[]{:S(2)}, u32[]{:S(2)}) collective-permute-start(bf16[128,768]{1,0:T(8,128)(2,1)S(1)} %get-tuple-element.42.a.refs_3_), channel_id=1, source_target_pairs={{0,8},{4,36},{8,16},{12,44},{16,24},{20,52},{24,0},{28,60},{32,40}... | collective-permute-start | bytes 589832 | tf_op jit(solution)/shard_map/ppermute | solution.py:41
  2.9 1.5 collective-permute-start.2
  4.4 2.1 %collective-permute-start.3 = (bf16[128,768]{1,0:T(8,128)(2,1)S(1)}, bf16[128,768]{1,0:T(8,128)(2,1)S(1)}, u32[]{:S(2)}, u32[]{:S(2)}) collective-permute-start(bf16[128,768]{1,0:T(8,128)(2,1)S(1)} %get-tuple-element.42.a.refs_3_), channel_id=1, source_target_pairs={{0,16},{4,68},{8,24},{12,76},{16,0},{20,84},{24,8},{28,92},{32,48}... | collective-permute-start | bytes 589832 | tf_op jit(solution)/shard_map/ppermute | solution.py:41
  6.5 0.1 pad_add_fusion.place
  6.6 2.0 %shard_map.191 = (s32[4,128]{1,0:T(4,128)S(1)}, bf16[128,1024]{1,0:T(8,128)(2,1)S(1)}, f32[8,128]{1,0:T(8,128)S(1)}, f32[8,384]{1,0:T(8,128)S(1)}, f32[8,512]{1,...) custom-call(s32[4]{0:T(128)S(1)} %pad_add_fusion.place, s32[4,32]{1,0:T(4,128)} %bitcast.20, ...), custom_call_target="tpu_custom_call" | custom-call | bytes 2097152 | tf_op jit(solution)/shard_map/pallas_call | solution.py:48
  8.6 3.0 %collective-permute-done.3.d = bf16[128,768]{1,0:T(8,128)(2,1)S(1)} collective-permute-done((bf16[128,768]{1,0:T(8,128)(2,1)S(1)}, bf16[128,768]{1,0:T(8,128)(2,1)S(1)}, u32[]{:S(2)}, u32[]{:S(2)}) %collective-permute-start.3) | collective-permute-done | bytes 196640 | tf_op jit(solution)/shard_map/ppermute | solution.py:41
  11.6 0.1 shard_map.192
  11.7 2.1 %collective-permute-start.4 = (bf16[2,128,768]{2,1,0:T(8,128)(2,1)S(1)}, bf16[2,128,768]{2,1,0:T(8,128)(2,1)S(1)}, u32[]{:S(2)}, u32[]{:S(2)}) collective-permute-start(bf16[2,128,768]{2,1,0:T(8,128)(2,1)S(1)} %get-tuple-element.45.refs_5_), channel_id=1, source_target_pairs={{0,32},{4,12},{8,40},{12,20},{16,48},{20,28},{24,56},{28,4},{32,64... | collective-permute-start | bytes 1179656 | tf_op jit(solution)/shard_map/ppermute | solution.py:41
  13.8 2.2 %collective-permute-start.6 = (bf16[2,128,768]{2,1,0:T(8,128)(2,1)S(1)}, bf16[2,128,768]{2,1,0:T(8,128)(2,1)S(1)}, u32[]{:S(2)}, u32[]{:S(2)}) collective-permute-start(bf16[2,128,768]{2,1,0:T(8,128)(2,1)S(1)} %get-tuple-element.46.refs_6_), channel_id=1, source_target_pairs={{0,96},{4,28},{8,104},{12,4},{16,112},{20,12},{24,120},{28,20},{32... | collective-permute-start | bytes 1179656 | tf_op jit(solution)/shard_map/ppermute | solution.py:41
  16.0 1.9 %collective-permute-start.8 = (bf16[2,128,768]{2,1,0:T(8,128)(2,1)S(1)}, bf16[2,128,768]{2,1,0:T(8,128)(2,1)S(1)}, u32[]{:S(2)}, u32[]{:S(2)}) collective-permute-start(bf16[2,128,768]{2,1,0:T(8,128)(2,1)S(1)} %get-tuple-element.45.refs_5_), channel_id=1, source_target_pairs={{0,96},{4,28},{8,104},{12,4},{16,112},{20,12},{24,120},{28,20},{32... | collective-permute-start | bytes 1179656 | tf_op jit(solution)/shard_map/ppermute | solution.py:41
  17.9 0.1 collective-permute-start.9
  18.0 3.6 %collective-permute-done.4.refs_3_ = bf16[2,128,768]{2,1,0:T(8,128)(2,1)S(1)} collective-permute-done((bf16[2,128,768]{2,1,0:T(8,128)(2,1)S(1)}, bf16[2,128,768]{2,1,0:T(8,128)(2,1)S(1)}, u32[]{:S(2)}, u32[]{:S(2)}) %collective-permute-start.4) | collective-permute-done | bytes 393248 | tf_op jit(solution)/shard_map/ppermute | solution.py:41
  21.6 3.3 %collective-permute-start.7 = (bf16[2,128,768]{2,1,0:T(8,128)(2,1)S(1)}, bf16[2,128,768]{2,1,0:T(8,128)(2,1)S(1)}, u32[]{:S(2)}, u32[]{:S(2)}) collective-permute-start(bf16[2,128,768]{2,1,0:T(8,128)(2,1)S(1)} %collective-permute-done.6.refs_4_), channel_id=1, source_target_pairs={{0,96},{4,28},{8,104},{12,4},{16,112},{20,12},{24,120},{28,20},{32... | collective-permute-start | bytes 1179656 | tf_op jit(solution)/shard_map/ppermute | solution.py:41
  25.0 1.9 %shard_map.193 = (f32[1536,128]{1,0:T(8,128)S(1)}, f32[1536,128]{1,0:T(8,128)S(1)}, f32[1024,128]{1,0:T(8,128)S(1)}, f32[512,256]{1,0:T(8,128)S(1)}) custom-call(bf16[128,1024]{1,0:T(8,128)(2,1)S(1)} %get-tuple-element.41.refs_0_, bf16[128,1024]{1,0:T(8,128)(2,1)S(1)} %collective-permute-done.refs_1_, s32[1]{0:T(128)} %bitcast.2.refs_2_, ...), custom_call_target="tpu_custom_call" | custom-call | flops 536870912 | bytes 4194304 | tf_op jit(solution)/shard_map/pallas_call | solution.py:370
  26.8 0.0 copy-start.1
  26.8 2.6 %shard_map.194 = (f32[1536,128]{1,0:T(8,128)S(1)}, f32[1536,128]{1,0:T(8,128)S(1)}, f32[1024,128]{1,0:T(8,128)S(1)}, f32[512,256]{1,0:T(8,128)S(1)}) custom-call(bf16[128,1024]{1,0:T(8,128)(2,1)S(1)} %get-tuple-element.41.refs_0_, bf16[128,1024]{1,0:T(8,128)(2,1)S(1)} %collective-permute-done.refs_1_, s32[1]{0:T(128)} %bitcast.2.refs_2_, ...), custom_call_target="tpu_custom_call" | custom-call | flops 536870912 | bytes 4194304 | tf_op jit(solution)/shard_map/pallas_call | solution.py:370
  29.5 2.6 %shard_map.195 = (f32[1536,128]{1,0:T(8,128)S(1)}, f32[1536,128]{1,0:T(8,128)S(1)}, f32[1024,128]{1,0:T(8,128)S(1)}, f32[512,256]{1,0:T(8,128)S(1)}) custom-call(bf16[128,1024]{1,0:T(8,128)(2,1)S(1)} %get-tuple-element.41.refs_0_, bf16[128,1024]{1,0:T(8,128)(2,1)S(1)} %collective-permute-done.refs_1_, s32[1]{0:T(128)} %bitcast.2.refs_2_, ...), custom_call_target="tpu_custom_call" | custom-call | flops 536870912 | bytes 4194304 | tf_op jit(solution)/shard_map/pallas_call | solution.py:370
  32.2 2.6 %shard_map.196 = (f32[128,1152]{1,0:T(8,128)S(1)}, bf16[128,1152]{1,0:T(8,128)(2,1)S(1)}) custom-call(bf16[128,1024]{1,0:T(8,128)(2,1)S(1)} %get-tuple-element.41.refs_0_, bf16[128,1024]{1,0:T(8,128)(2,1)S(1)} %collective-permute-done.refs_1_, s32[1]{0:T(128)} %bitcast.2.refs_2_, bf16[2,128,768]{2,1,0:T(8,128)(2,1)S(1)} %collective-permute-done.5.refs_3_, ...), custom_call_target="tpu_custom_call" | custom-call | flops 536870912 | bytes 4194304 | tf_op jit(solution)/shard_map/pallas_call | solution.py:370
  34.8 0.1 collective-permute-start.10
  34.9 1.6 collective-permute-done.10.other
  36.5 2.2 %shard_map.197 = (bf16[32,4096]{1,0:T(8,128)(2,1)S(1)}, bf16[32,4096]{1,0:T(8,128)(2,1)S(1)}, bf16[32,4096]{1,0:T(8,128)(2,1)S(1)}, bf16[32,4096]{1,0:T(8,128)(2,1)S(1)}) custom-call(s32[4]{0:T(128)S(1)} %pad_add_fusion.place, f32[128,1152]{1,0:T(8,128)S(1)} %get-tuple-element.63.own, bf16[128,1152]{1,0:T(8,128)(2,1)S(1)} %collective-permute-done.10.other, ...), custom_call_target="tpu_custom_call" | custom-call | flops 1073741824 | bytes 2097152 | tf_op jit(solution)/shard_map/pallas_call | solution.py:48
  38.7 1.6 collective-permute-start.11
  40.2 2.7 %collective-permute-start.12 = (bf16[32,4096]{1,0:T(8,128)(2,1)S(1)}, bf16[32,4096]{1,0:T(8,128)(2,1)S(1)}, u32[]{:S(2)}, u32[]{:S(2)}) collective-permute-start(bf16[32,4096]{1,0:T(8,128)(2,1)S(1)} %get-tuple-element.67), channel_id=1, source_target_pairs={{0,2},{1,3},{2,0},{3,1},{4,6},{5,7},{6,4},{7,5},{8,10},{9,11},{10,... | collective-permute-start | bytes 786440 | tf_op jit(solution)/shard_map/ppermute | solution.py:27
  42.9 1.4 collective-permute-start.13
  44.4 3.9 %collective-permute-done.11.p1 = bf16[32,4096]{1,0:T(8,128)(2,1)S(1)} collective-permute-done((bf16[32,4096]{1,0:T(8,128)(2,1)S(1)}, bf16[32,4096]{1,0:T(8,128)(2,1)S(1)}, u32[]{:S(2)}, u32[]{:S(2)}) %collective-permute-start.11) | collective-permute-done | bytes 262176 | tf_op jit(solution)/shard_map/ppermute | solution.py:27
  48.3 6.6 %collective-permute-done.12.p2 = bf16[32,4096]{1,0:T(8,128)(2,1)S(1)} collective-permute-done((bf16[32,4096]{1,0:T(8,128)(2,1)S(1)}, bf16[32,4096]{1,0:T(8,128)(2,1)S(1)}, u32[]{:S(2)}, u32[]{:S(2)}) %collective-permute-start.12) | collective-permute-done | bytes 262176 | tf_op jit(solution)/shard_map/ppermute | solution.py:27
  54.9 2.7 %shard_map.198 = (f32[32,4096]{1,0:T(8,128)}, bf16[32,4096]{1,0:T(8,128)(2,1)S(1)}, bf16[1024,1024]{1,0:T(8,128)(2,1)}) custom-call(s32[4]{0:T(128)S(1)} %pad_add_fusion.place, bf16[32,4096]{1,0:T(8,128)(2,1)S(1)} %get-tuple-element.65.p0, bf16[32,4096]{1,0:T(8,128)(2,1)S(1)} %collective-permute-done.11.p1, bf16[32,4096]{1,0:T(8,128)(2,1)S(1)} %collective-permute-done.12.p2, ...), custom_call_target="tpu_custom_call" | custom-call | flops 268435456 | bytes 2097152 | tf_op jit(solution)/shard_map/pallas_call | solution.py:48
  57.6 37.2 %all_to_all.10 = bf16[128,8,1024]{2,1,0:T(8,128)(2,1)S(1)} all-to-all(bf16[128,8,1024]{2,1,0:T(8,128)(2,1)} %bitcast.17), channel_id=1, replica_groups=mesh['z'=4,'y'=4,'c'=2,'tp'=4] {'z','y','c','tp'}, dimensions={0} | all-to-all | bytes 4194304 | tf_op jit(solution)/shard_map/all_to_all | solution.py:475
  94.9 5.7 %shard_map.199 = bf16[1024,1024]{1,0:T(8,128)(2,1)} custom-call(bf16[1024,1024]{1,0:T(8,128)(2,1)S(1)} %bitcast.13, bf16[1,4096,256]{2,1,0:T(8,128)(2,1)} %gate_hbm.2, bf16[1,4096,256]{2,1,0:T(8,128)(2,1)} %up_hbm.2, bf16[1,256,4096]{2,1,0:T(8,128)(2,1)} %down_hbm.2), custom_call_target="tpu_custom_call" | custom-call | flops 1610612736 | bytes 2097152 | tf_op jit(solution)/shard_map/pallas_call | solution.py:48
  100.6 4.7 %all-to-all-start.1 = ((bf16[128,8,1024]{2,1,0:T(8,128)(2,1)}), bf16[128,8,1024]{2,1,0:T(8,128)(2,1)S(1)}, u32[]{:S(2)}, u32[]{:S(2)}) async-start(bf16[128,8,1024]{2,1,0:T(8,128)(2,1)} %bitcast.16), calls=%async_computation.1 | async-start | bytes 4194304 | tf_op jit(solution)/shard_map/all_to_all | solution.py:517
  105.3 0.9 collective-permute-start.14
  106.2 2.7 %collective-permute-start.15 = (bf16[32,4096]{1,0:T(8,128)(2,1)S(1)}, bf16[32,4096]{1,0:T(8,128)(2,1)S(1)}, u32[]{:S(2)}, u32[]{:S(2)}) collective-permute-start(bf16[32,4096]{1,0:T(8,128)(2,1)S(1)} %get-tuple-element.72.n0), channel_id=1, source_target_pairs={{0,2},{1,3},{2,0},{3,1},{4,6},{5,7},{6,4},{7,5},{8,10},{9,11},{10,... | collective-permute-start | bytes 786440 | tf_op jit(solution)/shard_map/ppermute | solution.py:27
  108.9 1.4 collective-permute-start.16
  110.3 25.7 %collective-permute-done.14.n1 = bf16[32,4096]{1,0:T(8,128)(2,1)S(1)} collective-permute-done((bf16[32,4096]{1,0:T(8,128)(2,1)S(1)}, bf16[32,4096]{1,0:T(8,128)(2,1)S(1)}, u32[]{:S(2)}, u32[]{:S(2)}) %collective-permute-start.14) | collective-permute-done | bytes 262176 | tf_op jit(solution)/shard_map/ppermute | solution.py:27
  136.0 5.6 %collective-permute-done.15.n2 = bf16[32,4096]{1,0:T(8,128)(2,1)S(1)} collective-permute-done((bf16[32,4096]{1,0:T(8,128)(2,1)S(1)}, bf16[32,4096]{1,0:T(8,128)(2,1)S(1)}, u32[]{:S(2)}, u32[]{:S(2)}) %collective-permute-start.15) | collective-permute-done | bytes 262176 | tf_op jit(solution)/shard_map/ppermute | solution.py:27
  141.6 0.7 copy-done.7
  142.3 0.7 copy-done.8
  143.1 3.8 %shard_map.200 = (bf16[32,4096]{1,0:T(8,128)(2,1)S(1)}, bf16[32,4096]{1,0:T(8,128)(2,1)S(1)}, bf16[32,4096]{1,0:T(8,128)(2,1)S(1)}, bf16[32,4096]{1,0:T(8,128)(2,1)S(1)}) custom-call(bf16[32,4096]{1,0:T(8,128)(2,1)} %copy-done.3, bf16[32,4096]{1,0:T(8,128)(2,1)} %copy-done.6, bf16[32,4096]{1,0:T(8,128)(2,1)} %copy-done.7, bf16[32,4096]{1,0:T(8,128)(2,1)} %copy-done.8, ...), custom_call_target="tpu_custom_call" | custom-call | flops 805306368 | bytes 2097152 | tf_op jit(solution)/shard_map/pallas_call | solution.py:48
  146.9 0.7 copy-done.4
  147.6 1.3 collective-permute-start.18
  148.9 0.8 collective-permute-start.19
  149.6 7.1 %collective-permute-done.17.s1 = bf16[32,4096]{1,0:T(8,128)(2,1)S(1)} collective-permute-done((bf16[32,4096]{1,0:T(8,128)(2,1)S(1)}, bf16[32,4096]{1,0:T(8,128)(2,1)S(1)}, u32[]{:S(2)}, u32[]{:S(2)}) %collective-permute-start.17) | collective-permute-done | bytes 262176 | tf_op jit(solution)/shard_map/ppermute | solution.py:27
  156.8 1.5 collective-permute-done.18.s2
  158.3 4.1 %collective-permute-done.19.s3 = bf16[32,4096]{1,0:T(8,128)(2,1)S(1)} collective-permute-done((bf16[32,4096]{1,0:T(8,128)(2,1)S(1)}, bf16[32,4096]{1,0:T(8,128)(2,1)S(1)}, u32[]{:S(2)}, u32[]{:S(2)}) %collective-permute-start.19) | collective-permute-done | bytes 262176 | tf_op jit(solution)/shard_map/ppermute | solution.py:27
  162.5 0.7 copy-done.11
  163.2 1.5 shard_map.201.base
  164.7 1.2 shard_map.202
  (33 shorter events, 0.1 us)
Async XLA Ops:
  1.1 7.4 %collective-permute-start.1 = (bf16[128,768]{1,0:T(8,128)(2,1)S(1)}, bf16[128,768]{1,0:T(8,128)(2,1)S(1)}, u32[]{:S(2)}, u32[]{:S(2)}) collective-permute-start(bf16[128,768]{1,0:T(8,128)(2,1)S(1)} %get-tuple-element.42.a.refs_3_), channel_id=1, source_target_pairs={{0,8},{4,36},{8,16},{12,44},{16,24},{20,52},{24,0},{28,60},{32,40}... | collective-permute-start | bytes 589832 | tf_op jit(solution)/shard_map/ppermute | solution.py:41
  2.9 5.7 %collective-permute-start.2 = (bf16[128,768]{1,0:T(8,128)(2,1)S(1)}, bf16[128,768]{1,0:T(8,128)(2,1)S(1)}, u32[]{:S(2)}, u32[]{:S(2)}) collective-permute-start(bf16[128,768]{1,0:T(8,128)(2,1)S(1)} %get-tuple-element.42.a.refs_3_), channel_id=1, source_target_pairs={{0,24},{4,100},{8,0},{12,108},{16,8},{20,116},{24,16},{28,124},{32... | collective-permute-start | bytes 589832 | tf_op jit(solution)/shard_map/ppermute | solution.py:41
  4.4 7.2 %collective-permute-start.3 = (bf16[128,768]{1,0:T(8,128)(2,1)S(1)}, bf16[128,768]{1,0:T(8,128)(2,1)S(1)}, u32[]{:S(2)}, u32[]{:S(2)}) collective-permute-start(bf16[128,768]{1,0:T(8,128)(2,1)S(1)} %get-tuple-element.42.a.refs_3_), channel_id=1, source_target_pairs={{0,16},{4,68},{8,24},{12,76},{16,0},{20,84},{24,8},{28,92},{32,48}... | collective-permute-start | bytes 589832 | tf_op jit(solution)/shard_map/ppermute | solution.py:41
  11.7 10.0 %collective-permute-start.4 = (bf16[2,128,768]{2,1,0:T(8,128)(2,1)S(1)}, bf16[2,128,768]{2,1,0:T(8,128)(2,1)S(1)}, u32[]{:S(2)}, u32[]{:S(2)}) collective-permute-start(bf16[2,128,768]{2,1,0:T(8,128)(2,1)S(1)} %get-tuple-element.45.refs_5_), channel_id=1, source_target_pairs={{0,32},{4,12},{8,40},{12,20},{16,48},{20,28},{24,56},{28,4},{32,64... | collective-permute-start | bytes 1179656 | tf_op jit(solution)/shard_map/ppermute | solution.py:41
  13.8 7.9 %collective-permute-start.6 = (bf16[2,128,768]{2,1,0:T(8,128)(2,1)S(1)}, bf16[2,128,768]{2,1,0:T(8,128)(2,1)S(1)}, u32[]{:S(2)}, u32[]{:S(2)}) collective-permute-start(bf16[2,128,768]{2,1,0:T(8,128)(2,1)S(1)} %get-tuple-element.46.refs_6_), channel_id=1, source_target_pairs={{0,96},{4,28},{8,104},{12,4},{16,112},{20,12},{24,120},{28,20},{32... | collective-permute-start | bytes 1179656 | tf_op jit(solution)/shard_map/ppermute | solution.py:41
  16.0 13.5 %collective-permute-start.8 = (bf16[2,128,768]{2,1,0:T(8,128)(2,1)S(1)}, bf16[2,128,768]{2,1,0:T(8,128)(2,1)S(1)}, u32[]{:S(2)}, u32[]{:S(2)}) collective-permute-start(bf16[2,128,768]{2,1,0:T(8,128)(2,1)S(1)} %get-tuple-element.45.refs_5_), channel_id=1, source_target_pairs={{0,96},{4,28},{8,104},{12,4},{16,112},{20,12},{24,120},{28,20},{32... | collective-permute-start | bytes 1179656 | tf_op jit(solution)/shard_map/ppermute | solution.py:41
  17.9 11.6 %collective-permute-start.9 = (bf16[2,128,768]{2,1,0:T(8,128)(2,1)S(1)}, bf16[2,128,768]{2,1,0:T(8,128)(2,1)S(1)}, u32[]{:S(2)}, u32[]{:S(2)}) collective-permute-start(bf16[2,128,768]{2,1,0:T(8,128)(2,1)S(1)} %get-tuple-element.46.refs_6_), channel_id=1, source_target_pairs={{0,32},{4,12},{8,40},{12,20},{16,48},{20,28},{24,56},{28,4},{32,64... | collective-permute-start | bytes 1179656 | tf_op jit(solution)/shard_map/ppermute | solution.py:41
  18.0 7.0 %collective-permute-start = (bf16[128,1024]{1,0:T(8,128)(2,1)S(1)}, bf16[128,1024]{1,0:T(8,128)(2,1)S(1)}, u32[]{:S(2)}, u32[]{:S(2)}) collective-permute-start(bf16[128,1024]{1,0:T(8,128)(2,1)S(1)} %get-tuple-element.41.refs_0_), channel_id=1, source_target_pairs={{0,4},{4,0},{1,5},{5,1},{2,6},{6,2},{3,7},{7,3},{8,12},{12,8},{9,1... | collective-permute-start | bytes 786440 | tf_op jit(solution)/shard_map/ppermute | solution.py:31
  21.6 10.5 %collective-permute-start.5 = (bf16[2,128,768]{2,1,0:T(8,128)(2,1)S(1)}, bf16[2,128,768]{2,1,0:T(8,128)(2,1)S(1)}, u32[]{:S(2)}, u32[]{:S(2)}) collective-permute-start(bf16[2,128,768]{2,1,0:T(8,128)(2,1)S(1)} %collective-permute-done.4.refs_3_), channel_id=1, source_target_pairs={{0,32},{4,12},{8,40},{12,20},{16,48},{20,28},{24,56},{28,4},{32,64... | collective-permute-start | bytes 1179656 | tf_op jit(solution)/shard_map/ppermute | solution.py:41
  21.6 10.5 %collective-permute-start.7 = (bf16[2,128,768]{2,1,0:T(8,128)(2,1)S(1)}, bf16[2,128,768]{2,1,0:T(8,128)(2,1)S(1)}, u32[]{:S(2)}, u32[]{:S(2)}) collective-permute-start(bf16[2,128,768]{2,1,0:T(8,128)(2,1)S(1)} %collective-permute-done.6.refs_4_), channel_id=1, source_target_pairs={{0,96},{4,28},{8,104},{12,4},{16,112},{20,12},{24,120},{28,20},{32... | collective-permute-start | bytes 1179656 | tf_op jit(solution)/shard_map/ppermute | solution.py:41
  26.8 9.6 %copy-start.1 = (bf16[512,4096]{1,0:T(8,128)(2,1)S(1)}, bf16[512,4096]{1,0:T(8,128)(2,1)}, u32[]{:S(2)}) copy-start(bf16[512,4096]{1,0:T(8,128)(2,1)} %broad.1) | copy-start | bytes 12582916
  29.5 7.0 %copy-start = (bf16[512,4096]{1,0:T(8,128)(2,1)S(1)}, bf16[512,4096]{1,0:T(8,128)(2,1)}, u32[]{:S(2)}) copy-start(bf16[512,4096]{1,0:T(8,128)(2,1)} %narrow.1) | copy-start | bytes 12582916
  34.8 1.7 %collective-permute-start.10 = (bf16[128,1152]{1,0:T(8,128)(2,1)S(1)}, bf16[128,1152]{1,0:T(8,128)(2,1)S(1)}, u32[]{:S(2)}, u32[]{:S(2)}) collective-permute-start(bf16[128,1152]{1,0:T(8,128)(2,1)S(1)} %get-tuple-element.64), channel_id=1, source_target_pairs={{0,4},{4,0},{1,5},{5,1},{2,6},{6,2},{3,7},{7,3},{8,12},{12,8},{9,1... | collective-permute-start | bytes 884744 | tf_op jit(solution)/shard_map/ppermute | solution.py:31
  36.5 18.4 %copy-start.2 = (bf16[128,4096]{1,0:T(8,128)(2,1)S(1)}, bf16[128,4096]{1,0:T(8,128)(2,1)}, u32[]{:S(2)}) copy-start(bf16[128,4096]{1,0:T(8,128)(2,1)} %residual.1) | copy-start | bytes 3145732
  36.5 18.4 %copy-start.5 = (f32[4096]{0:T(1024)S(1)}, f32[4096]{0:T(1024)}, u32[]{:S(2)}) copy-start(f32[4096]{0:T(1024)} %param.31) | copy-start | bytes 49156
  38.7 9.6 %collective-permute-start.11 = (bf16[32,4096]{1,0:T(8,128)(2,1)S(1)}, bf16[32,4096]{1,0:T(8,128)(2,1)S(1)}, u32[]{:S(2)}, u32[]{:S(2)}) collective-permute-start(bf16[32,4096]{1,0:T(8,128)(2,1)S(1)} %get-tuple-element.66), channel_id=1, source_target_pairs={{0,1},{1,2},{2,3},{3,0},{4,5},{5,6},{6,7},{7,4},{8,9},{9,10},{10,1... | collective-permute-start | bytes 786440 | tf_op jit(solution)/shard_map/ppermute | solution.py:27
  40.2 14.7 %collective-permute-start.12 = (bf16[32,4096]{1,0:T(8,128)(2,1)S(1)}, bf16[32,4096]{1,0:T(8,128)(2,1)S(1)}, u32[]{:S(2)}, u32[]{:S(2)}) collective-permute-start(bf16[32,4096]{1,0:T(8,128)(2,1)S(1)} %get-tuple-element.67), channel_id=1, source_target_pairs={{0,2},{1,3},{2,0},{3,1},{4,6},{5,7},{6,4},{7,5},{8,10},{9,11},{10,... | collective-permute-start | bytes 786440 | tf_op jit(solution)/shard_map/ppermute | solution.py:27
  42.9 11.9 %collective-permute-start.13 = (bf16[32,4096]{1,0:T(8,128)(2,1)S(1)}, bf16[32,4096]{1,0:T(8,128)(2,1)S(1)}, u32[]{:S(2)}, u32[]{:S(2)}) collective-permute-start(bf16[32,4096]{1,0:T(8,128)(2,1)S(1)} %get-tuple-element.68), channel_id=1, source_target_pairs={{0,3},{1,0},{2,1},{3,2},{4,7},{5,4},{6,5},{7,6},{8,11},{9,8},{10,9... | collective-permute-start | bytes 786440 | tf_op jit(solution)/shard_map/ppermute | solution.py:27
  57.6 51.2 %copy-start.3 = (bf16[32,4096]{1,0:T(8,128)(2,1)}, bf16[32,4096]{1,0:T(8,128)(2,1)S(1)}, u32[]{:S(2)}) copy-start(bf16[32,4096]{1,0:T(8,128)(2,1)S(1)} %get-tuple-element.72.n0) | copy-start | bytes 786436
  100.6 64.1 %all-to-all-start.1 = ((bf16[128,8,1024]{2,1,0:T(8,128)(2,1)}), bf16[128,8,1024]{2,1,0:T(8,128)(2,1)S(1)}, u32[]{:S(2)}, u32[]{:S(2)}) async-start(bf16[128,8,1024]{2,1,0:T(8,128)(2,1)} %bitcast.16), calls=%async_computation.1 | async-start | bytes 4194304 | tf_op jit(solution)/shard_map/all_to_all | solution.py:517
  105.3 30.8 %collective-permute-start.14 = (bf16[32,4096]{1,0:T(8,128)(2,1)S(1)}, bf16[32,4096]{1,0:T(8,128)(2,1)S(1)}, u32[]{:S(2)}, u32[]{:S(2)}) collective-permute-start(bf16[32,4096]{1,0:T(8,128)(2,1)S(1)} %get-tuple-element.72.n0), channel_id=1, source_target_pairs={{0,1},{1,2},{2,3},{3,0},{4,5},{5,6},{6,7},{7,4},{8,9},{9,10},{10,1... | collective-permute-start | bytes 786440 | tf_op jit(solution)/shard_map/ppermute | solution.py:27
  106.2 35.5 %collective-permute-start.15 = (bf16[32,4096]{1,0:T(8,128)(2,1)S(1)}, bf16[32,4096]{1,0:T(8,128)(2,1)S(1)}, u32[]{:S(2)}, u32[]{:S(2)}) collective-permute-start(bf16[32,4096]{1,0:T(8,128)(2,1)S(1)} %get-tuple-element.72.n0), channel_id=1, source_target_pairs={{0,2},{1,3},{2,0},{3,1},{4,6},{5,7},{6,4},{7,5},{8,10},{9,11},{10,... | collective-permute-start | bytes 786440 | tf_op jit(solution)/shard_map/ppermute | solution.py:27
  108.9 32.8 %collective-permute-start.16 = (bf16[32,4096]{1,0:T(8,128)(2,1)S(1)}, bf16[32,4096]{1,0:T(8,128)(2,1)S(1)}, u32[]{:S(2)}, u32[]{:S(2)}) collective-permute-start(bf16[32,4096]{1,0:T(8,128)(2,1)S(1)} %get-tuple-element.72.n0), channel_id=1, source_target_pairs={{0,3},{1,0},{2,1},{3,2},{4,7},{5,4},{6,5},{7,6},{8,11},{9,8},{10,9... | collective-permute-start | bytes 786440 | tf_op jit(solution)/shard_map/ppermute | solution.py:27
  136.0 5.6 %copy-start.6 = (bf16[32,4096]{1,0:T(8,128)(2,1)}, bf16[32,4096]{1,0:T(8,128)(2,1)S(1)}, u32[]{:S(2)}) copy-start(bf16[32,4096]{1,0:T(8,128)(2,1)S(1)} %collective-permute-done.14.n1) | copy-start | bytes 786436
  141.6 0.7 copy-start.7
  142.3 0.7 copy-start.8
  146.9 0.7 copy-start.4
  147.6 9.2 %collective-permute-start.17 = (bf16[32,4096]{1,0:T(8,128)(2,1)S(1)}, bf16[32,4096]{1,0:T(8,128)(2,1)S(1)}, u32[]{:S(2)}, u32[]{:S(2)}) collective-permute-start(bf16[32,4096]{1,0:T(8,128)(2,1)S(1)} %get-tuple-element.74), channel_id=1, source_target_pairs={{0,3},{1,0},{2,1},{3,2},{4,7},{5,4},{6,5},{7,6},{8,11},{9,8},{10,9... | collective-permute-start | bytes 786440 | tf_op jit(solution)/shard_map/ppermute | solution.py:27
  147.6 10.7 %collective-permute-start.18 = (bf16[32,4096]{1,0:T(8,128)(2,1)S(1)}, bf16[32,4096]{1,0:T(8,128)(2,1)S(1)}, u32[]{:S(2)}, u32[]{:S(2)}) collective-permute-start(bf16[32,4096]{1,0:T(8,128)(2,1)S(1)} %get-tuple-element.75), channel_id=1, source_target_pairs={{0,2},{1,3},{2,0},{3,1},{4,6},{5,7},{6,4},{7,5},{8,10},{9,11},{10,... | collective-permute-start | bytes 786440 | tf_op jit(solution)/shard_map/ppermute | solution.py:27
  148.9 13.6 %collective-permute-start.19 = (bf16[32,4096]{1,0:T(8,128)(2,1)S(1)}, bf16[32,4096]{1,0:T(8,128)(2,1)S(1)}, u32[]{:S(2)}, u32[]{:S(2)}) collective-permute-start(bf16[32,4096]{1,0:T(8,128)(2,1)S(1)} %get-tuple-element.76), channel_id=1, source_target_pairs={{0,1},{1,2},{2,3},{3,0},{4,5},{5,6},{6,7},{7,4},{8,9},{9,10},{10,1... | collective-permute-start | bytes 786440 | tf_op jit(solution)/shard_map/ppermute | solution.py:27
  156.8 5.7 %copy-start.9 = (bf16[32,4096]{1,0:T(8,128)(2,1)}, bf16[32,4096]{1,0:T(8,128)(2,1)S(1)}, u32[]{:S(2)}) copy-start(bf16[32,4096]{1,0:T(8,128)(2,1)S(1)} %collective-permute-done.17.s1) | copy-start | bytes 786436
  158.3 4.2 %copy-start.10 = (bf16[32,4096]{1,0:T(8,128)(2,1)}, bf16[32,4096]{1,0:T(8,128)(2,1)S(1)}, u32[]{:S(2)}) copy-start(bf16[32,4096]{1,0:T(8,128)(2,1)S(1)} %collective-permute-done.18.s2) | copy-start | bytes 786436
  162.5 0.7 copy-start.11
